TPU v7x, 128 devices: a whole 4x4x4 slice. The times are simulated.
128 devices in a mesh: sp: 16 (over z, x), tp: 8 (over y, core).
Axes of the slice: x: 4, y: 4, z: 4, core: 2. Of those that a mesh axis runs over, the one named last changes fastest.
Arguments:
- tokens: bfloat16 [16384, 2048], P(('sp', 'tp')), may hold values from -6 to 6
- elapsed: float32 [16384], P(('sp', 'tp')), may hold values from 0 to 3, as said below
- norm_gain: float32 [2048], replicated, may hold values from 0.1 to 1.9
- in_weight: bfloat16 [2048, 1024], replicated, may hold values from -0.125 to 0.125
- state_input: bfloat16 [2, 2, 64, 64, 16], replicated, may hold values from -1.5 to 1.5
- state_output: float32 [2, 2, 64, 16, 64], replicated, may hold values from -0.375 to 0.375
- forget_rate: float32 [2, 64, 64], replicated, may hold values from 0 to 1, as said below
- decay_angle: float32 [2, 64, 64], replicated, may hold values from -3.140625 to 3.140625
- skip_gain: float32 [1024], replicated, may hold values from -4 to 4
- glu_weight: bfloat16 [1024, 1024], replicated, may hold values from -0.1875 to 0.1875
- glu_bias: float32 [1024], replicated, may hold values from -4 to 4
- out_weight: bfloat16 [1024, 2048], replicated, may hold values from -0.1875 to 0.1875
- out_gain: float32 [2048], replicated, may hold values from 0.1 to 1.9
Outputs:
- mixed: bfloat16 [16384, 2048], P(('sp', 'tp'))
Inputs may be any that keep to these rules, and one draw needn't show every extreme that they name: `elapsed`: positive time steps. `forget_rate`: positive rates.
All inputs are finite; a program needn't handle non-finite values.
Results may differ from a plain program's by a relative error of at most 0.0067.
Values sent between devices are 32-bit elements; how exact they have to be, the bound alone decides.
No kernel may reach another device: no remote copies, remote signals or barrier semaphores. Data moves between devices by JAX's collectives and lax.ppermute only.
A program may use at most 128 MiB of HBM per device.

v0:
```python
import functools
import math

import jax
import jax.numpy as jnp
from jax import lax
from jax.experimental import pallas as pl
from jax.experimental.pallas import tpu as pltpu
from jax.sharding import PartitionSpec as P

ROWS = 128
D = 2048
CHANNELS = 1024
DEVICES = 128
TILES = 8
SPAN = 16
SPANS = ROWS // SPAN
HALF_TILES = 4
EPSILON = 1e-06
AXES = ("sp", "tp")
VMEM = pltpu.VMEM
HIGHEST = lax.Precision.HIGHEST
F32 = jnp.float32
BF16 = jnp.bfloat16

SINE = (4.44288291, -7.30824512, 3.60634303, -0.84604096, 0.10968436)
COSINE = (1.4142135, -6.97885097, 5.73946067, -1.88355924, 0.31068962)
DAMP = (
    9.99999626e-01,
    -2.49992247e-01,
    5.20558088e-02,
    -7.77389543e-03,
    8.29541685e-04,
    -6.19250366e-05,
    2.98283721e-06,
    -7.10025954e-08,
)
SINE_SHORT = (4.44287876, -7.30776104, 3.5971931, -0.7896682)


def horner(coefficients, x):
    value = coefficients[-1] * x + coefficients[-2]
    for c in coefficients[-3::-1]:
        value = value * x + c
    return value


def unit_circle(turns, sine=SINE_SHORT):
    r = turns - jnp.round(turns)
    z = r * r
    s = r * horner(sine, z)
    c = horner(COSINE, z)
    return 1.0 - s * s, s * c


def nt(a, b):
    return lax.dot_general(a, b, (((1,), (1,)), ((), ())), preferred_element_type=F32)


def mm(a, b):
    return jnp.dot(a, b, preferred_element_type=F32)


def iotas(shape):
    return lax.broadcasted_iota(jnp.int32, shape, 0), lax.broadcasted_iota(jnp.int32, shape, 1)


def column_of(row):
    return jnp.broadcast_to(row, (ROWS, ROWS)).T


def exact_mm(a, b):
    return jnp.dot(a, b, preferred_element_type=F32, precision=HIGHEST)


def end_kernel(
    tokens, elapsed, gain, weight, inputs, turns, rates, rates2, root2,
    driven_ref, ends_ref, total_ref, bt_ref, normed, times,
):
    step = pl.program_id(0)

    @pl.when(step == 0)
    def _():
        x = tokens[...].astype(F32)
        scale = lax.rsqrt(jnp.mean(x * x, axis=-1, keepdims=True) + EPSILON)
        normed[...] = (x * scale * gain[...]).astype(BF16)
        steps = column_of(elapsed[...])
        row, col = iotas((ROWS, ROWS))
        times[0] = exact_mm((col > row).astype(F32), steps)
        times[1] = exact_mm((col < row).astype(F32), steps)
        times[2] = jnp.sqrt(steps)
        times[3] = steps
        total_ref[...] = exact_mm(jnp.ones((ROWS, ROWS), F32), steps)

    driven = mm(normed[...], weight[...]).astype(BF16)
    driven_ref[...] = driven
    flipped = driven.astype(F32).T.astype(BF16)
    lane = lax.broadcasted_iota(jnp.int32, (16, 128), 1)
    first = lane < 64
    row, col = iotas((16, 16))
    eye = (row == col).astype(BF16)
    for j in range(4):
        pair = step * 4 + j
        for k in range(2):
            th = turns[k, pl.ds(pair, 1), :]
            fl = rates[k, pl.ds(pair, 1), :]
            f2 = rates2[k, pl.ds(pair, 1), :]
            rt = root2[k, pl.ds(pair, 1), :]
            after = times[k]
            cosine, sine = unit_circle(after * th)
            damp = horner(DAMP, times[3] * f2) * (times[2] * rt)
            amp = jnp.exp2(after * fl) * damp
            pull = jnp.concatenate(
                [(amp * cosine).astype(BF16), (amp * sine).astype(BF16)], axis=1
            )
            mixed = mm(flipped[32 * j : 32 * j + 32], pull)
            m_re = jnp.where(first, mixed[:16, :128], mixed[16:, :128])
            m_im = jnp.where(first, mixed[:16, 128:], mixed[16:, 128:])
            b_re = nt(eye, inputs[k, 0, 2 * j : 2 * j + 2].reshape(128, 16))
            b_im = nt(eye, inputs[k, 1, 2 * j : 2 * j + 2].reshape(128, 16))
            bt_ref[j, k] = jnp.concatenate([b_re.astype(BF16), b_im.astype(BF16)], axis=1)
            x_re = jnp.sum(b_re * m_re - b_im * m_im, axis=0, keepdims=True)
            x_im = jnp.sum(b_re * m_im + b_im * m_re, axis=0, keepdims=True)
            lane1 = first[:1]
            row0 = jnp.where(lane1, x_re, pltpu.roll(x_im, 64, 1))
            row1 = jnp.where(lane1, pltpu.roll(x_re, 64, 1), x_im)
            ends_ref[pl.ds(64 * k + 2 * pair, 1), :] = row0
            ends_ref[pl.ds(64 * k + 2 * pair + 1, 1), :] = row1


def local_kernel(
    offset, elapsed, driven, bt, readout, turns, rates, rates2, root2, skip,
    out_ref, prefix_ref, table_ref, times,
):
    step = pl.program_id(0)

    @pl.when(step == 0)
    def _():
        steps = column_of(elapsed[...])
        row, col = iotas((ROWS, ROWS))
        same = row // SPAN == col // SPAN
        times[0] = exact_mm(((col <= row) & same).astype(F32), steps)
        times[1] = exact_mm(((col >= row) & same).astype(F32), steps)
        times[2] = jnp.sqrt(steps)
        times[3] = steps

    row, col = iotas((ROWS, ROWS))
    same = row // SPAN == col // SPAN
    triangles = (((col <= row) & same).astype(BF16), ((col >= row) & same).astype(BF16))
    lane = lax.broadcasted_iota(jnp.int32, (16, 256), 1) % 128
    zero_bt = jnp.zeros((16, 256), BF16)
    hole = jnp.zeros((16, 64), F32)
    x = driven[...]
    outs = []
    for j in range(4):
        pair = (step + offset) * 4 + j
        lhs = x[:, 32 * j : 32 * j + 32]
        total = None
        for k in range(2):
            th = turns[k, pl.ds(pair, 1), :]
            fl = rates[k, pl.ds(pair, 1), :]
            f2 = rates2[k, pl.ds(pair, 1), :]
            rt = root2[k, pl.ds(pair, 1), :]
            b = bt[j, k].astype(F32)
            rhs = jnp.concatenate(
                [jnp.where(lane < 64, b, 0.0).astype(BF16), jnp.where(lane < 64, 0.0, b).astype(BF16)], axis=0
            )
            proj = mm(lhs, rhs)
            p_re, p_im = proj[:, :128], proj[:, 128:]
            offs = times[k]
            cosine, sine = unit_circle(offs * th)
            damp = horner(DAMP, times[3] * f2) * (times[2] * rt)
            level = offs * fl
            grow = jnp.exp2(-level) * damp
            fade = jnp.exp2(level)
            a_re, a_im = grow * cosine, grow * sine
            lift = jnp.concatenate(
                [(a_re * p_re + a_im * p_im).astype(BF16), (a_re * p_im - a_im * p_re).astype(BF16)], axis=1
            )
            part = mm(triangles[k], lift)
            e_re, e_im = fade * cosine, fade * sine
            c_re = c_im = jnp.zeros((1, 128), F32)
            d_re, d_im = jnp.ones((1, 128), F32), jnp.zeros((1, 128), F32)
            states, prefixes = [None] * SPANS, [None] * SPANS
            for n in range(SPANS) if k == 0 else range(SPANS - 1, -1, -1):
                cut = slice(SPAN * n, SPAN * n + SPAN)
                er, ei = e_re[cut], e_im[cut]
                wr, wi = part[cut, :128] + c_re, part[cut, 128:] + c_im
                sr, si = er * wr - ei * wi, er * wi + ei * wr
                pr, pi = er * d_re - ei * d_im, er * d_im + ei * d_re
                edge = slice(SPAN - 1, SPAN) if k == 0 else slice(0, 1)
                c_re, c_im, d_re, d_im = sr[edge], si[edge], pr[edge], pi[edge]
                states[n] = jnp.concatenate([sr.astype(BF16), si.astype(BF16)], axis=1)
                prefixes[n] = jnp.concatenate([pr.astype(BF16), pi.astype(BF16)], axis=1)
            prefix_ref[j, k] = jnp.concatenate(prefixes, axis=0)
            tables = []
            for c in range(2):
                upper = jnp.concatenate([readout[k, c, 2 * j], hole], axis=1)
                lower = jnp.concatenate([hole, readout[k, c, 2 * j + 1]], axis=1)
                table = jnp.concatenate([upper, lower], axis=0)
                table_ref[j, k, c] = table
                tables.append(table)
            y = nt(
                jnp.concatenate(states, axis=0),
                jnp.concatenate([tables[0].astype(BF16), (-tables[1]).astype(BF16)], axis=1),
            )
            total = y if total is None else total + y
        outs.append(total)
    out_ref[...] = jnp.concatenate(outs, axis=1) + skip[...] * x.astype(F32)


def device_kernel(backward, ends, turns_hi, turns_lo, rate, out_ref, work):
    span = ends[:, 128:]
    u = span * turns_hi[...]
    r = (u - jnp.round(u)) + span * turns_lo[...]
    cosine, sine = unit_circle(r, SINE)
    fade = jnp.exp2(span * rate[...])
    work[0] = fade * cosine
    work[1] = fade * sine
    x = ends[:, :128]
    work[2] = x
    work[3] = pltpu.roll(x, 64, 1)
    back = backward[0]
    first = lax.broadcasted_iota(jnp.int32, (1, 128), 1) < 64

    def body(i, carry):
        re, im = carry
        d = jnp.where(back > 0, DEVICES - 1 - i, i)
        out_ref[pl.ds(d, 1), :] = jnp.where(first, re, pltpu.roll(im, 64, 1))
        ar, ai = work[0, pl.ds(d, 1), :], work[1, pl.ds(d, 1), :]
        xr, xi = work[2, pl.ds(d, 1), :], work[3, pl.ds(d, 1), :]
        return ar * re - ai * im + xr, ar * im + ai * re + xi

    zero = jnp.zeros((1, 128), F32)
    lax.fori_loop(0, DEVICES, body, (zero, zero), unroll=8)


def final_kernel(
    entering, near_a, near_b, prefix_a, prefix_b, table_a, table_b, glu, glu_bias, outw, out_gain,
    out_ref, prefix, glu_v, outw_v, response, sems,
):
    copies = [
        pltpu.make_async_copy(prefix_a, prefix.at[pl.ds(0, 16)], sems.at[0]),
        pltpu.make_async_copy(prefix_b, prefix.at[pl.ds(16, 16)], sems.at[1]),
        pltpu.make_async_copy(glu, glu_v, sems.at[2]),
        pltpu.make_async_copy(outw, outw_v, sems.at[3]),
    ]
    for copy in copies:
        copy.start()
    for half, (near, table) in enumerate(((near_a, table_a), (near_b, table_b))):
        copies[half].wait()

        def tile(i, _, half=half, near=near, table=table):
            outs = []
            for j in range(4):
                total = None
                for k in range(2):
                    at = 64 * k + 32 * half + 8 * i + 2 * j
                    e0, e1 = entering[pl.ds(at, 1), :], entering[pl.ds(at + 1, 1), :]
                    er = jnp.concatenate([e0[:, :64], e1[:, :64]], axis=1)
                    ei = jnp.concatenate([e0[:, 64:], e1[:, 64:]], axis=1)
                    cr, ci = table[4 * i + j, k, 0], table[4 * i + j, k, 1]
                    rhs = jnp.concatenate(
                        [(cr * er - ci * ei).astype(BF16), (-(cr * ei + ci * er)).astype(BF16)], axis=1
                    )
                    y = nt(prefix[16 * half + 4 * i + j, k], rhs)
                    total = y if total is None else total + y
                outs.append(total)
            at = pl.multiple_of(128 * i, 128)
            response[:, pl.ds(at + 512 * half, 128)] = jnp.concatenate(outs, axis=1) + near[:, pl.ds(at, 128)]
            return 0

        lax.fori_loop(0, HALF_TILES, tile, 0)
    x = response[...]
    active = 0.5 * x * (1.0 + jnp.tanh(math.sqrt(2.0 / math.pi) * (x + 0.044715 * (x * x * x))))
    copies[2].wait()
    gate = mm(active.astype(BF16), glu_v[...]) + glu_bias[...]
    gated = (active * jax.nn.sigmoid(gate)).astype(BF16)
    copies[3].wait()
    projected = mm(gated, outw_v[...])
    scale = lax.rsqrt(jnp.mean(projected * projected, axis=-1, keepdims=True) + EPSILON)
    out_ref[...] = (projected * scale * out_gain[...]).astype(BF16)


def whole(shape):
    return pl.BlockSpec(shape, lambda *_: (0,) * len(shape))


def sds(shape, dtype=F32):
    return jax.ShapeDtypeStruct(shape, dtype)


def params(limit=40):
    return pltpu.CompilerParams(vmem_limit_bytes=limit * 1024 * 1024)


def run_local(half, elapsed_row, driven, bt, state_output, rows, skip_row):
    row_spec = whole((2, 32, 128))
    return pl.pallas_call(
        functools.partial(local_kernel, half * HALF_TILES),
        name=f"local_{half}",
        grid=(HALF_TILES,),
        in_specs=[
            whole((1, ROWS)),
            pl.BlockSpec((ROWS, 128), lambda i: (0, i + half * HALF_TILES)),
            pl.BlockSpec((4, 2, 16, 256), lambda i: (i + half * HALF_TILES, 0, 0, 0)),
            pl.BlockSpec((2, 2, 8, 16, 64), lambda i: (0, 0, i + half * HALF_TILES, 0, 0)),
            row_spec, row_spec, row_spec, row_spec,
            pl.BlockSpec((1, 128), lambda i: (0, i + half * HALF_TILES)),
        ],
        out_specs=[
            pl.BlockSpec((ROWS, 128), lambda i: (0, i)),
            pl.BlockSpec((4, 2, ROWS, 256), lambda i: (i, 0, 0, 0)),
            pl.BlockSpec((4, 2, 2, 32, 128), lambda i: (i, 0, 0, 0, 0)),
        ],
        out_shape=[
            sds((ROWS, 512)),
            sds((16, 2, ROWS, 256), BF16),
            sds((16, 2, 2, 32, 128)),
        ],
        scratch_shapes=[VMEM((4, ROWS, ROWS), F32)],
        compiler_params=params(),
        cost_estimate=pl.CostEstimate(flops=2 * 10**9, bytes_accessed=8 * 2**20, transcendentals=0),
    )(elapsed_row, driven, bt, state_output, *rows, skip_row)


def local(
    tokens, elapsed, norm_gain, in_weight, state_input, state_output, forget_rate, decay_angle,
    skip_gain, glu_weight, glu_bias, out_weight, out_gain,
):
    elapsed_row = elapsed.reshape(1, ROWS)
    rate = forget_rate.reshape(2, 32, 128)
    angle = decay_angle.reshape(2, 32, 128)
    rows = (
        angle * (0.5 / math.pi),
        rate * (-1.0 / math.log(2.0)),
        rate * 2.0,
        jnp.sqrt(rate * 2.0),
    )
    row_spec = whole((2, 32, 128))
    driven, ends, total, bt = pl.pallas_call(
        end_kernel,
        name="ends",
        grid=(TILES,),
        in_specs=[
            whole((ROWS, D)),
            whole((1, ROWS)),
            whole((1, D)),
            pl.BlockSpec((D, 128), lambda i: (0, i)),
            pl.BlockSpec((2, 2, 8, 64, 16), lambda i: (0, 0, i, 0, 0)),
            row_spec, row_spec, row_spec, row_spec,
        ],
        out_specs=[
            pl.BlockSpec((ROWS, 128), lambda i: (0, i)),
            whole((ROWS, 128)),
            whole((ROWS, 128)),
            pl.BlockSpec((4, 2, 16, 256), lambda i: (i, 0, 0, 0)),
        ],
        out_shape=[
            sds((ROWS, CHANNELS), BF16),
            sds((DEVICES, 128)),
            sds((DEVICES, 128)),
            sds((32, 2, 16, 256), BF16),
        ],
        scratch_shapes=[VMEM((ROWS, D), BF16), VMEM((4, ROWS, ROWS), F32)],
        compiler_params=params(),
    )(tokens, elapsed_row, norm_gain.reshape(1, D), in_weight, state_input, *rows)

    me = lax.axis_index(AXES)
    flat_angle = lax.dynamic_slice(decay_angle.reshape(128, 64), (me, 0), (1, 64))
    flat_rate = lax.dynamic_slice(forget_rate.reshape(128, 64), (me, 0), (1, 64))
    mine = jnp.concatenate([flat_angle, flat_angle], axis=1)
    mine_rate = jnp.concatenate([flat_rate, flat_rate], axis=1) * (-1.0 / math.log(2.0))
    high = jnp.round(mine * (4096 * 0.5 / math.pi)) * (1.0 / 4096)
    coarse = 6433 / 1024
    low = ((mine - high * coarse) - high * (2 * math.pi - coarse)) * (0.5 / math.pi)
    backward = (me >= 64).astype(jnp.int32).reshape(1)

    seen = lax.all_to_all(jnp.concatenate([ends, total], axis=1), AXES, 0, 0, tiled=True)
    skip_row = skip_gain.reshape(1, CHANNELS)
    near_a, prefix_a, table_a = run_local(0, elapsed_row, driven, bt, state_output, rows, skip_row)
    carried = pl.pallas_call(
        device_kernel,
        name="across",
        in_specs=[pl.BlockSpec(memory_space=pltpu.SMEM)] + [pl.BlockSpec(memory_space=VMEM)] * 4,
        out_shape=sds((DEVICES, 128)),
        scratch_shapes=[VMEM((4, DEVICES, 128), F32)],
        compiler_params=params(8),
    )(backward, seen, high, low, mine_rate)
    entering = lax.all_to_all(carried, AXES, 0, 0, tiled=True)
    near_b, prefix_b, table_b = run_local(1, elapsed_row, driven, bt, state_output, rows, skip_row)

    any_spec = pl.BlockSpec(memory_space=pl.ANY)
    vmem_spec = pl.BlockSpec(memory_space=VMEM)
    return pl.pallas_call(
        final_kernel,
        name="final",
        in_specs=[
            vmem_spec, vmem_spec, vmem_spec, any_spec, any_spec, vmem_spec, vmem_spec,
            any_spec, vmem_spec, any_spec, vmem_spec,
        ],
        out_specs=vmem_spec,
        out_shape=sds((ROWS, D), BF16),
        scratch_shapes=[
            VMEM((32, 2, ROWS, 256), BF16),
            VMEM((CHANNELS, CHANNELS), BF16),
            VMEM((CHANNELS, D), BF16),
            VMEM((ROWS, CHANNELS), F32),
            pltpu.SemaphoreType.DMA((4,)),
        ],
        compiler_params=params(),
    )(
        entering, near_a, near_b, prefix_a, prefix_b, table_a, table_b,
        glu_weight, glu_bias.reshape(1, CHANNELS), out_weight, out_gain.reshape(1, D),
    )


def solution(mesh):
    split = P(AXES, None)
    placed = (split, P(AXES), P(), P(), P(), P(), P(), P(), P(), P(), P(), P(), P())
    return jax.shard_map(local, mesh=mesh, in_specs=placed, out_specs=split, check_vma=False)
```

profile of v0, /device:TPU:1, one launch (start us, length us, event | category | flops | bytes accessed | tf_op | source)
XLA Modules:
  0.0 94.6 jit_solution(7619819545823145076)
XLA Ops:
  0.0 0.8 broadcast_multiply_fusion.2
  0.8 0.1 mul.92.turns
  0.9 0.9 broadcast_multiply_fusion
  1.8 0.1 mul.97.rates2
  1.9 0.0 copy-start.15
  1.9 0.1 mul.95.rates
  2.0 0.0 copy-start.13
  2.0 0.0 copy-start.10
  2.0 0.0 copy-start.17
  2.0 0.0 copy-start.20
  2.0 4.7 %copy.15.inputs = bf16[2,2,64,64,16]{4,3,2,1,0:T(8,128)(2,1)} copy(bf16[2,2,64,64,16]{3,4,2,1,0:T(8,128)(2,1)} %param.17) | data formatting | bytes 1048576 | tf_op args[4]
  6.6 0.0 copy-done.10
  6.6 0.0 copy-done.17
  6.6 0.0 copy-done.20
  6.7 0.0 copy-start
  6.7 2.2 %copy-done = bf16[2,2,64,64,16]{4,3,2,1,0:T(8,128)(2,1)S(1)} copy-done((bf16[2,2,64,64,16]{4,3,2,1,0:T(8,128)(2,1)S(1)}, bf16[2,2,64,64,16]{4,3,2,1,0:T(8,128)(2,1)}, u32[]{:S(2)}) %copy-start) | copy-done | bytes 524312
  8.8 0.0 copy-start.2
  8.8 2.2 %copy-done.2 = bf16[2048,1024]{1,0:T(8,128)(2,1)S(1)} copy-done((bf16[2048,1024]{1,0:T(8,128)(2,1)S(1)}, bf16[2048,1024]{1,0:T(8,128)(2,1)}, u32[]{:S(2)}) %copy-start.2) | copy-done | bytes 4194328
  11.0 0.0 copy-start.27
  11.0 12.2 %ends.1 = (bf16[128,1024]{1,0:T(8,128)(2,1)S(1)}, f32[128,128]{1,0:T(8,128)S(1)}, f32[128,128]{1,0:T(8,128)S(1)}, bf16[32,2,16,256]{3,2,1,0:T(8,128)(2,1)S(1)}) custom-call(bf16[128,2048]{1,0:T(8,128)(2,1)S(1)} %copy-done.10, f32[1,128]{1,0:T(1,128)S(1)} %bitcast.22, f32[1,2048]{1,0:T(1,128)S(1)} %bitcast.19, bf16[2048,1024]{1,0:T(8,128)(2,1)S(1)} %copy-done.2, ...), custom_call_target="tpu_custom_call" | custom-call | tf_op jit(solution)/shard_map/ends/pallas_call | solution.py:341
  23.3 0.0 copy-start.23
  23.3 0.9 copy.16
  24.2 11.5 %all-to-all-start = ((f32[128,1,256]{2,1,0:T(1,128)}), f32[128,1,256]{2,1,0:T(1,128)S(1)}, u32[]{:S(2)}, u32[]{:S(2)}) async-start(f32[128,1,256]{2,1,0:T(1,128)} %copy.16), calls=%async_computation | async-start | bytes 262144 | tf_op jit(solution)/shard_map/all_to_all | solution.py:379
  35.7 0.7 constant_dynamic-slice_fusion.1
  36.4 0.0 copy-done.15
  36.4 0.0 copy-done.13
  36.4 0.0 copy-done.27
  36.4 0.0 copy-start.21
  36.4 1.6 %copy-done.21 = f32[2,2,64,16,64]{4,3,2,1,0:T(8,128)S(1)} copy-done((f32[2,2,64,16,64]{4,3,2,1,0:T(8,128)S(1)}, f32[2,2,64,16,64]{4,3,2,1,0:T(8,128)}, u32[]{:S(2)}) %copy-start.21) | copy-done | bytes 1048600
  38.0 9.8 %local_1.1 = (f32[128,512]{1,0:T(8,128)S(1)}, bf16[16,2,128,256]{3,2,1,0:T(8,128)(2,1)S(1)}, f32[16,2,2,32,128]{4,3,2,1,0:T(8,128)S(1)}) custom-call(f32[1,128]{1,0:T(1,128)S(1)} %bitcast.23, bf16[128,1024]{1,0:T(8,128)(2,1)S(1)} %get-tuple-element.17.driven, bf16[32,2,16,256]{3,2,1,0:T(8,128)(2,1)S(1)} %get-tuple-element.18.bt, ...), custom_call_target="tpu_custom_call" | custom-call | flops 2000000000 | bytes 8388608 | tf_op jit(solution)/shard_map/local_1/pallas_call | solution.py:299
  47.7 0.0 copy-done.23
  47.8 0.0 copy-done.25
  47.8 0.0 copy-start.4
  47.8 1.3 %copy-done.4 = bf16[16,2,128,256]{3,2,1,0:T(8,128)(2,1)} copy-done((bf16[16,2,128,256]{3,2,1,0:T(8,128)(2,1)}, bf16[16,2,128,256]{3,2,1,0:T(8,128)(2,1)S(1)}, u32[]{:S(2)}) %copy-start.4) | copy-done | bytes 2097176
  49.1 0.7 constant_dynamic-slice_fusion
  49.8 0.1 subtract_multiply_fusion
  49.9 0.0 all-to-all-done
  49.9 2.2 %across.1 = f32[128,128]{1,0:T(8,128)} custom-call(s32[1]{0:T(128)} %bitcast.backward, f32[128,256]{1,0:T(8,128)S(1)} %bitcast.17, f32[1,128]{1,0:T(1,128)S(1)} %get-tuple-element.28.turns_hi, f32[1,128]{1,0:T(1,128)S(1)} %get-tuple-element.27.turns_lo, f32[1,128]{1,0:T(1,128)S(1)} %get-tuple-element.29.rate), custom_call_target="tpu_custom_call" | custom-call | tf_op jit(solution)/shard_map/across/pallas_call | solution.py:382
  52.1 9.8 %all-to-all-start.1 = ((f32[128,1,128]{2,1,0:T(1,128)}), f32[128,1,128]{2,1,0:T(1,128)S(1)}, u32[]{:S(2)}, u32[]{:S(2)}) async-start(f32[128,1,128]{2,1,0:T(1,128)} %bitcast.7), calls=%async_computation.1 | async-start | bytes 131072 | tf_op jit(solution)/shard_map/all_to_all | solution.py:390
  61.9 0.0 copy-start.14
  61.9 0.7 copy-done.14
  62.6 0.0 copy-start.16
  62.6 0.8 copy-done.16
  63.4 0.0 copy-start.22
  63.4 1.6 %copy-done.22 = f32[2,2,64,16,64]{4,3,2,1,0:T(8,128)S(1)} copy-done((f32[2,2,64,16,64]{4,3,2,1,0:T(8,128)S(1)}, f32[2,2,64,16,64]{4,3,2,1,0:T(8,128)}, u32[]{:S(2)}) %copy-start.22) | copy-done | bytes 1048600
  65.0 1.0 %copy-done.24 = bf16[32,2,16,256]{3,2,1,0:T(8,128)(2,1)S(1)} copy-done((bf16[32,2,16,256]{3,2,1,0:T(8,128)(2,1)S(1)}, bf16[32,2,16,256]{3,2,1,0:T(8,128)(2,1)}, u32[]{:S(2)}) %copy-start.24) | copy-done | bytes 524312
  66.0 0.9 %copy-done.26 = bf16[128,1024]{1,0:T(8,128)(2,1)S(1)} copy-done((bf16[128,1024]{1,0:T(8,128)(2,1)S(1)}, bf16[128,1024]{1,0:T(8,128)(2,1)}, u32[]{:S(2)}) %copy-start.26) | copy-done | bytes 262168
  67.0 0.7 copy-done.28
  67.7 9.8 %local_0.1 = (f32[128,512]{1,0:T(8,128)S(1)}, bf16[16,2,128,256]{3,2,1,0:T(8,128)(2,1)S(1)}, f32[16,2,2,32,128]{4,3,2,1,0:T(8,128)S(1)}) custom-call(f32[1,128]{1,0:T(1,128)S(1)} %bitcast.24, bf16[128,1024]{1,0:T(8,128)(2,1)S(1)} %copy-done.26, bf16[32,2,16,256]{3,2,1,0:T(8,128)(2,1)S(1)} %copy-done.24, f32[2,2,64,16,64]{4,3,2,1,0:T(8,128)S(1)} %copy-done.22, ...), custom_call_target="tpu_custom_call" | custom-call | flops 2000000000 | bytes 8388608 | tf_op jit(solution)/shard_map/local_0/pallas_call | solution.py:299
  77.4 0.0 copy-start.6
  77.4 1.3 %copy-done.6 = bf16[16,2,128,256]{3,2,1,0:T(8,128)(2,1)} copy-done((bf16[16,2,128,256]{3,2,1,0:T(8,128)(2,1)}, bf16[16,2,128,256]{3,2,1,0:T(8,128)(2,1)S(1)}, u32[]{:S(2)}) %copy-start.6) | copy-done | bytes 2097176
  78.8 1.0 %copy-done.8 = f32[16,2,2,32,128]{4,3,2,1,0:T(8,128)} copy-done((f32[16,2,2,32,128]{4,3,2,1,0:T(8,128)}, f32[16,2,2,32,128]{4,3,2,1,0:T(8,128)S(1)}, u32[]{:S(2)}) %copy-start.8) | copy-done | bytes 1048600
  79.8 0.7 copy-done.11
  80.5 0.0 all-to-all-done.1
  80.5 0.0 copy-done.3
  80.5 0.0 copy-done.18
  80.5 0.0 copy-done.19
  80.5 0.0 copy-start.1
  80.5 2.2 %copy-done.1 = bf16[1024,2048]{1,0:T(8,128)(2,1)S(1)} copy-done((bf16[1024,2048]{1,0:T(8,128)(2,1)S(1)}, bf16[1024,2048]{1,0:T(8,128)(2,1)}, u32[]{:S(2)}) %copy-start.1) | copy-done | bytes 4194328
  82.7 1.6 %copy-done.5 = bf16[16,2,128,256]{3,2,1,0:T(8,128)(2,1)S(1)} copy-done((bf16[16,2,128,256]{3,2,1,0:T(8,128)(2,1)S(1)}, bf16[16,2,128,256]{3,2,1,0:T(8,128)(2,1)}, u32[]{:S(2)}) %copy-start.5) | copy-done | bytes 2097176
  84.3 1.6 %copy-done.7 = bf16[16,2,128,256]{3,2,1,0:T(8,128)(2,1)S(1)} copy-done((bf16[16,2,128,256]{3,2,1,0:T(8,128)(2,1)S(1)}, bf16[16,2,128,256]{3,2,1,0:T(8,128)(2,1)}, u32[]{:S(2)}) %copy-start.7) | copy-done | bytes 2097176
  85.9 1.2 %copy-done.9 = f32[16,2,2,32,128]{4,3,2,1,0:T(8,128)S(1)} copy-done((f32[16,2,2,32,128]{4,3,2,1,0:T(8,128)S(1)}, f32[16,2,2,32,128]{4,3,2,1,0:T(8,128)}, u32[]{:S(2)}) %copy-start.9) | copy-done | bytes 1048600
  87.1 0.9 %copy-done.12 = f32[128,512]{1,0:T(8,128)S(1)} copy-done((f32[128,512]{1,0:T(8,128)S(1)}, f32[128,512]{1,0:T(8,128)}, u32[]{:S(2)}) %copy-start.12) | copy-done | bytes 262168
  88.1 6.5 %final.1 = bf16[128,2048]{1,0:T(8,128)(2,1)} custom-call(f32[128,128]{1,0:T(8,128)S(1)} %bitcast.18, f32[128,512]{1,0:T(8,128)S(1)} %copy-done.12, f32[128,512]{1,0:T(8,128)S(1)} %get-tuple-element.20.near_b, bf16[16,2,128,256]{3,2,1,0:T(8,128)(2,1)S(1)} %copy-done.7, bf16[16,2,128,256]{3,2,1,0:T(8,128)(2,1)S(1)} %copy-done.5, ...), custom_call_target="tpu_custom_call" | custom-call | tf_op jit(solution)/shard_map/final/pallas_call | solution.py:395
  (16 shorter events, 0.1 us)
Async XLA Ops:
  1.9 34.5 %copy-start.15 = (f32[2,32,128]{2,1,0:T(8,128)}, f32[2,32,128]{2,1,0:T(8,128)S(1)}, u32[]{:S(2)}) copy-start(f32[2,32,128]{2,1,0:T(8,128)S(1)} %sqrt.3.root2) | copy-start | bytes 98308
  2.0 34.4 %copy-start.13 = (f32[2,32,128]{2,1,0:T(8,128)}, f32[2,32,128]{2,1,0:T(8,128)S(1)}, u32[]{:S(2)}) copy-start(f32[2,32,128]{2,1,0:T(8,128)S(1)} %mul.95.rates) | copy-start | bytes 98308
  2.0 4.7 %copy-start.10 = (bf16[128,2048]{1,0:T(8,128)(2,1)S(1)}, bf16[128,2048]{1,0:T(8,128)(2,1)}, u32[]{:S(2)}) copy-start(bf16[128,2048]{1,0:T(8,128)(2,1)} %tokens.1) | copy-start | bytes 1572868
  2.0 4.7 %copy-start.17 = (f32[2048]{0:T(1024)S(1)}, f32[2048]{0:T(1024)}, u32[]{:S(2)}) copy-start(f32[2048]{0:T(1024)} %param.15) | copy-start | bytes 24580
  2.0 4.7 %copy-start.20 = (f32[128]{0:T(128)S(1)}, f32[128]{0:T(128)}, u32[]{:S(2)}) copy-start(f32[128]{0:T(128)} %param.14) | copy-start | bytes 1540
  6.7 2.2 %copy-start = (bf16[2,2,64,64,16]{4,3,2,1,0:T(8,128)(2,1)S(1)}, bf16[2,2,64,64,16]{4,3,2,1,0:T(8,128)(2,1)}, u32[]{:S(2)}) copy-start(bf16[2,2,64,64,16]{4,3,2,1,0:T(8,128)(2,1)} %copy.15.inputs) | copy-start | bytes 1572868
  8.8 2.2 %copy-start.2 = (bf16[2048,1024]{1,0:T(8,128)(2,1)S(1)}, bf16[2048,1024]{1,0:T(8,128)(2,1)}, u32[]{:S(2)}) copy-start(bf16[2048,1024]{1,0:T(8,128)(2,1)} %weight.1) | copy-start | bytes 12582916
  11.0 25.3 %copy-start.27 = (f32[1024]{0:T(1024)S(1)}, f32[1024]{0:T(1024)}, u32[]{:S(2)}) copy-start(f32[1024]{0:T(1024)} %param.21) | copy-start | bytes 12292
  23.3 24.5 %copy-start.23 = (bf16[32,2,16,256]{3,2,1,0:T(8,128)(2,1)}, bf16[32,2,16,256]{3,2,1,0:T(8,128)(2,1)S(1)}, u32[]{:S(2)}) copy-start(bf16[32,2,16,256]{3,2,1,0:T(8,128)(2,1)S(1)} %get-tuple-element.18.bt) | copy-start | bytes 1572868
  23.3 24.5 %copy-start.25 = (bf16[128,1024]{1,0:T(8,128)(2,1)}, bf16[128,1024]{1,0:T(8,128)(2,1)S(1)}, u32[]{:S(2)}) copy-start(bf16[128,1024]{1,0:T(8,128)(2,1)S(1)} %get-tuple-element.17.driven) | copy-start | bytes 786436
  24.2 25.7 %all-to-all-start = ((f32[128,1,256]{2,1,0:T(1,128)}), f32[128,1,256]{2,1,0:T(1,128)S(1)}, u32[]{:S(2)}, u32[]{:S(2)}) async-start(f32[128,1,256]{2,1,0:T(1,128)} %copy.16), calls=%async_computation | async-start | bytes 262144 | tf_op jit(solution)/shard_map/all_to_all | solution.py:379
  36.4 1.6 %copy-start.21 = (f32[2,2,64,16,64]{4,3,2,1,0:T(8,128)S(1)}, f32[2,2,64,16,64]{4,3,2,1,0:T(8,128)}, u32[]{:S(2)}) copy-start(f32[2,2,64,16,64]{4,3,2,1,0:T(8,128)} %readout.3) | copy-start | bytes 3145732
  47.8 1.4 %copy-start.4 = (bf16[16,2,128,256]{3,2,1,0:T(8,128)(2,1)}, bf16[16,2,128,256]{3,2,1,0:T(8,128)(2,1)S(1)}, u32[]{:S(2)}) copy-start(bf16[16,2,128,256]{3,2,1,0:T(8,128)(2,1)S(1)} %get-tuple-element.22.prefix_b) | copy-start | bytes 6291460
  52.1 28.4 %all-to-all-start.1 = ((f32[128,1,128]{2,1,0:T(1,128)}), f32[128,1,128]{2,1,0:T(1,128)S(1)}, u32[]{:S(2)}, u32[]{:S(2)}) async-start(f32[128,1,128]{2,1,0:T(1,128)} %bitcast.7), calls=%async_computation.1 | async-start | bytes 131072 | tf_op jit(solution)/shard_map/all_to_all | solution.py:390
  61.9 0.8 copy-start.14
  62.6 0.8 copy-start.16
  63.4 1.6 %copy-start.22 = (f32[2,2,64,16,64]{4,3,2,1,0:T(8,128)S(1)}, f32[2,2,64,16,64]{4,3,2,1,0:T(8,128)}, u32[]{:S(2)}) copy-start(f32[2,2,64,16,64]{4,3,2,1,0:T(8,128)} %readout.3) | copy-start | bytes 3145732
  65.0 1.0 %copy-start.24 = (bf16[32,2,16,256]{3,2,1,0:T(8,128)(2,1)S(1)}, bf16[32,2,16,256]{3,2,1,0:T(8,128)(2,1)}, u32[]{:S(2)}) copy-start(bf16[32,2,16,256]{3,2,1,0:T(8,128)(2,1)} %copy-done.23) | copy-start | bytes 1572868
  66.0 0.9 %copy-start.26 = (bf16[128,1024]{1,0:T(8,128)(2,1)S(1)}, bf16[128,1024]{1,0:T(8,128)(2,1)}, u32[]{:S(2)}) copy-start(bf16[128,1024]{1,0:T(8,128)(2,1)} %copy-done.25) | copy-start | bytes 786436
  67.0 0.7 copy-start.28
  67.7 12.8 %copy-start.3 = (bf16[1024,1024]{1,0:T(8,128)(2,1)S(1)}, bf16[1024,1024]{1,0:T(8,128)(2,1)}, u32[]{:S(2)}) copy-start(bf16[1024,1024]{1,0:T(8,128)(2,1)} %glu.1) | copy-start | bytes 6291460
  67.7 12.8 %copy-start.18 = (f32[2048]{0:T(1024)S(1)}, f32[2048]{0:T(1024)}, u32[]{:S(2)}) copy-start(f32[2048]{0:T(1024)} %param.25) | copy-start | bytes 24580
  67.7 12.8 %copy-start.19 = (f32[1024]{0:T(1024)S(1)}, f32[1024]{0:T(1024)}, u32[]{:S(2)}) copy-start(f32[1024]{0:T(1024)} %param.23) | copy-start | bytes 12292
  77.4 1.3 %copy-start.6 = (bf16[16,2,128,256]{3,2,1,0:T(8,128)(2,1)}, bf16[16,2,128,256]{3,2,1,0:T(8,128)(2,1)S(1)}, u32[]{:S(2)}) copy-start(bf16[16,2,128,256]{3,2,1,0:T(8,128)(2,1)S(1)} %get-tuple-element.21.prefix_a) | copy-start | bytes 6291460
  78.8 1.0 %copy-start.8 = (f32[16,2,2,32,128]{4,3,2,1,0:T(8,128)}, f32[16,2,2,32,128]{4,3,2,1,0:T(8,128)S(1)}, u32[]{:S(2)}) copy-start(f32[16,2,2,32,128]{4,3,2,1,0:T(8,128)S(1)} %get-tuple-element.23.table_a) | copy-start | bytes 3145732
  79.8 0.7 copy-start.11
  80.5 2.2 %copy-start.1 = (bf16[1024,2048]{1,0:T(8,128)(2,1)S(1)}, bf16[1024,2048]{1,0:T(8,128)(2,1)}, u32[]{:S(2)}) copy-start(bf16[1024,2048]{1,0:T(8,128)(2,1)} %outw.1) | copy-start | bytes 12582916
  82.7 1.6 %copy-start.5 = (bf16[16,2,128,256]{3,2,1,0:T(8,128)(2,1)S(1)}, bf16[16,2,128,256]{3,2,1,0:T(8,128)(2,1)}, u32[]{:S(2)}) copy-start(bf16[16,2,128,256]{3,2,1,0:T(8,128)(2,1)} %copy-done.4) | copy-start | bytes 6291460
  84.3 1.6 %copy-start.7 = (bf16[16,2,128,256]{3,2,1,0:T(8,128)(2,1)S(1)}, bf16[16,2,128,256]{3,2,1,0:T(8,128)(2,1)}, u32[]{:S(2)}) copy-start(bf16[16,2,128,256]{3,2,1,0:T(8,128)(2,1)} %copy-done.6) | copy-start | bytes 6291460
  85.9 1.2 %copy-start.9 = (f32[16,2,2,32,128]{4,3,2,1,0:T(8,128)S(1)}, f32[16,2,2,32,128]{4,3,2,1,0:T(8,128)}, u32[]{:S(2)}) copy-start(f32[16,2,2,32,128]{4,3,2,1,0:T(8,128)} %copy-done.8) | copy-start | bytes 3145732
  87.1 0.9 %copy-start.12 = (f32[128,512]{1,0:T(8,128)S(1)}, f32[128,512]{1,0:T(8,128)}, u32[]{:S(2)}) copy-start(f32[128,512]{1,0:T(8,128)} %copy-done.11) | copy-start | bytes 786436
where the time goes:
time: 95.5 us; the launch traced here: 94.6 us
  Pallas kernels  40.4 us (42%)
  local copies, waits for them, and re-layouts  30.9 us (32%)
  starting transfers between devices  21.2 us (22%)
  other arithmetic  1.79 us (2%)
    unnamed x60, local copies, waits for them, and re-layouts  28.4 us
    pallas_call x2, Pallas kernels, run_local(): pl.pallas_call(functools.partial(local_kernel, half * HALF_TILES), name=f...  19.5 us
    pallas_call x1, Pallas kernels, local(): pl.pallas_call(end_kernel, name='ends', grid=(TILES,), in_specs=[whole((R...  12.2 us
    all_to_all x1, starting transfers between devices, local(): lax.all_to_all(jnp.concatenate([ends, total], axis=1), AXES, 0, 0, tiled=...  11.5 us
    all_to_all x1, starting transfers between devices, local(): entering = lax.all_to_all(carried, AXES, 0, 0, tiled=True)  9.76 us
    pallas_call x1, Pallas kernels, local(): pl.pallas_call(final_kernel, name='final', in_specs=[vmem_spec, vmem_spec...  6.51 us
    pallas_call x1, Pallas kernels, local(): pl.pallas_call(device_kernel, name='across', in_specs=[pl.BlockSpec(memor...  2.19 us
  transfers between devices with their start and end apart: 2, of which 0 were waited for; matrix products, arithmetic and copies ran while one was open for 2% of the time, Pallas kernels for 21%

commit v1 on v0

v1 whole, which is shorter than its diff:
```python
import functools
import math

import jax
import jax.numpy as jnp
from jax import lax
from jax.experimental import pallas as pl
from jax.experimental.pallas import tpu as pltpu
from jax.sharding import Mesh
from jax.sharding import PartitionSpec as P

ROWS = 128
D = 2048
CHANNELS = 1024
TILES = 8
SPAN = 16
SPANS = ROWS // SPAN
PIECES = (1, 2, 4, 1)
LOG2E = 1.0 / math.log(2.0)
EPSILON = 1e-06
AXES = ("sp", "y", "c")
VMEM = pltpu.VMEM
HIGHEST = lax.Precision.HIGHEST
F32 = jnp.float32
BF16 = jnp.bfloat16

SINE = (4.44288291, -7.30824512, 3.60634303, -0.84604096, 0.10968436)
COSINE = (1.4142135, -6.97885097, 5.73946067, -1.88355924, 0.31068962)
DAMP = (
    9.99999626e-01,
    -2.49992247e-01,
    5.20558088e-02,
    -7.77389543e-03,
    8.29541685e-04,
    -6.19250366e-05,
    2.98283721e-06,
    -7.10025954e-08,
)
SINE_SHORT = (4.44287876, -7.30776104, 3.5971931, -0.7896682)


def horner(coefficients, x):
    value = coefficients[-1] * x + coefficients[-2]
    for c in coefficients[-3::-1]:
        value = value * x + c
    return value


def unit_circle(turns, sine=SINE_SHORT):
    r = turns - jnp.round(turns)
    z = r * r
    s = r * horner(sine, z)
    c = horner(COSINE, z)
    return 1.0 - s * s, s * c


def nt(a, b):
    return lax.dot_general(a, b, (((1,), (1,)), ((), ())), preferred_element_type=F32)


def mm(a, b):
    return jnp.dot(a, b, preferred_element_type=F32)


def iotas(shape):
    return lax.broadcasted_iota(jnp.int32, shape, 0), lax.broadcasted_iota(jnp.int32, shape, 1)


def column_of(row):
    return jnp.broadcast_to(row, (ROWS, ROWS)).T


def exact_mm(a, b):
    return jnp.dot(a, b, preferred_element_type=F32, precision=HIGHEST)


def pair_row(ref, k, pair):
    return jnp.concatenate([ref[k, pl.ds(2 * pair, 1), :], ref[k, pl.ds(2 * pair + 1, 1), :]], axis=1)


def end_kernel(tokens, elapsed, gain, weight, inputs, angle, rate, driven_ref, ends_ref, pars_ref, normed, times):
    step = pl.program_id(0)
    core = lax.axis_index("c")

    @pl.when(step == 0)
    def _():
        x = tokens[...].astype(F32)
        scale = lax.rsqrt(jnp.mean(x * x, axis=-1, keepdims=True) + EPSILON)
        normed[...] = (x * scale * gain[...]).astype(BF16)
        steps = column_of(elapsed[...])
        row, col = iotas((ROWS, ROWS))
        times[0] = exact_mm((col > row).astype(F32), steps)
        times[1] = exact_mm((col < row).astype(F32), steps)
        times[2] = jnp.sqrt(steps)
        times[3] = steps
        total = exact_mm(jnp.ones((16, ROWS), F32), steps)
        ends_ref[0, 4] = total
        ends_ref[1, 4] = total

    driven = mm(normed[...], weight[...]).astype(BF16)
    driven_ref[...] = driven
    flipped = driven.astype(F32).T.astype(BF16)
    first = lax.broadcasted_iota(jnp.int32, (16, 128), 1) < 64
    away = jnp.where((step // 4) == core, 0, 1)
    for j in range(4):
        pair = step * 4 + j
        for k in range(2):
            f = pair_row(rate, k, pair)
            th = pair_row(angle, k, pair)
            pars_ref[k, 0, pl.ds(pair, 1), :] = th
            pars_ref[k, 1, pl.ds(pair, 1), :] = f
            f2 = f * 2.0
            after = times[k]
            cosine, sine = unit_circle(after * (th * (0.5 / math.pi)))
            damp = horner(DAMP, times[3] * f2) * (times[2] * jnp.sqrt(f2))
            amp = jnp.exp2(after * (f * -LOG2E)) * damp
            pull = jnp.concatenate([(amp * cosine).astype(BF16), (amp * sine).astype(BF16)], axis=1)
            mixed = mm(flipped[32 * j : 32 * j + 32], pull)
            m_re = jnp.where(first, mixed[:16, :128], mixed[16:, :128])
            m_im = jnp.where(first, mixed[:16, 128:], mixed[16:, 128:])
            b_re, b_im = (
                jnp.concatenate([inputs[k, c, 2 * j].astype(F32), inputs[k, c, 2 * j + 1].astype(F32)], axis=1)
                for c in range(2)
            )
            at = 4 * (step % 4) + j
            ends_ref[away, 2 * k, pl.ds(at, 1), :] = jnp.sum(b_re * m_re - b_im * m_im, axis=0, keepdims=True)
            ends_ref[away, 2 * k + 1, pl.ds(at, 1), :] = jnp.sum(b_re * m_im + b_im * m_re, axis=0, keepdims=True)


def local_kernel(
    offset, elapsed, driven, inputs, readout, angle, rate, skip,
    out_ref, prefix_ref, table_ref, times,
):
    step = pl.program_id(0)

    @pl.when(step == 0)
    def _():
        steps = column_of(elapsed[...])
        row, col = iotas((ROWS, ROWS))
        same = row // SPAN == col // SPAN
        times[0] = exact_mm(((col <= row) & same).astype(F32), steps)
        times[1] = exact_mm(((col >= row) & same).astype(F32), steps)
        times[2] = jnp.sqrt(steps)
        times[3] = steps

    row, col = iotas((ROWS, ROWS))
    same = row // SPAN == col // SPAN
    triangles = (((col <= row) & same).astype(BF16), ((col >= row) & same).astype(BF16))
    empty = jnp.zeros((16, 64), BF16)
    hole = jnp.zeros((16, 64), F32)
    x = driven[...]
    outs = []
    for j in range(4):
        pair = (step + offset) * 4 + j
        lhs = x[:, 32 * j : 32 * j + 32]
        total = None
        for k in range(2):
            f = pair_row(rate, k, pair)
            th = pair_row(angle, k, pair)
            f2 = f * 2.0
            b00, b01 = inputs[k, 0, 2 * j], inputs[k, 1, 2 * j]
            b10, b11 = inputs[k, 0, 2 * j + 1], inputs[k, 1, 2 * j + 1]
            rhs = jnp.concatenate(
                [
                    jnp.concatenate([b00, empty, b01, empty], axis=1),
                    jnp.concatenate([empty, b10, empty, b11], axis=1),
                ],
                axis=0,
            )
            proj = mm(lhs, rhs)
            p_re, p_im = proj[:, :128], proj[:, 128:]
            offs = times[k]
            cosine, sine = unit_circle(offs * (th * (0.5 / math.pi)))
            damp = horner(DAMP, times[3] * f2) * (times[2] * jnp.sqrt(f2))
            level = offs * (f * LOG2E)
            grow = jnp.exp2(level) * damp
            fade = jnp.exp2(-level)
            a_re, a_im = grow * cosine, grow * sine
            lift = jnp.concatenate(
                [(a_re * p_re + a_im * p_im).astype(BF16), (a_re * p_im - a_im * p_re).astype(BF16)], axis=1
            )
            part = mm(triangles[k], lift)
            e_re, e_im = fade * cosine, fade * sine
            c_re = c_im = jnp.zeros((1, 128), F32)
            d_re, d_im = jnp.ones((1, 128), F32), jnp.zeros((1, 128), F32)
            states, prefixes = [None] * SPANS, [None] * SPANS
            for n in range(SPANS) if k == 0 else range(SPANS - 1, -1, -1):
                cut = slice(SPAN * n, SPAN * n + SPAN)
                er, ei = e_re[cut], e_im[cut]
                wr, wi = part[cut, :128] + c_re, part[cut, 128:] + c_im
                sr, si = er * wr - ei * wi, er * wi + ei * wr
                pr, pi = er * d_re - ei * d_im, er * d_im + ei * d_re
                edge = slice(SPAN - 1, SPAN) if k == 0 else slice(0, 1)
                c_re, c_im, d_re, d_im = sr[edge], si[edge], pr[edge], pi[edge]
                states[n] = jnp.concatenate([sr.astype(BF16), si.astype(BF16)], axis=1)
                prefixes[n] = jnp.concatenate([pr.astype(BF16), pi.astype(BF16)], axis=1)
            prefix_ref[j, k] = jnp.concatenate(prefixes, axis=0)
            tables = []
            for c in range(2):
                upper = jnp.concatenate([readout[k, c, 2 * j], hole], axis=1)
                lower = jnp.concatenate([hole, readout[k, c, 2 * j + 1]], axis=1)
                table = jnp.concatenate([upper, lower], axis=0)
                table_ref[j, k, c] = table
                tables.append(table)
            y = nt(
                jnp.concatenate(states, axis=0),
                jnp.concatenate([tables[0].astype(BF16), (-tables[1]).astype(BF16)], axis=1),
            )
            total = y if total is None else total + y
        outs.append(total)
    out_ref[...] = jnp.concatenate(outs, axis=1) + skip[...] * x.astype(F32)


def times_of(a, b):
    return a[0] * b[0] - a[1] * b[1], a[0] * b[1] + a[1] * b[0]


def plus(a, b):
    return a[0] + b[0], a[1] + b[1]


def pick(condition, a, b):
    return tuple(jnp.where(condition, x, y) for x, y in zip(a, b))


def my_pars(pars):
    core = lax.axis_index("c")
    found = []
    for k in range(2):
        angle = pars[k, 0, pl.ds(16 * core, 16), :]
        rate = pars[k, 1, pl.ds(16 * core, 16), :]
        high = jnp.round(angle * (4096 * 0.5 / math.pi)) * (1.0 / 4096)
        coarse = 6433 / 1024
        low = ((angle - high * coarse) - high * (2 * math.pi - coarse)) * (0.5 / math.pi)
        found.append((high, low, rate * -LOG2E))
    return found


def decay_over(span, pars):
    high, low, level = pars
    u = span * high
    cosine, sine = unit_circle((u - jnp.round(u)) + span * low, SINE)
    fade = jnp.exp2(span * level)
    return fade * cosine, fade * sine


def states_of(ref, k):
    return ref[2 * k], ref[2 * k + 1]


def pair_kernel(own, other, pars, out_ref):
    core = lax.axis_index("c")
    mine = my_pars(pars)
    span, span_other = own[4], other[4]
    for k in range(2):
        ahead = core == k
        a, b = states_of(own, k), states_of(other, k)
        early, late = pick(ahead, a, b), pick(ahead, b, a)
        moved = times_of(decay_over(jnp.where(ahead, span_other, span), mine[k]), early)
        total = plus(moved, late)
        out_ref[2 * k], out_ref[2 * k + 1] = total
    out_ref[4] = span + span_other


def group_kernel(own, one, two, three, pars, send_ref, before_ref, data):
    y = lax.axis_index("y")
    here = lax.axis_index("sp")
    mine = my_pars(pars)
    data[y] = own[...]
    data[(y + 3) % 4] = one[...]
    data[(y + 2) % 4] = two[...]
    data[(y + 1) % 4] = three[...]
    zero = jnp.zeros((16, 128), F32)
    totals = []
    for k in range(2):
        state, decay = (zero, zero), (zero + 1.0, zero)
        before, before_decay = state, decay
        for n in range(4) if k == 0 else range(3, -1, -1):
            before = pick(n == y, state, before)
            before_decay = pick(n == y, decay, before_decay)
            step = decay_over(data[n, 4], mine[k])
            state = plus(times_of(step, state), (data[n, 2 * k], data[n, 2 * k + 1]))
            decay = times_of(step, decay)
        before_ref[2 * k], before_ref[2 * k + 1] = before
        before_ref[4 + 2 * k], before_ref[5 + 2 * k] = before_decay
        totals.append(state)
    span = data[0, 4] + data[1, 4] + data[2, 4] + data[3, 4]
    for n in range(16):
        sent = pick(n > here, totals[0], totals[1])
        send_ref[n, 0], send_ref[n, 1] = sent
        send_ref[n, 2] = span


def enter_kernel(seen, before, own, other, pars, mine_ref, theirs_ref):
    here = lax.axis_index("sp")
    core = lax.axis_index("c")
    mine = my_pars(pars)
    zero = jnp.zeros((16, 128), F32)
    steps = []
    for n in range(16):
        chosen = pick(n < here, mine[0], mine[1])
        steps.append(decay_over(seen[n, 2], chosen))
    for k in range(2):
        state = (zero, zero)
        for n in range(16) if k == 0 else range(15, -1, -1):
            active = n < here if k == 0 else n > here
            new = plus(times_of(steps[n], state), (seen[n, 0], seen[n, 1]))
            state = pick(active, new, state)
        state = plus(times_of((before[4 + 2 * k], before[5 + 2 * k]), state), states_of(before, k))
        ahead = core == k
        a, b = states_of(own, k), states_of(other, k)
        early = pick(ahead, a, b)
        later = plus(times_of(decay_over(jnp.where(ahead, own[4], other[4]), mine[k]), state), early)
        mine_ref[2 * k], mine_ref[2 * k + 1] = pick(ahead, state, later)
        theirs_ref[2 * k], theirs_ref[2 * k + 1] = pick(ahead, later, state)


def final_kernel(*refs):
    count = len(PIECES)
    own, other = refs[:2]
    nears, prefixes, tables = (refs[2 + count * n : 2 + count * n + count] for n in range(3))
    glu, glu_bias, outw, out_gain, out_ref, entering, response = refs[2 + 3 * count :]
    core = lax.axis_index("c")
    entering[core] = own[...]
    entering[1 - core] = other[...]
    start = 0
    for size, near, prefix, table in zip(PIECES, nears, prefixes, tables):

        def tile(i, _, start=start, near=near, prefix=prefix, table=table):
            outs = []
            for j in range(4):
                total = None
                for k in range(2):
                    pair = 4 * (start + i) + j
                    er = entering[pair // 16, 2 * k, pl.ds(pair % 16, 1), :]
                    ei = entering[pair // 16, 2 * k + 1, pl.ds(pair % 16, 1), :]
                    cr, ci = table[4 * i + j, k, 0], table[4 * i + j, k, 1]
                    rhs = jnp.concatenate(
                        [(cr * er - ci * ei).astype(BF16), (-(cr * ei + ci * er)).astype(BF16)], axis=1
                    )
                    y = nt(prefix[4 * i + j, k], rhs)
                    total = y if total is None else total + y
                outs.append(total)
            at = pl.multiple_of(128 * i, 128)
            response[:, pl.ds(at + 128 * start, 128)] = jnp.concatenate(outs, axis=1) + near[:, pl.ds(at, 128)]
            return 0

        lax.fori_loop(0, size, tile, 0)
        start += size
    x = response[...]
    active = 0.5 * x * (1.0 + jnp.tanh(math.sqrt(2.0 / math.pi) * (x + 0.044715 * (x * x * x))))
    gate = mm(active.astype(BF16), glu[...]) + glu_bias[...]
    gated = (active * jax.nn.sigmoid(gate)).astype(BF16)
    projected = mm(gated, outw[...])
    scale = lax.rsqrt(jnp.mean(projected * projected, axis=-1, keepdims=True) + EPSILON)
    out_ref[...] = (projected * scale * out_gain[...]).astype(BF16)


def whole(shape):
    return pl.BlockSpec(shape, lambda *_: (0,) * len(shape))


def sds(shape, dtype=F32):
    return jax.ShapeDtypeStruct(shape, dtype)


def params(limit):
    return pltpu.CompilerParams(vmem_limit_bytes=limit * 1024 * 1024)


def run_local(start, size, elapsed_row, driven, inputs, state_output, angle, rate, skip_row):
    row_spec = whole((2, 64, 64))
    return pl.pallas_call(
        functools.partial(local_kernel, start),
        name=f"local_{start}",
        grid=(size,),
        in_specs=[
            whole((1, ROWS)),
            pl.BlockSpec((ROWS, 128), lambda i: (0, i + start)),
            pl.BlockSpec((2, 2, 8, 16, 64), lambda i: (0, 0, i + start, 0, 0)),
            pl.BlockSpec((2, 2, 8, 16, 64), lambda i: (0, 0, i + start, 0, 0)),
            row_spec, row_spec,
            pl.BlockSpec((1, 128), lambda i: (0, i + start)),
        ],
        out_specs=[
            pl.BlockSpec((ROWS, 128), lambda i: (0, i)),
            pl.BlockSpec((4, 2, ROWS, 256), lambda i: (i, 0, 0, 0)),
            pl.BlockSpec((4, 2, 2, 32, 128), lambda i: (i, 0, 0, 0, 0)),
        ],
        out_shape=[
            sds((ROWS, 128 * size)),
            sds((4 * size, 2, ROWS, 256), BF16),
            sds((4 * size, 2, 2, 32, 128)),
        ],
        scratch_shapes=[VMEM((4, ROWS, ROWS), F32)],
        compiler_params=params(10),
        cost_estimate=pl.CostEstimate(flops=size * 5 * 10**8, bytes_accessed=size * 2 * 2**20, transcendentals=0),
    )(elapsed_row, driven, inputs, state_output, angle, rate, skip_row)


def simple(kernel, name, shapes, args, scratch=()):
    spec = pl.BlockSpec(memory_space=VMEM)
    return pl.pallas_call(
        kernel,
        name=name,
        in_specs=[spec] * len(args),
        out_specs=[spec] * len(shapes),
        out_shape=[sds(shape) for shape in shapes],
        scratch_shapes=scratch,
        compiler_params=params(4),
    )(*args)


def local(
    tokens, elapsed, norm_gain, in_weight, state_input, state_output, forget_rate, decay_angle,
    skip_gain, glu_weight, glu_bias, out_weight, out_gain,
):
    elapsed_row = elapsed.reshape(1, ROWS)
    inputs = jnp.swapaxes(state_input, 3, 4)
    row_spec = whole((2, 64, 64))
    driven, ends, pars = pl.pallas_call(
        end_kernel,
        name="ends",
        grid=(TILES,),
        in_specs=[
            whole((ROWS, D)),
            whole((1, ROWS)),
            whole((1, D)),
            pl.BlockSpec((D, 128), lambda i: (0, i)),
            pl.BlockSpec((2, 2, 8, 16, 64), lambda i: (0, 0, i, 0, 0)),
            row_spec, row_spec,
        ],
        out_specs=[
            pl.BlockSpec((ROWS, 128), lambda i: (0, i)),
            whole((2, 5, 16, 128)),
            whole((2, 2, 32, 128)),
        ],
        out_shape=[sds((ROWS, CHANNELS), BF16), sds((2, 5, 16, 128)), sds((2, 2, 32, 128))],
        scratch_shapes=[VMEM((ROWS, D), BF16), VMEM((4, ROWS, ROWS), F32)],
        compiler_params=params(10),
    )(
        tokens, elapsed_row, norm_gain.reshape(1, D), hbm(in_weight), hbm(inputs), decay_angle, forget_rate
    )

    skip_row = skip_gain.reshape(1, CHANNELS)
    pieces, start = [], 0
    for size in PIECES:
        pieces.append(
            run_local(
                start, size, elapsed_row, driven, inputs, state_output, decay_angle, forget_rate, skip_row
            )
        )
        start += size

    swap = [(0, 1), (1, 0)]
    keep = ends[0]
    partner = lax.ppermute(ends[1], "c", swap)
    (pair,) = simple(pair_kernel, "pair", [(5, 16, 128)], (keep, partner, pars))
    shifted = [lax.ppermute(pair, "y", [(i, (i + n) % 4) for i in range(4)]) for n in (2, 1, 3)]
    two, one, three = shifted
    send, before = simple(
        group_kernel, "group", [(16, 3, 16, 128), (8, 16, 128)], (pair, one, two, three, pars),
        [VMEM((4, 5, 16, 128), F32)],
    )
    seen = lax.all_to_all(send, "sp", 0, 0, tiled=True)
    mine, theirs = simple(
        enter_kernel, "enter", [(4, 16, 128), (4, 16, 128)], (seen, before, keep, partner, pars)
    )
    other = lax.ppermute(theirs, "c", swap)

    spec = pl.BlockSpec(memory_space=VMEM)
    args = (
        mine, other, *(p[0] for p in pieces), *(p[1] for p in pieces), *(p[2] for p in pieces),
        glu_weight, glu_bias.reshape(1, CHANNELS), out_weight, out_gain.reshape(1, D),
    )
    return pl.pallas_call(
        final_kernel,
        name="final",
        in_specs=[spec] * len(args),
        out_specs=spec,
        out_shape=sds((ROWS, D), BF16),
        scratch_shapes=[VMEM((2, 4, 16, 128), F32), VMEM((ROWS, CHANNELS), F32)],
        compiler_params=params(24),
    )(*args)


def hbm(x):
    return pltpu.with_memory_space_constraint(x, pltpu.HBM)


def solution(mesh):
    finer = Mesh(mesh.devices.reshape(16, 4, 2), AXES)
    split = P(AXES, None)
    placed = (split, P(AXES), P(), P(), P(), P(), P(), P(), P(), P(), P(), P(), P())
    return jax.shard_map(local, mesh=finer, in_specs=placed, out_specs=split, check_vma=False)
```

time: 95.5 us -> 86.9 us (0.910)
  starting transfers between devices: 21.2 us -> 15.3 us
  waiting for transfers between devices: 0.01 us -> 4.63 us
  Pallas kernels: 40.4 us -> 36.3 us
  other arithmetic: 1.79 us -> 0 us
  local copies, waits for them, and re-layouts: 30.9 us -> 29.4 us
    all_to_all x2 -> x1, starting transfers between devices: 21.2 us -> 7.59 us  [local(): seen = lax.all_to_all(send, 'sp', 0, 0, tiled=True)]
    ppermute x0 -> x5, starting transfers between devices: none -> 7.73 us  [the longest x3 3.96 us: local(): lax.ppermute(pair, 'y', [(i, (i + n) % 4) for i in range(4)])]
    ppermute x0 -> x5, waiting for transfers between devices: none -> 4.62 us  [the longest x3 3.75 us: local(): lax.ppermute(pair, 'y', [(i, (i + n) % 4) for i in range(4)])]
    pallas_call x4 -> x8, Pallas kernels: 28.2 us -> 25.3 us  [the longest x4 20.1 us: run_local(): pl.pallas_call(functools.partial(local_kernel, start), name=f'local_{star...]
    mul x3 -> x0, other arithmetic: 1.78 us -> none  [the longest x1 0.85 us: local(): rate * 2.0]
    dynamic_slice x2 -> x0, local copies, waits for them, and re-layouts: 1.39 us -> none  [the longest x1 0.7 us: local(): lax.dynamic_slice(decay_angle.reshape(128, 64), (me, 0), (1, 64))]
    pallas_call x1, Pallas kernels: 12.2 us -> 11 us  [local(): pl.pallas_call(end_kernel, name='ends', grid=(TILES,), in_specs=[whole((R...]
    unnamed x60 -> x94, local copies, waits for them, and re-layouts: 28.4 us -> 29.4 us
  transfers between devices with their start and end apart: 2 -> 6, of which waited for: 0 -> 4; matrix products, arithmetic and copies ran while one was open for 2% -> 0% of each run, Pallas kernels for 21% -> 23%
where the time goes in v1:
time: 86.9 us; the launch traced here: 85.9 us
  Pallas kernels  36.3 us (42%)
  local copies, waits for them, and re-layouts  29.4 us (34%)
  starting transfers between devices  15.3 us (18%)
  waiting for transfers between devices  4.63 us (5%)
    unnamed x94, local copies, waits for them, and re-layouts  29.4 us
    pallas_call x4, Pallas kernels, run_local(): pl.pallas_call(functools.partial(local_kernel, start), name=f'local_{star...  20.1 us
    pallas_call x1, Pallas kernels, local(): pl.pallas_call(end_kernel, name='ends', grid=(TILES,), in_specs=[whole((R...  11 us
    all_to_all x1, starting transfers between devices, local(): seen = lax.all_to_all(send, 'sp', 0, 0, tiled=True)  7.59 us
    pallas_call x1, Pallas kernels, local(): pl.pallas_call(final_kernel, name='final', in_specs=[spec] * len(args), o...  4.73 us
    ppermute x3, starting transfers between devices, local(): lax.ppermute(pair, 'y', [(i, (i + n) % 4) for i in range(4)])  3.96 us
    ppermute x3, waiting for transfers between devices, local(): lax.ppermute(pair, 'y', [(i, (i + n) % 4) for i in range(4)])  3.75 us
    ppermute x1, starting transfers between devices, local(): other = lax.ppermute(theirs, 'c', swap)  2.31 us
  transfers between devices with their start and end apart: 6, of which 4 were waited for; matrix products, arithmetic and copies ran while one was open for 0% of the time, Pallas kernels for 23%

profile of v1, /device:TPU:1, one launch (start us, length us, event | category | flops | bytes accessed | tf_op | source)
XLA Modules:
  0.0 85.9 jit_solution(2881899105802062164)
XLA Ops:
  0.0 0.8 copy-done.13
  0.8 0.8 copy-done.16
  1.7 1.0 %copy-done.21 = bf16[128,2048]{1,0:T(8,128)(2,1)S(1)} copy-done((bf16[128,2048]{1,0:T(8,128)(2,1)S(1)}, bf16[128,2048]{1,0:T(8,128)(2,1)}, u32[]{:S(2)}) %copy-start.21) | copy-done | bytes 524312
  2.7 0.7 copy-done.42
  3.4 0.7 copy-done.44
  4.1 11.0 %ends.1 = (bf16[128,1024]{1,0:T(8,128)(2,1)S(1)}, f32[2,5,16,128]{3,2,1,0:T(8,128)S(1)}, f32[2,2,32,128]{3,2,1,0:T(8,128)S(1)}) custom-call(bf16[128,2048]{1,0:T(8,128)(2,1)S(1)} %copy-done.21, f32[1,128]{1,0:T(1,128)S(1)} %bitcast.21, f32[1,2048]{1,0:T(1,128)S(1)} %bitcast.19, bf16[2048,1024]{1,0:T(8,128)(2,1)} %weight.1, ...), custom_call_target="tpu_custom_call" | custom-call | tf_op jit(solution)/shard_map/ends/pallas_call | solution.py:421
  15.1 0.7 copy-done.6
  15.8 1.5 %collective-permute-start = (f32[5,16,128]{2,1,0:T(8,128)S(1)}, f32[5,16,128]{2,1,0:T(8,128)S(1)}, u32[]{:S(2)}, u32[]{:S(2)}) collective-permute-start(f32[5,16,128]{2,1,0:T(8,128)S(1)} %get-tuple-element.43), channel_id=1, source_target_pairs={{0,1},{1,0},{2,3},{3,2},{4,5},{5,4},{6,7},{7,6},{8,9},{9,8},{10,11... | collective-permute-start | bytes 122888 | tf_op jit(solution)/shard_map/ppermute | solution.py:457
  17.2 0.9 %collective-permute-done.other = f32[5,16,128]{2,1,0:T(8,128)S(1)} collective-permute-done((f32[5,16,128]{2,1,0:T(8,128)S(1)}, f32[5,16,128]{2,1,0:T(8,128)S(1)}, u32[]{:S(2)}, u32[]{:S(2)}) %collective-permute-start) | collective-permute-done | bytes 40992 | tf_op jit(solution)/shard_map/ppermute | solution.py:457
  18.1 2.9 %collective-permute-start.3 = (f32[5,16,128]{2,1,0:T(8,128)S(1)}, f32[5,16,128]{2,1,0:T(8,128)S(1)}, u32[]{:S(2)}, u32[]{:S(2)}) collective-permute-start(f32[5,16,128]{2,1,0:T(8,128)S(1)} %pair.1.own), channel_id=1, source_target_pairs={{0,6},{2,0},{4,2},{6,4},{1,7},{3,1},{5,3},{7,5},{8,14},{10,8},{12,... | collective-permute-start | bytes 122888 | tf_op jit(solution)/shard_map/ppermute | solution.py:459
  21.1 0.3 collective-permute-start.2
  21.4 0.7 collective-permute-start.1
  22.1 0.1 collective-permute-done.3.three
  22.2 3.3 %collective-permute-done.2.two = f32[5,16,128]{2,1,0:T(8,128)S(1)} collective-permute-done((f32[5,16,128]{2,1,0:T(8,128)S(1)}, f32[5,16,128]{2,1,0:T(8,128)S(1)}, u32[]{:S(2)}, u32[]{:S(2)}) %collective-permute-start.2) | collective-permute-done | bytes 40992 | tf_op jit(solution)/shard_map/ppermute | solution.py:459
  25.5 0.0 copy-done.33
  25.5 0.4 collective-permute-done.1.one
  25.9 0.2 group.1
  26.0 0.7 copy-done.26
  26.8 0.6 copy-done.39
  27.4 7.6 %all-to-all-start = ((f32[16,3,16,128]{3,2,1,0:T(8,128)}), f32[16,3,16,128]{3,2,1,0:T(8,128)S(1)}, u32[]{:S(2)}, u32[]{:S(2)}) async-start(f32[16,3,16,128]{3,2,1,0:T(8,128)} %copy-done.26), calls=%async_computation | async-start | bytes 786432 | tf_op jit(solution)/shard_map/all_to_all | solution.py:465
  35.1 0.9 %copy-done.7 = bf16[128,1024]{1,0:T(8,128)(2,1)S(1)} copy-done((bf16[128,1024]{1,0:T(8,128)(2,1)S(1)}, bf16[128,1024]{1,0:T(8,128)(2,1)}, u32[]{:S(2)}) %copy-start.7) | copy-done | bytes 262168
  36.0 0.8 copy-done.14
  36.8 0.8 copy-done.17
  37.7 2.3 %local_7.1 = (f32[128,128]{1,0:T(8,128)S(1)}, bf16[4,2,128,256]{3,2,1,0:T(8,128)(2,1)S(1)}, f32[4,2,2,32,128]{4,3,2,1,0:T(8,128)S(1)}) custom-call(f32[1,128]{1,0:T(1,128)S(1)} %bitcast.22, bf16[128,1024]{1,0:T(8,128)(2,1)S(1)} %copy-done.7, bf16[2,2,64,16,64]{4,3,2,1,0:T(8,128)(2,1)S(1)} %bitcast.11, f32[2,2,64,16,64]{4,3,2,1,0:T(8,128)S(1)} %copy-done.1, ...), custom_call_target="tpu_custom_call" | custom-call | flops 500000000 | bytes 2097152 | tf_op jit(solution)/shard_map/local_7/pallas_call | solution.py:373
  40.0 0.0 copy-start.22
  40.0 0.8 copy-done.22
  40.8 0.7 copy-done.29
  41.4 0.6 copy-done.37
  42.1 5.3 %local_1.1 = (f32[128,256]{1,0:T(8,128)S(1)}, bf16[8,2,128,256]{3,2,1,0:T(8,128)(2,1)S(1)}, f32[8,2,2,32,128]{4,3,2,1,0:T(8,128)S(1)}) custom-call(f32[1,128]{1,0:T(1,128)S(1)} %bitcast.23, bf16[128,1024]{1,0:T(8,128)(2,1)S(1)} %copy-done.7, bf16[2,2,64,16,64]{4,3,2,1,0:T(8,128)(2,1)S(1)} %bitcast.12, f32[2,2,64,16,64]{4,3,2,1,0:T(8,128)S(1)} %copy-done.1, ...), custom_call_target="tpu_custom_call" | custom-call | flops 1000000000 | bytes 4194304 | tf_op jit(solution)/shard_map/local_1/pallas_call | solution.py:373
  47.4 1.0 %copy-done.9 = bf16[8,2,128,256]{3,2,1,0:T(8,128)(2,1)} copy-done((bf16[8,2,128,256]{3,2,1,0:T(8,128)(2,1)}, bf16[8,2,128,256]{3,2,1,0:T(8,128)(2,1)S(1)}, u32[]{:S(2)}) %copy-start.9) | copy-done | bytes 1048600
  48.3 0.8 copy-done.24
  49.1 0.7 copy-done.35
  49.8 10.2 %local_3.1 = (f32[128,512]{1,0:T(8,128)S(1)}, bf16[16,2,128,256]{3,2,1,0:T(8,128)(2,1)S(1)}, f32[16,2,2,32,128]{4,3,2,1,0:T(8,128)S(1)}) custom-call(f32[1,128]{1,0:T(1,128)S(1)} %bitcast.24, bf16[128,1024]{1,0:T(8,128)(2,1)S(1)} %copy-done.7, bf16[2,2,64,16,64]{4,3,2,1,0:T(8,128)(2,1)S(1)} %bitcast.13, f32[2,2,64,16,64]{4,3,2,1,0:T(8,128)S(1)} %copy-done.1, ...), custom_call_target="tpu_custom_call" | custom-call | flops 2000000000 | bytes 8388608 | tf_op jit(solution)/shard_map/local_3/pallas_call | solution.py:373
  60.0 0.0 copy-start.4
  60.1 1.4 %copy-done.4 = bf16[16,2,128,256]{3,2,1,0:T(8,128)(2,1)} copy-done((bf16[16,2,128,256]{3,2,1,0:T(8,128)(2,1)}, bf16[16,2,128,256]{3,2,1,0:T(8,128)(2,1)S(1)}, u32[]{:S(2)}) %copy-start.4) | copy-done | bytes 2097176
  61.4 1.0 %copy-done.11 = f32[16,2,2,32,128]{4,3,2,1,0:T(8,128)} copy-done((f32[16,2,2,32,128]{4,3,2,1,0:T(8,128)}, f32[16,2,2,32,128]{4,3,2,1,0:T(8,128)S(1)}, u32[]{:S(2)}) %copy-start.11) | copy-done | bytes 1048600
  62.4 0.7 copy-done.31
  63.1 0.0 all-to-all-done.seen
  63.1 1.0 %copy-done.20 = f32[2,2,32,128]{3,2,1,0:T(8,128)S(1)} copy-done((f32[2,2,32,128]{3,2,1,0:T(8,128)S(1)}, f32[2,2,32,128]{3,2,1,0:T(8,128)}, u32[]{:S(2)}) %copy-start.20) | copy-done | bytes 65560
  64.1 0.8 copy-done.28
  64.9 0.8 copy-done.34
  65.7 0.8 copy-done.40
  66.5 0.3 enter.1
  66.8 2.3 %collective-permute-start.4 = (f32[4,16,128]{2,1,0:T(8,128)S(1)}, f32[4,16,128]{2,1,0:T(8,128)S(1)}, u32[]{:S(2)}, u32[]{:S(2)}) collective-permute-start(f32[4,16,128]{2,1,0:T(8,128)S(1)} %get-tuple-element.29), channel_id=1, source_target_pairs={{0,1},{1,0},{2,3},{3,2},{4,5},{5,4},{6,7},{7,6},{8,9},{9,8},{10,11... | collective-permute-start | bytes 98312 | tf_op jit(solution)/shard_map/ppermute | solution.py:469
  69.1 0.9 %copy-done.8 = bf16[128,1024]{1,0:T(8,128)(2,1)S(1)} copy-done((bf16[128,1024]{1,0:T(8,128)(2,1)S(1)}, bf16[128,1024]{1,0:T(8,128)(2,1)}, u32[]{:S(2)}) %copy-start.8) | copy-done | bytes 262168
  70.1 0.8 copy-done.15
  70.9 0.8 copy-done.18
  71.8 0.0 copy-start.46
  71.8 2.3 %local_0.1 = (f32[128,128]{1,0:T(8,128)S(1)}, bf16[4,2,128,256]{3,2,1,0:T(8,128)(2,1)S(1)}, f32[4,2,2,32,128]{4,3,2,1,0:T(8,128)S(1)}) custom-call(f32[1,128]{1,0:T(1,128)S(1)} %bitcast.25, bf16[128,1024]{1,0:T(8,128)(2,1)S(1)} %copy-done.8, bf16[2,2,64,16,64]{4,3,2,1,0:T(8,128)(2,1)S(1)} %bitcast.14, f32[2,2,64,16,64]{4,3,2,1,0:T(8,128)S(1)} %copy-done.1, ...), custom_call_target="tpu_custom_call" | custom-call | flops 500000000 | bytes 2097152 | tf_op jit(solution)/shard_map/local_0/pallas_call | solution.py:373
  74.1 0.0 collective-permute-done.4.refs_1_
  74.1 0.0 copy-done.43
  74.1 0.0 copy-done.3
  74.1 0.0 copy-done.10
  74.1 0.0 copy-done.23
  74.1 0.0 copy-done.30
  74.1 0.0 copy-done.36
  74.1 0.0 copy-done.38
  74.2 0.0 copy-start.2
  74.2 2.2 %copy-done.2 = bf16[1024,2048]{1,0:T(8,128)(2,1)S(1)} copy-done((bf16[1024,2048]{1,0:T(8,128)(2,1)S(1)}, bf16[1024,2048]{1,0:T(8,128)(2,1)}, u32[]{:S(2)}) %copy-start.2) | copy-done | bytes 4194328
  76.3 1.6 %copy-done.5 = bf16[16,2,128,256]{3,2,1,0:T(8,128)(2,1)S(1)} copy-done((bf16[16,2,128,256]{3,2,1,0:T(8,128)(2,1)S(1)}, bf16[16,2,128,256]{3,2,1,0:T(8,128)(2,1)}, u32[]{:S(2)}) %copy-start.5) | copy-done | bytes 2097176
  77.9 1.2 %copy-done.12 = f32[16,2,2,32,128]{4,3,2,1,0:T(8,128)S(1)} copy-done((f32[16,2,2,32,128]{4,3,2,1,0:T(8,128)S(1)}, f32[16,2,2,32,128]{4,3,2,1,0:T(8,128)}, u32[]{:S(2)}) %copy-start.12) | copy-done | bytes 1048600
  79.2 1.0 %copy-done.25 = f32[8,2,2,32,128]{4,3,2,1,0:T(8,128)S(1)} copy-done((f32[8,2,2,32,128]{4,3,2,1,0:T(8,128)S(1)}, f32[8,2,2,32,128]{4,3,2,1,0:T(8,128)}, u32[]{:S(2)}) %copy-start.25) | copy-done | bytes 524312
  80.2 0.9 %copy-done.32 = f32[128,512]{1,0:T(8,128)S(1)} copy-done((f32[128,512]{1,0:T(8,128)S(1)}, f32[128,512]{1,0:T(8,128)}, u32[]{:S(2)}) %copy-start.32) | copy-done | bytes 262168
  81.2 4.7 %final.1 = bf16[128,2048]{1,0:T(8,128)(2,1)} custom-call(f32[4,16,128]{2,1,0:T(8,128)S(1)} %get-tuple-element.28.refs_0_, f32[4,16,128]{2,1,0:T(8,128)S(1)} %collective-permute-done.4.refs_1_, f32[128,128]{1,0:T(8,128)S(1)} %get-tuple-element.31.refs_2_, f32[128,256]{1,0:T(8,128)S(1)} %copy-done.36, f32[128,512]{1,0:T(8,128)S(1)} %copy-done.32, ...), custom_call_target="tpu_custom_call" | custom-call | tf_op jit(solution)/shard_map/final/pallas_call | solution.py:476
  (52 shorter events, 0.1 us)
Async XLA Ops:
  0.0 0.8 copy-start.13
  0.8 0.8 copy-start.16
  1.7 1.0 %copy-start.21 = (bf16[128,2048]{1,0:T(8,128)(2,1)S(1)}, bf16[128,2048]{1,0:T(8,128)(2,1)}, u32[]{:S(2)}) copy-start(bf16[128,2048]{1,0:T(8,128)(2,1)} %tokens.1) | copy-start | bytes 1572868
  2.7 0.7 copy-start.42
  3.4 0.7 copy-start.44
  4.1 30.9 %copy-start.1 = (f32[2,2,64,16,64]{4,3,2,1,0:T(8,128)S(1)}, f32[2,2,64,16,64]{4,3,2,1,0:T(8,128)}, u32[]{:S(2)}) copy-start(f32[2,2,64,16,64]{4,3,2,1,0:T(8,128)} %readout.7) | copy-start | bytes 3145732
  4.1 30.9 %copy-start.41 = (f32[1024]{0:T(1024)S(1)}, f32[1024]{0:T(1024)}, u32[]{:S(2)}) copy-start(f32[1024]{0:T(1024)} %param.21) | copy-start | bytes 12292
  4.1 30.9 %copy-start.45 = (f32[128]{0:T(128)S(1)}, f32[128]{0:T(128)}, u32[]{:S(2)}) copy-start(f32[128]{0:T(128)} %param.14) | copy-start | bytes 1540
  15.1 0.7 copy-start.6
  15.7 10.1 %copy-start.19 = (f32[2,2,32,128]{3,2,1,0:T(8,128)}, f32[2,2,32,128]{3,2,1,0:T(8,128)S(1)}, u32[]{:S(2)}) copy-start(f32[2,2,32,128]{3,2,1,0:T(8,128)S(1)} %get-tuple-element.25.pars) | copy-start | bytes 196612
  15.7 19.3 %copy-start = (bf16[2,2,64,64,16]{3,4,2,1,0:T(8,128)(2,1)S(1)}, bf16[2,2,64,64,16]{3,4,2,1,0:T(8,128)(2,1)}, u32[]{:S(2)}) copy-start(bf16[2,2,64,64,16]{3,4,2,1,0:T(8,128)(2,1)} %param.17) | copy-start | bytes 1572868
  15.8 10.3 %copy-start.27 = (f32[5,16,128]{2,1,0:T(8,128)}, f32[5,16,128]{2,1,0:T(8,128)S(1)}, u32[]{:S(2)}) copy-start(f32[5,16,128]{2,1,0:T(8,128)S(1)} %get-tuple-element.44.own) | copy-start | bytes 122884
  15.8 2.3 %collective-permute-start = (f32[5,16,128]{2,1,0:T(8,128)S(1)}, f32[5,16,128]{2,1,0:T(8,128)S(1)}, u32[]{:S(2)}, u32[]{:S(2)}) collective-permute-start(f32[5,16,128]{2,1,0:T(8,128)S(1)} %get-tuple-element.43), channel_id=1, source_target_pairs={{0,1},{1,0},{2,3},{3,2},{4,5},{5,4},{6,7},{7,6},{8,9},{9,8},{10,11... | collective-permute-start | bytes 122888 | tf_op jit(solution)/shard_map/ppermute | solution.py:457
  18.1 7.4 %copy-start.33 = (f32[5,16,128]{2,1,0:T(8,128)}, f32[5,16,128]{2,1,0:T(8,128)S(1)}, u32[]{:S(2)}) copy-start(f32[5,16,128]{2,1,0:T(8,128)S(1)} %collective-permute-done.other) | copy-start | bytes 122884
  18.1 4.0 %collective-permute-start.3 = (f32[5,16,128]{2,1,0:T(8,128)S(1)}, f32[5,16,128]{2,1,0:T(8,128)S(1)}, u32[]{:S(2)}, u32[]{:S(2)}) collective-permute-start(f32[5,16,128]{2,1,0:T(8,128)S(1)} %pair.1.own), channel_id=1, source_target_pairs={{0,6},{2,0},{4,2},{6,4},{1,7},{3,1},{5,3},{7,5},{8,14},{10,8},{12,... | collective-permute-start | bytes 122888 | tf_op jit(solution)/shard_map/ppermute | solution.py:459
  21.1 4.4 %collective-permute-start.2 = (f32[5,16,128]{2,1,0:T(8,128)S(1)}, f32[5,16,128]{2,1,0:T(8,128)S(1)}, u32[]{:S(2)}, u32[]{:S(2)}) collective-permute-start(f32[5,16,128]{2,1,0:T(8,128)S(1)} %pair.1.own), channel_id=1, source_target_pairs={{0,4},{2,6},{4,0},{6,2},{1,5},{3,7},{5,1},{7,3},{8,12},{10,14},{12... | collective-permute-start | bytes 122888 | tf_op jit(solution)/shard_map/ppermute | solution.py:459
  21.4 4.4 %collective-permute-start.1 = (f32[5,16,128]{2,1,0:T(8,128)S(1)}, f32[5,16,128]{2,1,0:T(8,128)S(1)}, u32[]{:S(2)}, u32[]{:S(2)}) collective-permute-start(f32[5,16,128]{2,1,0:T(8,128)S(1)} %pair.1.own), channel_id=1, source_target_pairs={{0,2},{2,4},{4,6},{6,0},{1,3},{3,5},{5,7},{7,1},{8,10},{10,12},{12... | collective-permute-start | bytes 122888 | tf_op jit(solution)/shard_map/ppermute | solution.py:459
  26.0 0.8 copy-start.26
  26.8 0.6 copy-start.39
  27.4 35.7 %all-to-all-start = ((f32[16,3,16,128]{3,2,1,0:T(8,128)}), f32[16,3,16,128]{3,2,1,0:T(8,128)S(1)}, u32[]{:S(2)}, u32[]{:S(2)}) async-start(f32[16,3,16,128]{3,2,1,0:T(8,128)} %copy-done.26), calls=%async_computation | async-start | bytes 786432 | tf_op jit(solution)/shard_map/all_to_all | solution.py:465
  35.0 1.0 %copy-start.7 = (bf16[128,1024]{1,0:T(8,128)(2,1)S(1)}, bf16[128,1024]{1,0:T(8,128)(2,1)}, u32[]{:S(2)}) copy-start(bf16[128,1024]{1,0:T(8,128)(2,1)} %copy-done.6) | copy-start | bytes 786436
  36.0 0.8 copy-start.14
  36.8 0.8 copy-start.17
  40.0 0.8 copy-start.22
  40.7 0.7 copy-start.29
  41.4 0.6 copy-start.37
  47.4 1.0 %copy-start.9 = (bf16[8,2,128,256]{3,2,1,0:T(8,128)(2,1)}, bf16[8,2,128,256]{3,2,1,0:T(8,128)(2,1)S(1)}, u32[]{:S(2)}) copy-start(bf16[8,2,128,256]{3,2,1,0:T(8,128)(2,1)S(1)} %get-tuple-element.36.refs_7_) | copy-start | bytes 3145732
  48.3 0.8 copy-start.24
  49.1 0.7 copy-start.35
  49.8 24.3 %copy-start.43 = (f32[2048]{0:T(1024)S(1)}, f32[2048]{0:T(1024)}, u32[]{:S(2)}) copy-start(f32[2048]{0:T(1024)} %param.25) | copy-start | bytes 24580
  60.0 1.4 %copy-start.4 = (bf16[16,2,128,256]{3,2,1,0:T(8,128)(2,1)}, bf16[16,2,128,256]{3,2,1,0:T(8,128)(2,1)S(1)}, u32[]{:S(2)}) copy-start(bf16[16,2,128,256]{3,2,1,0:T(8,128)(2,1)S(1)} %get-tuple-element.37.refs_8_) | copy-start | bytes 6291460
  61.4 1.0 %copy-start.11 = (f32[16,2,2,32,128]{4,3,2,1,0:T(8,128)}, f32[16,2,2,32,128]{4,3,2,1,0:T(8,128)S(1)}, u32[]{:S(2)}) copy-start(f32[16,2,2,32,128]{4,3,2,1,0:T(8,128)S(1)} %get-tuple-element.41.refs_12_) | copy-start | bytes 3145732
  62.4 0.7 copy-start.31
  63.1 11.0 %copy-start.3 = (bf16[1024,1024]{1,0:T(8,128)(2,1)S(1)}, bf16[1024,1024]{1,0:T(8,128)(2,1)}, u32[]{:S(2)}) copy-start(bf16[1024,1024]{1,0:T(8,128)(2,1)} %refs_14_.1) | copy-start | bytes 6291460
  63.1 1.0 %copy-start.20 = (f32[2,2,32,128]{3,2,1,0:T(8,128)S(1)}, f32[2,2,32,128]{3,2,1,0:T(8,128)}, u32[]{:S(2)}) copy-start(f32[2,2,32,128]{3,2,1,0:T(8,128)} %copy-done.19) | copy-start | bytes 196612
  64.1 0.8 copy-start.28
  64.9 0.8 copy-start.34
  65.7 0.8 copy-start.40
  66.8 7.3 %collective-permute-start.4 = (f32[4,16,128]{2,1,0:T(8,128)S(1)}, f32[4,16,128]{2,1,0:T(8,128)S(1)}, u32[]{:S(2)}, u32[]{:S(2)}) collective-permute-start(f32[4,16,128]{2,1,0:T(8,128)S(1)} %get-tuple-element.29), channel_id=1, source_target_pairs={{0,1},{1,0},{2,3},{3,2},{4,5},{5,4},{6,7},{7,6},{8,9},{9,8},{10,11... | collective-permute-start | bytes 98312 | tf_op jit(solution)/shard_map/ppermute | solution.py:469
  69.1 0.9 %copy-start.8 = (bf16[128,1024]{1,0:T(8,128)(2,1)S(1)}, bf16[128,1024]{1,0:T(8,128)(2,1)}, u32[]{:S(2)}) copy-start(bf16[128,1024]{1,0:T(8,128)(2,1)} %copy-done.6) | copy-start | bytes 786436
  70.1 0.8 copy-start.15
  70.9 0.8 copy-start.18
  71.7 2.3 %copy-start.10 = (bf16[8,2,128,256]{3,2,1,0:T(8,128)(2,1)S(1)}, bf16[8,2,128,256]{3,2,1,0:T(8,128)(2,1)}, u32[]{:S(2)}) copy-start(bf16[8,2,128,256]{3,2,1,0:T(8,128)(2,1)} %copy-done.9) | copy-start | bytes 3145732
  71.8 2.4 %copy-start.23 = (bf16[4,2,128,256]{3,2,1,0:T(8,128)(2,1)S(1)}, bf16[4,2,128,256]{3,2,1,0:T(8,128)(2,1)}, u32[]{:S(2)}) copy-start(bf16[4,2,128,256]{3,2,1,0:T(8,128)(2,1)} %copy-done.22) | copy-start | bytes 1572868
  71.8 2.4 %copy-start.30 = (f32[4,2,2,32,128]{4,3,2,1,0:T(8,128)S(1)}, f32[4,2,2,32,128]{4,3,2,1,0:T(8,128)}, u32[]{:S(2)}) copy-start(f32[4,2,2,32,128]{4,3,2,1,0:T(8,128)} %copy-done.29) | copy-start | bytes 786436
  71.8 2.4 %copy-start.36 = (f32[128,256]{1,0:T(8,128)S(1)}, f32[128,256]{1,0:T(8,128)}, u32[]{:S(2)}) copy-start(f32[128,256]{1,0:T(8,128)} %copy-done.35) | copy-start | bytes 393220
  71.8 2.4 %copy-start.38 = (f32[128,128]{1,0:T(8,128)S(1)}, f32[128,128]{1,0:T(8,128)}, u32[]{:S(2)}) copy-start(f32[128,128]{1,0:T(8,128)} %copy-done.37) | copy-start | bytes 196612
  71.8 2.4 %copy-start.46 = (f32[1024]{0:T(1024)S(1)}, f32[1024]{0:T(1024)}, u32[]{:S(2)}) copy-start(f32[1024]{0:T(1024)} %param.23) | copy-start | bytes 12292
  74.2 2.2 %copy-start.2 = (bf16[1024,2048]{1,0:T(8,128)(2,1)S(1)}, bf16[1024,2048]{1,0:T(8,128)(2,1)}, u32[]{:S(2)}) copy-start(bf16[1024,2048]{1,0:T(8,128)(2,1)} %refs_16_.1) | copy-start | bytes 12582916
  76.3 1.6 %copy-start.5 = (bf16[16,2,128,256]{3,2,1,0:T(8,128)(2,1)S(1)}, bf16[16,2,128,256]{3,2,1,0:T(8,128)(2,1)}, u32[]{:S(2)}) copy-start(bf16[16,2,128,256]{3,2,1,0:T(8,128)(2,1)} %copy-done.4) | copy-start | bytes 6291460
  77.9 1.2 %copy-start.12 = (f32[16,2,2,32,128]{4,3,2,1,0:T(8,128)S(1)}, f32[16,2,2,32,128]{4,3,2,1,0:T(8,128)}, u32[]{:S(2)}) copy-start(f32[16,2,2,32,128]{4,3,2,1,0:T(8,128)} %copy-done.11) | copy-start | bytes 3145732
  79.2 1.0 %copy-start.25 = (f32[8,2,2,32,128]{4,3,2,1,0:T(8,128)S(1)}, f32[8,2,2,32,128]{4,3,2,1,0:T(8,128)}, u32[]{:S(2)}) copy-start(f32[8,2,2,32,128]{4,3,2,1,0:T(8,128)} %copy-done.24) | copy-start | bytes 1572868
  80.2 0.9 %copy-start.32 = (f32[128,512]{1,0:T(8,128)S(1)}, f32[128,512]{1,0:T(8,128)}, u32[]{:S(2)}) copy-start(f32[128,512]{1,0:T(8,128)} %copy-done.31) | copy-start | bytes 786436

commit v2 on v1

--- a/solution.py
+++ b/solution.py
@@ -15,10 +15,10 @@
 TILES = 8
 SPAN = 16
 SPANS = ROWS // SPAN
-PIECES = (1, 2, 4, 1)
+PIECES = (1, 2, 2, 2, 1)
 LOG2E = 1.0 / math.log(2.0)
 EPSILON = 1e-06
-AXES = ("sp", "y", "c")
+AXES = ("z", "x", "y", "c")
 VMEM = pltpu.VMEM
 HIGHEST = lax.Precision.HIGHEST
 F32 = jnp.float32
@@ -262,51 +262,47 @@
     out_ref[4] = span + span_other
 
 
-def group_kernel(own, one, two, three, pars, send_ref, before_ref, data):
-    y = lax.axis_index("y")
-    here = lax.axis_index("sp")
+def gather_four(axis, own, one, two, three, data):
+    here = lax.axis_index(axis)
+    data[here] = own[...]
+    data[(here + 3) % 4] = one[...]
+    data[(here + 2) % 4] = two[...]
+    data[(here + 1) % 4] = three[...]
+    return here
+
+
+def run_over(here, data, mine, k):
+    zero = jnp.zeros((16, 128), F32)
+    state, decay = (zero, zero), (zero + 1.0, zero)
+    before, before_decay = state, decay
+    for n in range(4) if k == 0 else range(3, -1, -1):
+        before = pick(n == here, state, before)
+        before_decay = pick(n == here, decay, before_decay)
+        step = decay_over(data[n, 4], mine[k])
+        state = plus(times_of(step, state), (data[n, 2 * k], data[n, 2 * k + 1]))
+        decay = times_of(step, decay)
+    return state, before, before_decay
+
+
+def group_kernel(axis, own, one, two, three, pars, total_ref, before_ref, data):
+    here = gather_four(axis, own, one, two, three, data)
     mine = my_pars(pars)
-    data[y] = own[...]
-    data[(y + 3) % 4] = one[...]
-    data[(y + 2) % 4] = two[...]
-    data[(y + 1) % 4] = three[...]
-    zero = jnp.zeros((16, 128), F32)
-    totals = []
     for k in range(2):
-        state, decay = (zero, zero), (zero + 1.0, zero)
-        before, before_decay = state, decay
-        for n in range(4) if k == 0 else range(3, -1, -1):
-            before = pick(n == y, state, before)
-            before_decay = pick(n == y, decay, before_decay)
-            step = decay_over(data[n, 4], mine[k])
-            state = plus(times_of(step, state), (data[n, 2 * k], data[n, 2 * k + 1]))
-            decay = times_of(step, decay)
+        total, before, decay = run_over(here, data, mine, k)
+        total_ref[2 * k], total_ref[2 * k + 1] = total
         before_ref[2 * k], before_ref[2 * k + 1] = before
-        before_ref[4 + 2 * k], before_ref[5 + 2 * k] = before_decay
-        totals.append(state)
-    span = data[0, 4] + data[1, 4] + data[2, 4] + data[3, 4]
-    for n in range(16):
-        sent = pick(n > here, totals[0], totals[1])
-        send_ref[n, 0], send_ref[n, 1] = sent
-        send_ref[n, 2] = span
-
-
-def enter_kernel(seen, before, own, other, pars, mine_ref, theirs_ref):
-    here = lax.axis_index("sp")
+        before_ref[4 + 2 * k], before_ref[5 + 2 * k] = decay
+    total_ref[4] = data[0, 4] + data[1, 4] + data[2, 4] + data[3, 4]
+
+
+def enter_kernel(across, one, two, three, before_x, before_y, own, other, pars, mine_ref, theirs_ref, data):
+    here = gather_four("z", across, one, two, three, data)
     core = lax.axis_index("c")
     mine = my_pars(pars)
-    zero = jnp.zeros((16, 128), F32)
-    steps = []
-    for n in range(16):
-        chosen = pick(n < here, mine[0], mine[1])
-        steps.append(decay_over(seen[n, 2], chosen))
     for k in range(2):
-        state = (zero, zero)
-        for n in range(16) if k == 0 else range(15, -1, -1):
-            active = n < here if k == 0 else n > here
-            new = plus(times_of(steps[n], state), (seen[n, 0], seen[n, 1]))
-            state = pick(active, new, state)
-        state = plus(times_of((before[4 + 2 * k], before[5 + 2 * k]), state), states_of(before, k))
+        _, state, _ = run_over(here, data, mine, k)
+        for before in (before_x, before_y):
+            state = plus(times_of((before[4 + 2 * k], before[5 + 2 * k]), state), states_of(before, k))
         ahead = core == k
         a, b = states_of(own, k), states_of(other, k)
         early = pick(ahead, a, b)
@@ -439,34 +435,45 @@
         scratch_shapes=[VMEM((ROWS, D), BF16), VMEM((4, ROWS, ROWS), F32)],
         compiler_params=params(10),
     )(
-        tokens, elapsed_row, norm_gain.reshape(1, D), hbm(in_weight), hbm(inputs), decay_angle, forget_rate
+        *(hbm(a) for a in (tokens, elapsed_row, norm_gain.reshape(1, D), in_weight, inputs, decay_angle, forget_rate))
     )
 
     skip_row = skip_gain.reshape(1, CHANNELS)
     pieces, start = [], 0
-    for size in PIECES:
-        pieces.append(
-            run_local(
-                start, size, elapsed_row, driven, inputs, state_output, decay_angle, forget_rate, skip_row
-            )
+
+    def piece_between(before, after):
+        index = len(pieces)
+        start = sum(PIECES[:index])
+        driven_now, _ = lax.optimization_barrier((driven, before))
+        piece = run_local(
+            start, PIECES[index], elapsed_row, driven_now, inputs, state_output, decay_angle, forget_rate, skip_row
         )
-        start += size
+        *piece, after = lax.optimization_barrier((*piece, after))
+        pieces.append(piece)
+        return after
+
+    def around(value, axis):
+        return tuple(lax.ppermute(value, axis, [(i, (i + n) % 4) for i in range(4)]) for n in (1, 2, 3))
 
     swap = [(0, 1), (1, 0)]
+    four = VMEM((4, 5, 16, 128), F32)
     keep = ends[0]
-    partner = lax.ppermute(ends[1], "c", swap)
-    (pair,) = simple(pair_kernel, "pair", [(5, 16, 128)], (keep, partner, pars))
-    shifted = [lax.ppermute(pair, "y", [(i, (i + n) % 4) for i in range(4)]) for n in (2, 1, 3)]
-    two, one, three = shifted
-    send, before = simple(
-        group_kernel, "group", [(16, 3, 16, 128), (8, 16, 128)], (pair, one, two, three, pars),
-        [VMEM((4, 5, 16, 128), F32)],
+    partner = piece_between(keep, lax.ppermute(ends[1], "c", swap))
+    (total,) = simple(pair_kernel, "pair", [(5, 16, 128)], (keep, partner, pars))
+    befores = []
+    for axis in ("y", "x"):
+        others = piece_between(total, around(total, axis))
+        total, before = simple(
+            functools.partial(group_kernel, axis), f"group_{axis}", [(5, 16, 128), (8, 16, 128)],
+            (total, *others, pars), [four],
+        )
+        befores.append(before)
+    others = piece_between(total, around(total, "z"))
+    mine, theirs = simple(
+        enter_kernel, "enter", [(4, 16, 128), (4, 16, 128)],
+        (total, *others, befores[1], befores[0], keep, partner, pars), [four],
     )
-    seen = lax.all_to_all(send, "sp", 0, 0, tiled=True)
-    mine, theirs = simple(
-        enter_kernel, "enter", [(4, 16, 128), (4, 16, 128)], (seen, before, keep, partner, pars)
-    )
-    other = lax.ppermute(theirs, "c", swap)
+    other = piece_between(theirs, lax.ppermute(theirs, "c", swap))
 
     spec = pl.BlockSpec(memory_space=VMEM)
     args = (
@@ -480,7 +487,7 @@
         out_specs=spec,
         out_shape=sds((ROWS, D), BF16),
         scratch_shapes=[VMEM((2, 4, 16, 128), F32), VMEM((ROWS, CHANNELS), F32)],
-        compiler_params=params(24),
+        compiler_params=params(12),
     )(*args)
 
 
@@ -489,7 +496,7 @@
 
 
 def solution(mesh):
-    finer = Mesh(mesh.devices.reshape(16, 4, 2), AXES)
+    finer = Mesh(mesh.devices.reshape(4, 4, 4, 2), AXES)
     split = P(AXES, None)
     placed = (split, P(AXES), P(), P(), P(), P(), P(), P(), P(), P(), P(), P(), P())
     return jax.shard_map(local, mesh=finer, in_specs=placed, out_specs=split, check_vma=False)

time: 86.9 us -> 53.8 us (0.62)
  local copies, waits for them, and re-layouts: 29.4 us -> 0.06 us
  waiting for transfers between devices: 4.63 us -> 0.03 us
  starting transfers between devices: 15.3 us -> 16.3 us
    unnamed x94 -> x20, local copies, waits for them, and re-layouts: 29.4 us -> 0.05 us
    ppermute x5 -> x11, starting transfers between devices: 7.73 us -> 16.3 us  [the longest x9 12.2 us: around(): lax.ppermute(value, axis, [(i, (i + n) % 4) for i in range(4)])]
    all_to_all x1 -> x0, starting transfers between devices: 7.59 us -> none  [local(): seen = lax.all_to_all(send, 'sp', 0, 0, tiled=True)]
    ppermute x5 -> x11, waiting for transfers between devices: 4.62 us -> 0.03 us  [the longest x9 0.02 us: around(): lax.ppermute(value, axis, [(i, (i + n) % 4) for i in range(4)])]
    pallas_call x4 -> x5, Pallas kernels: 20.1 us -> 20.4 us  [run_local(): pl.pallas_call(functools.partial(local_kernel, start), name=f'local_{star...]
  transfers between devices with their start and end apart: 6 -> 11, of which waited for: 4 -> 0; matrix products, arithmetic and copies ran while one was open for 0% -> 0% of each run, Pallas kernels for 23% -> 38%
where the time goes in v2:
time: 53.8 us; the launch traced here: 53.6 us
  Pallas kernels  36.9 us (69%)
  starting transfers between devices  16.3 us (30%)
    pallas_call x5, Pallas kernels, run_local(): pl.pallas_call(functools.partial(local_kernel, start), name=f'local_{star...  20.4 us
    ppermute x9, starting transfers between devices, around(): lax.ppermute(value, axis, [(i, (i + n) % 4) for i in range(4)])  12.2 us
    pallas_call x1, Pallas kernels, local(): pl.pallas_call(end_kernel, name='ends', grid=(TILES,), in_specs=[whole((R...  11.3 us
    pallas_call x1, Pallas kernels, local(): pl.pallas_call(final_kernel, name='final', in_specs=[spec] * len(args), o...  4.76 us
    ppermute x1, starting transfers between devices, local(): other = piece_between(theirs, lax.ppermute(theirs, 'c', swap))  2.65 us
    ppermute x1, starting transfers between devices, local(): partner = piece_between(keep, lax.ppermute(ends[1], 'c', swap))  1.45 us
  transfers between devices with their start and end apart: 11, of which 0 were waited for; matrix products, arithmetic and copies ran while one was open for 0% of the time, Pallas kernels for 38%

profile of v2, /device:TPU:1, one launch (start us, length us, event | category | flops | bytes accessed | tf_op | source)
XLA Modules:
  0.0 53.6 jit_solution(316802878835865868)
XLA Ops:
  0.0 0.0 copy-start.4
  0.0 0.0 copy-start.5
  0.0 0.0 copy-start
  0.0 0.0 copy-start.8
  0.0 0.0 copy-start.1
  0.0 0.0 copy-start.6
  0.0 11.3 %ends.1 = (bf16[128,1024]{1,0:T(8,128)(2,1)S(1)}, f32[2,5,16,128]{3,2,1,0:T(8,128)S(1)}, f32[2,2,32,128]{3,2,1,0:T(8,128)S(1)}) custom-call(bf16[128,2048]{1,0:T(8,128)(2,1)} %tokens.1, f32[1,128]{1,0:T(1,128)} %bitcast.22, f32[1,2048]{1,0:T(1,128)} %bitcast.29, bf16[2048,1024]{1,0:T(8,128)(2,1)} %weight.1, bf16[2,2,64,16,64]{4,3,2,1,0:T(8,128)(2,1)} %bitcast.10, ...), custom_call_target="tpu_custom_call" | custom-call | tf_op jit(solution)/shard_map/ends/pallas_call | solution.py:417
  11.4 1.4 %collective-permute-start = (f32[5,16,128]{2,1,0:T(8,128)S(1)}, f32[5,16,128]{2,1,0:T(8,128)S(1)}, u32[]{:S(2)}, u32[]{:S(2)}) collective-permute-start(f32[5,16,128]{2,1,0:T(8,128)S(1)} %get-tuple-element.115), channel_id=1, source_target_pairs={{0,1},{1,0},{2,3},{3,2},{4,5},{5,4},{6,7},{7,6},{8,9},{9,8},{10,11... | collective-permute-start | bytes 122888 | tf_op jit(solution)/shard_map/ppermute | solution.py:461
  12.8 0.0 copy-done.4
  12.8 0.0 copy-done.5
  12.8 0.0 copy-done
  12.8 0.0 copy-done.8
  12.8 0.0 copy-done.1
  12.8 0.0 copy-done.6
  12.8 2.3 %local_0.1 = (f32[128,128]{1,0:T(8,128)S(1)}, bf16[4,2,128,256]{3,2,1,0:T(8,128)(2,1)S(1)}, f32[4,2,2,32,128]{4,3,2,1,0:T(8,128)S(1)}) custom-call(f32[1,128]{1,0:T(1,128)S(1)} %bitcast.23, bf16[128,1024]{1,0:T(8,128)(2,1)S(1)} %get-tuple-element.95.driven, bf16[2,2,64,16,64]{4,3,2,1,0:T(8,128)(2,1)S(1)} %bitcast.11, f32[2,2,64,16,64]{4,3,2,1,0:T(8,128)S(1)} %copy-done.1, ...), custom_call_target="tpu_custom_call" | custom-call | flops 500000000 | bytes 2097152 | tf_op jit(solution)/shard_map/local_0/pallas_call | solution.py:369
  15.1 0.0 collective-permute-done.other
  15.2 2.9 %collective-permute-start.3 = (f32[5,16,128]{2,1,0:T(8,128)S(1)}, f32[5,16,128]{2,1,0:T(8,128)S(1)}, u32[]{:S(2)}, u32[]{:S(2)}) collective-permute-start(f32[5,16,128]{2,1,0:T(8,128)S(1)} %pair.1.own), channel_id=1, source_target_pairs={{0,6},{2,0},{4,2},{6,4},{1,7},{3,1},{5,3},{7,5},{8,14},{10,8},{12,... | collective-permute-start | bytes 122888 | tf_op jit(solution)/shard_map/ppermute | solution.py:456
  18.1 0.3 collective-permute-start.2
  18.5 0.7 %collective-permute-start.1 = (f32[5,16,128]{2,1,0:T(8,128)S(1)}, f32[5,16,128]{2,1,0:T(8,128)S(1)}, u32[]{:S(2)}, u32[]{:S(2)}) collective-permute-start(f32[5,16,128]{2,1,0:T(8,128)S(1)} %pair.1.own), channel_id=1, source_target_pairs={{0,2},{2,4},{4,6},{6,0},{1,3},{3,5},{5,7},{7,1},{8,10},{10,12},{12... | collective-permute-start | bytes 122888 | tf_op jit(solution)/shard_map/ppermute | solution.py:456
  19.2 5.3 %local_1.1 = (f32[128,256]{1,0:T(8,128)S(1)}, bf16[8,2,128,256]{3,2,1,0:T(8,128)(2,1)S(1)}, f32[8,2,2,32,128]{4,3,2,1,0:T(8,128)S(1)}) custom-call(f32[1,128]{1,0:T(1,128)S(1)} %bitcast.24, bf16[128,1024]{1,0:T(8,128)(2,1)S(1)} %get-tuple-element.95.driven, bf16[2,2,64,16,64]{4,3,2,1,0:T(8,128)(2,1)S(1)} %bitcast.12, f32[2,2,64,16,64]{4,3,2,1,0:T(8,128)S(1)} %copy-done.1, ...), custom_call_target="tpu_custom_call" | custom-call | flops 1000000000 | bytes 4194304 | tf_op jit(solution)/shard_map/local_1/pallas_call | solution.py:369
  24.5 0.0 collective-permute-done.3.three
  24.5 0.0 collective-permute-done.2.two
  24.5 0.0 collective-permute-done.1.one
  24.5 0.1 group_y.1
  24.6 2.5 %collective-permute-start.6 = (f32[5,16,128]{2,1,0:T(8,128)S(1)}, f32[5,16,128]{2,1,0:T(8,128)S(1)}, u32[]{:S(2)}, u32[]{:S(2)}) collective-permute-start(f32[5,16,128]{2,1,0:T(8,128)S(1)} %get-tuple-element.75.own), channel_id=1, source_target_pairs={{0,24},{8,0},{16,8},{24,16},{1,25},{9,1},{17,9},{25,17},{2,26},{10... | collective-permute-start | bytes 122888 | tf_op jit(solution)/shard_map/ppermute | solution.py:456
  27.2 0.5 collective-permute-start.5
  27.7 0.6 %collective-permute-start.4 = (f32[5,16,128]{2,1,0:T(8,128)S(1)}, f32[5,16,128]{2,1,0:T(8,128)S(1)}, u32[]{:S(2)}, u32[]{:S(2)}) collective-permute-start(f32[5,16,128]{2,1,0:T(8,128)S(1)} %get-tuple-element.75.own), channel_id=1, source_target_pairs={{0,8},{8,16},{16,24},{24,0},{1,9},{9,17},{17,25},{25,1},{2,10},{10... | collective-permute-start | bytes 122888 | tf_op jit(solution)/shard_map/ppermute | solution.py:456
  28.3 5.3 %local_3.1 = (f32[128,256]{1,0:T(8,128)S(1)}, bf16[8,2,128,256]{3,2,1,0:T(8,128)(2,1)S(1)}, f32[8,2,2,32,128]{4,3,2,1,0:T(8,128)S(1)}) custom-call(f32[1,128]{1,0:T(1,128)S(1)} %bitcast.25, bf16[128,1024]{1,0:T(8,128)(2,1)S(1)} %get-tuple-element.95.driven, bf16[2,2,64,16,64]{4,3,2,1,0:T(8,128)(2,1)S(1)} %bitcast.13, f32[2,2,64,16,64]{4,3,2,1,0:T(8,128)S(1)} %copy-done.1, ...), custom_call_target="tpu_custom_call" | custom-call | flops 1000000000 | bytes 4194304 | tf_op jit(solution)/shard_map/local_3/pallas_call | solution.py:369
  33.6 0.0 copy-start.2
  33.6 0.0 copy-start.3
  33.6 0.0 copy-start.7
  33.6 0.0 copy-start.9
  33.7 0.0 collective-permute-done.6.three
  33.7 0.0 collective-permute-done.5.two
  33.7 0.0 collective-permute-done.4.one
  33.7 0.1 group_x.1
  33.8 3.8 %collective-permute-start.9 = (f32[5,16,128]{2,1,0:T(8,128)S(1)}, f32[5,16,128]{2,1,0:T(8,128)S(1)}, u32[]{:S(2)}, u32[]{:S(2)}) collective-permute-start(f32[5,16,128]{2,1,0:T(8,128)S(1)} %get-tuple-element.83.across), channel_id=1, source_target_pairs={{0,96},{32,0},{64,32},{96,64},{1,97},{33,1},{65,33},{97,65},{2,98}... | collective-permute-start | bytes 122888 | tf_op jit(solution)/shard_map/ppermute | solution.py:456
  37.7 0.0 collective-permute-start.8
  37.7 0.7 %collective-permute-start.7 = (f32[5,16,128]{2,1,0:T(8,128)S(1)}, f32[5,16,128]{2,1,0:T(8,128)S(1)}, u32[]{:S(2)}, u32[]{:S(2)}) collective-permute-start(f32[5,16,128]{2,1,0:T(8,128)S(1)} %get-tuple-element.83.across), channel_id=1, source_target_pairs={{0,32},{32,64},{64,96},{96,0},{1,33},{33,65},{65,97},{97,1},{2,34}... | collective-permute-start | bytes 122888 | tf_op jit(solution)/shard_map/ppermute | solution.py:456
  38.4 5.3 %local_5.1 = (f32[128,256]{1,0:T(8,128)S(1)}, bf16[8,2,128,256]{3,2,1,0:T(8,128)(2,1)S(1)}, f32[8,2,2,32,128]{4,3,2,1,0:T(8,128)S(1)}) custom-call(f32[1,128]{1,0:T(1,128)S(1)} %bitcast.26, bf16[128,1024]{1,0:T(8,128)(2,1)S(1)} %get-tuple-element.95.driven, bf16[2,2,64,16,64]{4,3,2,1,0:T(8,128)(2,1)S(1)} %bitcast.14, f32[2,2,64,16,64]{4,3,2,1,0:T(8,128)S(1)} %copy-done.1, ...), custom_call_target="tpu_custom_call" | custom-call | flops 1000000000 | bytes 4194304 | tf_op jit(solution)/shard_map/local_5/pallas_call | solution.py:369
  43.7 0.0 collective-permute-done.9.three
  43.7 0.0 collective-permute-done.8.two
  43.7 0.0 collective-permute-done.7.one
  43.7 0.1 enter.1
  43.8 2.6 %collective-permute-start.10 = (f32[4,16,128]{2,1,0:T(8,128)S(1)}, f32[4,16,128]{2,1,0:T(8,128)S(1)}, u32[]{:S(2)}, u32[]{:S(2)}) collective-permute-start(f32[4,16,128]{2,1,0:T(8,128)S(1)} %get-tuple-element.94), channel_id=1, source_target_pairs={{0,1},{1,0},{2,3},{3,2},{4,5},{5,4},{6,7},{7,6},{8,9},{9,8},{10,11... | collective-permute-start | bytes 98312 | tf_op jit(solution)/shard_map/ppermute | solution.py:476
  46.5 2.3 %local_7.1 = (f32[128,128]{1,0:T(8,128)S(1)}, bf16[4,2,128,256]{3,2,1,0:T(8,128)(2,1)S(1)}, f32[4,2,2,32,128]{4,3,2,1,0:T(8,128)S(1)}) custom-call(f32[1,128]{1,0:T(1,128)S(1)} %bitcast.27, bf16[128,1024]{1,0:T(8,128)(2,1)S(1)} %get-tuple-element.95.driven, bf16[2,2,64,16,64]{4,3,2,1,0:T(8,128)(2,1)S(1)} %bitcast.15, f32[2,2,64,16,64]{4,3,2,1,0:T(8,128)S(1)} %copy-done.1, ...), custom_call_target="tpu_custom_call" | custom-call | flops 500000000 | bytes 2097152 | tf_op jit(solution)/shard_map/local_7/pallas_call | solution.py:369
  48.8 0.0 collective-permute-done.10.refs_1_
  48.8 0.0 copy-done.2
  48.8 0.0 copy-done.3
  48.8 0.0 copy-done.7
  48.8 0.0 copy-done.9
  48.8 4.8 %final.1 = bf16[128,2048]{1,0:T(8,128)(2,1)} custom-call(f32[4,16,128]{2,1,0:T(8,128)S(1)} %get-tuple-element.93.refs_0_, f32[4,16,128]{2,1,0:T(8,128)S(1)} %collective-permute-done.10.refs_1_, f32[128,128]{1,0:T(8,128)S(1)} %get-tuple-element.100.refs_2_, f32[128,256]{1,0:T(8,128)S(1)} %get-tuple-element.101.refs_3_, ...), custom_call_target="tpu_custom_call" | custom-call | tf_op jit(solution)/shard_map/final/pallas_call | solution.py:483
  (2 shorter events, 0.1 us)
Async XLA Ops:
  0.0 12.8 %copy-start.4 = (f32[2,64,64]{2,1,0:T(8,128)S(1)}, f32[2,64,64]{2,1,0:T(8,128)}, u32[]{:S(2)}) copy-start(f32[2,64,64]{2,1,0:T(8,128)} %angle.11) | copy-start | bytes 98308
  0.0 12.8 %copy-start.5 = (f32[2,64,64]{2,1,0:T(8,128)S(1)}, f32[2,64,64]{2,1,0:T(8,128)}, u32[]{:S(2)}) copy-start(f32[2,64,64]{2,1,0:T(8,128)} %rate.11) | copy-start | bytes 98308
  0.0 12.8 %copy-start = (bf16[2,2,64,64,16]{3,4,2,1,0:T(8,128)(2,1)S(1)}, bf16[2,2,64,64,16]{3,4,2,1,0:T(8,128)(2,1)}, u32[]{:S(2)}) copy-start(bf16[2,2,64,64,16]{3,4,2,1,0:T(8,128)(2,1)} %param.17) | copy-start | bytes 1572868
  0.0 12.8 %copy-start.8 = (f32[128]{0:T(128)S(1)}, f32[128]{0:T(128)}, u32[]{:S(2)}) copy-start(f32[128]{0:T(128)} %param.14) | copy-start | bytes 1540
  0.0 12.8 %copy-start.1 = (f32[2,2,64,16,64]{4,3,2,1,0:T(8,128)S(1)}, f32[2,2,64,16,64]{4,3,2,1,0:T(8,128)}, u32[]{:S(2)}) copy-start(f32[2,2,64,16,64]{4,3,2,1,0:T(8,128)} %readout.9) | copy-start | bytes 3145732
  0.0 12.8 %copy-start.6 = (f32[1024]{0:T(1024)S(1)}, f32[1024]{0:T(1024)}, u32[]{:S(2)}) copy-start(f32[1024]{0:T(1024)} %param.21) | copy-start | bytes 12292
  11.4 3.8 %collective-permute-start = (f32[5,16,128]{2,1,0:T(8,128)S(1)}, f32[5,16,128]{2,1,0:T(8,128)S(1)}, u32[]{:S(2)}, u32[]{:S(2)}) collective-permute-start(f32[5,16,128]{2,1,0:T(8,128)S(1)} %get-tuple-element.115), channel_id=1, source_target_pairs={{0,1},{1,0},{2,3},{3,2},{4,5},{5,4},{6,7},{7,6},{8,9},{9,8},{10,11... | collective-permute-start | bytes 122888 | tf_op jit(solution)/shard_map/ppermute | solution.py:461
  15.2 9.3 %collective-permute-start.3 = (f32[5,16,128]{2,1,0:T(8,128)S(1)}, f32[5,16,128]{2,1,0:T(8,128)S(1)}, u32[]{:S(2)}, u32[]{:S(2)}) collective-permute-start(f32[5,16,128]{2,1,0:T(8,128)S(1)} %pair.1.own), channel_id=1, source_target_pairs={{0,6},{2,0},{4,2},{6,4},{1,7},{3,1},{5,3},{7,5},{8,14},{10,8},{12,... | collective-permute-start | bytes 122888 | tf_op jit(solution)/shard_map/ppermute | solution.py:456
  18.1 6.4 %collective-permute-start.2 = (f32[5,16,128]{2,1,0:T(8,128)S(1)}, f32[5,16,128]{2,1,0:T(8,128)S(1)}, u32[]{:S(2)}, u32[]{:S(2)}) collective-permute-start(f32[5,16,128]{2,1,0:T(8,128)S(1)} %pair.1.own), channel_id=1, source_target_pairs={{0,4},{2,6},{4,0},{6,2},{1,5},{3,7},{5,1},{7,3},{8,12},{10,14},{12... | collective-permute-start | bytes 122888 | tf_op jit(solution)/shard_map/ppermute | solution.py:456
  18.5 6.0 %collective-permute-start.1 = (f32[5,16,128]{2,1,0:T(8,128)S(1)}, f32[5,16,128]{2,1,0:T(8,128)S(1)}, u32[]{:S(2)}, u32[]{:S(2)}) collective-permute-start(f32[5,16,128]{2,1,0:T(8,128)S(1)} %pair.1.own), channel_id=1, source_target_pairs={{0,2},{2,4},{4,6},{6,0},{1,3},{3,5},{5,7},{7,1},{8,10},{10,12},{12... | collective-permute-start | bytes 122888 | tf_op jit(solution)/shard_map/ppermute | solution.py:456
  24.6 9.0 %collective-permute-start.6 = (f32[5,16,128]{2,1,0:T(8,128)S(1)}, f32[5,16,128]{2,1,0:T(8,128)S(1)}, u32[]{:S(2)}, u32[]{:S(2)}) collective-permute-start(f32[5,16,128]{2,1,0:T(8,128)S(1)} %get-tuple-element.75.own), channel_id=1, source_target_pairs={{0,24},{8,0},{16,8},{24,16},{1,25},{9,1},{17,9},{25,17},{2,26},{10... | collective-permute-start | bytes 122888 | tf_op jit(solution)/shard_map/ppermute | solution.py:456
  27.2 6.5 %collective-permute-start.5 = (f32[5,16,128]{2,1,0:T(8,128)S(1)}, f32[5,16,128]{2,1,0:T(8,128)S(1)}, u32[]{:S(2)}, u32[]{:S(2)}) collective-permute-start(f32[5,16,128]{2,1,0:T(8,128)S(1)} %get-tuple-element.75.own), channel_id=1, source_target_pairs={{0,16},{8,24},{16,0},{24,8},{1,17},{9,25},{17,1},{25,9},{2,18},{10... | collective-permute-start | bytes 122888 | tf_op jit(solution)/shard_map/ppermute | solution.py:456
  27.7 6.0 %collective-permute-start.4 = (f32[5,16,128]{2,1,0:T(8,128)S(1)}, f32[5,16,128]{2,1,0:T(8,128)S(1)}, u32[]{:S(2)}, u32[]{:S(2)}) collective-permute-start(f32[5,16,128]{2,1,0:T(8,128)S(1)} %get-tuple-element.75.own), channel_id=1, source_target_pairs={{0,8},{8,16},{16,24},{24,0},{1,9},{9,17},{17,25},{25,1},{2,10},{10... | collective-permute-start | bytes 122888 | tf_op jit(solution)/shard_map/ppermute | solution.py:456
  33.6 15.2 %copy-start.2 = (bf16[1024,2048]{1,0:T(8,128)(2,1)S(1)}, bf16[1024,2048]{1,0:T(8,128)(2,1)}, u32[]{:S(2)}) copy-start(bf16[1024,2048]{1,0:T(8,128)(2,1)} %refs_19_.1) | copy-start | bytes 12582916
  33.6 15.2 %copy-start.3 = (bf16[1024,1024]{1,0:T(8,128)(2,1)S(1)}, bf16[1024,1024]{1,0:T(8,128)(2,1)}, u32[]{:S(2)}) copy-start(bf16[1024,1024]{1,0:T(8,128)(2,1)} %refs_17_.1) | copy-start | bytes 6291460
  33.6 15.2 %copy-start.7 = (f32[2048]{0:T(1024)S(1)}, f32[2048]{0:T(1024)}, u32[]{:S(2)}) copy-start(f32[2048]{0:T(1024)} %param.25) | copy-start | bytes 24580
  33.6 15.2 %copy-start.9 = (f32[1024]{0:T(1024)S(1)}, f32[1024]{0:T(1024)}, u32[]{:S(2)}) copy-start(f32[1024]{0:T(1024)} %param.23) | copy-start | bytes 12292
  33.8 9.8 %collective-permute-start.9 = (f32[5,16,128]{2,1,0:T(8,128)S(1)}, f32[5,16,128]{2,1,0:T(8,128)S(1)}, u32[]{:S(2)}, u32[]{:S(2)}) collective-permute-start(f32[5,16,128]{2,1,0:T(8,128)S(1)} %get-tuple-element.83.across), channel_id=1, source_target_pairs={{0,96},{32,0},{64,32},{96,64},{1,97},{33,1},{65,33},{97,65},{2,98}... | collective-permute-start | bytes 122888 | tf_op jit(solution)/shard_map/ppermute | solution.py:456
  37.7 6.0 %collective-permute-start.8 = (f32[5,16,128]{2,1,0:T(8,128)S(1)}, f32[5,16,128]{2,1,0:T(8,128)S(1)}, u32[]{:S(2)}, u32[]{:S(2)}) collective-permute-start(f32[5,16,128]{2,1,0:T(8,128)S(1)} %get-tuple-element.83.across), channel_id=1, source_target_pairs={{0,64},{32,96},{64,0},{96,32},{1,65},{33,97},{65,1},{97,33},{2,66}... | collective-permute-start | bytes 122888 | tf_op jit(solution)/shard_map/ppermute | solution.py:456
  37.7 6.0 %collective-permute-start.7 = (f32[5,16,128]{2,1,0:T(8,128)S(1)}, f32[5,16,128]{2,1,0:T(8,128)S(1)}, u32[]{:S(2)}, u32[]{:S(2)}) collective-permute-start(f32[5,16,128]{2,1,0:T(8,128)S(1)} %get-tuple-element.83.across), channel_id=1, source_target_pairs={{0,32},{32,64},{64,96},{96,0},{1,33},{33,65},{65,97},{97,1},{2,34}... | collective-permute-start | bytes 122888 | tf_op jit(solution)/shard_map/ppermute | solution.py:456
  43.8 4.9 %collective-permute-start.10 = (f32[4,16,128]{2,1,0:T(8,128)S(1)}, f32[4,16,128]{2,1,0:T(8,128)S(1)}, u32[]{:S(2)}, u32[]{:S(2)}) collective-permute-start(f32[4,16,128]{2,1,0:T(8,128)S(1)} %get-tuple-element.94), channel_id=1, source_target_pairs={{0,1},{1,0},{2,3},{3,2},{4,5},{5,4},{6,7},{7,6},{8,9},{9,8},{10,11... | collective-permute-start | bytes 98312 | tf_op jit(solution)/shard_map/ppermute | solution.py:476

commit v3 on v2

--- a/solution.py
+++ b/solution.py
@@ -15,7 +15,7 @@
 TILES = 8
 SPAN = 16
 SPANS = ROWS // SPAN
-PIECES = (1, 2, 2, 2, 1)
+PIECES = (1,) * 8
 LOG2E = 1.0 / math.log(2.0)
 EPSILON = 1e-06
 AXES = ("z", "x", "y", "c")
@@ -26,17 +26,17 @@
 
 SINE = (4.44288291, -7.30824512, 3.60634303, -0.84604096, 0.10968436)
 COSINE = (1.4142135, -6.97885097, 5.73946067, -1.88355924, 0.31068962)
+SINE_SHORT = (4.44287876, -7.30776104, 3.5971931, -0.7896682)
+COSINE_SHORT = (1.41420407, -6.97764062, 5.71521917, -1.7282871)
 DAMP = (
-    9.99999626e-01,
-    -2.49992247e-01,
-    5.20558088e-02,
-    -7.77389543e-03,
-    8.29541685e-04,
-    -6.19250366e-05,
-    2.98283721e-06,
-    -7.10025954e-08,
+    9.99995989e-01,
+    -2.49939726e-01,
+    5.19269127e-02,
+    -7.65257696e-03,
+    7.74390930e-04,
+    -4.89307841e-05,
+    1.45423687e-06,
 )
-SINE_SHORT = (4.44287876, -7.30776104, 3.5971931, -0.7896682)
 
 
 def horner(coefficients, x):
@@ -46,11 +46,14 @@
     return value
 
 
-def unit_circle(turns, sine=SINE_SHORT):
+def half_turn(turns, sine=SINE_SHORT, cosine=COSINE_SHORT):
     r = turns - jnp.round(turns)
     z = r * r
-    s = r * horner(sine, z)
-    c = horner(COSINE, z)
+    return r * horner(sine, z), horner(cosine, z)
+
+
+def unit_circle(turns, *tables):
+    s, c = half_turn(turns, *tables)
     return 1.0 - s * s, s * c
 
 
@@ -78,7 +81,10 @@
     return jnp.concatenate([ref[k, pl.ds(2 * pair, 1), :], ref[k, pl.ds(2 * pair + 1, 1), :]], axis=1)
 
 
-def end_kernel(tokens, elapsed, gain, weight, inputs, angle, rate, driven_ref, ends_ref, pars_ref, normed, times):
+def end_kernel(
+    tokens, elapsed, gain, weight, inputs, angle, rate,
+    driven_ref, ends_ref, pars_ref, damp_ref, within_ref, normed, times,
+):
     step = pl.program_id(0)
     core = lax.axis_index("c")
 
@@ -89,13 +95,16 @@
         normed[...] = (x * scale * gain[...]).astype(BF16)
         steps = column_of(elapsed[...])
         row, col = iotas((ROWS, ROWS))
+        same = row // SPAN == col // SPAN
         times[0] = exact_mm((col > row).astype(F32), steps)
         times[1] = exact_mm((col < row).astype(F32), steps)
         times[2] = jnp.sqrt(steps)
         times[3] = steps
-        total = exact_mm(jnp.ones((16, ROWS), F32), steps)
-        ends_ref[0, 4] = total
-        ends_ref[1, 4] = total
+        within_ref[0] = exact_mm(((col <= row) & same).astype(F32), steps)
+        within_ref[1] = exact_mm(((col >= row) & same).astype(F32), steps)
+        total = exact_mm(jnp.ones((8, ROWS), F32), steps)
+        ends_ref[0, 64:] = total
+        ends_ref[1, 64:] = total
 
     driven = mm(normed[...], weight[...]).astype(BF16)
     driven_ref[...] = driven
@@ -110,11 +119,14 @@
             pars_ref[k, 0, pl.ds(pair, 1), :] = th
             pars_ref[k, 1, pl.ds(pair, 1), :] = f
             f2 = f * 2.0
+            root = jnp.sqrt(f2)
             after = times[k]
-            cosine, sine = unit_circle(after * (th * (0.5 / math.pi)))
-            damp = horner(DAMP, times[3] * f2) * (times[2] * jnp.sqrt(f2))
+            s, c = half_turn(after * (th * (0.5 / math.pi)))
+            damp = horner(DAMP, times[3] * f2) * times[2]
+            damp_ref[j, k] = damp
             amp = jnp.exp2(after * (f * -LOG2E)) * damp
-            pull = jnp.concatenate([(amp * cosine).astype(BF16), (amp * sine).astype(BF16)], axis=1)
+            tilted = amp * s
+            pull = jnp.concatenate([(amp - tilted * s).astype(BF16), (tilted * c).astype(BF16)], axis=1)
             mixed = mm(flipped[32 * j : 32 * j + 32], pull)
             m_re = jnp.where(first, mixed[:16, :128], mixed[16:, :128])
             m_im = jnp.where(first, mixed[:16, 128:], mixed[16:, 128:])
@@ -122,27 +134,16 @@
                 jnp.concatenate([inputs[k, c, 2 * j].astype(F32), inputs[k, c, 2 * j + 1].astype(F32)], axis=1)
                 for c in range(2)
             )
-            at = 4 * (step % 4) + j
-            ends_ref[away, 2 * k, pl.ds(at, 1), :] = jnp.sum(b_re * m_re - b_im * m_im, axis=0, keepdims=True)
-            ends_ref[away, 2 * k + 1, pl.ds(at, 1), :] = jnp.sum(b_re * m_im + b_im * m_re, axis=0, keepdims=True)
+            at = 32 * k + 4 * (step % 4) + j
+            ends_ref[away, pl.ds(at, 1), :] = root * jnp.sum(b_re * m_re - b_im * m_im, axis=0, keepdims=True)
+            ends_ref[away, pl.ds(at + 16, 1), :] = root * jnp.sum(b_re * m_im + b_im * m_re, axis=0, keepdims=True)
 
 
 def local_kernel(
-    offset, elapsed, driven, inputs, readout, angle, rate, skip,
-    out_ref, prefix_ref, table_ref, times,
+    offset, within, damps, driven, inputs, readout, angle, rate, skip,
+    out_ref, prefix_ref, table_ref,
 ):
     step = pl.program_id(0)
-
-    @pl.when(step == 0)
-    def _():
-        steps = column_of(elapsed[...])
-        row, col = iotas((ROWS, ROWS))
-        same = row // SPAN == col // SPAN
-        times[0] = exact_mm(((col <= row) & same).astype(F32), steps)
-        times[1] = exact_mm(((col >= row) & same).astype(F32), steps)
-        times[2] = jnp.sqrt(steps)
-        times[3] = steps
-
     row, col = iotas((ROWS, ROWS))
     same = row // SPAN == col // SPAN
     triangles = (((col <= row) & same).astype(BF16), ((col >= row) & same).astype(BF16))
@@ -157,7 +158,7 @@
         for k in range(2):
             f = pair_row(rate, k, pair)
             th = pair_row(angle, k, pair)
-            f2 = f * 2.0
+            root = jnp.sqrt(f * 2.0)
             b00, b01 = inputs[k, 0, 2 * j], inputs[k, 1, 2 * j]
             b10, b11 = inputs[k, 0, 2 * j + 1], inputs[k, 1, 2 * j + 1]
             rhs = jnp.concatenate(
@@ -169,12 +170,10 @@
             )
             proj = mm(lhs, rhs)
             p_re, p_im = proj[:, :128], proj[:, 128:]
-            offs = times[k]
+            offs = within[k]
             cosine, sine = unit_circle(offs * (th * (0.5 / math.pi)))
-            damp = horner(DAMP, times[3] * f2) * (times[2] * jnp.sqrt(f2))
-            level = offs * (f * LOG2E)
-            grow = jnp.exp2(level) * damp
-            fade = jnp.exp2(-level)
+            grow = jnp.exp2(offs * (f * LOG2E)) * damps[j, k]
+            fade = jnp.exp2(offs * (f * -LOG2E))
             a_re, a_im = grow * cosine, grow * sine
             lift = jnp.concatenate(
                 [(a_re * p_re + a_im * p_im).astype(BF16), (a_re * p_im - a_im * p_re).astype(BF16)], axis=1
@@ -201,7 +200,7 @@
                 lower = jnp.concatenate([hole, readout[k, c, 2 * j + 1]], axis=1)
                 table = jnp.concatenate([upper, lower], axis=0)
                 table_ref[j, k, c] = table
-                tables.append(table)
+                tables.append(table * root)
             y = nt(
                 jnp.concatenate(states, axis=0),
                 jnp.concatenate([tables[0].astype(BF16), (-tables[1]).astype(BF16)], axis=1),
@@ -239,76 +238,80 @@
 def decay_over(span, pars):
     high, low, level = pars
     u = span * high
-    cosine, sine = unit_circle((u - jnp.round(u)) + span * low, SINE)
+    cosine, sine = unit_circle((u - jnp.round(u)) + span * low, SINE, COSINE)
     fade = jnp.exp2(span * level)
     return fade * cosine, fade * sine
 
 
 def states_of(ref, k):
-    return ref[2 * k], ref[2 * k + 1]
-
-
-def pair_kernel(own, other, pars, out_ref):
-    core = lax.axis_index("c")
+    return ref[32 * k : 32 * k + 16, :], ref[32 * k + 16 : 32 * k + 32, :]
+
+
+def span_of(ref):
+    span = ref[64:72, :]
+    return jnp.concatenate([span, span], axis=0)
+
+
+def keep_at(ref, at, value):
+    ref[2 * at], ref[2 * at + 1] = value
+
+
+def upper(stage):
+    axis, kind = stage
+    here = lax.axis_index(axis)
+    return here >= 2 if kind == "high" else here % 2 == 1
+
+
+def merge(stage, own, other, mine, total_ref, k, decay, decay_other):
+    behind = upper(stage) if k == 0 else jnp.logical_not(upper(stage))
+    a, b = states_of(own, k), states_of(other, k)
+    early, late = pick(behind, b, a), pick(behind, a, b)
+    total = plus(times_of(pick(behind, decay, decay_other), early), late)
+    if total_ref is not None:
+        total_ref[32 * k : 32 * k + 16, :], total_ref[32 * k + 16 : 32 * k + 32, :] = total
+    return behind, b
+
+
+def pair_kernel(own, other, pars, total_ref, trail_ref):
     mine = my_pars(pars)
-    span, span_other = own[4], other[4]
+    zero = jnp.zeros((16, 128), F32)
     for k in range(2):
-        ahead = core == k
-        a, b = states_of(own, k), states_of(other, k)
-        early, late = pick(ahead, a, b), pick(ahead, b, a)
-        moved = times_of(decay_over(jnp.where(ahead, span_other, span), mine[k]), early)
-        total = plus(moved, late)
-        out_ref[2 * k], out_ref[2 * k + 1] = total
-    out_ref[4] = span + span_other
-
-
-def gather_four(axis, own, one, two, three, data):
-    here = lax.axis_index(axis)
-    data[here] = own[...]
-    data[(here + 3) % 4] = one[...]
-    data[(here + 2) % 4] = two[...]
-    data[(here + 1) % 4] = three[...]
-    return here
-
-
-def run_over(here, data, mine, k):
-    zero = jnp.zeros((16, 128), F32)
-    state, decay = (zero, zero), (zero + 1.0, zero)
-    before, before_decay = state, decay
-    for n in range(4) if k == 0 else range(3, -1, -1):
-        before = pick(n == here, state, before)
-        before_decay = pick(n == here, decay, before_decay)
-        step = decay_over(data[n, 4], mine[k])
-        state = plus(times_of(step, state), (data[n, 2 * k], data[n, 2 * k + 1]))
-        decay = times_of(step, decay)
-    return state, before, before_decay
-
-
-def group_kernel(axis, own, one, two, three, pars, total_ref, before_ref, data):
-    here = gather_four(axis, own, one, two, three, data)
+        decay, decay_other = decay_over(span_of(own), mine[k]), decay_over(span_of(other), mine[k])
+        merge(("c", "low"), own, other, mine, total_ref, k, decay, decay_other)
+        keep_at(trail_ref, k, (zero, zero))
+        keep_at(trail_ref, 2 + k, (zero + 1.0, zero))
+        keep_at(trail_ref, 4 + k, times_of(decay, decay_other))
+    total_ref[64:72, :] = own[64:72, :] + other[64:72, :]
+
+
+def trail_of(trail, at):
+    return trail[2 * at], trail[2 * at + 1]
+
+
+def stage_kernel(stage, own, other, trail, pars, total_ref, trail_ref):
     mine = my_pars(pars)
     for k in range(2):
-        total, before, decay = run_over(here, data, mine, k)
-        total_ref[2 * k], total_ref[2 * k + 1] = total
-        before_ref[2 * k], before_ref[2 * k + 1] = before
-        before_ref[4 + 2 * k], before_ref[5 + 2 * k] = decay
-    total_ref[4] = data[0, 4] + data[1, 4] + data[2, 4] + data[3, 4]
-
-
-def enter_kernel(across, one, two, three, before_x, before_y, own, other, pars, mine_ref, theirs_ref, data):
-    here = gather_four("z", across, one, two, three, data)
+        decay, decay_other = trail_of(trail, 4 + k), decay_over(span_of(other), mine[k])
+        behind, theirs = merge(stage, own, other, mine, total_ref, k, decay, decay_other)
+        state, fade = trail_of(trail, k), trail_of(trail, 2 + k)
+        keep_at(trail_ref, k, pick(behind, plus(times_of(fade, theirs), state), state))
+        keep_at(trail_ref, 2 + k, pick(behind, times_of(fade, decay_other), fade))
+        keep_at(trail_ref, 4 + k, times_of(decay, decay_other))
+    total_ref[64:72, :] = own[64:72, :] + other[64:72, :]
+
+
+def enter_kernel(stage, last, trail, own, other, pars, mine_ref, theirs_ref):
     core = lax.axis_index("c")
     mine = my_pars(pars)
     for k in range(2):
-        _, state, _ = run_over(here, data, mine, k)
-        for before in (before_x, before_y):
-            state = plus(times_of((before[4 + 2 * k], before[5 + 2 * k]), state), states_of(before, k))
+        behind = upper(stage) if k == 0 else jnp.logical_not(upper(stage))
+        state, fade = trail_of(trail, k), trail_of(trail, 2 + k)
+        state = pick(behind, plus(times_of(fade, states_of(last, k)), state), state)
         ahead = core == k
-        a, b = states_of(own, k), states_of(other, k)
-        early = pick(ahead, a, b)
-        later = plus(times_of(decay_over(jnp.where(ahead, own[4], other[4]), mine[k]), state), early)
-        mine_ref[2 * k], mine_ref[2 * k + 1] = pick(ahead, state, later)
-        theirs_ref[2 * k], theirs_ref[2 * k + 1] = pick(ahead, later, state)
+        early = pick(ahead, states_of(own, k), states_of(other, k))
+        later = plus(times_of(decay_over(jnp.where(ahead, span_of(own), span_of(other)), mine[k]), state), early)
+        keep_at(mine_ref, k, pick(ahead, state, later))
+        keep_at(theirs_ref, k, pick(ahead, later, state))
 
 
 def final_kernel(*refs):
@@ -364,14 +367,15 @@
     return pltpu.CompilerParams(vmem_limit_bytes=limit * 1024 * 1024)
 
 
-def run_local(start, size, elapsed_row, driven, inputs, state_output, angle, rate, skip_row):
+def run_local(start, size, within, damps, driven, inputs, state_output, angle, rate, skip_row):
     row_spec = whole((2, 64, 64))
     return pl.pallas_call(
         functools.partial(local_kernel, start),
         name=f"local_{start}",
         grid=(size,),
         in_specs=[
-            whole((1, ROWS)),
+            whole((2, ROWS, ROWS)),
+            pl.BlockSpec((4, 2, ROWS, ROWS), lambda i: (i + start, 0, 0, 0)),
             pl.BlockSpec((ROWS, 128), lambda i: (0, i + start)),
             pl.BlockSpec((2, 2, 8, 16, 64), lambda i: (0, 0, i + start, 0, 0)),
             pl.BlockSpec((2, 2, 8, 16, 64), lambda i: (0, 0, i + start, 0, 0)),
@@ -388,10 +392,9 @@
             sds((4 * size, 2, ROWS, 256), BF16),
             sds((4 * size, 2, 2, 32, 128)),
         ],
-        scratch_shapes=[VMEM((4, ROWS, ROWS), F32)],
         compiler_params=params(10),
         cost_estimate=pl.CostEstimate(flops=size * 5 * 10**8, bytes_accessed=size * 2 * 2**20, transcendentals=0),
-    )(elapsed_row, driven, inputs, state_output, angle, rate, skip_row)
+    )(within, damps, driven, inputs, state_output, angle, rate, skip_row)
 
 
 def simple(kernel, name, shapes, args, scratch=()):
@@ -414,7 +417,7 @@
     elapsed_row = elapsed.reshape(1, ROWS)
     inputs = jnp.swapaxes(state_input, 3, 4)
     row_spec = whole((2, 64, 64))
-    driven, ends, pars = pl.pallas_call(
+    driven, ends, pars, damps, within = pl.pallas_call(
         end_kernel,
         name="ends",
         grid=(TILES,),
@@ -428,10 +431,15 @@
         ],
         out_specs=[
             pl.BlockSpec((ROWS, 128), lambda i: (0, i)),
-            whole((2, 5, 16, 128)),
+            whole((2, 72, 128)),
             whole((2, 2, 32, 128)),
+            pl.BlockSpec((4, 2, ROWS, ROWS), lambda i: (i, 0, 0, 0)),
+            whole((2, ROWS, ROWS)),
         ],
-        out_shape=[sds((ROWS, CHANNELS), BF16), sds((2, 5, 16, 128)), sds((2, 2, 32, 128))],
+        out_shape=[
+            sds((ROWS, CHANNELS), BF16), sds((2, 72, 128)), sds((2, 2, 32, 128)),
+            sds((32, 2, ROWS, ROWS)), sds((2, ROWS, ROWS)),
+        ],
         scratch_shapes=[VMEM((ROWS, D), BF16), VMEM((4, ROWS, ROWS), F32)],
         compiler_params=params(10),
     )(
@@ -446,33 +454,31 @@
         start = sum(PIECES[:index])
         driven_now, _ = lax.optimization_barrier((driven, before))
         piece = run_local(
-            start, PIECES[index], elapsed_row, driven_now, inputs, state_output, decay_angle, forget_rate, skip_row
+            start, PIECES[index], within, damps, driven_now, inputs, state_output, decay_angle, forget_rate, skip_row
         )
         *piece, after = lax.optimization_barrier((*piece, after))
         pieces.append(piece)
         return after
 
-    def around(value, axis):
-        return tuple(lax.ppermute(value, axis, [(i, (i + n) % 4) for i in range(4)]) for n in (1, 2, 3))
-
     swap = [(0, 1), (1, 0)]
-    four = VMEM((4, 5, 16, 128), F32)
+    pairings = {"low": [(0, 1), (1, 0), (2, 3), (3, 2)], "high": [(0, 3), (3, 0), (1, 2), (2, 1)]}
+    stages = [(axis, kind) for axis in ("y", "x", "z") for kind in ("low", "high")]
     keep = ends[0]
     partner = piece_between(keep, lax.ppermute(ends[1], "c", swap))
-    (total,) = simple(pair_kernel, "pair", [(5, 16, 128)], (keep, partner, pars))
-    befores = []
-    for axis in ("y", "x"):
-        others = piece_between(total, around(total, axis))
-        total, before = simple(
-            functools.partial(group_kernel, axis), f"group_{axis}", [(5, 16, 128), (8, 16, 128)],
-            (total, *others, pars), [four],
-        )
-        befores.append(before)
-    others = piece_between(total, around(total, "z"))
-    mine, theirs = simple(
-        enter_kernel, "enter", [(4, 16, 128), (4, 16, 128)],
-        (total, *others, befores[1], befores[0], keep, partner, pars), [four],
-    )
+    total, trail = simple(pair_kernel, "pair", [(72, 128), (12, 16, 128)], (keep, partner, pars))
+    for stage in stages:
+        axis, kind = stage
+        other = piece_between(total, lax.ppermute(total, axis, pairings[kind]))
+        if stage == stages[-1]:
+            mine, theirs = simple(
+                functools.partial(enter_kernel, stage), "enter", [(4, 16, 128), (4, 16, 128)],
+                (other, trail, keep, partner, pars),
+            )
+        else:
+            total, trail = simple(
+                functools.partial(stage_kernel, stage), f"stage_{axis}_{kind}", [(72, 128), (12, 16, 128)],
+                (total, other, trail, pars),
+            )
     other = piece_between(theirs, lax.ppermute(theirs, "c", swap))
 
     spec = pl.BlockSpec(memory_space=VMEM)

time: 53.8 us -> 49.6 us (0.922)
  Pallas kernels: 36.9 us -> 30.9 us
  starting transfers between devices: 16.3 us -> 18.1 us
    pallas_call x5 -> x8, Pallas kernels: 20.4 us -> 16.6 us  [run_local(): pl.pallas_call(functools.partial(local_kernel, start), name=f'local_{star...]
    ppermute x1, starting transfers between devices: 2.65 us -> 4.76 us  [local(): other = piece_between(theirs, lax.ppermute(theirs, 'c', swap))]
    pallas_call x1, Pallas kernels: 4.76 us -> 3.34 us  [local(): pl.pallas_call(final_kernel, name='final', in_specs=[spec] * len(args), o...]
    pallas_call x1, Pallas kernels: 11.3 us -> 10.6 us  [local(): pl.pallas_call(end_kernel, name='ends', grid=(TILES,), in_specs=[whole((R...]
    ppermute x9 -> x6, starting transfers between devices: 12.2 us -> 11.9 us  [local(): other = piece_between(total, lax.ppermute(total, axis, pairings[kind]))]
  transfers between devices with their start and end apart: 11 -> 8, of which waited for: 0 -> 0; matrix products, arithmetic and copies ran while one was open for 0% -> 0% of each run, Pallas kernels for 38% -> 34%
where the time goes in v3:
time: 49.6 us; the launch traced here: 49.4 us
  Pallas kernels  30.9 us (62%)
  starting transfers between devices  18.1 us (36%)
    pallas_call x8, Pallas kernels, run_local(): pl.pallas_call(functools.partial(local_kernel, start), name=f'local_{star...  16.6 us
    ppermute x6, starting transfers between devices, local(): other = piece_between(total, lax.ppermute(total, axis, pairings[kind]))  11.9 us
    pallas_call x1, Pallas kernels, local(): pl.pallas_call(end_kernel, name='ends', grid=(TILES,), in_specs=[whole((R...  10.6 us
    ppermute x1, starting transfers between devices, local(): other = piece_between(theirs, lax.ppermute(theirs, 'c', swap))  4.76 us
    pallas_call x1, Pallas kernels, local(): pl.pallas_call(final_kernel, name='final', in_specs=[spec] * len(args), o...  3.34 us
    ppermute x1, starting transfers between devices, local(): partner = piece_between(keep, lax.ppermute(ends[1], 'c', swap))  1.44 us
  transfers between devices with their start and end apart: 8, of which 0 were waited for; matrix products, arithmetic and copies ran while one was open for 0% of the time, Pallas kernels for 34%

profile of v3, /device:TPU:1, one launch (start us, length us, event | category | flops | bytes accessed | tf_op | source)
XLA Modules:
  0.0 49.4 jit_solution(16878171979621695215)
XLA Ops:
  0.0 0.0 copy-start.2
  0.0 0.0 copy-start.3
  0.0 0.0 copy-start.1
  0.0 0.0 copy-start
  0.0 0.0 copy-start.6
  0.0 10.6 %ends.1 = (bf16[128,1024]{1,0:T(8,128)(2,1)S(1)}, f32[2,72,128]{2,1,0:T(8,128)S(1)}, f32[2,2,32,128]{3,2,1,0:T(8,128)S(1)}, f32[32,2,128,128]{3,2,1,0:T(8,128)S(1)}, f32[2,128,128]{2,1,0:T(8,128)S(1)}) custom-call(bf16[128,2048]{1,0:T(8,128)(2,1)} %tokens.1, f32[1,128]{1,0:T(1,128)} %bitcast.30, f32[1,2048]{1,0:T(1,128)} %bitcast.29, ...), custom_call_target="tpu_custom_call" | custom-call | tf_op jit(solution)/shard_map/ends/pallas_call | solution.py:420
  10.6 1.4 %collective-permute-start = (f32[72,128]{1,0:T(8,128)S(1)}, f32[72,128]{1,0:T(8,128)S(1)}, u32[]{:S(2)}, u32[]{:S(2)}) collective-permute-start(f32[72,128]{1,0:T(8,128)S(1)} %get-tuple-element.171), channel_id=1, source_target_pairs={{0,1},{1,0},{2,3},{3,2},{4,5},{5,4},{6,7},{7,6},{8,9},{9,8},{10,11... | collective-permute-start | bytes 110600 | tf_op jit(solution)/shard_map/ppermute | solution.py:467
  12.1 0.0 copy-done.2
  12.1 0.0 copy-done.3
  12.1 0.0 copy-done.1
  12.1 0.0 copy-done
  12.1 0.0 copy-done.6
  12.1 2.1 %local_0.1 = (f32[128,128]{1,0:T(8,128)S(1)}, bf16[4,2,128,256]{3,2,1,0:T(8,128)(2,1)S(1)}, f32[4,2,2,32,128]{4,3,2,1,0:T(8,128)S(1)}) custom-call(f32[2,128,128]{2,1,0:T(8,128)S(1)} %get-tuple-element.88.within, f32[32,2,128,128]{3,2,1,0:T(8,128)S(1)} %get-tuple-element.89.damps, bf16[128,1024]{1,0:T(8,128)(2,1)S(1)} %get-tuple-element.142.driven, ...), custom_call_target="tpu_custom_call" | custom-call | flops 500000000 | bytes 2097152 | tf_op jit(solution)/shard_map/local_0/pallas_call | solution.py:372
  14.2 0.0 collective-permute-done.other
  14.2 0.1 pair.1
  14.3 1.5 %collective-permute-start.1 = (f32[72,128]{1,0:T(8,128)S(1)}, f32[72,128]{1,0:T(8,128)S(1)}, u32[]{:S(2)}, u32[]{:S(2)}) collective-permute-start(f32[72,128]{1,0:T(8,128)S(1)} %get-tuple-element.98.own), channel_id=1, source_target_pairs={{0,2},{2,0},{4,6},{6,4},{1,3},{3,1},{5,7},{7,5},{8,10},{10,8},{12,... | collective-permute-start | bytes 110600 | tf_op jit(solution)/shard_map/ppermute | solution.py:471
  15.8 2.1 %local_1.1 = (f32[128,128]{1,0:T(8,128)S(1)}, bf16[4,2,128,256]{3,2,1,0:T(8,128)(2,1)S(1)}, f32[4,2,2,32,128]{4,3,2,1,0:T(8,128)S(1)}) custom-call(f32[2,128,128]{2,1,0:T(8,128)S(1)} %get-tuple-element.88.within, f32[32,2,128,128]{3,2,1,0:T(8,128)S(1)} %get-tuple-element.89.damps, bf16[128,1024]{1,0:T(8,128)(2,1)S(1)} %get-tuple-element.142.driven, ...), custom_call_target="tpu_custom_call" | custom-call | flops 500000000 | bytes 2097152 | tf_op jit(solution)/shard_map/local_1/pallas_call | solution.py:372
  17.9 0.0 collective-permute-done.1.other
  17.9 0.1 stage_y_low.1
  17.9 2.2 %collective-permute-start.2 = (f32[72,128]{1,0:T(8,128)S(1)}, f32[72,128]{1,0:T(8,128)S(1)}, u32[]{:S(2)}, u32[]{:S(2)}) collective-permute-start(f32[72,128]{1,0:T(8,128)S(1)} %get-tuple-element.105.own), channel_id=1, source_target_pairs={{0,6},{6,0},{2,4},{4,2},{1,7},{7,1},{3,5},{5,3},{8,14},{14,8},{10,... | collective-permute-start | bytes 110600 | tf_op jit(solution)/shard_map/ppermute | solution.py:471
  20.2 2.1 %local_2.1 = (f32[128,128]{1,0:T(8,128)S(1)}, bf16[4,2,128,256]{3,2,1,0:T(8,128)(2,1)S(1)}, f32[4,2,2,32,128]{4,3,2,1,0:T(8,128)S(1)}) custom-call(f32[2,128,128]{2,1,0:T(8,128)S(1)} %get-tuple-element.88.within, f32[32,2,128,128]{3,2,1,0:T(8,128)S(1)} %get-tuple-element.89.damps, bf16[128,1024]{1,0:T(8,128)(2,1)S(1)} %get-tuple-element.142.driven, ...), custom_call_target="tpu_custom_call" | custom-call | flops 500000000 | bytes 2097152 | tf_op jit(solution)/shard_map/local_2/pallas_call | solution.py:372
  22.2 0.0 collective-permute-done.2.other
  22.2 0.1 stage_y_high.1
  22.3 1.3 %collective-permute-start.3 = (f32[72,128]{1,0:T(8,128)S(1)}, f32[72,128]{1,0:T(8,128)S(1)}, u32[]{:S(2)}, u32[]{:S(2)}) collective-permute-start(f32[72,128]{1,0:T(8,128)S(1)} %get-tuple-element.112.own), channel_id=1, source_target_pairs={{0,8},{8,0},{16,24},{24,16},{1,9},{9,1},{17,25},{25,17},{2,10},{10... | collective-permute-start | bytes 110600 | tf_op jit(solution)/shard_map/ppermute | solution.py:471
  23.6 2.1 %local_3.1 = (f32[128,128]{1,0:T(8,128)S(1)}, bf16[4,2,128,256]{3,2,1,0:T(8,128)(2,1)S(1)}, f32[4,2,2,32,128]{4,3,2,1,0:T(8,128)S(1)}) custom-call(f32[2,128,128]{2,1,0:T(8,128)S(1)} %get-tuple-element.88.within, f32[32,2,128,128]{3,2,1,0:T(8,128)S(1)} %get-tuple-element.89.damps, bf16[128,1024]{1,0:T(8,128)(2,1)S(1)} %get-tuple-element.142.driven, ...), custom_call_target="tpu_custom_call" | custom-call | flops 500000000 | bytes 2097152 | tf_op jit(solution)/shard_map/local_3/pallas_call | solution.py:372
  25.7 0.0 collective-permute-done.3.other
  25.7 0.1 stage_x_low.1
  25.8 2.1 %collective-permute-start.4 = (f32[72,128]{1,0:T(8,128)S(1)}, f32[72,128]{1,0:T(8,128)S(1)}, u32[]{:S(2)}, u32[]{:S(2)}) collective-permute-start(f32[72,128]{1,0:T(8,128)S(1)} %get-tuple-element.119.own), channel_id=1, source_target_pairs={{0,24},{24,0},{8,16},{16,8},{1,25},{25,1},{9,17},{17,9},{2,26},{26... | collective-permute-start | bytes 110600 | tf_op jit(solution)/shard_map/ppermute | solution.py:471
  27.8 2.1 %local_4.1 = (f32[128,128]{1,0:T(8,128)S(1)}, bf16[4,2,128,256]{3,2,1,0:T(8,128)(2,1)S(1)}, f32[4,2,2,32,128]{4,3,2,1,0:T(8,128)S(1)}) custom-call(f32[2,128,128]{2,1,0:T(8,128)S(1)} %get-tuple-element.88.within, f32[32,2,128,128]{3,2,1,0:T(8,128)S(1)} %get-tuple-element.89.damps, bf16[128,1024]{1,0:T(8,128)(2,1)S(1)} %get-tuple-element.142.driven, ...), custom_call_target="tpu_custom_call" | custom-call | flops 500000000 | bytes 2097152 | tf_op jit(solution)/shard_map/local_4/pallas_call | solution.py:372
  29.9 0.0 collective-permute-done.4.other
  29.9 0.1 stage_x_high.1
  30.0 1.9 %collective-permute-start.5 = (f32[72,128]{1,0:T(8,128)S(1)}, f32[72,128]{1,0:T(8,128)S(1)}, u32[]{:S(2)}, u32[]{:S(2)}) collective-permute-start(f32[72,128]{1,0:T(8,128)S(1)} %get-tuple-element.126.own), channel_id=1, source_target_pairs={{0,32},{32,0},{64,96},{96,64},{1,33},{33,1},{65,97},{97,65},{2,34}... | collective-permute-start | bytes 110600 | tf_op jit(solution)/shard_map/ppermute | solution.py:471
  31.9 2.1 %local_5.1 = (f32[128,128]{1,0:T(8,128)S(1)}, bf16[4,2,128,256]{3,2,1,0:T(8,128)(2,1)S(1)}, f32[4,2,2,32,128]{4,3,2,1,0:T(8,128)S(1)}) custom-call(f32[2,128,128]{2,1,0:T(8,128)S(1)} %get-tuple-element.88.within, f32[32,2,128,128]{3,2,1,0:T(8,128)S(1)} %get-tuple-element.89.damps, bf16[128,1024]{1,0:T(8,128)(2,1)S(1)} %get-tuple-element.142.driven, ...), custom_call_target="tpu_custom_call" | custom-call | flops 500000000 | bytes 2097152 | tf_op jit(solution)/shard_map/local_5/pallas_call | solution.py:372
  34.0 0.0 collective-permute-done.5.other
  34.0 0.1 stage_z_low.1
  34.0 2.9 %collective-permute-start.6 = (f32[72,128]{1,0:T(8,128)S(1)}, f32[72,128]{1,0:T(8,128)S(1)}, u32[]{:S(2)}, u32[]{:S(2)}) collective-permute-start(f32[72,128]{1,0:T(8,128)S(1)} %get-tuple-element.133), channel_id=1, source_target_pairs={{0,96},{96,0},{32,64},{64,32},{1,97},{97,1},{33,65},{65,33},{2,98}... | collective-permute-start | bytes 110600 | tf_op jit(solution)/shard_map/ppermute | solution.py:471
  36.9 2.1 %local_6.1 = (f32[128,128]{1,0:T(8,128)S(1)}, bf16[4,2,128,256]{3,2,1,0:T(8,128)(2,1)S(1)}, f32[4,2,2,32,128]{4,3,2,1,0:T(8,128)S(1)}) custom-call(f32[2,128,128]{2,1,0:T(8,128)S(1)} %get-tuple-element.88.within, f32[32,2,128,128]{3,2,1,0:T(8,128)S(1)} %get-tuple-element.89.damps, bf16[128,1024]{1,0:T(8,128)(2,1)S(1)} %get-tuple-element.142.driven, ...), custom_call_target="tpu_custom_call" | custom-call | flops 500000000 | bytes 2097152 | tf_op jit(solution)/shard_map/local_6/pallas_call | solution.py:372
  39.0 0.0 copy-start.4
  39.0 0.0 copy-start.5
  39.0 0.0 copy-start.7
  39.1 0.0 copy-start.8
  39.1 0.0 collective-permute-done.6.last
  39.1 0.1 enter.1
  39.1 4.8 %collective-permute-start.7 = (f32[4,16,128]{2,1,0:T(8,128)S(1)}, f32[4,16,128]{2,1,0:T(8,128)S(1)}, u32[]{:S(2)}, u32[]{:S(2)}) collective-permute-start(f32[4,16,128]{2,1,0:T(8,128)S(1)} %get-tuple-element.141), channel_id=1, source_target_pairs={{0,1},{1,0},{2,3},{3,2},{4,5},{5,4},{6,7},{7,6},{8,9},{9,8},{10,11... | collective-permute-start | bytes 98312 | tf_op jit(solution)/shard_map/ppermute | solution.py:482
  43.9 2.1 %local_7.1 = (f32[128,128]{1,0:T(8,128)S(1)}, bf16[4,2,128,256]{3,2,1,0:T(8,128)(2,1)S(1)}, f32[4,2,2,32,128]{4,3,2,1,0:T(8,128)S(1)}) custom-call(f32[2,128,128]{2,1,0:T(8,128)S(1)} %get-tuple-element.88.within, f32[32,2,128,128]{3,2,1,0:T(8,128)S(1)} %get-tuple-element.89.damps, bf16[128,1024]{1,0:T(8,128)(2,1)S(1)} %get-tuple-element.142.driven, ...), custom_call_target="tpu_custom_call" | custom-call | flops 500000000 | bytes 2097152 | tf_op jit(solution)/shard_map/local_7/pallas_call | solution.py:372
  46.0 0.0 collective-permute-done.7.refs_1_
  46.0 0.0 copy-done.4
  46.0 0.0 copy-done.5
  46.0 0.0 copy-done.7
  46.0 0.0 copy-done.8
  46.0 3.3 %final.1 = bf16[128,2048]{1,0:T(8,128)(2,1)} custom-call(f32[4,16,128]{2,1,0:T(8,128)S(1)} %get-tuple-element.140.refs_0_, f32[4,16,128]{2,1,0:T(8,128)S(1)} %collective-permute-done.7.refs_1_, f32[128,128]{1,0:T(8,128)S(1)} %get-tuple-element.147.refs_2_, f32[128,128]{1,0:T(8,128)S(1)} %get-tuple-element.148.refs_3_, ...), custom_call_target="tpu_custom_call" | custom-call | tf_op jit(solution)/shard_map/final/pallas_call | solution.py:489
  (1 shorter events, 0.0 us)
Async XLA Ops:
  0.0 12.1 %copy-start.2 = (f32[2,64,64]{2,1,0:T(8,128)S(1)}, f32[2,64,64]{2,1,0:T(8,128)}, u32[]{:S(2)}) copy-start(f32[2,64,64]{2,1,0:T(8,128)} %angle.17) | copy-start | bytes 98308
  0.0 12.1 %copy-start.3 = (f32[2,64,64]{2,1,0:T(8,128)S(1)}, f32[2,64,64]{2,1,0:T(8,128)}, u32[]{:S(2)}) copy-start(f32[2,64,64]{2,1,0:T(8,128)} %rate.17) | copy-start | bytes 98308
  0.0 12.1 %copy-start.1 = (bf16[2,2,64,64,16]{3,4,2,1,0:T(8,128)(2,1)S(1)}, bf16[2,2,64,64,16]{3,4,2,1,0:T(8,128)(2,1)}, u32[]{:S(2)}) copy-start(bf16[2,2,64,64,16]{3,4,2,1,0:T(8,128)(2,1)} %param.17) | copy-start | bytes 1572868
  0.0 12.1 %copy-start = (f32[2,2,64,16,64]{4,3,2,1,0:T(8,128)S(1)}, f32[2,2,64,16,64]{4,3,2,1,0:T(8,128)}, u32[]{:S(2)}) copy-start(f32[2,2,64,16,64]{4,3,2,1,0:T(8,128)} %readout.15) | copy-start | bytes 3145732
  0.0 12.1 %copy-start.6 = (f32[1024]{0:T(1024)S(1)}, f32[1024]{0:T(1024)}, u32[]{:S(2)}) copy-start(f32[1024]{0:T(1024)} %param.21) | copy-start | bytes 12292
  10.6 3.6 %collective-permute-start = (f32[72,128]{1,0:T(8,128)S(1)}, f32[72,128]{1,0:T(8,128)S(1)}, u32[]{:S(2)}, u32[]{:S(2)}) collective-permute-start(f32[72,128]{1,0:T(8,128)S(1)} %get-tuple-element.171), channel_id=1, source_target_pairs={{0,1},{1,0},{2,3},{3,2},{4,5},{5,4},{6,7},{7,6},{8,9},{9,8},{10,11... | collective-permute-start | bytes 110600 | tf_op jit(solution)/shard_map/ppermute | solution.py:467
  14.3 3.6 %collective-permute-start.1 = (f32[72,128]{1,0:T(8,128)S(1)}, f32[72,128]{1,0:T(8,128)S(1)}, u32[]{:S(2)}, u32[]{:S(2)}) collective-permute-start(f32[72,128]{1,0:T(8,128)S(1)} %get-tuple-element.98.own), channel_id=1, source_target_pairs={{0,2},{2,0},{4,6},{6,4},{1,3},{3,1},{5,7},{7,5},{8,10},{10,8},{12,... | collective-permute-start | bytes 110600 | tf_op jit(solution)/shard_map/ppermute | solution.py:471
  17.9 4.3 %collective-permute-start.2 = (f32[72,128]{1,0:T(8,128)S(1)}, f32[72,128]{1,0:T(8,128)S(1)}, u32[]{:S(2)}, u32[]{:S(2)}) collective-permute-start(f32[72,128]{1,0:T(8,128)S(1)} %get-tuple-element.105.own), channel_id=1, source_target_pairs={{0,6},{6,0},{2,4},{4,2},{1,7},{7,1},{3,5},{5,3},{8,14},{14,8},{10,... | collective-permute-start | bytes 110600 | tf_op jit(solution)/shard_map/ppermute | solution.py:471
  22.3 3.4 %collective-permute-start.3 = (f32[72,128]{1,0:T(8,128)S(1)}, f32[72,128]{1,0:T(8,128)S(1)}, u32[]{:S(2)}, u32[]{:S(2)}) collective-permute-start(f32[72,128]{1,0:T(8,128)S(1)} %get-tuple-element.112.own), channel_id=1, source_target_pairs={{0,8},{8,0},{16,24},{24,16},{1,9},{9,1},{17,25},{25,17},{2,10},{10... | collective-permute-start | bytes 110600 | tf_op jit(solution)/shard_map/ppermute | solution.py:471
  25.8 4.1 %collective-permute-start.4 = (f32[72,128]{1,0:T(8,128)S(1)}, f32[72,128]{1,0:T(8,128)S(1)}, u32[]{:S(2)}, u32[]{:S(2)}) collective-permute-start(f32[72,128]{1,0:T(8,128)S(1)} %get-tuple-element.119.own), channel_id=1, source_target_pairs={{0,24},{24,0},{8,16},{16,8},{1,25},{25,1},{9,17},{17,9},{2,26},{26... | collective-permute-start | bytes 110600 | tf_op jit(solution)/shard_map/ppermute | solution.py:471
  30.0 4.0 %collective-permute-start.5 = (f32[72,128]{1,0:T(8,128)S(1)}, f32[72,128]{1,0:T(8,128)S(1)}, u32[]{:S(2)}, u32[]{:S(2)}) collective-permute-start(f32[72,128]{1,0:T(8,128)S(1)} %get-tuple-element.126.own), channel_id=1, source_target_pairs={{0,32},{32,0},{64,96},{96,64},{1,33},{33,1},{65,97},{97,65},{2,34}... | collective-permute-start | bytes 110600 | tf_op jit(solution)/shard_map/ppermute | solution.py:471
  34.0 5.0 %collective-permute-start.6 = (f32[72,128]{1,0:T(8,128)S(1)}, f32[72,128]{1,0:T(8,128)S(1)}, u32[]{:S(2)}, u32[]{:S(2)}) collective-permute-start(f32[72,128]{1,0:T(8,128)S(1)} %get-tuple-element.133), channel_id=1, source_target_pairs={{0,96},{96,0},{32,64},{64,32},{1,97},{97,1},{33,65},{65,33},{2,98}... | collective-permute-start | bytes 110600 | tf_op jit(solution)/shard_map/ppermute | solution.py:471
  39.0 7.0 %copy-start.4 = (bf16[1024,2048]{1,0:T(8,128)(2,1)S(1)}, bf16[1024,2048]{1,0:T(8,128)(2,1)}, u32[]{:S(2)}) copy-start(bf16[1024,2048]{1,0:T(8,128)(2,1)} %refs_28_.1) | copy-start | bytes 12582916
  39.0 7.0 %copy-start.5 = (bf16[1024,1024]{1,0:T(8,128)(2,1)S(1)}, bf16[1024,1024]{1,0:T(8,128)(2,1)}, u32[]{:S(2)}) copy-start(bf16[1024,1024]{1,0:T(8,128)(2,1)} %refs_26_.1) | copy-start | bytes 6291460
  39.0 7.0 %copy-start.7 = (f32[2048]{0:T(1024)S(1)}, f32[2048]{0:T(1024)}, u32[]{:S(2)}) copy-start(f32[2048]{0:T(1024)} %param.25) | copy-start | bytes 24580
  39.1 7.0 %copy-start.8 = (f32[1024]{0:T(1024)S(1)}, f32[1024]{0:T(1024)}, u32[]{:S(2)}) copy-start(f32[1024]{0:T(1024)} %param.23) | copy-start | bytes 12292
  39.1 6.9 %collective-permute-start.7 = (f32[4,16,128]{2,1,0:T(8,128)S(1)}, f32[4,16,128]{2,1,0:T(8,128)S(1)}, u32[]{:S(2)}, u32[]{:S(2)}) collective-permute-start(f32[4,16,128]{2,1,0:T(8,128)S(1)} %get-tuple-element.141), channel_id=1, source_target_pairs={{0,1},{1,0},{2,3},{3,2},{4,5},{5,4},{6,7},{7,6},{8,9},{9,8},{10,11... | collective-permute-start | bytes 98312 | tf_op jit(solution)/shard_map/ppermute | solution.py:482

commit v4 on v3

--- a/solution.py
+++ b/solution.py
@@ -86,7 +86,6 @@
     driven_ref, ends_ref, pars_ref, damp_ref, within_ref, normed, times,
 ):
     step = pl.program_id(0)
-    core = lax.axis_index("c")
 
     @pl.when(step == 0)
     def _():
@@ -103,14 +102,12 @@
         within_ref[0] = exact_mm(((col <= row) & same).astype(F32), steps)
         within_ref[1] = exact_mm(((col >= row) & same).astype(F32), steps)
         total = exact_mm(jnp.ones((8, ROWS), F32), steps)
-        ends_ref[0, 64:] = total
-        ends_ref[1, 64:] = total
+        ends_ref[128:, :] = total
 
     driven = mm(normed[...], weight[...]).astype(BF16)
     driven_ref[...] = driven
     flipped = driven.astype(F32).T.astype(BF16)
     first = lax.broadcasted_iota(jnp.int32, (16, 128), 1) < 64
-    away = jnp.where((step // 4) == core, 0, 1)
     for j in range(4):
         pair = step * 4 + j
         for k in range(2):
@@ -134,9 +131,9 @@
                 jnp.concatenate([inputs[k, c, 2 * j].astype(F32), inputs[k, c, 2 * j + 1].astype(F32)], axis=1)
                 for c in range(2)
             )
-            at = 32 * k + 4 * (step % 4) + j
-            ends_ref[away, pl.ds(at, 1), :] = root * jnp.sum(b_re * m_re - b_im * m_im, axis=0, keepdims=True)
-            ends_ref[away, pl.ds(at + 16, 1), :] = root * jnp.sum(b_re * m_im + b_im * m_re, axis=0, keepdims=True)
+            at = 64 * k + pair
+            ends_ref[pl.ds(at, 1), :] = root * jnp.sum(b_re * m_re - b_im * m_im, axis=0, keepdims=True)
+            ends_ref[pl.ds(at + 32, 1), :] = root * jnp.sum(b_re * m_im + b_im * m_re, axis=0, keepdims=True)
 
 
 def local_kernel(
@@ -223,11 +220,9 @@
 
 
 def my_pars(pars):
-    core = lax.axis_index("c")
     found = []
     for k in range(2):
-        angle = pars[k, 0, pl.ds(16 * core, 16), :]
-        rate = pars[k, 1, pl.ds(16 * core, 16), :]
+        angle, rate = pars[k, 0], pars[k, 1]
         high = jnp.round(angle * (4096 * 0.5 / math.pi)) * (1.0 / 4096)
         coarse = 6433 / 1024
         low = ((angle - high * coarse) - high * (2 * math.pi - coarse)) * (0.5 / math.pi)
@@ -244,16 +239,23 @@
 
 
 def states_of(ref, k):
-    return ref[32 * k : 32 * k + 16, :], ref[32 * k + 16 : 32 * k + 32, :]
+    return ref[64 * k : 64 * k + 32, :], ref[64 * k + 32 : 64 * k + 64, :]
+
+
+def keep_states(ref, k, value):
+    ref[64 * k : 64 * k + 32, :], ref[64 * k + 32 : 64 * k + 64, :] = value
 
 
 def span_of(ref):
-    span = ref[64:72, :]
-    return jnp.concatenate([span, span], axis=0)
-
-
-def keep_at(ref, at, value):
-    ref[2 * at], ref[2 * at + 1] = value
+    return jnp.concatenate([ref[128:136, :]] * 4, axis=0)
+
+
+def trail_of(trail, at):
+    return trail[2 * at], trail[2 * at + 1]
+
+
+def keep_trail(trail, at, value):
+    trail[2 * at], trail[2 * at + 1] = value
 
 
 def upper(stage):
@@ -262,56 +264,48 @@
     return here >= 2 if kind == "high" else here % 2 == 1
 
 
-def merge(stage, own, other, mine, total_ref, k, decay, decay_other):
-    behind = upper(stage) if k == 0 else jnp.logical_not(upper(stage))
-    a, b = states_of(own, k), states_of(other, k)
-    early, late = pick(behind, b, a), pick(behind, a, b)
-    total = plus(times_of(pick(behind, decay, decay_other), early), late)
-    if total_ref is not None:
-        total_ref[32 * k : 32 * k + 16, :], total_ref[32 * k + 16 : 32 * k + 32, :] = total
-    return behind, b
+def is_behind(stage, k):
+    return upper(stage) if k == 0 else jnp.logical_not(upper(stage))
 
 
 def pair_kernel(own, other, pars, total_ref, trail_ref):
     mine = my_pars(pars)
-    zero = jnp.zeros((16, 128), F32)
+    zero = jnp.zeros((32, 128), F32)
     for k in range(2):
         decay, decay_other = decay_over(span_of(own), mine[k]), decay_over(span_of(other), mine[k])
-        merge(("c", "low"), own, other, mine, total_ref, k, decay, decay_other)
-        keep_at(trail_ref, k, (zero, zero))
-        keep_at(trail_ref, 2 + k, (zero + 1.0, zero))
-        keep_at(trail_ref, 4 + k, times_of(decay, decay_other))
-    total_ref[64:72, :] = own[64:72, :] + other[64:72, :]
-
-
-def trail_of(trail, at):
-    return trail[2 * at], trail[2 * at + 1]
+        a, b = states_of(own, k), states_of(other, k)
+        total = plus(times_of(decay, b), a) if k == 0 else plus(times_of(decay_other, a), b)
+        keep_states(total_ref, k, total)
+        keep_trail(trail_ref, k, (zero, zero))
+        keep_trail(trail_ref, 2 + k, (zero + 1.0, zero))
+        keep_trail(trail_ref, 4 + k, times_of(decay, decay_other))
+    total_ref[128:136, :] = own[128:136, :] + other[128:136, :]
 
 
 def stage_kernel(stage, own, other, trail, pars, total_ref, trail_ref):
     mine = my_pars(pars)
     for k in range(2):
         decay, decay_other = trail_of(trail, 4 + k), decay_over(span_of(other), mine[k])
-        behind, theirs = merge(stage, own, other, mine, total_ref, k, decay, decay_other)
+        behind = is_behind(stage, k)
+        a, b = states_of(own, k), states_of(other, k)
+        early, late = pick(behind, b, a), pick(behind, a, b)
+        keep_states(total_ref, k, plus(times_of(pick(behind, decay, decay_other), early), late))
         state, fade = trail_of(trail, k), trail_of(trail, 2 + k)
-        keep_at(trail_ref, k, pick(behind, plus(times_of(fade, theirs), state), state))
-        keep_at(trail_ref, 2 + k, pick(behind, times_of(fade, decay_other), fade))
-        keep_at(trail_ref, 4 + k, times_of(decay, decay_other))
-    total_ref[64:72, :] = own[64:72, :] + other[64:72, :]
+        keep_trail(trail_ref, k, pick(behind, plus(times_of(fade, b), state), state))
+        keep_trail(trail_ref, 2 + k, pick(behind, times_of(fade, decay_other), fade))
+        keep_trail(trail_ref, 4 + k, times_of(decay, decay_other))
+    total_ref[128:136, :] = own[128:136, :] + other[128:136, :]
 
 
 def enter_kernel(stage, last, trail, own, other, pars, mine_ref, theirs_ref):
-    core = lax.axis_index("c")
     mine = my_pars(pars)
     for k in range(2):
-        behind = upper(stage) if k == 0 else jnp.logical_not(upper(stage))
         state, fade = trail_of(trail, k), trail_of(trail, 2 + k)
-        state = pick(behind, plus(times_of(fade, states_of(last, k)), state), state)
-        ahead = core == k
-        early = pick(ahead, states_of(own, k), states_of(other, k))
-        later = plus(times_of(decay_over(jnp.where(ahead, span_of(own), span_of(other)), mine[k]), state), early)
-        keep_at(mine_ref, k, pick(ahead, state, later))
-        keep_at(theirs_ref, k, pick(ahead, later, state))
+        state = pick(is_behind(stage, k), plus(times_of(fade, states_of(last, k)), state), state)
+        early = other if k == 0 else own
+        later = plus(times_of(decay_over(span_of(early), mine[k]), state), states_of(early, k))
+        keep_states(mine_ref, k, later if k == 0 else state)
+        keep_states(theirs_ref, k, state if k == 0 else later)
 
 
 def final_kernel(*refs):
@@ -319,9 +313,7 @@
     own, other = refs[:2]
     nears, prefixes, tables = (refs[2 + count * n : 2 + count * n + count] for n in range(3))
     glu, glu_bias, outw, out_gain, out_ref, entering, response = refs[2 + 3 * count :]
-    core = lax.axis_index("c")
-    entering[core] = own[...]
-    entering[1 - core] = other[...]
+    entering[...] = jnp.where(lax.axis_index("c") == 1, own[...], other[...])
     start = 0
     for size, near, prefix, table in zip(PIECES, nears, prefixes, tables):
 
@@ -331,8 +323,8 @@
                 total = None
                 for k in range(2):
                     pair = 4 * (start + i) + j
-                    er = entering[pair // 16, 2 * k, pl.ds(pair % 16, 1), :]
-                    ei = entering[pair // 16, 2 * k + 1, pl.ds(pair % 16, 1), :]
+                    er = entering[pl.ds(64 * k + pair, 1), :]
+                    ei = entering[pl.ds(64 * k + 32 + pair, 1), :]
                     cr, ci = table[4 * i + j, k, 0], table[4 * i + j, k, 1]
                     rhs = jnp.concatenate(
                         [(cr * er - ci * ei).astype(BF16), (-(cr * ei + ci * er)).astype(BF16)], axis=1
@@ -431,13 +423,13 @@
         ],
         out_specs=[
             pl.BlockSpec((ROWS, 128), lambda i: (0, i)),
-            whole((2, 72, 128)),
+            whole((136, 128)),
             whole((2, 2, 32, 128)),
             pl.BlockSpec((4, 2, ROWS, ROWS), lambda i: (i, 0, 0, 0)),
             whole((2, ROWS, ROWS)),
         ],
         out_shape=[
-            sds((ROWS, CHANNELS), BF16), sds((2, 72, 128)), sds((2, 2, 32, 128)),
+            sds((ROWS, CHANNELS), BF16), sds((136, 128)), sds((2, 2, 32, 128)),
             sds((32, 2, ROWS, ROWS)), sds((2, ROWS, ROWS)),
         ],
         scratch_shapes=[VMEM((ROWS, D), BF16), VMEM((4, ROWS, ROWS), F32)],
@@ -460,26 +452,25 @@
         pieces.append(piece)
         return after
 
-    swap = [(0, 1), (1, 0)]
-    pairings = {"low": [(0, 1), (1, 0), (2, 3), (3, 2)], "high": [(0, 3), (3, 0), (1, 2), (2, 1)]}
+    pairings = {"low": (1, 0, 3, 2), "high": (3, 2, 1, 0)}
     stages = [(axis, kind) for axis in ("y", "x", "z") for kind in ("low", "high")]
-    keep = ends[0]
-    partner = piece_between(keep, lax.ppermute(ends[1], "c", swap))
-    total, trail = simple(pair_kernel, "pair", [(72, 128), (12, 16, 128)], (keep, partner, pars))
+    partner = piece_between(ends, lax.ppermute(ends, "c", [(0, 1)]))
+    total, trail = simple(pair_kernel, "pair", [(136, 128), (12, 32, 128)], (ends, partner, pars))
     for stage in stages:
         axis, kind = stage
-        other = piece_between(total, lax.ppermute(total, axis, pairings[kind]))
+        pairs = [(2 * i + 1, 2 * j + 1) for i, j in enumerate(pairings[kind])]
+        other = piece_between(total, lax.ppermute(total, (axis, "c"), pairs))
         if stage == stages[-1]:
             mine, theirs = simple(
-                functools.partial(enter_kernel, stage), "enter", [(4, 16, 128), (4, 16, 128)],
-                (other, trail, keep, partner, pars),
+                functools.partial(enter_kernel, stage), "enter", [(128, 128), (128, 128)],
+                (other, trail, ends, partner, pars),
             )
         else:
             total, trail = simple(
-                functools.partial(stage_kernel, stage), f"stage_{axis}_{kind}", [(72, 128), (12, 16, 128)],
+                functools.partial(stage_kernel, stage), f"stage_{axis}_{kind}", [(136, 128), (12, 32, 128)],
                 (total, other, trail, pars),
             )
-    other = piece_between(theirs, lax.ppermute(theirs, "c", swap))
+    other = piece_between(theirs, lax.ppermute(theirs, "c", [(1, 0)]))
 
     spec = pl.BlockSpec(memory_space=VMEM)
     args = (
@@ -492,7 +483,7 @@
         in_specs=[spec] * len(args),
         out_specs=spec,
         out_shape=sds((ROWS, D), BF16),
-        scratch_shapes=[VMEM((2, 4, 16, 128), F32), VMEM((ROWS, CHANNELS), F32)],
+        scratch_shapes=[VMEM((128, 128), F32), VMEM((ROWS, CHANNELS), F32)],
         compiler_params=params(12),
     )(*args)
 

time: 49.6 us -> 59.3 us (1.20)
  starting transfers between devices: 18.1 us -> 27.4 us
    ppermute x8, starting transfers between devices: 18.1 us -> 27.4 us  [the longest x6 24.5 us: local(): other = piece_between(total, lax.ppermute(total, (axis, 'c'), pairs))]
  transfers between devices with their start and end apart: 8 -> 8, of which waited for: 0 -> 0; matrix products, arithmetic and copies ran while one was open for 0% -> 0% of each run, Pallas kernels for 34% -> 28%
where the time goes in v4:
time: 59.3 us; the launch traced here: 59 us
  Pallas kernels  31.1 us (52%)
  starting transfers between devices  27.4 us (46%)
    ppermute x6, starting transfers between devices, local(): other = piece_between(total, lax.ppermute(total, (axis, 'c'), pairs))  24.5 us
    pallas_call x8, Pallas kernels, run_local(): pl.pallas_call(functools.partial(local_kernel, start), name=f'local_{star...  16.6 us
    pallas_call x1, Pallas kernels, local(): pl.pallas_call(end_kernel, name='ends', grid=(TILES,), in_specs=[whole((R...  10.5 us
    pallas_call x1, Pallas kernels, local(): pl.pallas_call(final_kernel, name='final', in_specs=[spec] * len(args), o...  3.32 us
    ppermute x1, starting transfers between devices, local(): other = piece_between(theirs, lax.ppermute(theirs, 'c', [(1, 0)]))  1.56 us
    ppermute x1, starting transfers between devices, local(): partner = piece_between(ends, lax.ppermute(ends, 'c', [(0, 1)]))  1.29 us
  transfers between devices with their start and end apart: 8, of which 0 were waited for; matrix products, arithmetic and copies ran while one was open for 0% of the time, Pallas kernels for 28%

profile of v4, /device:TPU:1, one launch (start us, length us, event | category | flops | bytes accessed | tf_op | source)
XLA Modules:
  0.0 59.0 jit_solution(16312328480434546763)
XLA Ops:
  0.0 0.0 copy-start.2
  0.0 0.0 copy-start.3
  0.0 0.0 copy-start.1
  0.0 0.0 copy-start
  0.0 0.0 copy-start.6
  0.0 10.5 %ends.1 = (bf16[128,1024]{1,0:T(8,128)(2,1)S(1)}, f32[136,128]{1,0:T(8,128)S(1)}, f32[2,2,32,128]{3,2,1,0:T(8,128)S(1)}, f32[32,2,128,128]{3,2,1,0:T(8,128)S(1)}, f32[2,128,128]{2,1,0:T(8,128)S(1)}) custom-call(bf16[128,2048]{1,0:T(8,128)(2,1)} %tokens.1, f32[1,128]{1,0:T(1,128)} %bitcast.26, f32[1,2048]{1,0:T(1,128)} %bitcast.25, ...), custom_call_target="tpu_custom_call" | custom-call | tf_op jit(solution)/shard_map/ends/pallas_call | solution.py:412
  10.6 1.3 %collective-permute-start = (f32[136,128]{1,0:T(8,128)S(1)}, f32[136,128]{1,0:T(8,128)S(1)}, u32[]{:S(2)}, u32[]{:S(2)}) collective-permute-start(f32[136,128]{1,0:T(8,128)S(1)} %get-tuple-element.91.own), channel_id=1, source_target_pairs={{0,1},{2,3},{4,5},{6,7},{8,9},{10,11},{12,13},{14,15},{16,17},{18,... | collective-permute-start | bytes 208904 | tf_op jit(solution)/shard_map/ppermute | solution.py:457
  11.9 0.0 copy-done.2
  11.9 0.0 copy-done.3
  11.9 0.0 copy-done.1
  11.9 0.0 copy-done
  11.9 0.0 copy-done.6
  11.9 2.1 %local_0.1 = (f32[128,128]{1,0:T(8,128)S(1)}, bf16[4,2,128,256]{3,2,1,0:T(8,128)(2,1)S(1)}, f32[4,2,2,32,128]{4,3,2,1,0:T(8,128)S(1)}) custom-call(f32[2,128,128]{2,1,0:T(8,128)S(1)} %get-tuple-element.88.within, f32[32,2,128,128]{3,2,1,0:T(8,128)S(1)} %get-tuple-element.89.damps, bf16[128,1024]{1,0:T(8,128)(2,1)S(1)} %get-tuple-element.142.driven, ...), custom_call_target="tpu_custom_call" | custom-call | flops 500000000 | bytes 2097152 | tf_op jit(solution)/shard_map/local_0/pallas_call | solution.py:364
  14.0 0.0 collective-permute-done.other
  14.0 0.1 pair.1
  14.1 4.0 %collective-permute-start.1 = (f32[136,128]{1,0:T(8,128)S(1)}, f32[136,128]{1,0:T(8,128)S(1)}, u32[]{:S(2)}, u32[]{:S(2)}) collective-permute-start(f32[136,128]{1,0:T(8,128)S(1)} %get-tuple-element.98.own), channel_id=1, source_target_pairs={{1,3},{3,1},{5,7},{7,5},{9,11},{11,9},{13,15},{15,13},{17,19},{19,... | collective-permute-start | bytes 208904 | tf_op jit(solution)/shard_map/ppermute | solution.py:462
  18.2 2.1 %local_1.1 = (f32[128,128]{1,0:T(8,128)S(1)}, bf16[4,2,128,256]{3,2,1,0:T(8,128)(2,1)S(1)}, f32[4,2,2,32,128]{4,3,2,1,0:T(8,128)S(1)}) custom-call(f32[2,128,128]{2,1,0:T(8,128)S(1)} %get-tuple-element.88.within, f32[32,2,128,128]{3,2,1,0:T(8,128)S(1)} %get-tuple-element.89.damps, bf16[128,1024]{1,0:T(8,128)(2,1)S(1)} %get-tuple-element.142.driven, ...), custom_call_target="tpu_custom_call" | custom-call | flops 500000000 | bytes 2097152 | tf_op jit(solution)/shard_map/local_1/pallas_call | solution.py:364
  20.3 0.0 collective-permute-done.1.other
  20.3 0.1 stage_y_low.1
  20.4 4.4 %collective-permute-start.2 = (f32[136,128]{1,0:T(8,128)S(1)}, f32[136,128]{1,0:T(8,128)S(1)}, u32[]{:S(2)}, u32[]{:S(2)}) collective-permute-start(f32[136,128]{1,0:T(8,128)S(1)} %get-tuple-element.105.own), channel_id=1, source_target_pairs={{1,7},{3,5},{5,3},{7,1},{9,15},{11,13},{13,11},{15,9},{17,23},{19,... | collective-permute-start | bytes 208904 | tf_op jit(solution)/shard_map/ppermute | solution.py:462
  24.8 2.1 %local_2.1 = (f32[128,128]{1,0:T(8,128)S(1)}, bf16[4,2,128,256]{3,2,1,0:T(8,128)(2,1)S(1)}, f32[4,2,2,32,128]{4,3,2,1,0:T(8,128)S(1)}) custom-call(f32[2,128,128]{2,1,0:T(8,128)S(1)} %get-tuple-element.88.within, f32[32,2,128,128]{3,2,1,0:T(8,128)S(1)} %get-tuple-element.89.damps, bf16[128,1024]{1,0:T(8,128)(2,1)S(1)} %get-tuple-element.142.driven, ...), custom_call_target="tpu_custom_call" | custom-call | flops 500000000 | bytes 2097152 | tf_op jit(solution)/shard_map/local_2/pallas_call | solution.py:364
  26.8 0.0 collective-permute-done.2.other
  26.9 0.1 stage_y_high.1
  27.0 3.1 %collective-permute-start.3 = (f32[136,128]{1,0:T(8,128)S(1)}, f32[136,128]{1,0:T(8,128)S(1)}, u32[]{:S(2)}, u32[]{:S(2)}) collective-permute-start(f32[136,128]{1,0:T(8,128)S(1)} %get-tuple-element.112.own), channel_id=1, source_target_pairs={{1,9},{9,1},{17,25},{25,17},{3,11},{11,3},{19,27},{27,19},{5,13},{... | collective-permute-start | bytes 208904 | tf_op jit(solution)/shard_map/ppermute | solution.py:462
  30.1 2.1 %local_3.1 = (f32[128,128]{1,0:T(8,128)S(1)}, bf16[4,2,128,256]{3,2,1,0:T(8,128)(2,1)S(1)}, f32[4,2,2,32,128]{4,3,2,1,0:T(8,128)S(1)}) custom-call(f32[2,128,128]{2,1,0:T(8,128)S(1)} %get-tuple-element.88.within, f32[32,2,128,128]{3,2,1,0:T(8,128)S(1)} %get-tuple-element.89.damps, bf16[128,1024]{1,0:T(8,128)(2,1)S(1)} %get-tuple-element.142.driven, ...), custom_call_target="tpu_custom_call" | custom-call | flops 500000000 | bytes 2097152 | tf_op jit(solution)/shard_map/local_3/pallas_call | solution.py:364
  32.2 0.0 collective-permute-done.3.other
  32.2 0.1 stage_x_low.1
  32.3 4.2 %collective-permute-start.4 = (f32[136,128]{1,0:T(8,128)S(1)}, f32[136,128]{1,0:T(8,128)S(1)}, u32[]{:S(2)}, u32[]{:S(2)}) collective-permute-start(f32[136,128]{1,0:T(8,128)S(1)} %get-tuple-element.119.own), channel_id=1, source_target_pairs={{1,25},{9,17},{17,9},{25,1},{3,27},{11,19},{19,11},{27,3},{5,29},{... | collective-permute-start | bytes 208904 | tf_op jit(solution)/shard_map/ppermute | solution.py:462
  36.5 2.1 %local_4.1 = (f32[128,128]{1,0:T(8,128)S(1)}, bf16[4,2,128,256]{3,2,1,0:T(8,128)(2,1)S(1)}, f32[4,2,2,32,128]{4,3,2,1,0:T(8,128)S(1)}) custom-call(f32[2,128,128]{2,1,0:T(8,128)S(1)} %get-tuple-element.88.within, f32[32,2,128,128]{3,2,1,0:T(8,128)S(1)} %get-tuple-element.89.damps, bf16[128,1024]{1,0:T(8,128)(2,1)S(1)} %get-tuple-element.142.driven, ...), custom_call_target="tpu_custom_call" | custom-call | flops 500000000 | bytes 2097152 | tf_op jit(solution)/shard_map/local_4/pallas_call | solution.py:364
  38.6 0.0 collective-permute-done.4.other
  38.6 0.1 stage_x_high.1
  38.7 3.5 %collective-permute-start.5 = (f32[136,128]{1,0:T(8,128)S(1)}, f32[136,128]{1,0:T(8,128)S(1)}, u32[]{:S(2)}, u32[]{:S(2)}) collective-permute-start(f32[136,128]{1,0:T(8,128)S(1)} %get-tuple-element.126.own), channel_id=1, source_target_pairs={{1,33},{33,1},{65,97},{97,65},{3,35},{35,3},{67,99},{99,67},{5,37}... | collective-permute-start | bytes 208904 | tf_op jit(solution)/shard_map/ppermute | solution.py:462
  42.3 2.1 %local_5.1 = (f32[128,128]{1,0:T(8,128)S(1)}, bf16[4,2,128,256]{3,2,1,0:T(8,128)(2,1)S(1)}, f32[4,2,2,32,128]{4,3,2,1,0:T(8,128)S(1)}) custom-call(f32[2,128,128]{2,1,0:T(8,128)S(1)} %get-tuple-element.88.within, f32[32,2,128,128]{3,2,1,0:T(8,128)S(1)} %get-tuple-element.89.damps, bf16[128,1024]{1,0:T(8,128)(2,1)S(1)} %get-tuple-element.142.driven, ...), custom_call_target="tpu_custom_call" | custom-call | flops 500000000 | bytes 2097152 | tf_op jit(solution)/shard_map/local_5/pallas_call | solution.py:364
  44.3 0.0 collective-permute-done.5.other
  44.3 0.1 stage_z_low.1
  44.4 5.3 %collective-permute-start.6 = (f32[136,128]{1,0:T(8,128)S(1)}, f32[136,128]{1,0:T(8,128)S(1)}, u32[]{:S(2)}, u32[]{:S(2)}) collective-permute-start(f32[136,128]{1,0:T(8,128)S(1)} %get-tuple-element.133), channel_id=1, source_target_pairs={{1,97},{33,65},{65,33},{97,1},{3,99},{35,67},{67,35},{99,3},{5,101... | collective-permute-start | bytes 208904 | tf_op jit(solution)/shard_map/ppermute | solution.py:462
  49.7 2.1 %local_6.1 = (f32[128,128]{1,0:T(8,128)S(1)}, bf16[4,2,128,256]{3,2,1,0:T(8,128)(2,1)S(1)}, f32[4,2,2,32,128]{4,3,2,1,0:T(8,128)S(1)}) custom-call(f32[2,128,128]{2,1,0:T(8,128)S(1)} %get-tuple-element.88.within, f32[32,2,128,128]{3,2,1,0:T(8,128)S(1)} %get-tuple-element.89.damps, bf16[128,1024]{1,0:T(8,128)(2,1)S(1)} %get-tuple-element.142.driven, ...), custom_call_target="tpu_custom_call" | custom-call | flops 500000000 | bytes 2097152 | tf_op jit(solution)/shard_map/local_6/pallas_call | solution.py:364
  51.8 0.0 copy-start.4
  51.8 0.0 copy-start.5
  51.8 0.0 copy-start.7
  51.8 0.0 copy-start.8
  51.8 0.0 collective-permute-done.6.last
  51.8 0.1 enter.1
  51.9 1.6 %collective-permute-start.7 = (f32[128,128]{1,0:T(8,128)S(1)}, f32[128,128]{1,0:T(8,128)S(1)}, u32[]{:S(2)}, u32[]{:S(2)}) collective-permute-start(f32[128,128]{1,0:T(8,128)S(1)} %get-tuple-element.141), channel_id=1, source_target_pairs={{1,0},{3,2},{5,4},{7,6},{9,8},{11,10},{13,12},{15,14},{17,16},{19,... | collective-permute-start | bytes 196616 | tf_op jit(solution)/shard_map/ppermute | solution.py:473
  53.5 2.1 %local_7.1 = (f32[128,128]{1,0:T(8,128)S(1)}, bf16[4,2,128,256]{3,2,1,0:T(8,128)(2,1)S(1)}, f32[4,2,2,32,128]{4,3,2,1,0:T(8,128)S(1)}) custom-call(f32[2,128,128]{2,1,0:T(8,128)S(1)} %get-tuple-element.88.within, f32[32,2,128,128]{3,2,1,0:T(8,128)S(1)} %get-tuple-element.89.damps, bf16[128,1024]{1,0:T(8,128)(2,1)S(1)} %get-tuple-element.142.driven, ...), custom_call_target="tpu_custom_call" | custom-call | flops 500000000 | bytes 2097152 | tf_op jit(solution)/shard_map/local_7/pallas_call | solution.py:364
  55.6 0.0 collective-permute-done.7.refs_1_
  55.6 0.0 copy-done.4
  55.6 0.0 copy-done.5
  55.6 0.0 copy-done.7
  55.6 0.0 copy-done.8
  55.6 3.3 %final.1 = bf16[128,2048]{1,0:T(8,128)(2,1)} custom-call(f32[128,128]{1,0:T(8,128)S(1)} %get-tuple-element.140.refs_0_, f32[128,128]{1,0:T(8,128)S(1)} %collective-permute-done.7.refs_1_, f32[128,128]{1,0:T(8,128)S(1)} %get-tuple-element.147.refs_2_, f32[128,128]{1,0:T(8,128)S(1)} %get-tuple-element.148.refs_3_, f32[128,128]{1,0:T(8,128)S(1)} %get-tuple-element.149.refs_4_, ...), custom_call_target="tpu_custom_call" | custom-call | tf_op jit(solution)/shard_map/final/pallas_call | solution.py:480
Async XLA Ops:
  0.0 11.9 %copy-start.2 = (f32[2,64,64]{2,1,0:T(8,128)S(1)}, f32[2,64,64]{2,1,0:T(8,128)}, u32[]{:S(2)}) copy-start(f32[2,64,64]{2,1,0:T(8,128)} %angle.17) | copy-start | bytes 98308
  0.0 11.9 %copy-start.3 = (f32[2,64,64]{2,1,0:T(8,128)S(1)}, f32[2,64,64]{2,1,0:T(8,128)}, u32[]{:S(2)}) copy-start(f32[2,64,64]{2,1,0:T(8,128)} %rate.17) | copy-start | bytes 98308
  0.0 11.9 %copy-start.1 = (bf16[2,2,64,64,16]{3,4,2,1,0:T(8,128)(2,1)S(1)}, bf16[2,2,64,64,16]{3,4,2,1,0:T(8,128)(2,1)}, u32[]{:S(2)}) copy-start(bf16[2,2,64,64,16]{3,4,2,1,0:T(8,128)(2,1)} %param.17) | copy-start | bytes 1572868
  0.0 11.9 %copy-start = (f32[2,2,64,16,64]{4,3,2,1,0:T(8,128)S(1)}, f32[2,2,64,16,64]{4,3,2,1,0:T(8,128)}, u32[]{:S(2)}) copy-start(f32[2,2,64,16,64]{4,3,2,1,0:T(8,128)} %readout.15) | copy-start | bytes 3145732
  0.0 11.9 %copy-start.6 = (f32[1024]{0:T(1024)S(1)}, f32[1024]{0:T(1024)}, u32[]{:S(2)}) copy-start(f32[1024]{0:T(1024)} %param.21) | copy-start | bytes 12292
  10.6 3.4 %collective-permute-start = (f32[136,128]{1,0:T(8,128)S(1)}, f32[136,128]{1,0:T(8,128)S(1)}, u32[]{:S(2)}, u32[]{:S(2)}) collective-permute-start(f32[136,128]{1,0:T(8,128)S(1)} %get-tuple-element.91.own), channel_id=1, source_target_pairs={{0,1},{2,3},{4,5},{6,7},{8,9},{10,11},{12,13},{14,15},{16,17},{18,... | collective-permute-start | bytes 208904 | tf_op jit(solution)/shard_map/ppermute | solution.py:457
  14.1 6.1 %collective-permute-start.1 = (f32[136,128]{1,0:T(8,128)S(1)}, f32[136,128]{1,0:T(8,128)S(1)}, u32[]{:S(2)}, u32[]{:S(2)}) collective-permute-start(f32[136,128]{1,0:T(8,128)S(1)} %get-tuple-element.98.own), channel_id=1, source_target_pairs={{1,3},{3,1},{5,7},{7,5},{9,11},{11,9},{13,15},{15,13},{17,19},{19,... | collective-permute-start | bytes 208904 | tf_op jit(solution)/shard_map/ppermute | solution.py:462
  20.4 6.5 %collective-permute-start.2 = (f32[136,128]{1,0:T(8,128)S(1)}, f32[136,128]{1,0:T(8,128)S(1)}, u32[]{:S(2)}, u32[]{:S(2)}) collective-permute-start(f32[136,128]{1,0:T(8,128)S(1)} %get-tuple-element.105.own), channel_id=1, source_target_pairs={{1,7},{3,5},{5,3},{7,1},{9,15},{11,13},{13,11},{15,9},{17,23},{19,... | collective-permute-start | bytes 208904 | tf_op jit(solution)/shard_map/ppermute | solution.py:462
  27.0 5.2 %collective-permute-start.3 = (f32[136,128]{1,0:T(8,128)S(1)}, f32[136,128]{1,0:T(8,128)S(1)}, u32[]{:S(2)}, u32[]{:S(2)}) collective-permute-start(f32[136,128]{1,0:T(8,128)S(1)} %get-tuple-element.112.own), channel_id=1, source_target_pairs={{1,9},{9,1},{17,25},{25,17},{3,11},{11,3},{19,27},{27,19},{5,13},{... | collective-permute-start | bytes 208904 | tf_op jit(solution)/shard_map/ppermute | solution.py:462
  32.3 6.3 %collective-permute-start.4 = (f32[136,128]{1,0:T(8,128)S(1)}, f32[136,128]{1,0:T(8,128)S(1)}, u32[]{:S(2)}, u32[]{:S(2)}) collective-permute-start(f32[136,128]{1,0:T(8,128)S(1)} %get-tuple-element.119.own), channel_id=1, source_target_pairs={{1,25},{9,17},{17,9},{25,1},{3,27},{11,19},{19,11},{27,3},{5,29},{... | collective-permute-start | bytes 208904 | tf_op jit(solution)/shard_map/ppermute | solution.py:462
  38.7 5.6 %collective-permute-start.5 = (f32[136,128]{1,0:T(8,128)S(1)}, f32[136,128]{1,0:T(8,128)S(1)}, u32[]{:S(2)}, u32[]{:S(2)}) collective-permute-start(f32[136,128]{1,0:T(8,128)S(1)} %get-tuple-element.126.own), channel_id=1, source_target_pairs={{1,33},{33,1},{65,97},{97,65},{3,35},{35,3},{67,99},{99,67},{5,37}... | collective-permute-start | bytes 208904 | tf_op jit(solution)/shard_map/ppermute | solution.py:462
  44.4 7.4 %collective-permute-start.6 = (f32[136,128]{1,0:T(8,128)S(1)}, f32[136,128]{1,0:T(8,128)S(1)}, u32[]{:S(2)}, u32[]{:S(2)}) collective-permute-start(f32[136,128]{1,0:T(8,128)S(1)} %get-tuple-element.133), channel_id=1, source_target_pairs={{1,97},{33,65},{65,33},{97,1},{3,99},{35,67},{67,35},{99,3},{5,101... | collective-permute-start | bytes 208904 | tf_op jit(solution)/shard_map/ppermute | solution.py:462
  51.8 3.8 %copy-start.4 = (bf16[1024,2048]{1,0:T(8,128)(2,1)S(1)}, bf16[1024,2048]{1,0:T(8,128)(2,1)}, u32[]{:S(2)}) copy-start(bf16[1024,2048]{1,0:T(8,128)(2,1)} %refs_28_.1) | copy-start | bytes 12582916
  51.8 3.8 %copy-start.5 = (bf16[1024,1024]{1,0:T(8,128)(2,1)S(1)}, bf16[1024,1024]{1,0:T(8,128)(2,1)}, u32[]{:S(2)}) copy-start(bf16[1024,1024]{1,0:T(8,128)(2,1)} %refs_26_.1) | copy-start | bytes 6291460
  51.8 3.8 %copy-start.7 = (f32[2048]{0:T(1024)S(1)}, f32[2048]{0:T(1024)}, u32[]{:S(2)}) copy-start(f32[2048]{0:T(1024)} %param.25) | copy-start | bytes 24580
  51.8 3.8 %copy-start.8 = (f32[1024]{0:T(1024)S(1)}, f32[1024]{0:T(1024)}, u32[]{:S(2)}) copy-start(f32[1024]{0:T(1024)} %param.23) | copy-start | bytes 12292
  51.9 3.7 %collective-permute-start.7 = (f32[128,128]{1,0:T(8,128)S(1)}, f32[128,128]{1,0:T(8,128)S(1)}, u32[]{:S(2)}, u32[]{:S(2)}) collective-permute-start(f32[128,128]{1,0:T(8,128)S(1)} %get-tuple-element.141), channel_id=1, source_target_pairs={{1,0},{3,2},{5,4},{7,6},{9,8},{11,10},{13,12},{15,14},{17,16},{19,... | collective-permute-start | bytes 196616 | tf_op jit(solution)/shard_map/ppermute | solution.py:473

commit v5 on v4

--- a/solution.py
+++ b/solution.py
@@ -17,10 +17,10 @@
 SPANS = ROWS // SPAN
 PIECES = (1,) * 8
 LOG2E = 1.0 / math.log(2.0)
+TINY = 1e-37
 EPSILON = 1e-06
 AXES = ("z", "x", "y", "c")
 VMEM = pltpu.VMEM
-HIGHEST = lax.Precision.HIGHEST
 F32 = jnp.float32
 BF16 = jnp.bfloat16
 
@@ -28,15 +28,6 @@
 COSINE = (1.4142135, -6.97885097, 5.73946067, -1.88355924, 0.31068962)
 SINE_SHORT = (4.44287876, -7.30776104, 3.5971931, -0.7896682)
 COSINE_SHORT = (1.41420407, -6.97764062, 5.71521917, -1.7282871)
-DAMP = (
-    9.99995989e-01,
-    -2.49939726e-01,
-    5.19269127e-02,
-    -7.65257696e-03,
-    7.74390930e-04,
-    -4.89307841e-05,
-    1.45423687e-06,
-)
 
 
 def horner(coefficients, x):
@@ -73,8 +64,15 @@
     return jnp.broadcast_to(row, (ROWS, ROWS)).T
 
 
-def exact_mm(a, b):
-    return jnp.dot(a, b, preferred_element_type=F32, precision=HIGHEST)
+def in_parts(x):
+    high = x.astype(BF16)
+    rest = x - high.astype(F32)
+    middle = rest.astype(BF16)
+    return high, middle, (rest - middle.astype(F32)).astype(BF16)
+
+
+def sums_of(chosen, parts):
+    return sum(mm(chosen.astype(BF16), part) for part in parts)
 
 
 def pair_row(ref, k, pair):
@@ -93,15 +91,15 @@
         scale = lax.rsqrt(jnp.mean(x * x, axis=-1, keepdims=True) + EPSILON)
         normed[...] = (x * scale * gain[...]).astype(BF16)
         steps = column_of(elapsed[...])
+        parts = in_parts(steps)
         row, col = iotas((ROWS, ROWS))
         same = row // SPAN == col // SPAN
-        times[0] = exact_mm((col > row).astype(F32), steps)
-        times[1] = exact_mm((col < row).astype(F32), steps)
-        times[2] = jnp.sqrt(steps)
-        times[3] = steps
-        within_ref[0] = exact_mm(((col <= row) & same).astype(F32), steps)
-        within_ref[1] = exact_mm(((col >= row) & same).astype(F32), steps)
-        total = exact_mm(jnp.ones((8, ROWS), F32), steps)
+        times[0] = sums_of(col > row, parts)
+        times[1] = sums_of(col < row, parts)
+        times[2] = steps
+        within_ref[0] = sums_of((col <= row) & same, parts)
+        within_ref[1] = sums_of((col >= row) & same, parts)
+        total = sums_of(jnp.ones((8, ROWS), F32), parts)
         ends_ref[128:, :] = total
 
     driven = mm(normed[...], weight[...]).astype(BF16)
@@ -115,11 +113,10 @@
             th = pair_row(angle, k, pair)
             pars_ref[k, 0, pl.ds(pair, 1), :] = th
             pars_ref[k, 1, pl.ds(pair, 1), :] = f
-            f2 = f * 2.0
-            root = jnp.sqrt(f2)
             after = times[k]
             s, c = half_turn(after * (th * (0.5 / math.pi)))
-            damp = horner(DAMP, times[3] * f2) * times[2]
+            bend = jnp.tanh(times[2] * f)
+            damp = bend * lax.rsqrt(bend * (0.5 + 0.5 * bend) + TINY)
             damp_ref[j, k] = damp
             amp = jnp.exp2(after * (f * -LOG2E)) * damp
             tilted = amp * s
@@ -132,8 +129,8 @@
                 for c in range(2)
             )
             at = 64 * k + pair
-            ends_ref[pl.ds(at, 1), :] = root * jnp.sum(b_re * m_re - b_im * m_im, axis=0, keepdims=True)
-            ends_ref[pl.ds(at + 32, 1), :] = root * jnp.sum(b_re * m_im + b_im * m_re, axis=0, keepdims=True)
+            ends_ref[pl.ds(at, 1), :] = jnp.sum(b_re * m_re - b_im * m_im, axis=0, keepdims=True)
+            ends_ref[pl.ds(at + 32, 1), :] = jnp.sum(b_re * m_im + b_im * m_re, axis=0, keepdims=True)
 
 
 def local_kernel(
@@ -155,7 +152,6 @@
         for k in range(2):
             f = pair_row(rate, k, pair)
             th = pair_row(angle, k, pair)
-            root = jnp.sqrt(f * 2.0)
             b00, b01 = inputs[k, 0, 2 * j], inputs[k, 1, 2 * j]
             b10, b11 = inputs[k, 0, 2 * j + 1], inputs[k, 1, 2 * j + 1]
             rhs = jnp.concatenate(
@@ -197,7 +193,7 @@
                 lower = jnp.concatenate([hole, readout[k, c, 2 * j + 1]], axis=1)
                 table = jnp.concatenate([upper, lower], axis=0)
                 table_ref[j, k, c] = table
-                tables.append(table * root)
+                tables.append(table)
             y = nt(
                 jnp.concatenate(states, axis=0),
                 jnp.concatenate([tables[0].astype(BF16), (-tables[1]).astype(BF16)], axis=1),
@@ -432,7 +428,7 @@
             sds((ROWS, CHANNELS), BF16), sds((136, 128)), sds((2, 2, 32, 128)),
             sds((32, 2, ROWS, ROWS)), sds((2, ROWS, ROWS)),
         ],
-        scratch_shapes=[VMEM((ROWS, D), BF16), VMEM((4, ROWS, ROWS), F32)],
+        scratch_shapes=[VMEM((ROWS, D), BF16), VMEM((3, ROWS, ROWS), F32)],
         compiler_params=params(10),
     )(
         *(hbm(a) for a in (tokens, elapsed_row, norm_gain.reshape(1, D), in_weight, inputs, decay_angle, forget_rate))
@@ -452,13 +448,14 @@
         pieces.append(piece)
         return after
 
+    swap = [(0, 1), (1, 0)]
     pairings = {"low": (1, 0, 3, 2), "high": (3, 2, 1, 0)}
     stages = [(axis, kind) for axis in ("y", "x", "z") for kind in ("low", "high")]
-    partner = piece_between(ends, lax.ppermute(ends, "c", [(0, 1)]))
+    partner = piece_between(ends, lax.ppermute(ends, "c", swap))
     total, trail = simple(pair_kernel, "pair", [(136, 128), (12, 32, 128)], (ends, partner, pars))
     for stage in stages:
         axis, kind = stage
-        pairs = [(2 * i + 1, 2 * j + 1) for i, j in enumerate(pairings[kind])]
+        pairs = [pair for i, j in enumerate(pairings[kind]) for pair in ((2 * i, 2 * i), (2 * i + 1, 2 * j + 1))]
         other = piece_between(total, lax.ppermute(total, (axis, "c"), pairs))
         if stage == stages[-1]:
             mine, theirs = simple(
@@ -470,7 +467,7 @@
                 functools.partial(stage_kernel, stage), f"stage_{axis}_{kind}", [(136, 128), (12, 32, 128)],
                 (total, other, trail, pars),
             )
-    other = piece_between(theirs, lax.ppermute(theirs, "c", [(1, 0)]))
+    other = piece_between(theirs, lax.ppermute(theirs, "c", swap))
 
     spec = pl.BlockSpec(memory_space=VMEM)
     args = (

time: 59.3 us -> 57.2 us (0.965)
  starting transfers between devices: 27.4 us -> 25.3 us
    ppermute x2, starting transfers between devices: 2.85 us -> 1.53 us  [the longest x1 1.45 us: local(): partner = piece_between(ends, lax.ppermute(ends, 'c', swap))]
    ppermute x6, starting transfers between devices: 24.5 us -> 23.8 us  [local(): other = piece_between(total, lax.ppermute(total, (axis, 'c'), pairs))]
  transfers between devices with their start and end apart: 8 -> 8, of which waited for: 0 -> 0; matrix products, arithmetic and copies ran while one was open for 0% -> 0% of each run, Pallas kernels for 28% -> 29%
where the time goes in v5:
time: 57.2 us; the launch traced here: 56.9 us
  Pallas kernels  30.7 us (54%)
  starting transfers between devices  25.3 us (44%)
    ppermute x6, starting transfers between devices, local(): other = piece_between(total, lax.ppermute(total, (axis, 'c'), pairs))  23.8 us
    pallas_call x8, Pallas kernels, run_local(): pl.pallas_call(functools.partial(local_kernel, start), name=f'local_{star...  16.8 us
    pallas_call x1, Pallas kernels, local(): pl.pallas_call(end_kernel, name='ends', grid=(TILES,), in_specs=[whole((R...  9.96 us
    pallas_call x1, Pallas kernels, local(): pl.pallas_call(final_kernel, name='final', in_specs=[spec] * len(args), o...  3.28 us
    ppermute x1, starting transfers between devices, local(): partner = piece_between(ends, lax.ppermute(ends, 'c', swap))  1.45 us
  transfers between devices with their start and end apart: 8, of which 0 were waited for; matrix products, arithmetic and copies ran while one was open for 0% of the time, Pallas kernels for 29%

profile of v5, /device:TPU:1, one launch (start us, length us, event | category | flops | bytes accessed | tf_op | source)
XLA Modules:
  0.0 56.9 jit_solution(6850747253566071560)
XLA Ops:
  0.0 0.0 copy-start.2
  0.0 0.0 copy-start.3
  0.0 0.0 copy-start.1
  0.0 0.0 copy-start
  0.0 0.0 copy-start.6
  0.0 10.0 %ends.1 = (bf16[128,1024]{1,0:T(8,128)(2,1)S(1)}, f32[136,128]{1,0:T(8,128)S(1)}, f32[2,2,32,128]{3,2,1,0:T(8,128)S(1)}, f32[32,2,128,128]{3,2,1,0:T(8,128)S(1)}, f32[2,128,128]{2,1,0:T(8,128)S(1)}) custom-call(bf16[128,2048]{1,0:T(8,128)(2,1)} %tokens.1, f32[1,128]{1,0:T(1,128)} %bitcast.26, f32[1,2048]{1,0:T(1,128)} %bitcast.25, ...), custom_call_target="tpu_custom_call" | custom-call | tf_op jit(solution)/shard_map/ends/pallas_call | solution.py:408
  10.0 1.4 %collective-permute-start = (f32[136,128]{1,0:T(8,128)S(1)}, f32[136,128]{1,0:T(8,128)S(1)}, u32[]{:S(2)}, u32[]{:S(2)}) collective-permute-start(f32[136,128]{1,0:T(8,128)S(1)} %get-tuple-element.91.own), channel_id=1, source_target_pairs={{0,1},{1,0},{2,3},{3,2},{4,5},{5,4},{6,7},{7,6},{8,9},{9,8},{10,11... | collective-permute-start | bytes 208904 | tf_op jit(solution)/shard_map/ppermute | solution.py:454
  11.4 0.0 copy-done.2
  11.4 0.0 copy-done.3
  11.4 0.0 copy-done.1
  11.5 0.0 copy-done
  11.5 0.0 copy-done.6
  11.5 2.1 %local_0.1 = (f32[128,128]{1,0:T(8,128)S(1)}, bf16[4,2,128,256]{3,2,1,0:T(8,128)(2,1)S(1)}, f32[4,2,2,32,128]{4,3,2,1,0:T(8,128)S(1)}) custom-call(f32[2,128,128]{2,1,0:T(8,128)S(1)} %get-tuple-element.88.within, f32[32,2,128,128]{3,2,1,0:T(8,128)S(1)} %get-tuple-element.89.damps, bf16[128,1024]{1,0:T(8,128)(2,1)S(1)} %get-tuple-element.142.driven, ...), custom_call_target="tpu_custom_call" | custom-call | flops 500000000 | bytes 2097152 | tf_op jit(solution)/shard_map/local_0/pallas_call | solution.py:360
  13.6 0.0 collective-permute-done.other
  13.6 0.1 pair.1
  13.7 3.3 %collective-permute-start.1 = (f32[136,128]{1,0:T(8,128)S(1)}, f32[136,128]{1,0:T(8,128)S(1)}, u32[]{:S(2)}, u32[]{:S(2)}) collective-permute-start(f32[136,128]{1,0:T(8,128)S(1)} %get-tuple-element.98.own), channel_id=1, source_target_pairs={{0,0},{1,3},{2,2},{3,1},{4,4},{5,7},{6,6},{7,5},{8,8},{9,11},{10,1... | collective-permute-start | bytes 208904 | tf_op jit(solution)/shard_map/ppermute | solution.py:459
  17.0 2.1 %local_1.1 = (f32[128,128]{1,0:T(8,128)S(1)}, bf16[4,2,128,256]{3,2,1,0:T(8,128)(2,1)S(1)}, f32[4,2,2,32,128]{4,3,2,1,0:T(8,128)S(1)}) custom-call(f32[2,128,128]{2,1,0:T(8,128)S(1)} %get-tuple-element.88.within, f32[32,2,128,128]{3,2,1,0:T(8,128)S(1)} %get-tuple-element.89.damps, bf16[128,1024]{1,0:T(8,128)(2,1)S(1)} %get-tuple-element.142.driven, ...), custom_call_target="tpu_custom_call" | custom-call | flops 500000000 | bytes 2097152 | tf_op jit(solution)/shard_map/local_1/pallas_call | solution.py:360
  19.1 0.0 collective-permute-done.1.other
  19.1 0.1 stage_y_low.1
  19.3 4.4 %collective-permute-start.2 = (f32[136,128]{1,0:T(8,128)S(1)}, f32[136,128]{1,0:T(8,128)S(1)}, u32[]{:S(2)}, u32[]{:S(2)}) collective-permute-start(f32[136,128]{1,0:T(8,128)S(1)} %get-tuple-element.105.own), channel_id=1, source_target_pairs={{0,0},{1,7},{2,2},{3,5},{4,4},{5,3},{6,6},{7,1},{8,8},{9,15},{10,1... | collective-permute-start | bytes 208904 | tf_op jit(solution)/shard_map/ppermute | solution.py:459
  23.6 2.1 %local_2.1 = (f32[128,128]{1,0:T(8,128)S(1)}, bf16[4,2,128,256]{3,2,1,0:T(8,128)(2,1)S(1)}, f32[4,2,2,32,128]{4,3,2,1,0:T(8,128)S(1)}) custom-call(f32[2,128,128]{2,1,0:T(8,128)S(1)} %get-tuple-element.88.within, f32[32,2,128,128]{3,2,1,0:T(8,128)S(1)} %get-tuple-element.89.damps, bf16[128,1024]{1,0:T(8,128)(2,1)S(1)} %get-tuple-element.142.driven, ...), custom_call_target="tpu_custom_call" | custom-call | flops 500000000 | bytes 2097152 | tf_op jit(solution)/shard_map/local_2/pallas_call | solution.py:360
  25.7 0.0 collective-permute-done.2.other
  25.7 0.1 stage_y_high.1
  25.8 3.1 %collective-permute-start.3 = (f32[136,128]{1,0:T(8,128)S(1)}, f32[136,128]{1,0:T(8,128)S(1)}, u32[]{:S(2)}, u32[]{:S(2)}) collective-permute-start(f32[136,128]{1,0:T(8,128)S(1)} %get-tuple-element.112.own), channel_id=1, source_target_pairs={{0,0},{1,9},{8,8},{9,1},{16,16},{17,25},{24,24},{25,17},{2,2},{3,1... | collective-permute-start | bytes 208904 | tf_op jit(solution)/shard_map/ppermute | solution.py:459
  29.0 2.1 %local_3.1 = (f32[128,128]{1,0:T(8,128)S(1)}, bf16[4,2,128,256]{3,2,1,0:T(8,128)(2,1)S(1)}, f32[4,2,2,32,128]{4,3,2,1,0:T(8,128)S(1)}) custom-call(f32[2,128,128]{2,1,0:T(8,128)S(1)} %get-tuple-element.88.within, f32[32,2,128,128]{3,2,1,0:T(8,128)S(1)} %get-tuple-element.89.damps, bf16[128,1024]{1,0:T(8,128)(2,1)S(1)} %get-tuple-element.142.driven, ...), custom_call_target="tpu_custom_call" | custom-call | flops 500000000 | bytes 2097152 | tf_op jit(solution)/shard_map/local_3/pallas_call | solution.py:360
  31.1 0.0 collective-permute-done.3.other
  31.1 0.1 stage_x_low.1
  31.2 4.2 %collective-permute-start.4 = (f32[136,128]{1,0:T(8,128)S(1)}, f32[136,128]{1,0:T(8,128)S(1)}, u32[]{:S(2)}, u32[]{:S(2)}) collective-permute-start(f32[136,128]{1,0:T(8,128)S(1)} %get-tuple-element.119.own), channel_id=1, source_target_pairs={{0,0},{1,25},{8,8},{9,17},{16,16},{17,9},{24,24},{25,1},{2,2},{3,2... | collective-permute-start | bytes 208904 | tf_op jit(solution)/shard_map/ppermute | solution.py:459
  35.4 2.1 %local_4.1 = (f32[128,128]{1,0:T(8,128)S(1)}, bf16[4,2,128,256]{3,2,1,0:T(8,128)(2,1)S(1)}, f32[4,2,2,32,128]{4,3,2,1,0:T(8,128)S(1)}) custom-call(f32[2,128,128]{2,1,0:T(8,128)S(1)} %get-tuple-element.88.within, f32[32,2,128,128]{3,2,1,0:T(8,128)S(1)} %get-tuple-element.89.damps, bf16[128,1024]{1,0:T(8,128)(2,1)S(1)} %get-tuple-element.142.driven, ...), custom_call_target="tpu_custom_call" | custom-call | flops 500000000 | bytes 2097152 | tf_op jit(solution)/shard_map/local_4/pallas_call | solution.py:360
  37.5 0.0 collective-permute-done.4.other
  37.5 0.1 stage_x_high.1
  37.6 3.5 %collective-permute-start.5 = (f32[136,128]{1,0:T(8,128)S(1)}, f32[136,128]{1,0:T(8,128)S(1)}, u32[]{:S(2)}, u32[]{:S(2)}) collective-permute-start(f32[136,128]{1,0:T(8,128)S(1)} %get-tuple-element.126.own), channel_id=1, source_target_pairs={{0,0},{1,33},{32,32},{33,1},{64,64},{65,97},{96,96},{97,65},{2,2},... | collective-permute-start | bytes 208904 | tf_op jit(solution)/shard_map/ppermute | solution.py:459
  41.1 2.1 %local_5.1 = (f32[128,128]{1,0:T(8,128)S(1)}, bf16[4,2,128,256]{3,2,1,0:T(8,128)(2,1)S(1)}, f32[4,2,2,32,128]{4,3,2,1,0:T(8,128)S(1)}) custom-call(f32[2,128,128]{2,1,0:T(8,128)S(1)} %get-tuple-element.88.within, f32[32,2,128,128]{3,2,1,0:T(8,128)S(1)} %get-tuple-element.89.damps, bf16[128,1024]{1,0:T(8,128)(2,1)S(1)} %get-tuple-element.142.driven, ...), custom_call_target="tpu_custom_call" | custom-call | flops 500000000 | bytes 2097152 | tf_op jit(solution)/shard_map/local_5/pallas_call | solution.py:360
  43.2 0.0 collective-permute-done.5.other
  43.3 0.1 stage_z_low.1
  43.4 5.2 %collective-permute-start.6 = (f32[136,128]{1,0:T(8,128)S(1)}, f32[136,128]{1,0:T(8,128)S(1)}, u32[]{:S(2)}, u32[]{:S(2)}) collective-permute-start(f32[136,128]{1,0:T(8,128)S(1)} %get-tuple-element.133), channel_id=1, source_target_pairs={{0,0},{1,97},{32,32},{33,65},{64,64},{65,33},{96,96},{97,1},{2,2},... | collective-permute-start | bytes 208904 | tf_op jit(solution)/shard_map/ppermute | solution.py:459
  48.6 2.1 %local_6.1 = (f32[128,128]{1,0:T(8,128)S(1)}, bf16[4,2,128,256]{3,2,1,0:T(8,128)(2,1)S(1)}, f32[4,2,2,32,128]{4,3,2,1,0:T(8,128)S(1)}) custom-call(f32[2,128,128]{2,1,0:T(8,128)S(1)} %get-tuple-element.88.within, f32[32,2,128,128]{3,2,1,0:T(8,128)S(1)} %get-tuple-element.89.damps, bf16[128,1024]{1,0:T(8,128)(2,1)S(1)} %get-tuple-element.142.driven, ...), custom_call_target="tpu_custom_call" | custom-call | flops 500000000 | bytes 2097152 | tf_op jit(solution)/shard_map/local_6/pallas_call | solution.py:360
  50.7 0.0 copy-start.4
  50.7 0.0 copy-start.5
  50.7 0.0 copy-start.7
  50.7 0.0 copy-start.8
  50.7 0.0 collective-permute-done.6.last
  50.8 0.1 enter.1
  50.8 0.1 collective-permute-start.7
  50.9 2.1 %local_7.1 = (f32[128,128]{1,0:T(8,128)S(1)}, bf16[4,2,128,256]{3,2,1,0:T(8,128)(2,1)S(1)}, f32[4,2,2,32,128]{4,3,2,1,0:T(8,128)S(1)}) custom-call(f32[2,128,128]{2,1,0:T(8,128)S(1)} %get-tuple-element.88.within, f32[32,2,128,128]{3,2,1,0:T(8,128)S(1)} %get-tuple-element.89.damps, bf16[128,1024]{1,0:T(8,128)(2,1)S(1)} %get-tuple-element.142.driven, ...), custom_call_target="tpu_custom_call" | custom-call | flops 500000000 | bytes 2097152 | tf_op jit(solution)/shard_map/local_7/pallas_call | solution.py:360
  53.0 0.0 collective-permute-done.7.refs_1_
  53.0 0.0 copy-done.4
  53.1 0.5 copy-done.5
  53.6 0.0 copy-done.7
  53.6 0.0 copy-done.8
  53.6 3.3 %final.1 = bf16[128,2048]{1,0:T(8,128)(2,1)} custom-call(f32[128,128]{1,0:T(8,128)S(1)} %get-tuple-element.140.refs_0_, f32[128,128]{1,0:T(8,128)S(1)} %collective-permute-done.7.refs_1_, f32[128,128]{1,0:T(8,128)S(1)} %get-tuple-element.147.refs_2_, f32[128,128]{1,0:T(8,128)S(1)} %get-tuple-element.148.refs_3_, f32[128,128]{1,0:T(8,128)S(1)} %get-tuple-element.149.refs_4_, ...), custom_call_target="tpu_custom_call" | custom-call | tf_op jit(solution)/shard_map/final/pallas_call | solution.py:477
Async XLA Ops:
  0.0 11.4 %copy-start.2 = (f32[2,64,64]{2,1,0:T(8,128)S(1)}, f32[2,64,64]{2,1,0:T(8,128)}, u32[]{:S(2)}) copy-start(f32[2,64,64]{2,1,0:T(8,128)} %angle.17) | copy-start | bytes 98308
  0.0 11.4 %copy-start.3 = (f32[2,64,64]{2,1,0:T(8,128)S(1)}, f32[2,64,64]{2,1,0:T(8,128)}, u32[]{:S(2)}) copy-start(f32[2,64,64]{2,1,0:T(8,128)} %rate.17) | copy-start | bytes 98308
  0.0 11.4 %copy-start.1 = (bf16[2,2,64,64,16]{3,4,2,1,0:T(8,128)(2,1)S(1)}, bf16[2,2,64,64,16]{3,4,2,1,0:T(8,128)(2,1)}, u32[]{:S(2)}) copy-start(bf16[2,2,64,64,16]{3,4,2,1,0:T(8,128)(2,1)} %param.17) | copy-start | bytes 1572868
  0.0 11.4 %copy-start = (f32[2,2,64,16,64]{4,3,2,1,0:T(8,128)S(1)}, f32[2,2,64,16,64]{4,3,2,1,0:T(8,128)}, u32[]{:S(2)}) copy-start(f32[2,2,64,16,64]{4,3,2,1,0:T(8,128)} %readout.15) | copy-start | bytes 3145732
  0.0 11.4 %copy-start.6 = (f32[1024]{0:T(1024)S(1)}, f32[1024]{0:T(1024)}, u32[]{:S(2)}) copy-start(f32[1024]{0:T(1024)} %param.21) | copy-start | bytes 12292
  10.0 3.6 %collective-permute-start = (f32[136,128]{1,0:T(8,128)S(1)}, f32[136,128]{1,0:T(8,128)S(1)}, u32[]{:S(2)}, u32[]{:S(2)}) collective-permute-start(f32[136,128]{1,0:T(8,128)S(1)} %get-tuple-element.91.own), channel_id=1, source_target_pairs={{0,1},{1,0},{2,3},{3,2},{4,5},{5,4},{6,7},{7,6},{8,9},{9,8},{10,11... | collective-permute-start | bytes 208904 | tf_op jit(solution)/shard_map/ppermute | solution.py:454
  13.7 5.4 %collective-permute-start.1 = (f32[136,128]{1,0:T(8,128)S(1)}, f32[136,128]{1,0:T(8,128)S(1)}, u32[]{:S(2)}, u32[]{:S(2)}) collective-permute-start(f32[136,128]{1,0:T(8,128)S(1)} %get-tuple-element.98.own), channel_id=1, source_target_pairs={{0,0},{1,3},{2,2},{3,1},{4,4},{5,7},{6,6},{7,5},{8,8},{9,11},{10,1... | collective-permute-start | bytes 208904 | tf_op jit(solution)/shard_map/ppermute | solution.py:459
  19.3 6.5 %collective-permute-start.2 = (f32[136,128]{1,0:T(8,128)S(1)}, f32[136,128]{1,0:T(8,128)S(1)}, u32[]{:S(2)}, u32[]{:S(2)}) collective-permute-start(f32[136,128]{1,0:T(8,128)S(1)} %get-tuple-element.105.own), channel_id=1, source_target_pairs={{0,0},{1,7},{2,2},{3,5},{4,4},{5,3},{6,6},{7,1},{8,8},{9,15},{10,1... | collective-permute-start | bytes 208904 | tf_op jit(solution)/shard_map/ppermute | solution.py:459
  25.8 5.2 %collective-permute-start.3 = (f32[136,128]{1,0:T(8,128)S(1)}, f32[136,128]{1,0:T(8,128)S(1)}, u32[]{:S(2)}, u32[]{:S(2)}) collective-permute-start(f32[136,128]{1,0:T(8,128)S(1)} %get-tuple-element.112.own), channel_id=1, source_target_pairs={{0,0},{1,9},{8,8},{9,1},{16,16},{17,25},{24,24},{25,17},{2,2},{3,1... | collective-permute-start | bytes 208904 | tf_op jit(solution)/shard_map/ppermute | solution.py:459
  31.2 6.3 %collective-permute-start.4 = (f32[136,128]{1,0:T(8,128)S(1)}, f32[136,128]{1,0:T(8,128)S(1)}, u32[]{:S(2)}, u32[]{:S(2)}) collective-permute-start(f32[136,128]{1,0:T(8,128)S(1)} %get-tuple-element.119.own), channel_id=1, source_target_pairs={{0,0},{1,25},{8,8},{9,17},{16,16},{17,9},{24,24},{25,1},{2,2},{3,2... | collective-permute-start | bytes 208904 | tf_op jit(solution)/shard_map/ppermute | solution.py:459
  37.6 5.7 %collective-permute-start.5 = (f32[136,128]{1,0:T(8,128)S(1)}, f32[136,128]{1,0:T(8,128)S(1)}, u32[]{:S(2)}, u32[]{:S(2)}) collective-permute-start(f32[136,128]{1,0:T(8,128)S(1)} %get-tuple-element.126.own), channel_id=1, source_target_pairs={{0,0},{1,33},{32,32},{33,1},{64,64},{65,97},{96,96},{97,65},{2,2},... | collective-permute-start | bytes 208904 | tf_op jit(solution)/shard_map/ppermute | solution.py:459
  43.4 7.4 %collective-permute-start.6 = (f32[136,128]{1,0:T(8,128)S(1)}, f32[136,128]{1,0:T(8,128)S(1)}, u32[]{:S(2)}, u32[]{:S(2)}) collective-permute-start(f32[136,128]{1,0:T(8,128)S(1)} %get-tuple-element.133), channel_id=1, source_target_pairs={{0,0},{1,97},{32,32},{33,65},{64,64},{65,33},{96,96},{97,1},{2,2},... | collective-permute-start | bytes 208904 | tf_op jit(solution)/shard_map/ppermute | solution.py:459
  50.7 2.3 %copy-start.4 = (bf16[1024,2048]{1,0:T(8,128)(2,1)S(1)}, bf16[1024,2048]{1,0:T(8,128)(2,1)}, u32[]{:S(2)}) copy-start(bf16[1024,2048]{1,0:T(8,128)(2,1)} %refs_28_.1) | copy-start | bytes 12582916
  50.7 2.9 %copy-start.5 = (bf16[1024,1024]{1,0:T(8,128)(2,1)S(1)}, bf16[1024,1024]{1,0:T(8,128)(2,1)}, u32[]{:S(2)}) copy-start(bf16[1024,1024]{1,0:T(8,128)(2,1)} %refs_26_.1) | copy-start | bytes 6291460
  50.7 2.9 %copy-start.7 = (f32[2048]{0:T(1024)S(1)}, f32[2048]{0:T(1024)}, u32[]{:S(2)}) copy-start(f32[2048]{0:T(1024)} %param.25) | copy-start | bytes 24580
  50.7 2.8 %copy-start.8 = (f32[1024]{0:T(1024)S(1)}, f32[1024]{0:T(1024)}, u32[]{:S(2)}) copy-start(f32[1024]{0:T(1024)} %param.23) | copy-start | bytes 12292
  50.8 2.2 %collective-permute-start.7 = (f32[128,128]{1,0:T(8,128)S(1)}, f32[128,128]{1,0:T(8,128)S(1)}, u32[]{:S(2)}, u32[]{:S(2)}) collective-permute-start(f32[128,128]{1,0:T(8,128)S(1)} %get-tuple-element.141), channel_id=1, source_target_pairs={{0,1},{1,0},{2,3},{3,2},{4,5},{5,4},{6,7},{7,6},{8,9},{9,8},{10,11... | collective-permute-start | bytes 196616 | tf_op jit(solution)/shard_map/ppermute | solution.py:470

commit v6 on v3

--- a/solution.py
+++ b/solution.py
@@ -17,10 +17,10 @@
 SPANS = ROWS // SPAN
 PIECES = (1,) * 8
 LOG2E = 1.0 / math.log(2.0)
+TINY = 1e-37
 EPSILON = 1e-06
 AXES = ("z", "x", "y", "c")
 VMEM = pltpu.VMEM
-HIGHEST = lax.Precision.HIGHEST
 F32 = jnp.float32
 BF16 = jnp.bfloat16
 
@@ -28,15 +28,6 @@
 COSINE = (1.4142135, -6.97885097, 5.73946067, -1.88355924, 0.31068962)
 SINE_SHORT = (4.44287876, -7.30776104, 3.5971931, -0.7896682)
 COSINE_SHORT = (1.41420407, -6.97764062, 5.71521917, -1.7282871)
-DAMP = (
-    9.99995989e-01,
-    -2.49939726e-01,
-    5.19269127e-02,
-    -7.65257696e-03,
-    7.74390930e-04,
-    -4.89307841e-05,
-    1.45423687e-06,
-)
 
 
 def horner(coefficients, x):
@@ -73,8 +64,15 @@
     return jnp.broadcast_to(row, (ROWS, ROWS)).T
 
 
-def exact_mm(a, b):
-    return jnp.dot(a, b, preferred_element_type=F32, precision=HIGHEST)
+def in_parts(x):
+    high = x.astype(BF16)
+    rest = x - high.astype(F32)
+    middle = rest.astype(BF16)
+    return high, middle, (rest - middle.astype(F32)).astype(BF16)
+
+
+def sums_of(chosen, parts):
+    return sum(mm(chosen.astype(BF16), part) for part in parts)
 
 
 def pair_row(ref, k, pair):
@@ -83,84 +81,95 @@
 
 def end_kernel(
     tokens, elapsed, gain, weight, inputs, angle, rate,
-    driven_ref, ends_ref, pars_ref, damp_ref, within_ref, normed, times,
+    driven_ref, ends_ref, pars_ref, damp_ref, within_ref, inputs_ref, normed, times, chunks, weight_sems, input_sems,
 ):
-    step = pl.program_id(0)
     core = lax.axis_index("c")
 
-    @pl.when(step == 0)
-    def _():
-        x = tokens[...].astype(F32)
-        scale = lax.rsqrt(jnp.mean(x * x, axis=-1, keepdims=True) + EPSILON)
-        normed[...] = (x * scale * gain[...]).astype(BF16)
-        steps = column_of(elapsed[...])
-        row, col = iotas((ROWS, ROWS))
-        same = row // SPAN == col // SPAN
-        times[0] = exact_mm((col > row).astype(F32), steps)
-        times[1] = exact_mm((col < row).astype(F32), steps)
-        times[2] = jnp.sqrt(steps)
-        times[3] = steps
-        within_ref[0] = exact_mm(((col <= row) & same).astype(F32), steps)
-        within_ref[1] = exact_mm(((col >= row) & same).astype(F32), steps)
-        total = exact_mm(jnp.ones((8, ROWS), F32), steps)
-        ends_ref[0, 64:] = total
-        ends_ref[1, 64:] = total
-
-    driven = mm(normed[...], weight[...]).astype(BF16)
-    driven_ref[...] = driven
-    flipped = driven.astype(F32).T.astype(BF16)
+    def fetch(i):
+        return (
+            pltpu.make_async_copy(
+                weight.at[:, pl.ds(pl.multiple_of(128 * i, 128), 128)], chunks.at[i], weight_sems.at[i]
+            ),
+            pltpu.make_async_copy(inputs.at[:, :, pl.ds(8 * i, 8)], inputs_ref.at[:, :, pl.ds(8 * i, 8)], input_sems.at[i]),
+        )
+
+    for i in range(TILES):
+        for copy in fetch(i):
+            copy.start()
+    steps = column_of(elapsed[...])
+    parts = in_parts(steps)
+    row, col = iotas((ROWS, ROWS))
+    same = row // SPAN == col // SPAN
+    times[0] = sums_of(col > row, parts)
+    times[1] = sums_of(col < row, parts)
+    times[2] = steps
+    within_ref[0] = sums_of((col <= row) & same, parts)
+    within_ref[1] = sums_of((col >= row) & same, parts)
+    total = sums_of(jnp.ones((8, ROWS), F32), parts)
+    ends_ref[0, 64:] = total
+    ends_ref[1, 64:] = total
+    x = tokens[...].astype(F32)
+    scale = lax.rsqrt(jnp.mean(x * x, axis=-1, keepdims=True) + EPSILON)
+    normed[...] = (x * scale * gain[...]).astype(BF16)
     first = lax.broadcasted_iota(jnp.int32, (16, 128), 1) < 64
-    away = jnp.where((step // 4) == core, 0, 1)
-    for j in range(4):
-        pair = step * 4 + j
-        for k in range(2):
-            f = pair_row(rate, k, pair)
-            th = pair_row(angle, k, pair)
-            pars_ref[k, 0, pl.ds(pair, 1), :] = th
-            pars_ref[k, 1, pl.ds(pair, 1), :] = f
-            f2 = f * 2.0
-            root = jnp.sqrt(f2)
-            after = times[k]
-            s, c = half_turn(after * (th * (0.5 / math.pi)))
-            damp = horner(DAMP, times[3] * f2) * times[2]
-            damp_ref[j, k] = damp
-            amp = jnp.exp2(after * (f * -LOG2E)) * damp
-            tilted = amp * s
-            pull = jnp.concatenate([(amp - tilted * s).astype(BF16), (tilted * c).astype(BF16)], axis=1)
-            mixed = mm(flipped[32 * j : 32 * j + 32], pull)
-            m_re = jnp.where(first, mixed[:16, :128], mixed[16:, :128])
-            m_im = jnp.where(first, mixed[:16, 128:], mixed[16:, 128:])
-            b_re, b_im = (
-                jnp.concatenate([inputs[k, c, 2 * j].astype(F32), inputs[k, c, 2 * j + 1].astype(F32)], axis=1)
-                for c in range(2)
-            )
-            at = 32 * k + 4 * (step % 4) + j
-            ends_ref[away, pl.ds(at, 1), :] = root * jnp.sum(b_re * m_re - b_im * m_im, axis=0, keepdims=True)
-            ends_ref[away, pl.ds(at + 16, 1), :] = root * jnp.sum(b_re * m_im + b_im * m_re, axis=0, keepdims=True)
+
+    def tile(step, _):
+        for copy in fetch(step):
+            copy.wait()
+        driven = mm(normed[...], chunks[step]).astype(BF16)
+        driven_ref[:, pl.ds(pl.multiple_of(128 * step, 128), 128)] = driven
+        flipped = driven.astype(F32).T.astype(BF16)
+        away = jnp.where((step // 4) == core, 0, 1)
+        for j in range(4):
+            pair = step * 4 + j
+            for k in range(2):
+                f = pair_row(rate, k, pair)
+                th = pair_row(angle, k, pair)
+                pars_ref[k, 0, pl.ds(pair, 1), :] = th
+                pars_ref[k, 1, pl.ds(pair, 1), :] = f
+                after = times[k]
+                s, c = half_turn(after * (th * (0.5 / math.pi)))
+                bend = jnp.tanh(times[2] * f)
+                damp = bend * lax.rsqrt(bend * (0.5 + 0.5 * bend) + TINY)
+                damp_ref[pair, k] = damp
+                amp = jnp.exp2(after * (f * -LOG2E)) * damp
+                tilted = amp * s
+                pull = jnp.concatenate([(amp - tilted * s).astype(BF16), (tilted * c).astype(BF16)], axis=1)
+                mixed = mm(flipped[32 * j : 32 * j + 32], pull)
+                m_re = jnp.where(first, mixed[:16, :128], mixed[16:, :128])
+                m_im = jnp.where(first, mixed[:16, 128:], mixed[16:, 128:])
+                b_re, b_im = (
+                    jnp.concatenate([inputs_ref[k, c, 2 * pair].astype(F32), inputs_ref[k, c, 2 * pair + 1].astype(F32)], axis=1)
+                    for c in range(2)
+                )
+                at = 32 * k + 4 * (step % 4) + j
+                ends_ref[away, pl.ds(at, 1), :] = jnp.sum(b_re * m_re - b_im * m_im, axis=0, keepdims=True)
+                ends_ref[away, pl.ds(at + 16, 1), :] = jnp.sum(b_re * m_im + b_im * m_re, axis=0, keepdims=True)
+        return 0
+
+    lax.fori_loop(0, TILES, tile, 0)
 
 
 def local_kernel(
-    offset, within, damps, driven, inputs, readout, angle, rate, skip,
+    start, size, within, damps, driven, inputs, readout, angle, rate, skip,
     out_ref, prefix_ref, table_ref,
 ):
-    step = pl.program_id(0)
     row, col = iotas((ROWS, ROWS))
     same = row // SPAN == col // SPAN
     triangles = (((col <= row) & same).astype(BF16), ((col >= row) & same).astype(BF16))
     empty = jnp.zeros((16, 64), BF16)
     hole = jnp.zeros((16, 64), F32)
-    x = driven[...]
+    x = driven[:, 32 * start : 32 * (start + size)]
     outs = []
-    for j in range(4):
-        pair = (step + offset) * 4 + j
+    for j in range(size):
+        pair = start + j
         lhs = x[:, 32 * j : 32 * j + 32]
         total = None
         for k in range(2):
             f = pair_row(rate, k, pair)
             th = pair_row(angle, k, pair)
-            root = jnp.sqrt(f * 2.0)
-            b00, b01 = inputs[k, 0, 2 * j], inputs[k, 1, 2 * j]
-            b10, b11 = inputs[k, 0, 2 * j + 1], inputs[k, 1, 2 * j + 1]
+            b00, b01 = inputs[k, 0, 2 * pair], inputs[k, 1, 2 * pair]
+            b10, b11 = inputs[k, 0, 2 * pair + 1], inputs[k, 1, 2 * pair + 1]
             rhs = jnp.concatenate(
                 [
                     jnp.concatenate([b00, empty, b01, empty], axis=1),
@@ -172,7 +181,7 @@
             p_re, p_im = proj[:, :128], proj[:, 128:]
             offs = within[k]
             cosine, sine = unit_circle(offs * (th * (0.5 / math.pi)))
-            grow = jnp.exp2(offs * (f * LOG2E)) * damps[j, k]
+            grow = jnp.exp2(offs * (f * LOG2E)) * damps[pair, k]
             fade = jnp.exp2(offs * (f * -LOG2E))
             a_re, a_im = grow * cosine, grow * sine
             lift = jnp.concatenate(
@@ -196,18 +205,18 @@
             prefix_ref[j, k] = jnp.concatenate(prefixes, axis=0)
             tables = []
             for c in range(2):
-                upper = jnp.concatenate([readout[k, c, 2 * j], hole], axis=1)
-                lower = jnp.concatenate([hole, readout[k, c, 2 * j + 1]], axis=1)
+                upper = jnp.concatenate([readout[k, c, 2 * pair], hole], axis=1)
+                lower = jnp.concatenate([hole, readout[k, c, 2 * pair + 1]], axis=1)
                 table = jnp.concatenate([upper, lower], axis=0)
                 table_ref[j, k, c] = table
-                tables.append(table * root)
+                tables.append(table)
             y = nt(
                 jnp.concatenate(states, axis=0),
                 jnp.concatenate([tables[0].astype(BF16), (-tables[1]).astype(BF16)], axis=1),
             )
             total = y if total is None else total + y
         outs.append(total)
-    out_ref[...] = jnp.concatenate(outs, axis=1) + skip[...] * x.astype(F32)
+    out_ref[...] = jnp.concatenate(outs, axis=1) + skip[:, 32 * start : 32 * (start + size)] * x.astype(F32)
 
 
 def times_of(a, b):
@@ -355,10 +364,6 @@
     out_ref[...] = (projected * scale * out_gain[...]).astype(BF16)
 
 
-def whole(shape):
-    return pl.BlockSpec(shape, lambda *_: (0,) * len(shape))
-
-
 def sds(shape, dtype=F32):
     return jax.ShapeDtypeStruct(shape, dtype)
 
@@ -367,34 +372,21 @@
     return pltpu.CompilerParams(vmem_limit_bytes=limit * 1024 * 1024)
 
 
-def run_local(start, size, within, damps, driven, inputs, state_output, angle, rate, skip_row):
-    row_spec = whole((2, 64, 64))
+def run_local(start, size, args):
+    spec = pl.BlockSpec(memory_space=VMEM)
     return pl.pallas_call(
-        functools.partial(local_kernel, start),
+        functools.partial(local_kernel, 4 * start, 4 * size),
         name=f"local_{start}",
-        grid=(size,),
-        in_specs=[
-            whole((2, ROWS, ROWS)),
-            pl.BlockSpec((4, 2, ROWS, ROWS), lambda i: (i + start, 0, 0, 0)),
-            pl.BlockSpec((ROWS, 128), lambda i: (0, i + start)),
-            pl.BlockSpec((2, 2, 8, 16, 64), lambda i: (0, 0, i + start, 0, 0)),
-            pl.BlockSpec((2, 2, 8, 16, 64), lambda i: (0, 0, i + start, 0, 0)),
-            row_spec, row_spec,
-            pl.BlockSpec((1, 128), lambda i: (0, i + start)),
-        ],
-        out_specs=[
-            pl.BlockSpec((ROWS, 128), lambda i: (0, i)),
-            pl.BlockSpec((4, 2, ROWS, 256), lambda i: (i, 0, 0, 0)),
-            pl.BlockSpec((4, 2, 2, 32, 128), lambda i: (i, 0, 0, 0, 0)),
-        ],
+        in_specs=[spec] * len(args),
+        out_specs=[spec] * 3,
         out_shape=[
             sds((ROWS, 128 * size)),
             sds((4 * size, 2, ROWS, 256), BF16),
             sds((4 * size, 2, 2, 32, 128)),
         ],
-        compiler_params=params(10),
+        compiler_params=params(6),
         cost_estimate=pl.CostEstimate(flops=size * 5 * 10**8, bytes_accessed=size * 2 * 2**20, transcendentals=0),
-    )(within, damps, driven, inputs, state_output, angle, rate, skip_row)
+    )(*args)
 
 
 def simple(kernel, name, shapes, args, scratch=()):
@@ -416,32 +408,21 @@
 ):
     elapsed_row = elapsed.reshape(1, ROWS)
     inputs = jnp.swapaxes(state_input, 3, 4)
-    row_spec = whole((2, 64, 64))
-    driven, ends, pars, damps, within = pl.pallas_call(
+    spec, distant = pl.BlockSpec(memory_space=VMEM), pl.BlockSpec(memory_space=pltpu.HBM)
+    driven, ends, pars, damps, within, inputs_here = pl.pallas_call(
         end_kernel,
         name="ends",
-        grid=(TILES,),
-        in_specs=[
-            whole((ROWS, D)),
-            whole((1, ROWS)),
-            whole((1, D)),
-            pl.BlockSpec((D, 128), lambda i: (0, i)),
-            pl.BlockSpec((2, 2, 8, 16, 64), lambda i: (0, 0, i, 0, 0)),
-            row_spec, row_spec,
-        ],
-        out_specs=[
-            pl.BlockSpec((ROWS, 128), lambda i: (0, i)),
-            whole((2, 72, 128)),
-            whole((2, 2, 32, 128)),
-            pl.BlockSpec((4, 2, ROWS, ROWS), lambda i: (i, 0, 0, 0)),
-            whole((2, ROWS, ROWS)),
-        ],
+        in_specs=[spec, spec, spec, distant, distant, spec, spec],
+        out_specs=[spec] * 6,
         out_shape=[
             sds((ROWS, CHANNELS), BF16), sds((2, 72, 128)), sds((2, 2, 32, 128)),
-            sds((32, 2, ROWS, ROWS)), sds((2, ROWS, ROWS)),
+            sds((32, 2, ROWS, ROWS)), sds((2, ROWS, ROWS)), sds((2, 2, 64, 16, 64), BF16),
         ],
-        scratch_shapes=[VMEM((ROWS, D), BF16), VMEM((4, ROWS, ROWS), F32)],
-        compiler_params=params(10),
+        scratch_shapes=[
+            VMEM((ROWS, D), BF16), VMEM((3, ROWS, ROWS), F32), VMEM((TILES, D, 128), BF16),
+            pltpu.SemaphoreType.DMA((TILES,)), pltpu.SemaphoreType.DMA((TILES,)),
+        ],
+        compiler_params=params(12),
     )(
         *(hbm(a) for a in (tokens, elapsed_row, norm_gain.reshape(1, D), in_weight, inputs, decay_angle, forget_rate))
     )
@@ -454,7 +435,8 @@
         start = sum(PIECES[:index])
         driven_now, _ = lax.optimization_barrier((driven, before))
         piece = run_local(
-            start, PIECES[index], within, damps, driven_now, inputs, state_output, decay_angle, forget_rate, skip_row
+            start, PIECES[index],
+            (within, damps, driven_now, inputs_here, state_output, decay_angle, forget_rate, skip_row),
         )
         *piece, after = lax.optimization_barrier((*piece, after))
         pieces.append(piece)

time: 49.6 us -> 48.9 us (0.986)
  Pallas kernels: 30.9 us -> 30.4 us
    pallas_call x9, Pallas kernels: 27.2 us -> 26.7 us  [the longest x8 16.7 us: run_local(): pl.pallas_call(functools.partial(local_kernel, 4 * start, 4 * size), name...]
where the time goes in v6:
time: 48.9 us; the launch traced here: 48.8 us
  Pallas kernels  30.4 us (62%)
  starting transfers between devices  18.1 us (37%)
    pallas_call x8, Pallas kernels, run_local(): pl.pallas_call(functools.partial(local_kernel, 4 * start, 4 * size), name...  16.7 us
    ppermute x6, starting transfers between devices, local(): other = piece_between(total, lax.ppermute(total, axis, pairings[kind]))  11.9 us
    pallas_call x1, Pallas kernels, local(): pl.pallas_call(end_kernel, name='ends', in_specs=[spec, spec, spec, dista...  10 us
    ppermute x1, starting transfers between devices, local(): other = piece_between(theirs, lax.ppermute(theirs, 'c', swap))  4.76 us
    pallas_call x1, Pallas kernels, local(): pl.pallas_call(final_kernel, name='final', in_specs=[spec] * len(args), o...  3.34 us
    ppermute x1, starting transfers between devices, local(): partner = piece_between(keep, lax.ppermute(ends[1], 'c', swap))  1.45 us
  transfers between devices with their start and end apart: 8, of which 0 were waited for; matrix products, arithmetic and copies ran while one was open for 0% of the time, Pallas kernels for 34%

profile of v6, /device:TPU:1, one launch (start us, length us, event | category | flops | bytes accessed | tf_op | source)
XLA Modules:
  0.0 48.8 jit_solution(3480782555162009797)
XLA Ops:
  0.0 0.0 copy-start.1
  0.0 0.0 copy-start.2
  0.0 0.0 copy-start
  0.0 0.0 copy-start.5
  0.0 10.0 %ends.1 = (bf16[128,1024]{1,0:T(8,128)(2,1)S(1)}, f32[2,72,128]{2,1,0:T(8,128)S(1)}, f32[2,2,32,128]{3,2,1,0:T(8,128)S(1)}, f32[32,2,128,128]{3,2,1,0:T(8,128)S(...) custom-call(bf16[128,2048]{1,0:T(8,128)(2,1)} %tokens.1, f32[1,128]{1,0:T(1,128)} %bitcast.22, ...), custom_call_target="tpu_custom_call" | custom-call | tf_op jit(solution)/shard_map/ends/pallas_call | solution.py:412
  10.1 1.4 %collective-permute-start = (f32[72,128]{1,0:T(8,128)S(1)}, f32[72,128]{1,0:T(8,128)S(1)}, u32[]{:S(2)}, u32[]{:S(2)}) collective-permute-start(f32[72,128]{1,0:T(8,128)S(1)} %get-tuple-element.173), channel_id=1, source_target_pairs={{0,1},{1,0},{2,3},{3,2},{4,5},{5,4},{6,7},{7,6},{8,9},{9,8},{10,11... | collective-permute-start | bytes 110600 | tf_op jit(solution)/shard_map/ppermute | solution.py:449
  11.5 0.0 copy-done.1
  11.5 0.0 copy-done.2
  11.5 0.0 copy-done
  11.5 0.0 copy-done.5
  11.5 2.1 %local_0.1 = (f32[128,128]{1,0:T(8,128)S(1)}, bf16[4,2,128,256]{3,2,1,0:T(8,128)(2,1)S(1)}, f32[4,2,2,32,128]{4,3,2,1,0:T(8,128)S(1)}) custom-call(f32[2,128,128]{2,1,0:T(8,128)S(1)} %get-tuple-element.89.within, f32[32,2,128,128]{3,2,1,0:T(8,128)S(1)} %get-tuple-element.90.damps, bf16[128,1024]{1,0:T(8,128)(2,1)S(1)} %get-tuple-element.144.driven, ...), custom_call_target="tpu_custom_call" | custom-call | flops 500000000 | bytes 2097152 | tf_op jit(solution)/shard_map/local_0/pallas_call | solution.py:377
  13.6 0.0 collective-permute-done.other
  13.6 0.1 pair.1
  13.7 1.5 %collective-permute-start.1 = (f32[72,128]{1,0:T(8,128)S(1)}, f32[72,128]{1,0:T(8,128)S(1)}, u32[]{:S(2)}, u32[]{:S(2)}) collective-permute-start(f32[72,128]{1,0:T(8,128)S(1)} %get-tuple-element.100.own), channel_id=1, source_target_pairs={{0,2},{2,0},{4,6},{6,4},{1,3},{3,1},{5,7},{7,5},{8,10},{10,8},{12,... | collective-permute-start | bytes 110600 | tf_op jit(solution)/shard_map/ppermute | solution.py:453
  15.2 2.1 %local_1.1 = (f32[128,128]{1,0:T(8,128)S(1)}, bf16[4,2,128,256]{3,2,1,0:T(8,128)(2,1)S(1)}, f32[4,2,2,32,128]{4,3,2,1,0:T(8,128)S(1)}) custom-call(f32[2,128,128]{2,1,0:T(8,128)S(1)} %get-tuple-element.89.within, f32[32,2,128,128]{3,2,1,0:T(8,128)S(1)} %get-tuple-element.90.damps, bf16[128,1024]{1,0:T(8,128)(2,1)S(1)} %get-tuple-element.144.driven, ...), custom_call_target="tpu_custom_call" | custom-call | flops 500000000 | bytes 2097152 | tf_op jit(solution)/shard_map/local_1/pallas_call | solution.py:377
  17.3 0.0 collective-permute-done.1.other
  17.3 0.1 stage_y_low.1
  17.4 2.2 %collective-permute-start.2 = (f32[72,128]{1,0:T(8,128)S(1)}, f32[72,128]{1,0:T(8,128)S(1)}, u32[]{:S(2)}, u32[]{:S(2)}) collective-permute-start(f32[72,128]{1,0:T(8,128)S(1)} %get-tuple-element.107.own), channel_id=1, source_target_pairs={{0,6},{6,0},{2,4},{4,2},{1,7},{7,1},{3,5},{5,3},{8,14},{14,8},{10,... | collective-permute-start | bytes 110600 | tf_op jit(solution)/shard_map/ppermute | solution.py:453
  19.6 2.1 %local_2.1 = (f32[128,128]{1,0:T(8,128)S(1)}, bf16[4,2,128,256]{3,2,1,0:T(8,128)(2,1)S(1)}, f32[4,2,2,32,128]{4,3,2,1,0:T(8,128)S(1)}) custom-call(f32[2,128,128]{2,1,0:T(8,128)S(1)} %get-tuple-element.89.within, f32[32,2,128,128]{3,2,1,0:T(8,128)S(1)} %get-tuple-element.90.damps, bf16[128,1024]{1,0:T(8,128)(2,1)S(1)} %get-tuple-element.144.driven, ...), custom_call_target="tpu_custom_call" | custom-call | flops 500000000 | bytes 2097152 | tf_op jit(solution)/shard_map/local_2/pallas_call | solution.py:377
  21.7 0.0 collective-permute-done.2.other
  21.7 0.1 stage_y_high.1
  21.8 1.3 %collective-permute-start.3 = (f32[72,128]{1,0:T(8,128)S(1)}, f32[72,128]{1,0:T(8,128)S(1)}, u32[]{:S(2)}, u32[]{:S(2)}) collective-permute-start(f32[72,128]{1,0:T(8,128)S(1)} %get-tuple-element.114.own), channel_id=1, source_target_pairs={{0,8},{8,0},{16,24},{24,16},{1,9},{9,1},{17,25},{25,17},{2,10},{10... | collective-permute-start | bytes 110600 | tf_op jit(solution)/shard_map/ppermute | solution.py:453
  23.0 2.1 %local_3.1 = (f32[128,128]{1,0:T(8,128)S(1)}, bf16[4,2,128,256]{3,2,1,0:T(8,128)(2,1)S(1)}, f32[4,2,2,32,128]{4,3,2,1,0:T(8,128)S(1)}) custom-call(f32[2,128,128]{2,1,0:T(8,128)S(1)} %get-tuple-element.89.within, f32[32,2,128,128]{3,2,1,0:T(8,128)S(1)} %get-tuple-element.90.damps, bf16[128,1024]{1,0:T(8,128)(2,1)S(1)} %get-tuple-element.144.driven, ...), custom_call_target="tpu_custom_call" | custom-call | flops 500000000 | bytes 2097152 | tf_op jit(solution)/shard_map/local_3/pallas_call | solution.py:377
  25.1 0.0 collective-permute-done.3.other
  25.1 0.1 stage_x_low.1
  25.2 2.1 %collective-permute-start.4 = (f32[72,128]{1,0:T(8,128)S(1)}, f32[72,128]{1,0:T(8,128)S(1)}, u32[]{:S(2)}, u32[]{:S(2)}) collective-permute-start(f32[72,128]{1,0:T(8,128)S(1)} %get-tuple-element.121.own), channel_id=1, source_target_pairs={{0,24},{24,0},{8,16},{16,8},{1,25},{25,1},{9,17},{17,9},{2,26},{26... | collective-permute-start | bytes 110600 | tf_op jit(solution)/shard_map/ppermute | solution.py:453
  27.3 2.1 %local_4.1 = (f32[128,128]{1,0:T(8,128)S(1)}, bf16[4,2,128,256]{3,2,1,0:T(8,128)(2,1)S(1)}, f32[4,2,2,32,128]{4,3,2,1,0:T(8,128)S(1)}) custom-call(f32[2,128,128]{2,1,0:T(8,128)S(1)} %get-tuple-element.89.within, f32[32,2,128,128]{3,2,1,0:T(8,128)S(1)} %get-tuple-element.90.damps, bf16[128,1024]{1,0:T(8,128)(2,1)S(1)} %get-tuple-element.144.driven, ...), custom_call_target="tpu_custom_call" | custom-call | flops 500000000 | bytes 2097152 | tf_op jit(solution)/shard_map/local_4/pallas_call | solution.py:377
  29.3 0.0 collective-permute-done.4.other
  29.4 0.1 stage_x_high.1
  29.4 1.9 %collective-permute-start.5 = (f32[72,128]{1,0:T(8,128)S(1)}, f32[72,128]{1,0:T(8,128)S(1)}, u32[]{:S(2)}, u32[]{:S(2)}) collective-permute-start(f32[72,128]{1,0:T(8,128)S(1)} %get-tuple-element.128.own), channel_id=1, source_target_pairs={{0,32},{32,0},{64,96},{96,64},{1,33},{33,1},{65,97},{97,65},{2,34}... | collective-permute-start | bytes 110600 | tf_op jit(solution)/shard_map/ppermute | solution.py:453
  31.3 2.1 %local_5.1 = (f32[128,128]{1,0:T(8,128)S(1)}, bf16[4,2,128,256]{3,2,1,0:T(8,128)(2,1)S(1)}, f32[4,2,2,32,128]{4,3,2,1,0:T(8,128)S(1)}) custom-call(f32[2,128,128]{2,1,0:T(8,128)S(1)} %get-tuple-element.89.within, f32[32,2,128,128]{3,2,1,0:T(8,128)S(1)} %get-tuple-element.90.damps, bf16[128,1024]{1,0:T(8,128)(2,1)S(1)} %get-tuple-element.144.driven, ...), custom_call_target="tpu_custom_call" | custom-call | flops 500000000 | bytes 2097152 | tf_op jit(solution)/shard_map/local_5/pallas_call | solution.py:377
  33.4 0.0 collective-permute-done.5.other
  33.4 0.1 stage_z_low.1
  33.5 2.9 %collective-permute-start.6 = (f32[72,128]{1,0:T(8,128)S(1)}, f32[72,128]{1,0:T(8,128)S(1)}, u32[]{:S(2)}, u32[]{:S(2)}) collective-permute-start(f32[72,128]{1,0:T(8,128)S(1)} %get-tuple-element.135), channel_id=1, source_target_pairs={{0,96},{96,0},{32,64},{64,32},{1,97},{97,1},{33,65},{65,33},{2,98}... | collective-permute-start | bytes 110600 | tf_op jit(solution)/shard_map/ppermute | solution.py:453
  36.4 2.1 %local_6.1 = (f32[128,128]{1,0:T(8,128)S(1)}, bf16[4,2,128,256]{3,2,1,0:T(8,128)(2,1)S(1)}, f32[4,2,2,32,128]{4,3,2,1,0:T(8,128)S(1)}) custom-call(f32[2,128,128]{2,1,0:T(8,128)S(1)} %get-tuple-element.89.within, f32[32,2,128,128]{3,2,1,0:T(8,128)S(1)} %get-tuple-element.90.damps, bf16[128,1024]{1,0:T(8,128)(2,1)S(1)} %get-tuple-element.144.driven, ...), custom_call_target="tpu_custom_call" | custom-call | flops 500000000 | bytes 2097152 | tf_op jit(solution)/shard_map/local_6/pallas_call | solution.py:377
  38.5 0.0 copy-start.3
  38.5 0.0 copy-start.4
  38.5 0.0 copy-start.6
  38.5 0.0 copy-start.7
  38.5 0.0 collective-permute-done.6.last
  38.5 0.1 enter.1
  38.6 4.8 %collective-permute-start.7 = (f32[4,16,128]{2,1,0:T(8,128)S(1)}, f32[4,16,128]{2,1,0:T(8,128)S(1)}, u32[]{:S(2)}, u32[]{:S(2)}) collective-permute-start(f32[4,16,128]{2,1,0:T(8,128)S(1)} %get-tuple-element.143), channel_id=1, source_target_pairs={{0,1},{1,0},{2,3},{3,2},{4,5},{5,4},{6,7},{7,6},{8,9},{9,8},{10,11... | collective-permute-start | bytes 98312 | tf_op jit(solution)/shard_map/ppermute | solution.py:464
  43.3 2.1 %local_7.1 = (f32[128,128]{1,0:T(8,128)S(1)}, bf16[4,2,128,256]{3,2,1,0:T(8,128)(2,1)S(1)}, f32[4,2,2,32,128]{4,3,2,1,0:T(8,128)S(1)}) custom-call(f32[2,128,128]{2,1,0:T(8,128)S(1)} %get-tuple-element.89.within, f32[32,2,128,128]{3,2,1,0:T(8,128)S(1)} %get-tuple-element.90.damps, bf16[128,1024]{1,0:T(8,128)(2,1)S(1)} %get-tuple-element.144.driven, ...), custom_call_target="tpu_custom_call" | custom-call | flops 500000000 | bytes 2097152 | tf_op jit(solution)/shard_map/local_7/pallas_call | solution.py:377
  45.4 0.0 collective-permute-done.7.refs_1_
  45.4 0.0 copy-done.3
  45.4 0.0 copy-done.4
  45.5 0.0 copy-done.6
  45.5 0.0 copy-done.7
  45.5 3.3 %final.1 = bf16[128,2048]{1,0:T(8,128)(2,1)} custom-call(f32[4,16,128]{2,1,0:T(8,128)S(1)} %get-tuple-element.142.refs_0_, f32[4,16,128]{2,1,0:T(8,128)S(1)} %collective-permute-done.7.refs_1_, f32[128,128]{1,0:T(8,128)S(1)} %get-tuple-element.149.refs_2_, f32[128,128]{1,0:T(8,128)S(1)} %get-tuple-element.150.refs_3_, ...), custom_call_target="tpu_custom_call" | custom-call | tf_op jit(solution)/shard_map/final/pallas_call | solution.py:471
  (1 shorter events, 0.0 us)
Async XLA Ops:
  0.0 11.5 %copy-start.1 = (f32[2,64,64]{2,1,0:T(8,128)S(1)}, f32[2,64,64]{2,1,0:T(8,128)}, u32[]{:S(2)}) copy-start(f32[2,64,64]{2,1,0:T(8,128)} %angle.17) | copy-start | bytes 98308
  0.0 11.5 %copy-start.2 = (f32[2,64,64]{2,1,0:T(8,128)S(1)}, f32[2,64,64]{2,1,0:T(8,128)}, u32[]{:S(2)}) copy-start(f32[2,64,64]{2,1,0:T(8,128)} %rate.17) | copy-start | bytes 98308
  0.0 11.5 %copy-start = (f32[2,2,64,16,64]{4,3,2,1,0:T(8,128)S(1)}, f32[2,2,64,16,64]{4,3,2,1,0:T(8,128)}, u32[]{:S(2)}) copy-start(f32[2,2,64,16,64]{4,3,2,1,0:T(8,128)} %readout.15) | copy-start | bytes 3145732
  0.0 11.5 %copy-start.5 = (f32[1024]{0:T(1024)S(1)}, f32[1024]{0:T(1024)}, u32[]{:S(2)}) copy-start(f32[1024]{0:T(1024)} %param.21) | copy-start | bytes 12292
  10.1 3.6 %collective-permute-start = (f32[72,128]{1,0:T(8,128)S(1)}, f32[72,128]{1,0:T(8,128)S(1)}, u32[]{:S(2)}, u32[]{:S(2)}) collective-permute-start(f32[72,128]{1,0:T(8,128)S(1)} %get-tuple-element.173), channel_id=1, source_target_pairs={{0,1},{1,0},{2,3},{3,2},{4,5},{5,4},{6,7},{7,6},{8,9},{9,8},{10,11... | collective-permute-start | bytes 110600 | tf_op jit(solution)/shard_map/ppermute | solution.py:449
  13.7 3.6 %collective-permute-start.1 = (f32[72,128]{1,0:T(8,128)S(1)}, f32[72,128]{1,0:T(8,128)S(1)}, u32[]{:S(2)}, u32[]{:S(2)}) collective-permute-start(f32[72,128]{1,0:T(8,128)S(1)} %get-tuple-element.100.own), channel_id=1, source_target_pairs={{0,2},{2,0},{4,6},{6,4},{1,3},{3,1},{5,7},{7,5},{8,10},{10,8},{12,... | collective-permute-start | bytes 110600 | tf_op jit(solution)/shard_map/ppermute | solution.py:453
  17.4 4.3 %collective-permute-start.2 = (f32[72,128]{1,0:T(8,128)S(1)}, f32[72,128]{1,0:T(8,128)S(1)}, u32[]{:S(2)}, u32[]{:S(2)}) collective-permute-start(f32[72,128]{1,0:T(8,128)S(1)} %get-tuple-element.107.own), channel_id=1, source_target_pairs={{0,6},{6,0},{2,4},{4,2},{1,7},{7,1},{3,5},{5,3},{8,14},{14,8},{10,... | collective-permute-start | bytes 110600 | tf_op jit(solution)/shard_map/ppermute | solution.py:453
  21.8 3.4 %collective-permute-start.3 = (f32[72,128]{1,0:T(8,128)S(1)}, f32[72,128]{1,0:T(8,128)S(1)}, u32[]{:S(2)}, u32[]{:S(2)}) collective-permute-start(f32[72,128]{1,0:T(8,128)S(1)} %get-tuple-element.114.own), channel_id=1, source_target_pairs={{0,8},{8,0},{16,24},{24,16},{1,9},{9,1},{17,25},{25,17},{2,10},{10... | collective-permute-start | bytes 110600 | tf_op jit(solution)/shard_map/ppermute | solution.py:453
  25.2 4.1 %collective-permute-start.4 = (f32[72,128]{1,0:T(8,128)S(1)}, f32[72,128]{1,0:T(8,128)S(1)}, u32[]{:S(2)}, u32[]{:S(2)}) collective-permute-start(f32[72,128]{1,0:T(8,128)S(1)} %get-tuple-element.121.own), channel_id=1, source_target_pairs={{0,24},{24,0},{8,16},{16,8},{1,25},{25,1},{9,17},{17,9},{2,26},{26... | collective-permute-start | bytes 110600 | tf_op jit(solution)/shard_map/ppermute | solution.py:453
  29.4 4.0 %collective-permute-start.5 = (f32[72,128]{1,0:T(8,128)S(1)}, f32[72,128]{1,0:T(8,128)S(1)}, u32[]{:S(2)}, u32[]{:S(2)}) collective-permute-start(f32[72,128]{1,0:T(8,128)S(1)} %get-tuple-element.128.own), channel_id=1, source_target_pairs={{0,32},{32,0},{64,96},{96,64},{1,33},{33,1},{65,97},{97,65},{2,34}... | collective-permute-start | bytes 110600 | tf_op jit(solution)/shard_map/ppermute | solution.py:453
  33.5 5.0 %collective-permute-start.6 = (f32[72,128]{1,0:T(8,128)S(1)}, f32[72,128]{1,0:T(8,128)S(1)}, u32[]{:S(2)}, u32[]{:S(2)}) collective-permute-start(f32[72,128]{1,0:T(8,128)S(1)} %get-tuple-element.135), channel_id=1, source_target_pairs={{0,96},{96,0},{32,64},{64,32},{1,97},{97,1},{33,65},{65,33},{2,98}... | collective-permute-start | bytes 110600 | tf_op jit(solution)/shard_map/ppermute | solution.py:453
  38.5 7.0 %copy-start.3 = (bf16[1024,2048]{1,0:T(8,128)(2,1)S(1)}, bf16[1024,2048]{1,0:T(8,128)(2,1)}, u32[]{:S(2)}) copy-start(bf16[1024,2048]{1,0:T(8,128)(2,1)} %refs_28_.1) | copy-start | bytes 12582916
  38.5 7.0 %copy-start.4 = (bf16[1024,1024]{1,0:T(8,128)(2,1)S(1)}, bf16[1024,1024]{1,0:T(8,128)(2,1)}, u32[]{:S(2)}) copy-start(bf16[1024,1024]{1,0:T(8,128)(2,1)} %refs_26_.1) | copy-start | bytes 6291460
  38.5 7.0 %copy-start.6 = (f32[2048]{0:T(1024)S(1)}, f32[2048]{0:T(1024)}, u32[]{:S(2)}) copy-start(f32[2048]{0:T(1024)} %param.25) | copy-start | bytes 24580
  38.5 7.0 %copy-start.7 = (f32[1024]{0:T(1024)S(1)}, f32[1024]{0:T(1024)}, u32[]{:S(2)}) copy-start(f32[1024]{0:T(1024)} %param.23) | copy-start | bytes 12292
  38.6 6.9 %collective-permute-start.7 = (f32[4,16,128]{2,1,0:T(8,128)S(1)}, f32[4,16,128]{2,1,0:T(8,128)S(1)}, u32[]{:S(2)}, u32[]{:S(2)}) collective-permute-start(f32[4,16,128]{2,1,0:T(8,128)S(1)} %get-tuple-element.143), channel_id=1, source_target_pairs={{0,1},{1,0},{2,3},{3,2},{4,5},{5,4},{6,7},{7,6},{8,9},{9,8},{10,11... | collective-permute-start | bytes 98312 | tf_op jit(solution)/shard_map/ppermute | solution.py:464

commit v7 on v6

--- a/solution.py
+++ b/solution.py
@@ -15,7 +15,7 @@
 TILES = 8
 SPAN = 16
 SPANS = ROWS // SPAN
-PIECES = (1,) * 8
+PIECES = (1, 2, 2, 2, 1)
 LOG2E = 1.0 / math.log(2.0)
 TINY = 1e-37
 EPSILON = 1e-06
@@ -81,7 +81,7 @@
 
 def end_kernel(
     tokens, elapsed, gain, weight, inputs, angle, rate,
-    driven_ref, ends_ref, pars_ref, damp_ref, within_ref, inputs_ref, normed, times, chunks, weight_sems, input_sems,
+    driven_ref, pairs_ref, ends_ref, pars_ref, damp_ref, within_ref, inputs_ref, normed, times, chunks, weight_sems, input_sems,
 ):
     core = lax.axis_index("c")
 
@@ -122,6 +122,7 @@
         away = jnp.where((step // 4) == core, 0, 1)
         for j in range(4):
             pair = step * 4 + j
+            pairs_ref[pair] = driven[:, 32 * j : 32 * j + 32]
             for k in range(2):
                 f = pair_row(rate, k, pair)
                 th = pair_row(angle, k, pair)
@@ -151,23 +152,21 @@
 
 
 def local_kernel(
-    start, size, within, damps, driven, inputs, readout, angle, rate, skip,
-    out_ref, prefix_ref, table_ref,
+    start, size, within, damps, driven, inputs, readout, pars, out_ref, prefix_ref, table_ref, triangles,
 ):
     row, col = iotas((ROWS, ROWS))
     same = row // SPAN == col // SPAN
-    triangles = (((col <= row) & same).astype(BF16), ((col >= row) & same).astype(BF16))
+    triangles[0] = ((col <= row) & same).astype(BF16)
+    triangles[1] = ((col >= row) & same).astype(BF16)
     empty = jnp.zeros((16, 64), BF16)
     hole = jnp.zeros((16, 64), F32)
-    x = driven[:, 32 * start : 32 * (start + size)]
-    outs = []
-    for j in range(size):
+
+    def both(j, _):
         pair = start + j
-        lhs = x[:, 32 * j : 32 * j + 32]
+        lhs = driven[pair]
         total = None
         for k in range(2):
-            f = pair_row(rate, k, pair)
-            th = pair_row(angle, k, pair)
+            th, f = pars[k, 0, pl.ds(pair, 1), :], pars[k, 1, pl.ds(pair, 1), :]
             b00, b01 = inputs[k, 0, 2 * pair], inputs[k, 1, 2 * pair]
             b10, b11 = inputs[k, 0, 2 * pair + 1], inputs[k, 1, 2 * pair + 1]
             rhs = jnp.concatenate(
@@ -191,7 +190,7 @@
             e_re, e_im = fade * cosine, fade * sine
             c_re = c_im = jnp.zeros((1, 128), F32)
             d_re, d_im = jnp.ones((1, 128), F32), jnp.zeros((1, 128), F32)
-            states, prefixes = [None] * SPANS, [None] * SPANS
+            states = [None] * SPANS
             for n in range(SPANS) if k == 0 else range(SPANS - 1, -1, -1):
                 cut = slice(SPAN * n, SPAN * n + SPAN)
                 er, ei = e_re[cut], e_im[cut]
@@ -201,8 +200,7 @@
                 edge = slice(SPAN - 1, SPAN) if k == 0 else slice(0, 1)
                 c_re, c_im, d_re, d_im = sr[edge], si[edge], pr[edge], pi[edge]
                 states[n] = jnp.concatenate([sr.astype(BF16), si.astype(BF16)], axis=1)
-                prefixes[n] = jnp.concatenate([pr.astype(BF16), pi.astype(BF16)], axis=1)
-            prefix_ref[j, k] = jnp.concatenate(prefixes, axis=0)
+                prefix_ref[j, k, cut, :] = jnp.concatenate([pr.astype(BF16), pi.astype(BF16)], axis=1)
             tables = []
             for c in range(2):
                 upper = jnp.concatenate([readout[k, c, 2 * pair], hole], axis=1)
@@ -215,8 +213,10 @@
                 jnp.concatenate([tables[0].astype(BF16), (-tables[1]).astype(BF16)], axis=1),
             )
             total = y if total is None else total + y
-        outs.append(total)
-    out_ref[...] = jnp.concatenate(outs, axis=1) + skip[:, 32 * start : 32 * (start + size)] * x.astype(F32)
+        out_ref[j] = total
+        return 0
+
+    lax.fori_loop(0, size, both, 0)
 
 
 def times_of(a, b):
@@ -261,61 +261,67 @@
     return jnp.concatenate([span, span], axis=0)
 
 
+def keep_states(ref, k, value):
+    ref[32 * k : 32 * k + 16, :], ref[32 * k + 16 : 32 * k + 32, :] = value
+
+
 def keep_at(ref, at, value):
     ref[2 * at], ref[2 * at + 1] = value
 
 
-def upper(stage):
-    axis, kind = stage
-    here = lax.axis_index(axis)
-    return here >= 2 if kind == "high" else here % 2 == 1
-
-
-def merge(stage, own, other, mine, total_ref, k, decay, decay_other):
-    behind = upper(stage) if k == 0 else jnp.logical_not(upper(stage))
-    a, b = states_of(own, k), states_of(other, k)
-    early, late = pick(behind, b, a), pick(behind, a, b)
-    total = plus(times_of(pick(behind, decay, decay_other), early), late)
-    if total_ref is not None:
-        total_ref[32 * k : 32 * k + 16, :], total_ref[32 * k + 16 : 32 * k + 32, :] = total
-    return behind, b
-
-
-def pair_kernel(own, other, pars, total_ref, trail_ref):
-    mine = my_pars(pars)
-    zero = jnp.zeros((16, 128), F32)
-    for k in range(2):
-        decay, decay_other = decay_over(span_of(own), mine[k]), decay_over(span_of(other), mine[k])
-        merge(("c", "low"), own, other, mine, total_ref, k, decay, decay_other)
-        keep_at(trail_ref, k, (zero, zero))
-        keep_at(trail_ref, 2 + k, (zero + 1.0, zero))
-        keep_at(trail_ref, 4 + k, times_of(decay, decay_other))
-    total_ref[64:72, :] = own[64:72, :] + other[64:72, :]
-
-
-def trail_of(trail, at):
-    return trail[2 * at], trail[2 * at + 1]
-
-
-def stage_kernel(stage, own, other, trail, pars, total_ref, trail_ref):
-    mine = my_pars(pars)
-    for k in range(2):
-        decay, decay_other = trail_of(trail, 4 + k), decay_over(span_of(other), mine[k])
-        behind, theirs = merge(stage, own, other, mine, total_ref, k, decay, decay_other)
-        state, fade = trail_of(trail, k), trail_of(trail, 2 + k)
-        keep_at(trail_ref, k, pick(behind, plus(times_of(fade, theirs), state), state))
-        keep_at(trail_ref, 2 + k, pick(behind, times_of(fade, decay_other), fade))
-        keep_at(trail_ref, 4 + k, times_of(decay, decay_other))
-    total_ref[64:72, :] = own[64:72, :] + other[64:72, :]
-
-
-def enter_kernel(stage, last, trail, own, other, pars, mine_ref, theirs_ref):
+def pair_kernel(own, other, pars, total_ref):
     core = lax.axis_index("c")
     mine = my_pars(pars)
     for k in range(2):
-        behind = upper(stage) if k == 0 else jnp.logical_not(upper(stage))
-        state, fade = trail_of(trail, k), trail_of(trail, 2 + k)
-        state = pick(behind, plus(times_of(fade, states_of(last, k)), state), state)
+        ahead = core == k
+        a, b = states_of(own, k), states_of(other, k)
+        early, late = pick(ahead, a, b), pick(ahead, b, a)
+        step = decay_over(jnp.where(ahead, span_of(other), span_of(own)), mine[k])
+        keep_states(total_ref, k, plus(times_of(step, early), late))
+    total_ref[64:72, :] = own[64:72, :] + other[64:72, :]
+
+
+def gather_four(axis, own, one, two, three, data):
+    here = lax.axis_index(axis)
+    data[here] = own[...]
+    data[here + 1 - 2 * (here % 2)] = one[...]
+    data[(here + 2) % 4] = two[...]
+    data[3 - here] = three[...]
+    return here
+
+
+def run_over(here, data, mine, k):
+    zero = jnp.zeros((16, 128), F32)
+    state, decay = (zero, zero), (zero + 1.0, zero)
+    before, before_decay = state, decay
+    for n in range(4) if k == 0 else range(3, -1, -1):
+        before = pick(n == here, state, before)
+        before_decay = pick(n == here, decay, before_decay)
+        step = decay_over(span_of(data.at[n]), mine[k])
+        state = plus(times_of(step, state), states_of(data.at[n], k))
+        decay = times_of(step, decay)
+    return state, before, before_decay
+
+
+def group_kernel(axis, own, one, two, three, pars, total_ref, before_ref, data):
+    here = gather_four(axis, own, one, two, three, data)
+    mine = my_pars(pars)
+    for k in range(2):
+        total, before, decay = run_over(here, data, mine, k)
+        keep_states(total_ref, k, total)
+        keep_at(before_ref, k, before)
+        keep_at(before_ref, 2 + k, decay)
+    total_ref[64:72, :] = own[64:72, :] + one[64:72, :] + two[64:72, :] + three[64:72, :]
+
+
+def enter_kernel(across, one, two, three, before_x, before_y, own, other, pars, mine_ref, theirs_ref, data):
+    here = gather_four("z", across, one, two, three, data)
+    core = lax.axis_index("c")
+    mine = my_pars(pars)
+    for k in range(2):
+        _, state, _ = run_over(here, data, mine, k)
+        for before in (before_x, before_y):
+            state = plus(times_of((before[4 + 2 * k], before[5 + 2 * k]), state), (before[2 * k], before[2 * k + 1]))
         ahead = core == k
         early = pick(ahead, states_of(own, k), states_of(other, k))
         later = plus(times_of(decay_over(jnp.where(ahead, span_of(own), span_of(other)), mine[k]), state), early)
@@ -327,7 +333,7 @@
     count = len(PIECES)
     own, other = refs[:2]
     nears, prefixes, tables = (refs[2 + count * n : 2 + count * n + count] for n in range(3))
-    glu, glu_bias, outw, out_gain, out_ref, entering, response = refs[2 + 3 * count :]
+    driven, skip, glu, glu_bias, outw, out_gain, out_ref, entering, response = refs[2 + 3 * count :]
     core = lax.axis_index("c")
     entering[core] = own[...]
     entering[1 - core] = other[...]
@@ -348,14 +354,14 @@
                     )
                     y = nt(prefix[4 * i + j, k], rhs)
                     total = y if total is None else total + y
-                outs.append(total)
+                outs.append(total + near[4 * i + j])
             at = pl.multiple_of(128 * i, 128)
-            response[:, pl.ds(at + 128 * start, 128)] = jnp.concatenate(outs, axis=1) + near[:, pl.ds(at, 128)]
+            response[:, pl.ds(at + 128 * start, 128)] = jnp.concatenate(outs, axis=1)
             return 0
 
         lax.fori_loop(0, size, tile, 0)
         start += size
-    x = response[...]
+    x = response[...] + skip[...] * driven[...].astype(F32)
     active = 0.5 * x * (1.0 + jnp.tanh(math.sqrt(2.0 / math.pi) * (x + 0.044715 * (x * x * x))))
     gate = mm(active.astype(BF16), glu[...]) + glu_bias[...]
     gated = (active * jax.nn.sigmoid(gate)).astype(BF16)
@@ -380,10 +386,11 @@
         in_specs=[spec] * len(args),
         out_specs=[spec] * 3,
         out_shape=[
-            sds((ROWS, 128 * size)),
+            sds((4 * size, ROWS, 32)),
             sds((4 * size, 2, ROWS, 256), BF16),
             sds((4 * size, 2, 2, 32, 128)),
         ],
+        scratch_shapes=[VMEM((2, ROWS, ROWS), BF16)],
         compiler_params=params(6),
         cost_estimate=pl.CostEstimate(flops=size * 5 * 10**8, bytes_accessed=size * 2 * 2**20, transcendentals=0),
     )(*args)
@@ -409,13 +416,13 @@
     elapsed_row = elapsed.reshape(1, ROWS)
     inputs = jnp.swapaxes(state_input, 3, 4)
     spec, distant = pl.BlockSpec(memory_space=VMEM), pl.BlockSpec(memory_space=pltpu.HBM)
-    driven, ends, pars, damps, within, inputs_here = pl.pallas_call(
+    driven, pairs, ends, pars, damps, within, inputs_here = pl.pallas_call(
         end_kernel,
         name="ends",
         in_specs=[spec, spec, spec, distant, distant, spec, spec],
-        out_specs=[spec] * 6,
+        out_specs=[spec] * 7,
         out_shape=[
-            sds((ROWS, CHANNELS), BF16), sds((2, 72, 128)), sds((2, 2, 32, 128)),
+            sds((ROWS, CHANNELS), BF16), sds((32, ROWS, 32), BF16), sds((2, 72, 128)), sds((2, 2, 32, 128)),
             sds((32, 2, ROWS, ROWS)), sds((2, ROWS, ROWS)), sds((2, 2, 64, 16, 64), BF16),
         ],
         scratch_shapes=[
@@ -427,46 +434,45 @@
         *(hbm(a) for a in (tokens, elapsed_row, norm_gain.reshape(1, D), in_weight, inputs, decay_angle, forget_rate))
     )
 
-    skip_row = skip_gain.reshape(1, CHANNELS)
     pieces, start = [], 0
 
     def piece_between(before, after):
         index = len(pieces)
         start = sum(PIECES[:index])
-        driven_now, _ = lax.optimization_barrier((driven, before))
+        pairs_now, _ = lax.optimization_barrier((pairs, before))
         piece = run_local(
             start, PIECES[index],
-            (within, damps, driven_now, inputs_here, state_output, decay_angle, forget_rate, skip_row),
+            (within, damps, pairs_now, inputs_here, state_output, pars),
         )
         *piece, after = lax.optimization_barrier((*piece, after))
         pieces.append(piece)
         return after
 
     swap = [(0, 1), (1, 0)]
-    pairings = {"low": [(0, 1), (1, 0), (2, 3), (3, 2)], "high": [(0, 3), (3, 0), (1, 2), (2, 1)]}
-    stages = [(axis, kind) for axis in ("y", "x", "z") for kind in ("low", "high")]
+    swaps = ([(0, 1), (1, 0), (2, 3), (3, 2)], [(0, 2), (2, 0), (1, 3), (3, 1)], [(0, 3), (3, 0), (1, 2), (2, 1)])
+    four = VMEM((4, 72, 128), F32)
     keep = ends[0]
     partner = piece_between(keep, lax.ppermute(ends[1], "c", swap))
-    total, trail = simple(pair_kernel, "pair", [(72, 128), (12, 16, 128)], (keep, partner, pars))
-    for stage in stages:
-        axis, kind = stage
-        other = piece_between(total, lax.ppermute(total, axis, pairings[kind]))
-        if stage == stages[-1]:
-            mine, theirs = simple(
-                functools.partial(enter_kernel, stage), "enter", [(4, 16, 128), (4, 16, 128)],
-                (other, trail, keep, partner, pars),
-            )
-        else:
-            total, trail = simple(
-                functools.partial(stage_kernel, stage), f"stage_{axis}_{kind}", [(72, 128), (12, 16, 128)],
-                (total, other, trail, pars),
-            )
+    (total,) = simple(pair_kernel, "pair", [(72, 128)], (keep, partner, pars))
+    befores = []
+    for axis in ("y", "x"):
+        others = piece_between(total, tuple(lax.ppermute(total, axis, pairs) for pairs in swaps))
+        total, before = simple(
+            functools.partial(group_kernel, axis), f"group_{axis}", [(72, 128), (8, 16, 128)],
+            (total, *others, pars), [four],
+        )
+        befores.append(before)
+    others = piece_between(total, tuple(lax.ppermute(total, "z", pairs) for pairs in swaps))
+    mine, theirs = simple(
+        enter_kernel, "enter", [(4, 16, 128), (4, 16, 128)],
+        (total, *others, befores[1], befores[0], keep, partner, pars), [four],
+    )
     other = piece_between(theirs, lax.ppermute(theirs, "c", swap))
 
     spec = pl.BlockSpec(memory_space=VMEM)
     args = (
         mine, other, *(p[0] for p in pieces), *(p[1] for p in pieces), *(p[2] for p in pieces),
-        glu_weight, glu_bias.reshape(1, CHANNELS), out_weight, out_gain.reshape(1, D),
+        driven, skip_gain.reshape(1, CHANNELS), glu_weight, glu_bias.reshape(1, CHANNELS), out_weight, out_gain.reshape(1, D),
     )
     return pl.pallas_call(
         final_kernel,

time: 48.9 us -> 52 us (1.063)
  Pallas kernels: 30.4 us -> 36.5 us
  starting transfers between devices: 18.1 us -> 15.1 us
    pallas_call x8 -> x5, Pallas kernels: 16.7 us -> 21.1 us  [run_local(): pl.pallas_call(functools.partial(local_kernel, 4 * start, 4 * size), name...]
    ppermute x1, starting transfers between devices: 4.76 us -> 2.2 us  [local(): other = piece_between(theirs, lax.ppermute(theirs, 'c', swap))]
    pallas_call x1, Pallas kernels: 3.34 us -> 4.79 us  [local(): pl.pallas_call(final_kernel, name='final', in_specs=[spec] * len(args), o...]
    ppermute x6 -> x9, starting transfers between devices: 11.9 us -> 11.4 us  [the longest x6 6.93 us: local(): lax.ppermute(total, axis, pairs)]
  transfers between devices with their start and end apart: 8 -> 11, of which waited for: 0 -> 0; matrix products, arithmetic and copies ran while one was open for 0% -> 0% of each run, Pallas kernels for 34% -> 41%
where the time goes in v7:
time: 52 us; the launch traced here: 51.9 us
  Pallas kernels  36.5 us (70%)
  starting transfers between devices  15.1 us (29%)
    pallas_call x5, Pallas kernels, run_local(): pl.pallas_call(functools.partial(local_kernel, 4 * start, 4 * size), name...  21.1 us
    pallas_call x1, Pallas kernels, local(): pl.pallas_call(end_kernel, name='ends', in_specs=[spec, spec, spec, dista...  10.1 us
    ppermute x6, starting transfers between devices, local(): lax.ppermute(total, axis, pairs)  6.93 us
    pallas_call x1, Pallas kernels, local(): pl.pallas_call(final_kernel, name='final', in_specs=[spec] * len(args), o...  4.79 us
    ppermute x3, starting transfers between devices, local(): lax.ppermute(total, 'z', pairs)  4.5 us
    ppermute x1, starting transfers between devices, local(): other = piece_between(theirs, lax.ppermute(theirs, 'c', swap))  2.2 us
    ppermute x1, starting transfers between devices, local(): partner = piece_between(keep, lax.ppermute(ends[1], 'c', swap))  1.46 us
  transfers between devices with their start and end apart: 11, of which 0 were waited for; matrix products, arithmetic and copies ran while one was open for 0% of the time, Pallas kernels for 41%

profile of v7, /device:TPU:1, one launch (start us, length us, event | category | flops | bytes accessed | tf_op | source)
XLA Modules:
  0.0 51.9 jit_solution(5522655771860848551)
XLA Ops:
  0.0 0.0 copy-start
  0.0 10.1 %ends.1 = (bf16[128,1024]{1,0:T(8,128)(2,1)S(1)}, bf16[32,128,32]{2,1,0:T(8,128)(2,1)S(1)}, f32[2,72,128]{2,1,0:T(8,128)S(1)}, f32[2,2,32,128]{3,2,1,0:T(8,128)S...) custom-call(bf16[128,2048]{1,0:T(8,128)(2,1)} %tokens.1, ...), custom_call_target="tpu_custom_call" | custom-call | tf_op jit(solution)/shard_map/ends/pallas_call | solution.py:419
  10.1 1.5 %collective-permute-start = (f32[72,128]{1,0:T(8,128)S(1)}, f32[72,128]{1,0:T(8,128)S(1)}, u32[]{:S(2)}, u32[]{:S(2)}) collective-permute-start(f32[72,128]{1,0:T(8,128)S(1)} %get-tuple-element.123), channel_id=1, source_target_pairs={{0,1},{1,0},{2,3},{3,2},{4,5},{5,4},{6,7},{7,6},{8,9},{9,8},{10,11... | collective-permute-start | bytes 110600 | tf_op jit(solution)/shard_map/ppermute | solution.py:455
  11.6 0.0 copy-done
  11.6 2.6 %local_0.1 = (f32[4,128,32]{2,1,0:T(8,128)S(1)}, bf16[4,2,128,256]{3,2,1,0:T(8,128)(2,1)S(1)}, f32[4,2,2,32,128]{4,3,2,1,0:T(8,128)S(1)}) custom-call(f32[2,128,128]{2,1,0:T(8,128)S(1)} %get-tuple-element.65.within, f32[32,2,128,128]{3,2,1,0:T(8,128)S(1)} %get-tuple-element.66.damps, bf16[32,128,32]{2,1,0:T(8,128)(2,1)S(1)} %get-tuple-element.102.driven, ...), custom_call_target="tpu_custom_call" | custom-call | flops 500000000 | bytes 2097152 | tf_op jit(solution)/shard_map/local_0/pallas_call | solution.py:383
  14.3 0.0 collective-permute-done.other
  14.3 2.9 %collective-permute-start.3 = (f32[72,128]{1,0:T(8,128)S(1)}, f32[72,128]{1,0:T(8,128)S(1)}, u32[]{:S(2)}, u32[]{:S(2)}) collective-permute-start(f32[72,128]{1,0:T(8,128)S(1)} %pair.1.own), channel_id=1, source_target_pairs={{0,6},{6,0},{2,4},{4,2},{1,7},{7,1},{3,5},{5,3},{8,14},{14,8},{10,... | collective-permute-start | bytes 110600 | tf_op jit(solution)/shard_map/ppermute | solution.py:459
  17.2 0.3 collective-permute-start.2
  17.6 0.3 collective-permute-start.1
  17.9 5.3 %local_1.1 = (f32[8,128,32]{2,1,0:T(8,128)S(1)}, bf16[8,2,128,256]{3,2,1,0:T(8,128)(2,1)S(1)}, f32[8,2,2,32,128]{4,3,2,1,0:T(8,128)S(1)}) custom-call(f32[2,128,128]{2,1,0:T(8,128)S(1)} %get-tuple-element.65.within, f32[32,2,128,128]{3,2,1,0:T(8,128)S(1)} %get-tuple-element.66.damps, bf16[32,128,32]{2,1,0:T(8,128)(2,1)S(1)} %get-tuple-element.102.driven, ...), custom_call_target="tpu_custom_call" | custom-call | flops 1000000000 | bytes 4194304 | tf_op jit(solution)/shard_map/local_1/pallas_call | solution.py:383
  23.2 0.0 collective-permute-done.3.three
  23.2 0.0 collective-permute-done.2.two
  23.2 0.0 collective-permute-done.1.one
  23.2 0.1 group_y.1
  23.4 2.6 %collective-permute-start.6 = (f32[72,128]{1,0:T(8,128)S(1)}, f32[72,128]{1,0:T(8,128)S(1)}, u32[]{:S(2)}, u32[]{:S(2)}) collective-permute-start(f32[72,128]{1,0:T(8,128)S(1)} %get-tuple-element.82.own), channel_id=1, source_target_pairs={{0,24},{24,0},{8,16},{16,8},{1,25},{25,1},{9,17},{17,9},{2,26},{26... | collective-permute-start | bytes 110600 | tf_op jit(solution)/shard_map/ppermute | solution.py:459
  25.9 0.5 collective-permute-start.5
  26.4 0.3 collective-permute-start.4
  26.7 5.3 %local_3.1 = (f32[8,128,32]{2,1,0:T(8,128)S(1)}, bf16[8,2,128,256]{3,2,1,0:T(8,128)(2,1)S(1)}, f32[8,2,2,32,128]{4,3,2,1,0:T(8,128)S(1)}) custom-call(f32[2,128,128]{2,1,0:T(8,128)S(1)} %get-tuple-element.65.within, f32[32,2,128,128]{3,2,1,0:T(8,128)S(1)} %get-tuple-element.66.damps, bf16[32,128,32]{2,1,0:T(8,128)(2,1)S(1)} %get-tuple-element.102.driven, ...), custom_call_target="tpu_custom_call" | custom-call | flops 1000000000 | bytes 4194304 | tf_op jit(solution)/shard_map/local_3/pallas_call | solution.py:383
  32.0 0.0 collective-permute-done.6.three
  32.0 0.0 collective-permute-done.5.two
  32.0 0.0 collective-permute-done.4.one
  32.0 0.1 group_x.1
  32.1 3.8 %collective-permute-start.9 = (f32[72,128]{1,0:T(8,128)S(1)}, f32[72,128]{1,0:T(8,128)S(1)}, u32[]{:S(2)}, u32[]{:S(2)}) collective-permute-start(f32[72,128]{1,0:T(8,128)S(1)} %get-tuple-element.90.across), channel_id=1, source_target_pairs={{0,96},{96,0},{32,64},{64,32},{1,97},{97,1},{33,65},{65,33},{2,98}... | collective-permute-start | bytes 110600 | tf_op jit(solution)/shard_map/ppermute | solution.py:465
  36.0 0.0 collective-permute-start.8
  36.0 0.7 %collective-permute-start.7 = (f32[72,128]{1,0:T(8,128)S(1)}, f32[72,128]{1,0:T(8,128)S(1)}, u32[]{:S(2)}, u32[]{:S(2)}) collective-permute-start(f32[72,128]{1,0:T(8,128)S(1)} %get-tuple-element.90.across), channel_id=1, source_target_pairs={{0,32},{32,0},{64,96},{96,64},{1,33},{33,1},{65,97},{97,65},{2,34}... | collective-permute-start | bytes 110600 | tf_op jit(solution)/shard_map/ppermute | solution.py:465
  36.6 5.3 %local_5.1 = (f32[8,128,32]{2,1,0:T(8,128)S(1)}, bf16[8,2,128,256]{3,2,1,0:T(8,128)(2,1)S(1)}, f32[8,2,2,32,128]{4,3,2,1,0:T(8,128)S(1)}) custom-call(f32[2,128,128]{2,1,0:T(8,128)S(1)} %get-tuple-element.65.within, f32[32,2,128,128]{3,2,1,0:T(8,128)S(1)} %get-tuple-element.66.damps, bf16[32,128,32]{2,1,0:T(8,128)(2,1)S(1)} %get-tuple-element.102.driven, ...), custom_call_target="tpu_custom_call" | custom-call | flops 1000000000 | bytes 4194304 | tf_op jit(solution)/shard_map/local_5/pallas_call | solution.py:383
  41.9 0.0 collective-permute-done.9.three
  41.9 0.0 collective-permute-done.8.two
  42.0 0.0 collective-permute-done.7.one
  42.0 0.1 enter.1
  42.1 0.0 copy-start.1
  42.1 0.0 copy-start.2
  42.1 0.0 copy-start.3
  42.1 0.0 copy-start.4
  42.2 0.0 copy-start.5
  42.2 2.2 %collective-permute-start.10 = (f32[4,16,128]{2,1,0:T(8,128)S(1)}, f32[4,16,128]{2,1,0:T(8,128)S(1)}, u32[]{:S(2)}, u32[]{:S(2)}) collective-permute-start(f32[4,16,128]{2,1,0:T(8,128)S(1)} %get-tuple-element.101), channel_id=1, source_target_pairs={{0,1},{1,0},{2,3},{3,2},{4,5},{5,4},{6,7},{7,6},{8,9},{9,8},{10,11... | collective-permute-start | bytes 98312 | tf_op jit(solution)/shard_map/ppermute | solution.py:470
  44.4 2.6 %local_7.1 = (f32[4,128,32]{2,1,0:T(8,128)S(1)}, bf16[4,2,128,256]{3,2,1,0:T(8,128)(2,1)S(1)}, f32[4,2,2,32,128]{4,3,2,1,0:T(8,128)S(1)}) custom-call(f32[2,128,128]{2,1,0:T(8,128)S(1)} %get-tuple-element.65.within, f32[32,2,128,128]{3,2,1,0:T(8,128)S(1)} %get-tuple-element.66.damps, bf16[32,128,32]{2,1,0:T(8,128)(2,1)S(1)} %get-tuple-element.102.driven, ...), custom_call_target="tpu_custom_call" | custom-call | flops 500000000 | bytes 2097152 | tf_op jit(solution)/shard_map/local_7/pallas_call | solution.py:383
  47.0 0.0 collective-permute-done.10.refs_1_
  47.0 0.0 copy-done.1
  47.0 0.0 copy-done.2
  47.0 0.0 copy-done.3
  47.1 0.0 copy-done.4
  47.1 0.0 copy-done.5
  47.1 4.8 %final.1 = bf16[128,2048]{1,0:T(8,128)(2,1)} custom-call(f32[4,16,128]{2,1,0:T(8,128)S(1)} %get-tuple-element.100.refs_0_, f32[4,16,128]{2,1,0:T(8,128)S(1)} %collective-permute-done.10.refs_1_, f32[4,128,32]{2,1,0:T(8,128)S(1)} %get-tuple-element.107.refs_2_, f32[8,128,32]{2,1,0:T(8,128)S(1)} %get-tuple-element.108.refs_3_, ...), custom_call_target="tpu_custom_call" | custom-call | tf_op jit(solution)/shard_map/final/pallas_call | solution.py:477
  (2 shorter events, 0.1 us)
Async XLA Ops:
  0.0 11.6 %copy-start = (f32[2,2,64,16,64]{4,3,2,1,0:T(8,128)S(1)}, f32[2,2,64,16,64]{4,3,2,1,0:T(8,128)}, u32[]{:S(2)}) copy-start(f32[2,2,64,16,64]{4,3,2,1,0:T(8,128)} %readout.9) | copy-start | bytes 3145732
  10.1 4.1 %collective-permute-start = (f32[72,128]{1,0:T(8,128)S(1)}, f32[72,128]{1,0:T(8,128)S(1)}, u32[]{:S(2)}, u32[]{:S(2)}) collective-permute-start(f32[72,128]{1,0:T(8,128)S(1)} %get-tuple-element.123), channel_id=1, source_target_pairs={{0,1},{1,0},{2,3},{3,2},{4,5},{5,4},{6,7},{7,6},{8,9},{9,8},{10,11... | collective-permute-start | bytes 110600 | tf_op jit(solution)/shard_map/ppermute | solution.py:455
  14.3 8.9 %collective-permute-start.3 = (f32[72,128]{1,0:T(8,128)S(1)}, f32[72,128]{1,0:T(8,128)S(1)}, u32[]{:S(2)}, u32[]{:S(2)}) collective-permute-start(f32[72,128]{1,0:T(8,128)S(1)} %pair.1.own), channel_id=1, source_target_pairs={{0,6},{6,0},{2,4},{4,2},{1,7},{7,1},{3,5},{5,3},{8,14},{14,8},{10,... | collective-permute-start | bytes 110600 | tf_op jit(solution)/shard_map/ppermute | solution.py:459
  17.2 6.0 %collective-permute-start.2 = (f32[72,128]{1,0:T(8,128)S(1)}, f32[72,128]{1,0:T(8,128)S(1)}, u32[]{:S(2)}, u32[]{:S(2)}) collective-permute-start(f32[72,128]{1,0:T(8,128)S(1)} %pair.1.own), channel_id=1, source_target_pairs={{0,4},{4,0},{2,6},{6,2},{1,5},{5,1},{3,7},{7,3},{8,12},{12,8},{10,... | collective-permute-start | bytes 110600 | tf_op jit(solution)/shard_map/ppermute | solution.py:459
  17.6 5.6 %collective-permute-start.1 = (f32[72,128]{1,0:T(8,128)S(1)}, f32[72,128]{1,0:T(8,128)S(1)}, u32[]{:S(2)}, u32[]{:S(2)}) collective-permute-start(f32[72,128]{1,0:T(8,128)S(1)} %pair.1.own), channel_id=1, source_target_pairs={{0,2},{2,0},{4,6},{6,4},{1,3},{3,1},{5,7},{7,5},{8,10},{10,8},{12,... | collective-permute-start | bytes 110600 | tf_op jit(solution)/shard_map/ppermute | solution.py:459
  23.4 8.6 %collective-permute-start.6 = (f32[72,128]{1,0:T(8,128)S(1)}, f32[72,128]{1,0:T(8,128)S(1)}, u32[]{:S(2)}, u32[]{:S(2)}) collective-permute-start(f32[72,128]{1,0:T(8,128)S(1)} %get-tuple-element.82.own), channel_id=1, source_target_pairs={{0,24},{24,0},{8,16},{16,8},{1,25},{25,1},{9,17},{17,9},{2,26},{26... | collective-permute-start | bytes 110600 | tf_op jit(solution)/shard_map/ppermute | solution.py:459
  25.9 6.1 %collective-permute-start.5 = (f32[72,128]{1,0:T(8,128)S(1)}, f32[72,128]{1,0:T(8,128)S(1)}, u32[]{:S(2)}, u32[]{:S(2)}) collective-permute-start(f32[72,128]{1,0:T(8,128)S(1)} %get-tuple-element.82.own), channel_id=1, source_target_pairs={{0,16},{16,0},{8,24},{24,8},{1,17},{17,1},{9,25},{25,9},{2,18},{18... | collective-permute-start | bytes 110600 | tf_op jit(solution)/shard_map/ppermute | solution.py:459
  26.4 5.6 %collective-permute-start.4 = (f32[72,128]{1,0:T(8,128)S(1)}, f32[72,128]{1,0:T(8,128)S(1)}, u32[]{:S(2)}, u32[]{:S(2)}) collective-permute-start(f32[72,128]{1,0:T(8,128)S(1)} %get-tuple-element.82.own), channel_id=1, source_target_pairs={{0,8},{8,0},{16,24},{24,16},{1,9},{9,1},{17,25},{25,17},{2,10},{10... | collective-permute-start | bytes 110600 | tf_op jit(solution)/shard_map/ppermute | solution.py:459
  32.1 9.8 %collective-permute-start.9 = (f32[72,128]{1,0:T(8,128)S(1)}, f32[72,128]{1,0:T(8,128)S(1)}, u32[]{:S(2)}, u32[]{:S(2)}) collective-permute-start(f32[72,128]{1,0:T(8,128)S(1)} %get-tuple-element.90.across), channel_id=1, source_target_pairs={{0,96},{96,0},{32,64},{64,32},{1,97},{97,1},{33,65},{65,33},{2,98}... | collective-permute-start | bytes 110600 | tf_op jit(solution)/shard_map/ppermute | solution.py:465
  36.0 6.0 %collective-permute-start.8 = (f32[72,128]{1,0:T(8,128)S(1)}, f32[72,128]{1,0:T(8,128)S(1)}, u32[]{:S(2)}, u32[]{:S(2)}) collective-permute-start(f32[72,128]{1,0:T(8,128)S(1)} %get-tuple-element.90.across), channel_id=1, source_target_pairs={{0,64},{64,0},{32,96},{96,32},{1,65},{65,1},{33,97},{97,33},{2,66}... | collective-permute-start | bytes 110600 | tf_op jit(solution)/shard_map/ppermute | solution.py:465
  36.0 6.0 %collective-permute-start.7 = (f32[72,128]{1,0:T(8,128)S(1)}, f32[72,128]{1,0:T(8,128)S(1)}, u32[]{:S(2)}, u32[]{:S(2)}) collective-permute-start(f32[72,128]{1,0:T(8,128)S(1)} %get-tuple-element.90.across), channel_id=1, source_target_pairs={{0,32},{32,0},{64,96},{96,64},{1,33},{33,1},{65,97},{97,65},{2,34}... | collective-permute-start | bytes 110600 | tf_op jit(solution)/shard_map/ppermute | solution.py:465
  42.1 4.9 %copy-start.1 = (bf16[1024,2048]{1,0:T(8,128)(2,1)S(1)}, bf16[1024,2048]{1,0:T(8,128)(2,1)}, u32[]{:S(2)}) copy-start(bf16[1024,2048]{1,0:T(8,128)(2,1)} %refs_21_.1) | copy-start | bytes 12582916
  42.1 4.9 %copy-start.2 = (bf16[1024,1024]{1,0:T(8,128)(2,1)S(1)}, bf16[1024,1024]{1,0:T(8,128)(2,1)}, u32[]{:S(2)}) copy-start(bf16[1024,1024]{1,0:T(8,128)(2,1)} %refs_19_.1) | copy-start | bytes 6291460
  42.1 4.9 %copy-start.3 = (f32[2048]{0:T(1024)S(1)}, f32[2048]{0:T(1024)}, u32[]{:S(2)}) copy-start(f32[2048]{0:T(1024)} %param.25) | copy-start | bytes 24580
  42.1 4.9 %copy-start.4 = (f32[1024]{0:T(1024)S(1)}, f32[1024]{0:T(1024)}, u32[]{:S(2)}) copy-start(f32[1024]{0:T(1024)} %param.21) | copy-start | bytes 12292
  42.2 4.9 %copy-start.5 = (f32[1024]{0:T(1024)S(1)}, f32[1024]{0:T(1024)}, u32[]{:S(2)}) copy-start(f32[1024]{0:T(1024)} %param.23) | copy-start | bytes 12292
  42.2 4.9 %collective-permute-start.10 = (f32[4,16,128]{2,1,0:T(8,128)S(1)}, f32[4,16,128]{2,1,0:T(8,128)S(1)}, u32[]{:S(2)}, u32[]{:S(2)}) collective-permute-start(f32[4,16,128]{2,1,0:T(8,128)S(1)} %get-tuple-element.101), channel_id=1, source_target_pairs={{0,1},{1,0},{2,3},{3,2},{4,5},{5,4},{6,7},{7,6},{8,9},{9,8},{10,11... | collective-permute-start | bytes 98312 | tf_op jit(solution)/shard_map/ppermute | solution.py:470

commit v8 on v7

--- a/solution.py
+++ b/solution.py
@@ -12,9 +12,12 @@
 ROWS = 128
 D = 2048
 CHANNELS = 1024
-TILES = 8
+CHUNKS = 4
+LAG = 10
+DRIVE_AT = (6, 16, 32, 48)
 SPAN = 16
 SPANS = ROWS // SPAN
+SLOTS = 6
 PIECES = (1, 2, 2, 2, 1)
 LOG2E = 1.0 / math.log(2.0)
 TINY = 1e-37
@@ -81,19 +84,19 @@
 
 def end_kernel(
     tokens, elapsed, gain, weight, inputs, angle, rate,
-    driven_ref, pairs_ref, ends_ref, pars_ref, damp_ref, within_ref, inputs_ref, normed, times, chunks, weight_sems, input_sems,
+    driven_ref, pairs_ref, ends_ref, pars_ref, damp_ref, within_ref, inputs_ref, normed, times, chunks, flipped, pulls, weight_sems, input_sems,
 ):
     core = lax.axis_index("c")
 
     def fetch(i):
         return (
             pltpu.make_async_copy(
-                weight.at[:, pl.ds(pl.multiple_of(128 * i, 128), 128)], chunks.at[i], weight_sems.at[i]
+                weight.at[:, pl.ds(256 * i, 256)], chunks.at[i], weight_sems.at[i]
             ),
-            pltpu.make_async_copy(inputs.at[:, :, pl.ds(8 * i, 8)], inputs_ref.at[:, :, pl.ds(8 * i, 8)], input_sems.at[i]),
+            pltpu.make_async_copy(inputs.at[:, :, pl.ds(16 * i, 16)], inputs_ref.at[:, :, pl.ds(16 * i, 16)], input_sems.at[i]),
         )
 
-    for i in range(TILES):
+    for i in range(CHUNKS):
         for copy in fetch(i):
             copy.start()
     steps = column_of(elapsed[...])
@@ -113,46 +116,62 @@
     normed[...] = (x * scale * gain[...]).astype(BF16)
     first = lax.broadcasted_iota(jnp.int32, (16, 128), 1) < 64
 
-    def tile(step, _):
+    def drive(step):
         for copy in fetch(step):
             copy.wait()
         driven = mm(normed[...], chunks[step]).astype(BF16)
-        driven_ref[:, pl.ds(pl.multiple_of(128 * step, 128), 128)] = driven
-        flipped = driven.astype(F32).T.astype(BF16)
-        away = jnp.where((step // 4) == core, 0, 1)
-        for j in range(4):
-            pair = step * 4 + j
-            pairs_ref[pair] = driven[:, 32 * j : 32 * j + 32]
-            for k in range(2):
-                f = pair_row(rate, k, pair)
-                th = pair_row(angle, k, pair)
-                pars_ref[k, 0, pl.ds(pair, 1), :] = th
-                pars_ref[k, 1, pl.ds(pair, 1), :] = f
-                after = times[k]
-                s, c = half_turn(after * (th * (0.5 / math.pi)))
-                bend = jnp.tanh(times[2] * f)
-                damp = bend * lax.rsqrt(bend * (0.5 + 0.5 * bend) + TINY)
-                damp_ref[pair, k] = damp
-                amp = jnp.exp2(after * (f * -LOG2E)) * damp
-                tilted = amp * s
-                pull = jnp.concatenate([(amp - tilted * s).astype(BF16), (tilted * c).astype(BF16)], axis=1)
-                mixed = mm(flipped[32 * j : 32 * j + 32], pull)
-                m_re = jnp.where(first, mixed[:16, :128], mixed[16:, :128])
-                m_im = jnp.where(first, mixed[:16, 128:], mixed[16:, 128:])
-                b_re, b_im = (
-                    jnp.concatenate([inputs_ref[k, c, 2 * pair].astype(F32), inputs_ref[k, c, 2 * pair + 1].astype(F32)], axis=1)
-                    for c in range(2)
-                )
-                at = 32 * k + 4 * (step % 4) + j
-                ends_ref[away, pl.ds(at, 1), :] = jnp.sum(b_re * m_re - b_im * m_im, axis=0, keepdims=True)
-                ends_ref[away, pl.ds(at + 16, 1), :] = jnp.sum(b_re * m_im + b_im * m_re, axis=0, keepdims=True)
-        return 0
-
-    lax.fori_loop(0, TILES, tile, 0)
+        driven_ref[:, 256 * step : 256 * step + 256] = driven
+        for j in range(8):
+            pairs_ref[8 * step + j] = driven[:, 32 * j : 32 * j + 32]
+        flipped[step % 2] = driven.astype(F32).T.astype(BF16)
+
+    def pull(pair, k):
+        f = pair_row(rate, k, pair)
+        th = pair_row(angle, k, pair)
+        pars_ref[k, 0, pair : pair + 1, :] = th
+        pars_ref[k, 1, pair : pair + 1, :] = f
+        after = times[k]
+        s, c = half_turn(after * (th * (0.5 / math.pi)))
+        bend = jnp.tanh(times[2] * f)
+        damp = bend * lax.rsqrt(bend * (0.5 + 0.5 * bend) + TINY)
+        damp_ref[pair, k] = damp
+        amp = jnp.exp2(after * (f * -LOG2E)) * damp
+        tilted = amp * s
+        pulls[pair % 8, k, :, :128] = (amp - tilted * s).astype(BF16)
+        pulls[pair % 8, k, :, 128:] = (tilted * c).astype(BF16)
+
+    def finish(pair, k):
+        mixed = mm(flipped[pair // 8 % 2, 32 * (pair % 8) : 32 * (pair % 8) + 32], pulls[pair % 8, k])
+        m_re = jnp.where(first, mixed[:16, :128], mixed[16:, :128])
+        m_im = jnp.where(first, mixed[:16, 128:], mixed[16:, 128:])
+        b_re, b_im = (
+            jnp.concatenate([inputs_ref[k, c, 2 * pair].astype(F32), inputs_ref[k, c, 2 * pair + 1].astype(F32)], axis=1)
+            for c in range(2)
+        )
+        away = jnp.where(pair // 16 == core, 0, 1)
+        at = 32 * k + pair % 16
+        ends_ref[away, at : at + 1, :] = jnp.sum(b_re * m_re - b_im * m_im, axis=0, keepdims=True)
+        ends_ref[away, at + 16 : at + 17, :] = jnp.sum(b_re * m_im + b_im * m_re, axis=0, keepdims=True)
+
+    units = [(pair, k) for pair in range(32) for k in range(2)]
+    for n in range(len(units) + LAG):
+        if n in DRIVE_AT:
+            drive(DRIVE_AT.index(n))
+        if n < len(units):
+            pull(*units[n])
+        if n >= LAG:
+            finish(*units[n - LAG])
+
+
+def shifted_rows(x, by, fill):
+    row = lax.broadcasted_iota(jnp.int32, (SPANS, 128), 0)
+    moved = pltpu.roll(x, by % SPANS, 0)
+    return jnp.where(row >= by if by > 0 else row < SPANS + by, moved, fill)
 
 
 def local_kernel(
-    start, size, within, damps, driven, inputs, readout, pars, out_ref, prefix_ref, table_ref, triangles,
+    start, size, within, damps, driven, inputs, readout, pars, out_ref, prefix_ref, table_ref,
+    triangles, proj, turn, lifts, part, states, carry,
 ):
     row, col = iotas((ROWS, ROWS))
     same = row // SPAN == col // SPAN
@@ -161,62 +180,82 @@
     empty = jnp.zeros((16, 64), BF16)
     hole = jnp.zeros((16, 64), F32)
 
-    def both(j, _):
+    def project(j, k, slot):
         pair = start + j
-        lhs = driven[pair]
-        total = None
+        b00, b01 = inputs[k, 0, 2 * pair], inputs[k, 1, 2 * pair]
+        b10, b11 = inputs[k, 0, 2 * pair + 1], inputs[k, 1, 2 * pair + 1]
+        rhs = jnp.concatenate(
+            [
+                jnp.concatenate([b00, empty, b01, empty], axis=1),
+                jnp.concatenate([empty, b10, empty, b11], axis=1),
+            ],
+            axis=0,
+        )
+        proj[slot] = mm(driven[pair], rhs)
+
+    def lift(j, k, slot):
+        pair = start + j
+        th, f = pars[k, 0, pair : pair + 1, :], pars[k, 1, pair : pair + 1, :]
+        offs = within[k]
+        cosine, sine = unit_circle(offs * (th * (0.5 / math.pi)))
+        grow = jnp.exp2(offs * (f * LOG2E)) * damps[pair, k]
+        fade = jnp.exp2(offs * (f * -LOG2E))
+        turn[slot, 0], turn[slot, 1] = fade * cosine, fade * sine
+        a_re, a_im = grow * cosine, grow * sine
+        p_re, p_im = proj[slot, :, :128], proj[slot, :, 128:]
+        lifts[slot, :, :128] = (a_re * p_re + a_im * p_im).astype(BF16)
+        lifts[slot, :, 128:] = (a_re * p_im - a_im * p_re).astype(BF16)
+
+    def add_up(j, k, slot):
+        total = mm(triangles[k], lifts[slot])
+        part[slot, 0], part[slot, 1] = total[:, :128], total[:, 128:]
+
+    def carry_on(j, k, slot):
+        edge = pl.ds(SPAN - 1 if k == 0 else 0, SPANS, stride=SPAN)
+        d = turn[slot, 0, edge, :], turn[slot, 1, edge, :]
+        s = times_of(d, (part[slot, 0, edge, :], part[slot, 1, edge, :]))
+        sign = 1 if k == 0 else -1
+        for by in (1, 2, 4):
+            s_old = tuple(shifted_rows(x, sign * by, 0.0) for x in s)
+            d_old = shifted_rows(d[0], sign * by, 1.0), shifted_rows(d[1], sign * by, 0.0)
+            s = plus(times_of(d, s_old), s)
+            d = times_of(d, d_old)
+        carry[slot, 0], carry[slot, 1] = (shifted_rows(x, sign, 0.0) for x in s)
+        carry[slot, 2], carry[slot, 3] = shifted_rows(d[0], sign, 1.0), shifted_rows(d[1], sign, 0.0)
+
+    def spread(j, k, slot):
+        for n in range(SPANS):
+            cut = slice(SPAN * n, SPAN * n + SPAN)
+            e = turn[slot, 0, cut, :], turn[slot, 1, cut, :]
+            c_re, c_im, d_re, d_im = (jnp.broadcast_to(carry[slot, i, n : n + 1, :], (SPAN, 128)) for i in range(4))
+            state = times_of(e, (part[slot, 0, cut, :] + c_re, part[slot, 1, cut, :] + c_im))
+            states[j % 2, cut, 256 * k : 256 * k + 128] = state[0].astype(BF16)
+            states[j % 2, cut, 256 * k + 128 : 256 * k + 256] = state[1].astype(BF16)
+            prefix = times_of(e, (d_re, d_im))
+            prefix_ref[j, k, cut, :128] = prefix[0].astype(BF16)
+            prefix_ref[j, k, cut, 128:] = prefix[1].astype(BF16)
+
+    def read(j):
+        pair = start + j
+        tables = []
         for k in range(2):
-            th, f = pars[k, 0, pl.ds(pair, 1), :], pars[k, 1, pl.ds(pair, 1), :]
-            b00, b01 = inputs[k, 0, 2 * pair], inputs[k, 1, 2 * pair]
-            b10, b11 = inputs[k, 0, 2 * pair + 1], inputs[k, 1, 2 * pair + 1]
-            rhs = jnp.concatenate(
-                [
-                    jnp.concatenate([b00, empty, b01, empty], axis=1),
-                    jnp.concatenate([empty, b10, empty, b11], axis=1),
-                ],
-                axis=0,
-            )
-            proj = mm(lhs, rhs)
-            p_re, p_im = proj[:, :128], proj[:, 128:]
-            offs = within[k]
-            cosine, sine = unit_circle(offs * (th * (0.5 / math.pi)))
-            grow = jnp.exp2(offs * (f * LOG2E)) * damps[pair, k]
-            fade = jnp.exp2(offs * (f * -LOG2E))
-            a_re, a_im = grow * cosine, grow * sine
-            lift = jnp.concatenate(
-                [(a_re * p_re + a_im * p_im).astype(BF16), (a_re * p_im - a_im * p_re).astype(BF16)], axis=1
-            )
-            part = mm(triangles[k], lift)
-            e_re, e_im = fade * cosine, fade * sine
-            c_re = c_im = jnp.zeros((1, 128), F32)
-            d_re, d_im = jnp.ones((1, 128), F32), jnp.zeros((1, 128), F32)
-            states = [None] * SPANS
-            for n in range(SPANS) if k == 0 else range(SPANS - 1, -1, -1):
-                cut = slice(SPAN * n, SPAN * n + SPAN)
-                er, ei = e_re[cut], e_im[cut]
-                wr, wi = part[cut, :128] + c_re, part[cut, 128:] + c_im
-                sr, si = er * wr - ei * wi, er * wi + ei * wr
-                pr, pi = er * d_re - ei * d_im, er * d_im + ei * d_re
-                edge = slice(SPAN - 1, SPAN) if k == 0 else slice(0, 1)
-                c_re, c_im, d_re, d_im = sr[edge], si[edge], pr[edge], pi[edge]
-                states[n] = jnp.concatenate([sr.astype(BF16), si.astype(BF16)], axis=1)
-                prefix_ref[j, k, cut, :] = jnp.concatenate([pr.astype(BF16), pi.astype(BF16)], axis=1)
-            tables = []
             for c in range(2):
                 upper = jnp.concatenate([readout[k, c, 2 * pair], hole], axis=1)
                 lower = jnp.concatenate([hole, readout[k, c, 2 * pair + 1]], axis=1)
                 table = jnp.concatenate([upper, lower], axis=0)
                 table_ref[j, k, c] = table
-                tables.append(table)
-            y = nt(
-                jnp.concatenate(states, axis=0),
-                jnp.concatenate([tables[0].astype(BF16), (-tables[1]).astype(BF16)], axis=1),
-            )
-            total = y if total is None else total + y
-        out_ref[j] = total
-        return 0
-
-    lax.fori_loop(0, size, both, 0)
+                tables.append((table if c == 0 else -table).astype(BF16))
+        out_ref[j] = nt(states[j % 2], jnp.concatenate(tables, axis=1))
+
+    units = [(j, k) for j in range(size) for k in range(2)]
+    for turn_of in range(len(units) + 6):
+        for late, act in ((0, project), (1, lift), (2, add_up), (3, carry_on), (4, spread)):
+            at = turn_of - late
+            if 0 <= at < len(units):
+                act(*units[at], at % SLOTS)
+        at = turn_of - 5
+        if 0 <= at < len(units) and units[at][1] == 1:
+            read(units[at][0])
 
 
 def times_of(a, b):
@@ -340,7 +379,7 @@
     start = 0
     for size, near, prefix, table in zip(PIECES, nears, prefixes, tables):
 
-        def tile(i, _, start=start, near=near, prefix=prefix, table=table):
+        def tile(i, start=start, near=near, prefix=prefix, table=table):
             outs = []
             for j in range(4):
                 total = None
@@ -355,11 +394,11 @@
                     y = nt(prefix[4 * i + j, k], rhs)
                     total = y if total is None else total + y
                 outs.append(total + near[4 * i + j])
-            at = pl.multiple_of(128 * i, 128)
+            at = 128 * i
             response[:, pl.ds(at + 128 * start, 128)] = jnp.concatenate(outs, axis=1)
-            return 0
-
-        lax.fori_loop(0, size, tile, 0)
+
+        for i in range(size):
+            tile(i)
         start += size
     x = response[...] + skip[...] * driven[...].astype(F32)
     active = 0.5 * x * (1.0 + jnp.tanh(math.sqrt(2.0 / math.pi) * (x + 0.044715 * (x * x * x))))
@@ -390,8 +429,12 @@
             sds((4 * size, 2, ROWS, 256), BF16),
             sds((4 * size, 2, 2, 32, 128)),
         ],
-        scratch_shapes=[VMEM((2, ROWS, ROWS), BF16)],
-        compiler_params=params(6),
+        scratch_shapes=[
+            VMEM((2, ROWS, ROWS), BF16), VMEM((SLOTS, ROWS, 256), F32), VMEM((SLOTS, 2, ROWS, 128), F32),
+            VMEM((SLOTS, ROWS, 256), BF16), VMEM((SLOTS, 2, ROWS, 128), F32), VMEM((2, ROWS, 512), BF16),
+            VMEM((SLOTS, 4, SPANS, 128), F32),
+        ],
+        compiler_params=params(8),
         cost_estimate=pl.CostEstimate(flops=size * 5 * 10**8, bytes_accessed=size * 2 * 2**20, transcendentals=0),
     )(*args)
 
@@ -426,8 +469,9 @@
             sds((32, 2, ROWS, ROWS)), sds((2, ROWS, ROWS)), sds((2, 2, 64, 16, 64), BF16),
         ],
         scratch_shapes=[
-            VMEM((ROWS, D), BF16), VMEM((3, ROWS, ROWS), F32), VMEM((TILES, D, 128), BF16),
-            pltpu.SemaphoreType.DMA((TILES,)), pltpu.SemaphoreType.DMA((TILES,)),
+            VMEM((ROWS, D), BF16), VMEM((3, ROWS, ROWS), F32), VMEM((CHUNKS, D, 256), BF16), VMEM((2, 256, ROWS), BF16),
+            VMEM((8, 2, ROWS, 256), BF16),
+            pltpu.SemaphoreType.DMA((CHUNKS,)), pltpu.SemaphoreType.DMA((CHUNKS,)),
         ],
         compiler_params=params(12),
     )(

time: 52 us -> 45.2 us (0.87)
  Pallas kernels: 36.5 us -> 24.8 us
  starting transfers between devices: 15.1 us -> 17.6 us
  waiting for transfers between devices: 0.03 us -> 2.43 us
    pallas_call x5, Pallas kernels: 21.1 us -> 11.3 us  [run_local(): pl.pallas_call(functools.partial(local_kernel, 4 * start, 4 * size), name...]
    ppermute x1, starting transfers between devices: 2.2 us -> 4.69 us  [local(): other = piece_between(theirs, lax.ppermute(theirs, 'c', swap))]
    ppermute x6, waiting for transfers between devices: 0.02 us -> 1.57 us  [local(): lax.ppermute(total, axis, pairs)]
    pallas_call x1, Pallas kernels: 4.79 us -> 3.27 us  [local(): pl.pallas_call(final_kernel, name='final', in_specs=[spec] * len(args), o...]
    ppermute x3, waiting for transfers between devices: 0.01 us -> 0.85 us  [local(): lax.ppermute(total, 'z', pairs)]
  transfers between devices with their start and end apart: 11 -> 11, of which waited for: 0 -> 3; matrix products, arithmetic and copies ran while one was open for 0% -> 0% of each run, Pallas kernels for 41% -> 25%
where the time goes in v8:
time: 45.2 us; the launch traced here: 45.1 us
  Pallas kernels  24.8 us (55%)
  starting transfers between devices  17.6 us (39%)
  waiting for transfers between devices  2.43 us (5%)
    pallas_call x5, Pallas kernels, run_local(): pl.pallas_call(functools.partial(local_kernel, 4 * start, 4 * size), name...  11.3 us
    pallas_call x1, Pallas kernels, local(): pl.pallas_call(end_kernel, name='ends', in_specs=[spec, spec, spec, dista...  9.75 us
    ppermute x6, starting transfers between devices, local(): lax.ppermute(total, axis, pairs)  6.93 us
    ppermute x1, starting transfers between devices, local(): other = piece_between(theirs, lax.ppermute(theirs, 'c', swap))  4.69 us
    ppermute x3, starting transfers between devices, local(): lax.ppermute(total, 'z', pairs)  4.51 us
    pallas_call x1, Pallas kernels, local(): pl.pallas_call(final_kernel, name='final', in_specs=[spec] * len(args), o...  3.27 us
    ppermute x6, waiting for transfers between devices, local(): lax.ppermute(total, axis, pairs)  1.57 us
    ppermute x1, starting transfers between devices, local(): partner = piece_between(keep, lax.ppermute(ends[1], 'c', swap))  1.46 us
  transfers between devices with their start and end apart: 11, of which 3 were waited for; matrix products, arithmetic and copies ran while one was open for 0% of the time, Pallas kernels for 25%

profile of v8, /device:TPU:1, one launch (start us, length us, event | category | flops | bytes accessed | tf_op | source)
XLA Modules:
  0.0 45.1 jit_solution(12047108115875453211)
XLA Ops:
  0.0 0.0 copy-start
  0.0 9.8 %ends.1 = (bf16[128,1024]{1,0:T(8,128)(2,1)S(1)}, bf16[32,128,32]{2,1,0:T(8,128)(2,1)S(1)}, f32[2,72,128]{2,1,0:T(8,128)S(1)}, f32[2,2,32,128]{3,2,1,0:T(8,128)S...) custom-call(bf16[128,2048]{1,0:T(8,128)(2,1)} %tokens.1, ...), custom_call_target="tpu_custom_call" | custom-call | tf_op jit(solution)/shard_map/ends/pallas_call | solution.py:462
  9.8 1.5 %collective-permute-start = (f32[72,128]{1,0:T(8,128)S(1)}, f32[72,128]{1,0:T(8,128)S(1)}, u32[]{:S(2)}, u32[]{:S(2)}) collective-permute-start(f32[72,128]{1,0:T(8,128)S(1)} %get-tuple-element.123), channel_id=1, source_target_pairs={{0,1},{1,0},{2,3},{3,2},{4,5},{5,4},{6,7},{7,6},{8,9},{9,8},{10,11... | collective-permute-start | bytes 110600 | tf_op jit(solution)/shard_map/ppermute | solution.py:499
  11.2 0.0 copy-done
  11.2 1.5 %local_0.1 = (f32[4,128,32]{2,1,0:T(8,128)S(1)}, bf16[4,2,128,256]{3,2,1,0:T(8,128)(2,1)S(1)}, f32[4,2,2,32,128]{4,3,2,1,0:T(8,128)S(1)}) custom-call(f32[2,128,128]{2,1,0:T(8,128)S(1)} %get-tuple-element.65.within, f32[32,2,128,128]{3,2,1,0:T(8,128)S(1)} %get-tuple-element.66.damps, bf16[32,128,32]{2,1,0:T(8,128)(2,1)S(1)} %get-tuple-element.102.driven, ...), custom_call_target="tpu_custom_call" | custom-call | flops 500000000 | bytes 2097152 | tf_op jit(solution)/shard_map/local_0/pallas_call | solution.py:422
  12.7 0.0 collective-permute-done.other
  12.8 2.9 %collective-permute-start.3 = (f32[72,128]{1,0:T(8,128)S(1)}, f32[72,128]{1,0:T(8,128)S(1)}, u32[]{:S(2)}, u32[]{:S(2)}) collective-permute-start(f32[72,128]{1,0:T(8,128)S(1)} %pair.1.own), channel_id=1, source_target_pairs={{0,6},{6,0},{2,4},{4,2},{1,7},{7,1},{3,5},{5,3},{8,14},{14,8},{10,... | collective-permute-start | bytes 110600 | tf_op jit(solution)/shard_map/ppermute | solution.py:503
  15.7 0.4 collective-permute-start.2
  16.1 0.3 collective-permute-start.1
  16.4 2.8 %local_1.1 = (f32[8,128,32]{2,1,0:T(8,128)S(1)}, bf16[8,2,128,256]{3,2,1,0:T(8,128)(2,1)S(1)}, f32[8,2,2,32,128]{4,3,2,1,0:T(8,128)S(1)}) custom-call(f32[2,128,128]{2,1,0:T(8,128)S(1)} %get-tuple-element.65.within, f32[32,2,128,128]{3,2,1,0:T(8,128)S(1)} %get-tuple-element.66.damps, bf16[32,128,32]{2,1,0:T(8,128)(2,1)S(1)} %get-tuple-element.102.driven, ...), custom_call_target="tpu_custom_call" | custom-call | flops 1000000000 | bytes 4194304 | tf_op jit(solution)/shard_map/local_1/pallas_call | solution.py:422
  19.2 0.0 collective-permute-done.3.three
  19.2 0.8 %collective-permute-done.2.two = f32[72,128]{1,0:T(8,128)S(1)} collective-permute-done((f32[72,128]{1,0:T(8,128)S(1)}, f32[72,128]{1,0:T(8,128)S(1)}, u32[]{:S(2)}, u32[]{:S(2)}) %collective-permute-start.2) | collective-permute-done | bytes 36896 | tf_op jit(solution)/shard_map/ppermute | solution.py:503
  20.0 0.0 collective-permute-done.1.one
  20.0 0.1 group_y.1
  20.2 2.6 %collective-permute-start.6 = (f32[72,128]{1,0:T(8,128)S(1)}, f32[72,128]{1,0:T(8,128)S(1)}, u32[]{:S(2)}, u32[]{:S(2)}) collective-permute-start(f32[72,128]{1,0:T(8,128)S(1)} %get-tuple-element.82.own), channel_id=1, source_target_pairs={{0,24},{24,0},{8,16},{16,8},{1,25},{25,1},{9,17},{17,9},{2,26},{26... | collective-permute-start | bytes 110600 | tf_op jit(solution)/shard_map/ppermute | solution.py:503
  22.7 0.5 %collective-permute-start.5 = (f32[72,128]{1,0:T(8,128)S(1)}, f32[72,128]{1,0:T(8,128)S(1)}, u32[]{:S(2)}, u32[]{:S(2)}) collective-permute-start(f32[72,128]{1,0:T(8,128)S(1)} %get-tuple-element.82.own), channel_id=1, source_target_pairs={{0,16},{16,0},{8,24},{24,8},{1,17},{17,1},{9,25},{25,9},{2,18},{18... | collective-permute-start | bytes 110600 | tf_op jit(solution)/shard_map/ppermute | solution.py:503
  23.2 0.3 collective-permute-start.4
  23.5 2.8 %local_3.1 = (f32[8,128,32]{2,1,0:T(8,128)S(1)}, bf16[8,2,128,256]{3,2,1,0:T(8,128)(2,1)S(1)}, f32[8,2,2,32,128]{4,3,2,1,0:T(8,128)S(1)}) custom-call(f32[2,128,128]{2,1,0:T(8,128)S(1)} %get-tuple-element.65.within, f32[32,2,128,128]{3,2,1,0:T(8,128)S(1)} %get-tuple-element.66.damps, bf16[32,128,32]{2,1,0:T(8,128)(2,1)S(1)} %get-tuple-element.102.driven, ...), custom_call_target="tpu_custom_call" | custom-call | flops 1000000000 | bytes 4194304 | tf_op jit(solution)/shard_map/local_3/pallas_call | solution.py:422
  26.3 0.0 collective-permute-done.6.three
  26.3 0.7 %collective-permute-done.5.two = f32[72,128]{1,0:T(8,128)S(1)} collective-permute-done((f32[72,128]{1,0:T(8,128)S(1)}, f32[72,128]{1,0:T(8,128)S(1)}, u32[]{:S(2)}, u32[]{:S(2)}) %collective-permute-start.5) | collective-permute-done | bytes 36896 | tf_op jit(solution)/shard_map/ppermute | solution.py:503
  27.0 0.0 collective-permute-done.4.one
  27.0 0.1 group_x.1
  27.2 3.8 %collective-permute-start.9 = (f32[72,128]{1,0:T(8,128)S(1)}, f32[72,128]{1,0:T(8,128)S(1)}, u32[]{:S(2)}, u32[]{:S(2)}) collective-permute-start(f32[72,128]{1,0:T(8,128)S(1)} %get-tuple-element.90.across), channel_id=1, source_target_pairs={{0,96},{96,0},{32,64},{64,32},{1,97},{97,1},{33,65},{65,33},{2,98}... | collective-permute-start | bytes 110600 | tf_op jit(solution)/shard_map/ppermute | solution.py:509
  31.0 0.0 collective-permute-start.8
  31.0 0.7 %collective-permute-start.7 = (f32[72,128]{1,0:T(8,128)S(1)}, f32[72,128]{1,0:T(8,128)S(1)}, u32[]{:S(2)}, u32[]{:S(2)}) collective-permute-start(f32[72,128]{1,0:T(8,128)S(1)} %get-tuple-element.90.across), channel_id=1, source_target_pairs={{0,32},{32,0},{64,96},{96,64},{1,33},{33,1},{65,97},{97,65},{2,34}... | collective-permute-start | bytes 110600 | tf_op jit(solution)/shard_map/ppermute | solution.py:509
  31.7 2.8 %local_5.1 = (f32[8,128,32]{2,1,0:T(8,128)S(1)}, bf16[8,2,128,256]{3,2,1,0:T(8,128)(2,1)S(1)}, f32[8,2,2,32,128]{4,3,2,1,0:T(8,128)S(1)}) custom-call(f32[2,128,128]{2,1,0:T(8,128)S(1)} %get-tuple-element.65.within, f32[32,2,128,128]{3,2,1,0:T(8,128)S(1)} %get-tuple-element.66.damps, bf16[32,128,32]{2,1,0:T(8,128)(2,1)S(1)} %get-tuple-element.102.driven, ...), custom_call_target="tpu_custom_call" | custom-call | flops 1000000000 | bytes 4194304 | tf_op jit(solution)/shard_map/local_5/pallas_call | solution.py:422
  34.5 0.0 collective-permute-done.9.three
  34.5 0.8 %collective-permute-done.8.two = f32[72,128]{1,0:T(8,128)S(1)} collective-permute-done((f32[72,128]{1,0:T(8,128)S(1)}, f32[72,128]{1,0:T(8,128)S(1)}, u32[]{:S(2)}, u32[]{:S(2)}) %collective-permute-start.8) | collective-permute-done | bytes 36896 | tf_op jit(solution)/shard_map/ppermute | solution.py:509
  35.4 0.0 collective-permute-done.7.one
  35.4 0.1 enter.1
  35.5 0.0 copy-start.1
  35.5 0.0 copy-start.2
  35.5 0.0 copy-start.3
  35.5 0.0 copy-start.4
  35.5 0.0 copy-start.5
  35.6 4.7 %collective-permute-start.10 = (f32[4,16,128]{2,1,0:T(8,128)S(1)}, f32[4,16,128]{2,1,0:T(8,128)S(1)}, u32[]{:S(2)}, u32[]{:S(2)}) collective-permute-start(f32[4,16,128]{2,1,0:T(8,128)S(1)} %get-tuple-element.101), channel_id=1, source_target_pairs={{0,1},{1,0},{2,3},{3,2},{4,5},{5,4},{6,7},{7,6},{8,9},{9,8},{10,11... | collective-permute-start | bytes 98312 | tf_op jit(solution)/shard_map/ppermute | solution.py:514
  40.2 1.5 %local_7.1 = (f32[4,128,32]{2,1,0:T(8,128)S(1)}, bf16[4,2,128,256]{3,2,1,0:T(8,128)(2,1)S(1)}, f32[4,2,2,32,128]{4,3,2,1,0:T(8,128)S(1)}) custom-call(f32[2,128,128]{2,1,0:T(8,128)S(1)} %get-tuple-element.65.within, f32[32,2,128,128]{3,2,1,0:T(8,128)S(1)} %get-tuple-element.66.damps, bf16[32,128,32]{2,1,0:T(8,128)(2,1)S(1)} %get-tuple-element.102.driven, ...), custom_call_target="tpu_custom_call" | custom-call | flops 500000000 | bytes 2097152 | tf_op jit(solution)/shard_map/local_7/pallas_call | solution.py:422
  41.7 0.0 collective-permute-done.10.refs_1_
  41.7 0.0 copy-done.1
  41.7 0.0 copy-done.2
  41.8 0.0 copy-done.3
  41.8 0.0 copy-done.4
  41.8 0.0 copy-done.5
  41.8 3.3 %final.1 = bf16[128,2048]{1,0:T(8,128)(2,1)} custom-call(f32[4,16,128]{2,1,0:T(8,128)S(1)} %get-tuple-element.100.refs_0_, f32[4,16,128]{2,1,0:T(8,128)S(1)} %collective-permute-done.10.refs_1_, f32[4,128,32]{2,1,0:T(8,128)S(1)} %get-tuple-element.107.refs_2_, f32[8,128,32]{2,1,0:T(8,128)S(1)} %get-tuple-element.108.refs_3_, ...), custom_call_target="tpu_custom_call" | custom-call | tf_op jit(solution)/shard_map/final/pallas_call | solution.py:521
  (2 shorter events, 0.1 us)
Async XLA Ops:
  0.0 11.2 %copy-start = (f32[2,2,64,16,64]{4,3,2,1,0:T(8,128)S(1)}, f32[2,2,64,16,64]{4,3,2,1,0:T(8,128)}, u32[]{:S(2)}) copy-start(f32[2,2,64,16,64]{4,3,2,1,0:T(8,128)} %readout.9) | copy-start | bytes 3145732
  9.8 3.0 %collective-permute-start = (f32[72,128]{1,0:T(8,128)S(1)}, f32[72,128]{1,0:T(8,128)S(1)}, u32[]{:S(2)}, u32[]{:S(2)}) collective-permute-start(f32[72,128]{1,0:T(8,128)S(1)} %get-tuple-element.123), channel_id=1, source_target_pairs={{0,1},{1,0},{2,3},{3,2},{4,5},{5,4},{6,7},{7,6},{8,9},{9,8},{10,11... | collective-permute-start | bytes 110600 | tf_op jit(solution)/shard_map/ppermute | solution.py:499
  12.8 6.4 %collective-permute-start.3 = (f32[72,128]{1,0:T(8,128)S(1)}, f32[72,128]{1,0:T(8,128)S(1)}, u32[]{:S(2)}, u32[]{:S(2)}) collective-permute-start(f32[72,128]{1,0:T(8,128)S(1)} %pair.1.own), channel_id=1, source_target_pairs={{0,6},{6,0},{2,4},{4,2},{1,7},{7,1},{3,5},{5,3},{8,14},{14,8},{10,... | collective-permute-start | bytes 110600 | tf_op jit(solution)/shard_map/ppermute | solution.py:503
  15.7 4.3 %collective-permute-start.2 = (f32[72,128]{1,0:T(8,128)S(1)}, f32[72,128]{1,0:T(8,128)S(1)}, u32[]{:S(2)}, u32[]{:S(2)}) collective-permute-start(f32[72,128]{1,0:T(8,128)S(1)} %pair.1.own), channel_id=1, source_target_pairs={{0,4},{4,0},{2,6},{6,2},{1,5},{5,1},{3,7},{7,3},{8,12},{12,8},{10,... | collective-permute-start | bytes 110600 | tf_op jit(solution)/shard_map/ppermute | solution.py:503
  16.1 4.0 %collective-permute-start.1 = (f32[72,128]{1,0:T(8,128)S(1)}, f32[72,128]{1,0:T(8,128)S(1)}, u32[]{:S(2)}, u32[]{:S(2)}) collective-permute-start(f32[72,128]{1,0:T(8,128)S(1)} %pair.1.own), channel_id=1, source_target_pairs={{0,2},{2,0},{4,6},{6,4},{1,3},{3,1},{5,7},{7,5},{8,10},{10,8},{12,... | collective-permute-start | bytes 110600 | tf_op jit(solution)/shard_map/ppermute | solution.py:503
  20.2 6.1 %collective-permute-start.6 = (f32[72,128]{1,0:T(8,128)S(1)}, f32[72,128]{1,0:T(8,128)S(1)}, u32[]{:S(2)}, u32[]{:S(2)}) collective-permute-start(f32[72,128]{1,0:T(8,128)S(1)} %get-tuple-element.82.own), channel_id=1, source_target_pairs={{0,24},{24,0},{8,16},{16,8},{1,25},{25,1},{9,17},{17,9},{2,26},{26... | collective-permute-start | bytes 110600 | tf_op jit(solution)/shard_map/ppermute | solution.py:503
  22.7 4.3 %collective-permute-start.5 = (f32[72,128]{1,0:T(8,128)S(1)}, f32[72,128]{1,0:T(8,128)S(1)}, u32[]{:S(2)}, u32[]{:S(2)}) collective-permute-start(f32[72,128]{1,0:T(8,128)S(1)} %get-tuple-element.82.own), channel_id=1, source_target_pairs={{0,16},{16,0},{8,24},{24,8},{1,17},{17,1},{9,25},{25,9},{2,18},{18... | collective-permute-start | bytes 110600 | tf_op jit(solution)/shard_map/ppermute | solution.py:503
  23.2 3.8 %collective-permute-start.4 = (f32[72,128]{1,0:T(8,128)S(1)}, f32[72,128]{1,0:T(8,128)S(1)}, u32[]{:S(2)}, u32[]{:S(2)}) collective-permute-start(f32[72,128]{1,0:T(8,128)S(1)} %get-tuple-element.82.own), channel_id=1, source_target_pairs={{0,8},{8,0},{16,24},{24,16},{1,9},{9,1},{17,25},{25,17},{2,10},{10... | collective-permute-start | bytes 110600 | tf_op jit(solution)/shard_map/ppermute | solution.py:503
  27.2 7.3 %collective-permute-start.9 = (f32[72,128]{1,0:T(8,128)S(1)}, f32[72,128]{1,0:T(8,128)S(1)}, u32[]{:S(2)}, u32[]{:S(2)}) collective-permute-start(f32[72,128]{1,0:T(8,128)S(1)} %get-tuple-element.90.across), channel_id=1, source_target_pairs={{0,96},{96,0},{32,64},{64,32},{1,97},{97,1},{33,65},{65,33},{2,98}... | collective-permute-start | bytes 110600 | tf_op jit(solution)/shard_map/ppermute | solution.py:509
  31.0 4.3 %collective-permute-start.8 = (f32[72,128]{1,0:T(8,128)S(1)}, f32[72,128]{1,0:T(8,128)S(1)}, u32[]{:S(2)}, u32[]{:S(2)}) collective-permute-start(f32[72,128]{1,0:T(8,128)S(1)} %get-tuple-element.90.across), channel_id=1, source_target_pairs={{0,64},{64,0},{32,96},{96,32},{1,65},{65,1},{33,97},{97,33},{2,66}... | collective-permute-start | bytes 110600 | tf_op jit(solution)/shard_map/ppermute | solution.py:509
  31.0 4.3 %collective-permute-start.7 = (f32[72,128]{1,0:T(8,128)S(1)}, f32[72,128]{1,0:T(8,128)S(1)}, u32[]{:S(2)}, u32[]{:S(2)}) collective-permute-start(f32[72,128]{1,0:T(8,128)S(1)} %get-tuple-element.90.across), channel_id=1, source_target_pairs={{0,32},{32,0},{64,96},{96,64},{1,33},{33,1},{65,97},{97,65},{2,34}... | collective-permute-start | bytes 110600 | tf_op jit(solution)/shard_map/ppermute | solution.py:509
  35.5 6.2 %copy-start.1 = (bf16[1024,2048]{1,0:T(8,128)(2,1)S(1)}, bf16[1024,2048]{1,0:T(8,128)(2,1)}, u32[]{:S(2)}) copy-start(bf16[1024,2048]{1,0:T(8,128)(2,1)} %refs_21_.1) | copy-start | bytes 12582916
  35.5 6.2 %copy-start.2 = (bf16[1024,1024]{1,0:T(8,128)(2,1)S(1)}, bf16[1024,1024]{1,0:T(8,128)(2,1)}, u32[]{:S(2)}) copy-start(bf16[1024,1024]{1,0:T(8,128)(2,1)} %refs_19_.1) | copy-start | bytes 6291460
  35.5 6.2 %copy-start.3 = (f32[2048]{0:T(1024)S(1)}, f32[2048]{0:T(1024)}, u32[]{:S(2)}) copy-start(f32[2048]{0:T(1024)} %param.25) | copy-start | bytes 24580
  35.5 6.2 %copy-start.4 = (f32[1024]{0:T(1024)S(1)}, f32[1024]{0:T(1024)}, u32[]{:S(2)}) copy-start(f32[1024]{0:T(1024)} %param.21) | copy-start | bytes 12292
  35.5 6.2 %copy-start.5 = (f32[1024]{0:T(1024)S(1)}, f32[1024]{0:T(1024)}, u32[]{:S(2)}) copy-start(f32[1024]{0:T(1024)} %param.23) | copy-start | bytes 12292
  35.6 6.2 %collective-permute-start.10 = (f32[4,16,128]{2,1,0:T(8,128)S(1)}, f32[4,16,128]{2,1,0:T(8,128)S(1)}, u32[]{:S(2)}, u32[]{:S(2)}) collective-permute-start(f32[4,16,128]{2,1,0:T(8,128)S(1)} %get-tuple-element.101), channel_id=1, source_target_pairs={{0,1},{1,0},{2,3},{3,2},{4,5},{5,4},{6,7},{7,6},{8,9},{9,8},{10,11... | collective-permute-start | bytes 98312 | tf_op jit(solution)/shard_map/ppermute | solution.py:514

commit v9 on v8

--- a/solution.py
+++ b/solution.py
@@ -111,9 +111,10 @@
     total = sums_of(jnp.ones((8, ROWS), F32), parts)
     ends_ref[0, 64:] = total
     ends_ref[1, 64:] = total
-    x = tokens[...].astype(F32)
-    scale = lax.rsqrt(jnp.mean(x * x, axis=-1, keepdims=True) + EPSILON)
-    normed[...] = (x * scale * gain[...]).astype(BF16)
+    for r in range(0, ROWS, 16):
+        x = tokens[r : r + 16, :].astype(F32)
+        scale = lax.rsqrt(jnp.mean(x * x, axis=-1, keepdims=True) + EPSILON)
+        normed[r : r + 16, :] = (x * scale * gain[...]).astype(BF16)
     first = lax.broadcasted_iota(jnp.int32, (16, 128), 1) < 64
 
     def drive(step):
@@ -169,10 +170,19 @@
     return jnp.where(row >= by if by > 0 else row < SPANS + by, moved, fill)
 
 
-def local_kernel(
-    start, size, within, damps, driven, inputs, readout, pars, out_ref, prefix_ref, table_ref,
-    triangles, proj, turn, lifts, part, states, carry,
-):
+def local_kernel(start, size, fetching, within, damps, driven, inputs, readout, pars, *refs):
+    copies = []
+    if fetching:
+        *refs, sems = refs
+        sources, refs = refs[:fetching], refs[fetching:]
+        out_ref, prefix_ref, table_ref, *refs = refs
+        targets, refs = refs[:fetching], refs[fetching:]
+        for n in range(fetching):
+            copies.append(pltpu.make_async_copy(sources[n], targets[n], sems.at[n]))
+            copies[n].start()
+    else:
+        out_ref, prefix_ref, table_ref, *refs = refs
+    triangles, proj, turn, lifts, part, states, carry = refs
     row, col = iotas((ROWS, ROWS))
     same = row // SPAN == col // SPAN
     triangles[0] = ((col <= row) & same).astype(BF16)
@@ -256,6 +266,8 @@
         at = turn_of - 5
         if 0 <= at < len(units) and units[at][1] == 1:
             read(units[at][0])
+    for copy in copies:
+        copy.wait()
 
 
 def times_of(a, b):
@@ -342,23 +354,44 @@
     return state, before, before_decay
 
 
-def group_kernel(axis, own, one, two, three, pars, total_ref, before_ref, data):
+def group_kernel(axis, own, one, two, three, pars, *refs):
+    *sends, before_ref, data = refs
     here = gather_four(axis, own, one, two, three, data)
     mine = my_pars(pars)
+    totals = []
     for k in range(2):
         total, before, decay = run_over(here, data, mine, k)
-        keep_states(total_ref, k, total)
+        totals.append(total)
         keep_at(before_ref, k, before)
         keep_at(before_ref, 2 + k, decay)
-    total_ref[64:72, :] = own[64:72, :] + one[64:72, :] + two[64:72, :] + three[64:72, :]
-
-
-def enter_kernel(across, one, two, three, before_x, before_y, own, other, pars, mine_ref, theirs_ref, data):
-    here = gather_four("z", across, one, two, three, data)
+    span = own[64:72, :] + one[64:72, :] + two[64:72, :] + three[64:72, :]
+    if len(sends) == 1:
+        for k in range(2):
+            keep_states(sends[0], k, totals[k])
+        sends[0][64:72, :] = span
+        return
+    here = lax.axis_index("z")
+    partners = (here + 1 - 2 * (here % 2), (here + 2) % 4, 3 - here)
+    for partner, send in zip(partners, sends):
+        keep_states(send, 0, pick(partner > here, totals[0], totals[1]))
+        send[32:40, :] = span
+
+
+def enter_kernel(one, two, three, before_x, before_y, own, other, pars, mine_ref, theirs_ref, data):
+    here = lax.axis_index("z")
+    data[here] = one[...]
+    data[here + 1 - 2 * (here % 2)] = one[...]
+    data[(here + 2) % 4] = two[...]
+    data[3 - here] = three[...]
     core = lax.axis_index("c")
     mine = my_pars(pars)
+    zero = jnp.zeros((16, 128), F32)
     for k in range(2):
-        _, state, _ = run_over(here, data, mine, k)
+        state = (zero, zero)
+        for n in range(3) if k == 0 else range(3, 0, -1):
+            span = jnp.concatenate([data[n, 32:40, :]] * 2, axis=0)
+            new = plus(times_of(decay_over(span, mine[k]), state), states_of(data.at[n], 0))
+            state = pick(n < here if k == 0 else n > here, new, state)
         for before in (before_x, before_y):
             state = plus(times_of((before[4 + 2 * k], before[5 + 2 * k]), state), (before[2 * k], before[2 * k + 1]))
         ahead = core == k
@@ -417,26 +450,29 @@
     return pltpu.CompilerParams(vmem_limit_bytes=limit * 1024 * 1024)
 
 
-def run_local(start, size, args):
-    spec = pl.BlockSpec(memory_space=VMEM)
+def run_local(start, size, args, weights):
+    spec, distant = pl.BlockSpec(memory_space=VMEM), pl.BlockSpec(memory_space=pltpu.HBM)
+    count = len(weights)
     return pl.pallas_call(
-        functools.partial(local_kernel, 4 * start, 4 * size),
+        functools.partial(local_kernel, 4 * start, 4 * size, count),
         name=f"local_{start}",
-        in_specs=[spec] * len(args),
-        out_specs=[spec] * 3,
+        in_specs=[spec] * len(args) + [distant] * count,
+        out_specs=[spec] * (3 + count),
         out_shape=[
             sds((4 * size, ROWS, 32)),
             sds((4 * size, 2, ROWS, 256), BF16),
             sds((4 * size, 2, 2, 32, 128)),
+            *(sds(weight.shape, BF16) for weight in weights),
         ],
         scratch_shapes=[
             VMEM((2, ROWS, ROWS), BF16), VMEM((SLOTS, ROWS, 256), F32), VMEM((SLOTS, 2, ROWS, 128), F32),
             VMEM((SLOTS, ROWS, 256), BF16), VMEM((SLOTS, 2, ROWS, 128), F32), VMEM((2, ROWS, 512), BF16),
             VMEM((SLOTS, 4, SPANS, 128), F32),
+            *([pltpu.SemaphoreType.DMA((count,))] if count else []),
         ],
         compiler_params=params(8),
         cost_estimate=pl.CostEstimate(flops=size * 5 * 10**8, bytes_accessed=size * 2 * 2**20, transcendentals=0),
-    )(*args)
+    )(*args, *weights)
 
 
 def simple(kernel, name, shapes, args, scratch=()):
@@ -480,13 +516,13 @@
 
     pieces, start = [], 0
 
-    def piece_between(before, after):
+    def piece_between(before, after, weights=()):
         index = len(pieces)
         start = sum(PIECES[:index])
         pairs_now, _ = lax.optimization_barrier((pairs, before))
         piece = run_local(
             start, PIECES[index],
-            (within, damps, pairs_now, inputs_here, state_output, pars),
+            (within, damps, pairs_now, inputs_here, state_output, pars), weights,
         )
         *piece, after = lax.optimization_barrier((*piece, after))
         pieces.append(piece)
@@ -501,22 +537,28 @@
     befores = []
     for axis in ("y", "x"):
         others = piece_between(total, tuple(lax.ppermute(total, axis, pairs) for pairs in swaps))
-        total, before = simple(
-            functools.partial(group_kernel, axis), f"group_{axis}", [(72, 128), (8, 16, 128)],
+        *totals, before = simple(
+            functools.partial(group_kernel, axis), f"group_{axis}",
+            [(72, 128)] * (axis == "y") + [(40, 128)] * (3 * (axis == "x")) + [(8, 16, 128)],
             (total, *others, pars), [four],
         )
+        total = totals[0]
         befores.append(before)
-    others = piece_between(total, tuple(lax.ppermute(total, "z", pairs) for pairs in swaps))
+    others = piece_between(
+        total, tuple(lax.ppermute(value, "z", pairs) for value, pairs in zip(totals, swaps)),
+        (hbm(glu_weight), hbm(out_weight)),
+    )
+    glu_here, outw_here = pieces[-1][3:]
     mine, theirs = simple(
         enter_kernel, "enter", [(4, 16, 128), (4, 16, 128)],
-        (total, *others, befores[1], befores[0], keep, partner, pars), [four],
+        (*others, befores[1], befores[0], keep, partner, pars), [VMEM((4, 40, 128), F32)],
     )
     other = piece_between(theirs, lax.ppermute(theirs, "c", swap))
 
     spec = pl.BlockSpec(memory_space=VMEM)
     args = (
         mine, other, *(p[0] for p in pieces), *(p[1] for p in pieces), *(p[2] for p in pieces),
-        driven, skip_gain.reshape(1, CHANNELS), glu_weight, glu_bias.reshape(1, CHANNELS), out_weight, out_gain.reshape(1, D),
+        driven, skip_gain.reshape(1, CHANNELS), glu_here, glu_bias.reshape(1, CHANNELS), outw_here, out_gain.reshape(1, D),
     )
     return pl.pallas_call(
         final_kernel,

time: 45.2 us -> 46.1 us (1.020)
  starting transfers between devices: 17.6 us -> 18.4 us
    ppermute x3, starting transfers between devices: 4.51 us -> 5.03 us  [local(): lax.ppermute(value, 'z', pairs)]
where the time goes in v9:
time: 46.1 us; the launch traced here: 46 us
  Pallas kernels  24.8 us (54%)
  starting transfers between devices  18.4 us (40%)
  waiting for transfers between devices  2.6 us (6%)
    pallas_call x5, Pallas kernels, run_local(): pl.pallas_call(functools.partial(local_kernel, 4 * start, 4 * size, count...  11.3 us
    pallas_call x1, Pallas kernels, local(): pl.pallas_call(end_kernel, name='ends', in_specs=[spec, spec, spec, dista...  9.75 us
    ppermute x6, starting transfers between devices, local(): lax.ppermute(total, axis, pairs)  6.93 us
    ppermute x3, starting transfers between devices, local(): lax.ppermute(value, 'z', pairs)  5.03 us
    ppermute x1, starting transfers between devices, local(): other = piece_between(theirs, lax.ppermute(theirs, 'c', swap))  4.99 us
    pallas_call x1, Pallas kernels, local(): pl.pallas_call(final_kernel, name='final', in_specs=[spec] * len(args), o...  3.25 us
    ppermute x6, waiting for transfers between devices, local(): lax.ppermute(total, axis, pairs)  1.6 us
    ppermute x1, starting transfers between devices, local(): partner = piece_between(keep, lax.ppermute(ends[1], 'c', swap))  1.46 us
  transfers between devices with their start and end apart: 11, of which 3 were waited for; matrix products, arithmetic and copies ran while one was open for 0% of the time, Pallas kernels for 25%

profile of v9, /device:TPU:1, one launch (start us, length us, event | category | flops | bytes accessed | tf_op | source)
XLA Modules:
  0.0 46.0 jit_solution(10390241337344331501)
XLA Ops:
  0.0 0.0 copy-start
  0.0 9.8 %ends.1 = (bf16[128,1024]{1,0:T(8,128)(2,1)S(1)}, bf16[32,128,32]{2,1,0:T(8,128)(2,1)S(1)}, f32[2,72,128]{2,1,0:T(8,128)S(1)}, f32[2,2,32,128]{3,2,1,0:T(8,128)S...) custom-call(bf16[128,2048]{1,0:T(8,128)(2,1)} %tokens.1, ...), custom_call_target="tpu_custom_call" | custom-call | tf_op jit(solution)/shard_map/ends/pallas_call | solution.py:498
  9.8 1.5 %collective-permute-start = (f32[72,128]{1,0:T(8,128)S(1)}, f32[72,128]{1,0:T(8,128)S(1)}, u32[]{:S(2)}, u32[]{:S(2)}) collective-permute-start(f32[72,128]{1,0:T(8,128)S(1)} %get-tuple-element.135), channel_id=1, source_target_pairs={{0,1},{1,0},{2,3},{3,2},{4,5},{5,4},{6,7},{7,6},{8,9},{9,8},{10,11... | collective-permute-start | bytes 110600 | tf_op jit(solution)/shard_map/ppermute | solution.py:535
  11.2 0.0 copy-done
  11.2 1.5 %local_0.1 = (f32[4,128,32]{2,1,0:T(8,128)S(1)}, bf16[4,2,128,256]{3,2,1,0:T(8,128)(2,1)S(1)}, f32[4,2,2,32,128]{4,3,2,1,0:T(8,128)S(1)}) custom-call(f32[2,128,128]{2,1,0:T(8,128)S(1)} %get-tuple-element.70.within, f32[32,2,128,128]{3,2,1,0:T(8,128)S(1)} %get-tuple-element.71.damps, bf16[32,128,32]{2,1,0:T(8,128)(2,1)S(1)} %get-tuple-element.112.driven, ...), custom_call_target="tpu_custom_call" | custom-call | flops 500000000 | bytes 2097152 | tf_op jit(solution)/shard_map/local_0/pallas_call | solution.py:456
  12.7 0.0 collective-permute-done.other
  12.8 2.9 %collective-permute-start.3 = (f32[72,128]{1,0:T(8,128)S(1)}, f32[72,128]{1,0:T(8,128)S(1)}, u32[]{:S(2)}, u32[]{:S(2)}) collective-permute-start(f32[72,128]{1,0:T(8,128)S(1)} %pair.1.own), channel_id=1, source_target_pairs={{0,6},{6,0},{2,4},{4,2},{1,7},{7,1},{3,5},{5,3},{8,14},{14,8},{10,... | collective-permute-start | bytes 110600 | tf_op jit(solution)/shard_map/ppermute | solution.py:539
  15.7 0.4 collective-permute-start.2
  16.1 0.3 collective-permute-start.1
  16.4 2.8 %local_1.1 = (f32[8,128,32]{2,1,0:T(8,128)S(1)}, bf16[8,2,128,256]{3,2,1,0:T(8,128)(2,1)S(1)}, f32[8,2,2,32,128]{4,3,2,1,0:T(8,128)S(1)}) custom-call(f32[2,128,128]{2,1,0:T(8,128)S(1)} %get-tuple-element.70.within, f32[32,2,128,128]{3,2,1,0:T(8,128)S(1)} %get-tuple-element.71.damps, bf16[32,128,32]{2,1,0:T(8,128)(2,1)S(1)} %get-tuple-element.112.driven, ...), custom_call_target="tpu_custom_call" | custom-call | flops 1000000000 | bytes 4194304 | tf_op jit(solution)/shard_map/local_1/pallas_call | solution.py:456
  19.2 0.0 collective-permute-done.3.three
  19.2 0.8 %collective-permute-done.2.two = f32[72,128]{1,0:T(8,128)S(1)} collective-permute-done((f32[72,128]{1,0:T(8,128)S(1)}, f32[72,128]{1,0:T(8,128)S(1)}, u32[]{:S(2)}, u32[]{:S(2)}) %collective-permute-start.2) | collective-permute-done | bytes 36896 | tf_op jit(solution)/shard_map/ppermute | solution.py:539
  20.0 0.0 collective-permute-done.1.one
  20.0 0.1 group_y.1
  20.2 2.6 %collective-permute-start.6 = (f32[72,128]{1,0:T(8,128)S(1)}, f32[72,128]{1,0:T(8,128)S(1)}, u32[]{:S(2)}, u32[]{:S(2)}) collective-permute-start(f32[72,128]{1,0:T(8,128)S(1)} %get-tuple-element.88.own), channel_id=1, source_target_pairs={{0,24},{24,0},{8,16},{16,8},{1,25},{25,1},{9,17},{17,9},{2,26},{26... | collective-permute-start | bytes 110600 | tf_op jit(solution)/shard_map/ppermute | solution.py:539
  22.7 0.5 %collective-permute-start.5 = (f32[72,128]{1,0:T(8,128)S(1)}, f32[72,128]{1,0:T(8,128)S(1)}, u32[]{:S(2)}, u32[]{:S(2)}) collective-permute-start(f32[72,128]{1,0:T(8,128)S(1)} %get-tuple-element.88.own), channel_id=1, source_target_pairs={{0,16},{16,0},{8,24},{24,8},{1,17},{17,1},{9,25},{25,9},{2,18},{18... | collective-permute-start | bytes 110600 | tf_op jit(solution)/shard_map/ppermute | solution.py:539
  23.2 0.3 collective-permute-start.4
  23.5 2.8 %local_3.1 = (f32[8,128,32]{2,1,0:T(8,128)S(1)}, bf16[8,2,128,256]{3,2,1,0:T(8,128)(2,1)S(1)}, f32[8,2,2,32,128]{4,3,2,1,0:T(8,128)S(1)}) custom-call(f32[2,128,128]{2,1,0:T(8,128)S(1)} %get-tuple-element.70.within, f32[32,2,128,128]{3,2,1,0:T(8,128)S(1)} %get-tuple-element.71.damps, bf16[32,128,32]{2,1,0:T(8,128)(2,1)S(1)} %get-tuple-element.112.driven, ...), custom_call_target="tpu_custom_call" | custom-call | flops 1000000000 | bytes 4194304 | tf_op jit(solution)/shard_map/local_3/pallas_call | solution.py:456
  26.3 0.0 collective-permute-done.6.three
  26.3 0.7 %collective-permute-done.5.two = f32[72,128]{1,0:T(8,128)S(1)} collective-permute-done((f32[72,128]{1,0:T(8,128)S(1)}, f32[72,128]{1,0:T(8,128)S(1)}, u32[]{:S(2)}, u32[]{:S(2)}) %collective-permute-start.5) | collective-permute-done | bytes 36896 | tf_op jit(solution)/shard_map/ppermute | solution.py:539
  27.0 0.0 collective-permute-done.4.one
  27.0 0.1 group_x.1
  27.2 1.7 %collective-permute-start.7 = (f32[40,128]{1,0:T(8,128)S(1)}, f32[40,128]{1,0:T(8,128)S(1)}, u32[]{:S(2)}, u32[]{:S(2)}) collective-permute-start(f32[40,128]{1,0:T(8,128)S(1)} %get-tuple-element.96), channel_id=1, source_target_pairs={{0,32},{32,0},{64,96},{96,64},{1,33},{33,1},{65,97},{97,65},{2,34}... | collective-permute-start | bytes 61448 | tf_op jit(solution)/shard_map/ppermute | solution.py:548
  28.9 3.3 %collective-permute-start.8 = (f32[40,128]{1,0:T(8,128)S(1)}, f32[40,128]{1,0:T(8,128)S(1)}, u32[]{:S(2)}, u32[]{:S(2)}) collective-permute-start(f32[40,128]{1,0:T(8,128)S(1)} %get-tuple-element.103), channel_id=1, source_target_pairs={{0,64},{64,0},{32,96},{96,32},{1,65},{65,1},{33,97},{97,33},{2,66}... | collective-permute-start | bytes 61448 | tf_op jit(solution)/shard_map/ppermute | solution.py:548
  32.2 0.0 collective-permute-start.9
  32.2 2.8 %local_5.1 = (f32[8,128,32]{2,1,0:T(8,128)S(1)}, bf16[8,2,128,256]{3,2,1,0:T(8,128)(2,1)S(1)}, f32[8,2,2,32,128]{4,3,2,1,0:T(8,128)S(1)}, bf16[1024,1024]{1,0:T(8,128)(2,1)S(1)}, bf16[1024,2048]{1,0:T(8,128)(2,1)S(1)}) custom-call(f32[2,128,128]{2,1,0:T(8,128)S(1)} %get-tuple-element.70.within, f32[32,2,128,128]{3,2,1,0:T(8,128)S(1)} %get-tuple-element.71.damps, ...), custom_call_target="tpu_custom_call" | custom-call | flops 1000000000 | bytes 4194304 | tf_op jit(solution)/shard_map/local_5/pallas_call | solution.py:456
  35.1 0.0 collective-permute-done.8.two
  35.1 1.0 %collective-permute-done.9.three = f32[40,128]{1,0:T(8,128)S(1)} collective-permute-done((f32[40,128]{1,0:T(8,128)S(1)}, f32[40,128]{1,0:T(8,128)S(1)}, u32[]{:S(2)}, u32[]{:S(2)}) %collective-permute-start.9) | collective-permute-done | bytes 20512 | tf_op jit(solution)/shard_map/ppermute | solution.py:548
  36.0 0.0 collective-permute-done.7.one
  36.0 0.1 enter.1
  36.2 0.0 copy-start.1
  36.2 0.0 copy-start.2
  36.2 0.0 copy-start.3
  36.2 5.0 %collective-permute-start.10 = (f32[4,16,128]{2,1,0:T(8,128)S(1)}, f32[4,16,128]{2,1,0:T(8,128)S(1)}, u32[]{:S(2)}, u32[]{:S(2)}) collective-permute-start(f32[4,16,128]{2,1,0:T(8,128)S(1)} %get-tuple-element.111), channel_id=1, source_target_pairs={{0,1},{1,0},{2,3},{3,2},{4,5},{5,4},{6,7},{7,6},{8,9},{9,8},{10,11... | collective-permute-start | bytes 98312 | tf_op jit(solution)/shard_map/ppermute | solution.py:556
  41.2 1.5 %local_7.1 = (f32[4,128,32]{2,1,0:T(8,128)S(1)}, bf16[4,2,128,256]{3,2,1,0:T(8,128)(2,1)S(1)}, f32[4,2,2,32,128]{4,3,2,1,0:T(8,128)S(1)}) custom-call(f32[2,128,128]{2,1,0:T(8,128)S(1)} %get-tuple-element.70.within, f32[32,2,128,128]{3,2,1,0:T(8,128)S(1)} %get-tuple-element.71.damps, bf16[32,128,32]{2,1,0:T(8,128)(2,1)S(1)} %get-tuple-element.112.driven, ...), custom_call_target="tpu_custom_call" | custom-call | flops 500000000 | bytes 2097152 | tf_op jit(solution)/shard_map/local_7/pallas_call | solution.py:456
  42.7 0.0 collective-permute-done.10.refs_1_
  42.7 0.0 copy-done.1
  42.7 0.0 copy-done.2
  42.7 0.0 copy-done.3
  42.7 3.2 %final.1 = bf16[128,2048]{1,0:T(8,128)(2,1)} custom-call(f32[4,16,128]{2,1,0:T(8,128)S(1)} %get-tuple-element.110.refs_0_, f32[4,16,128]{2,1,0:T(8,128)S(1)} %collective-permute-done.10.refs_1_, f32[4,128,32]{2,1,0:T(8,128)S(1)} %get-tuple-element.117.refs_2_, f32[8,128,32]{2,1,0:T(8,128)S(1)} %get-tuple-element.118.refs_3_, ...), custom_call_target="tpu_custom_call" | custom-call | tf_op jit(solution)/shard_map/final/pallas_call | solution.py:563
  (2 shorter events, 0.1 us)
Async XLA Ops:
  0.0 11.2 %copy-start = (f32[2,2,64,16,64]{4,3,2,1,0:T(8,128)S(1)}, f32[2,2,64,16,64]{4,3,2,1,0:T(8,128)}, u32[]{:S(2)}) copy-start(f32[2,2,64,16,64]{4,3,2,1,0:T(8,128)} %readout.9) | copy-start | bytes 3145732
  9.8 2.9 %collective-permute-start = (f32[72,128]{1,0:T(8,128)S(1)}, f32[72,128]{1,0:T(8,128)S(1)}, u32[]{:S(2)}, u32[]{:S(2)}) collective-permute-start(f32[72,128]{1,0:T(8,128)S(1)} %get-tuple-element.135), channel_id=1, source_target_pairs={{0,1},{1,0},{2,3},{3,2},{4,5},{5,4},{6,7},{7,6},{8,9},{9,8},{10,11... | collective-permute-start | bytes 110600 | tf_op jit(solution)/shard_map/ppermute | solution.py:535
  12.8 6.4 %collective-permute-start.3 = (f32[72,128]{1,0:T(8,128)S(1)}, f32[72,128]{1,0:T(8,128)S(1)}, u32[]{:S(2)}, u32[]{:S(2)}) collective-permute-start(f32[72,128]{1,0:T(8,128)S(1)} %pair.1.own), channel_id=1, source_target_pairs={{0,6},{6,0},{2,4},{4,2},{1,7},{7,1},{3,5},{5,3},{8,14},{14,8},{10,... | collective-permute-start | bytes 110600 | tf_op jit(solution)/shard_map/ppermute | solution.py:539
  15.7 4.3 %collective-permute-start.2 = (f32[72,128]{1,0:T(8,128)S(1)}, f32[72,128]{1,0:T(8,128)S(1)}, u32[]{:S(2)}, u32[]{:S(2)}) collective-permute-start(f32[72,128]{1,0:T(8,128)S(1)} %pair.1.own), channel_id=1, source_target_pairs={{0,4},{4,0},{2,6},{6,2},{1,5},{5,1},{3,7},{7,3},{8,12},{12,8},{10,... | collective-permute-start | bytes 110600 | tf_op jit(solution)/shard_map/ppermute | solution.py:539
  16.1 4.0 %collective-permute-start.1 = (f32[72,128]{1,0:T(8,128)S(1)}, f32[72,128]{1,0:T(8,128)S(1)}, u32[]{:S(2)}, u32[]{:S(2)}) collective-permute-start(f32[72,128]{1,0:T(8,128)S(1)} %pair.1.own), channel_id=1, source_target_pairs={{0,2},{2,0},{4,6},{6,4},{1,3},{3,1},{5,7},{7,5},{8,10},{10,8},{12,... | collective-permute-start | bytes 110600 | tf_op jit(solution)/shard_map/ppermute | solution.py:539
  20.2 6.1 %collective-permute-start.6 = (f32[72,128]{1,0:T(8,128)S(1)}, f32[72,128]{1,0:T(8,128)S(1)}, u32[]{:S(2)}, u32[]{:S(2)}) collective-permute-start(f32[72,128]{1,0:T(8,128)S(1)} %get-tuple-element.88.own), channel_id=1, source_target_pairs={{0,24},{24,0},{8,16},{16,8},{1,25},{25,1},{9,17},{17,9},{2,26},{26... | collective-permute-start | bytes 110600 | tf_op jit(solution)/shard_map/ppermute | solution.py:539
  22.7 4.3 %collective-permute-start.5 = (f32[72,128]{1,0:T(8,128)S(1)}, f32[72,128]{1,0:T(8,128)S(1)}, u32[]{:S(2)}, u32[]{:S(2)}) collective-permute-start(f32[72,128]{1,0:T(8,128)S(1)} %get-tuple-element.88.own), channel_id=1, source_target_pairs={{0,16},{16,0},{8,24},{24,8},{1,17},{17,1},{9,25},{25,9},{2,18},{18... | collective-permute-start | bytes 110600 | tf_op jit(solution)/shard_map/ppermute | solution.py:539
  23.2 3.8 %collective-permute-start.4 = (f32[72,128]{1,0:T(8,128)S(1)}, f32[72,128]{1,0:T(8,128)S(1)}, u32[]{:S(2)}, u32[]{:S(2)}) collective-permute-start(f32[72,128]{1,0:T(8,128)S(1)} %get-tuple-element.88.own), channel_id=1, source_target_pairs={{0,8},{8,0},{16,24},{24,16},{1,9},{9,1},{17,25},{25,17},{2,10},{10... | collective-permute-start | bytes 110600 | tf_op jit(solution)/shard_map/ppermute | solution.py:539
  27.2 8.9 %collective-permute-start.7 = (f32[40,128]{1,0:T(8,128)S(1)}, f32[40,128]{1,0:T(8,128)S(1)}, u32[]{:S(2)}, u32[]{:S(2)}) collective-permute-start(f32[40,128]{1,0:T(8,128)S(1)} %get-tuple-element.96), channel_id=1, source_target_pairs={{0,32},{32,0},{64,96},{96,64},{1,33},{33,1},{65,97},{97,65},{2,34}... | collective-permute-start | bytes 61448 | tf_op jit(solution)/shard_map/ppermute | solution.py:548
  28.9 6.2 %collective-permute-start.8 = (f32[40,128]{1,0:T(8,128)S(1)}, f32[40,128]{1,0:T(8,128)S(1)}, u32[]{:S(2)}, u32[]{:S(2)}) collective-permute-start(f32[40,128]{1,0:T(8,128)S(1)} %get-tuple-element.103), channel_id=1, source_target_pairs={{0,64},{64,0},{32,96},{96,32},{1,65},{65,1},{33,97},{97,33},{2,66}... | collective-permute-start | bytes 61448 | tf_op jit(solution)/shard_map/ppermute | solution.py:548
  32.2 3.8 %collective-permute-start.9 = (f32[40,128]{1,0:T(8,128)S(1)}, f32[40,128]{1,0:T(8,128)S(1)}, u32[]{:S(2)}, u32[]{:S(2)}) collective-permute-start(f32[40,128]{1,0:T(8,128)S(1)} %get-tuple-element.104), channel_id=1, source_target_pairs={{0,96},{96,0},{32,64},{64,32},{1,97},{97,1},{33,65},{65,33},{2,98}... | collective-permute-start | bytes 61448 | tf_op jit(solution)/shard_map/ppermute | solution.py:548
  36.2 6.5 %copy-start.1 = (f32[2048]{0:T(1024)S(1)}, f32[2048]{0:T(1024)}, u32[]{:S(2)}) copy-start(f32[2048]{0:T(1024)} %param.25) | copy-start | bytes 24580
  36.2 6.5 %copy-start.2 = (f32[1024]{0:T(1024)S(1)}, f32[1024]{0:T(1024)}, u32[]{:S(2)}) copy-start(f32[1024]{0:T(1024)} %param.21) | copy-start | bytes 12292
  36.2 6.5 %copy-start.3 = (f32[1024]{0:T(1024)S(1)}, f32[1024]{0:T(1024)}, u32[]{:S(2)}) copy-start(f32[1024]{0:T(1024)} %param.23) | copy-start | bytes 12292
  36.2 6.5 %collective-permute-start.10 = (f32[4,16,128]{2,1,0:T(8,128)S(1)}, f32[4,16,128]{2,1,0:T(8,128)S(1)}, u32[]{:S(2)}, u32[]{:S(2)}) collective-permute-start(f32[4,16,128]{2,1,0:T(8,128)S(1)} %get-tuple-element.111), channel_id=1, source_target_pairs={{0,1},{1,0},{2,3},{3,2},{4,5},{5,4},{6,7},{7,6},{8,9},{9,8},{10,11... | collective-permute-start | bytes 98312 | tf_op jit(solution)/shard_map/ppermute | solution.py:556

commit v10 on v9

--- a/solution.py
+++ b/solution.py
@@ -13,8 +13,8 @@
 D = 2048
 CHANNELS = 1024
 CHUNKS = 4
-LAG = 10
-DRIVE_AT = (6, 16, 32, 48)
+LAG = 12
+DRIVE_AT = (6, 7, 8, 9, 13, 16, 19, 22, 29, 32, 35, 38, 45, 48, 51, 54)
 SPAN = 16
 SPANS = ROWS // SPAN
 SLOTS = 6
@@ -84,7 +84,7 @@
 
 def end_kernel(
     tokens, elapsed, gain, weight, inputs, angle, rate,
-    driven_ref, pairs_ref, ends_ref, pars_ref, damp_ref, within_ref, inputs_ref, normed, times, chunks, flipped, pulls, weight_sems, input_sems,
+    driven_ref, pairs_ref, ends_ref, pars_ref, damp_ref, within_ref, inputs_ref, normed, times, chunks, flipped, summed, pulls, weight_sems, input_sems,
 ):
     core = lax.axis_index("c")
 
@@ -117,10 +117,18 @@
         normed[r : r + 16, :] = (x * scale * gain[...]).astype(BF16)
     first = lax.broadcasted_iota(jnp.int32, (16, 128), 1) < 64
 
+    def gather_in(step, quarter):
+        if quarter == 0:
+            for copy in fetch(step):
+                copy.wait()
+        cut = slice(512 * quarter, 512 * quarter + 512)
+        value = mm(normed[:, cut], chunks[step, cut, :])
+        summed[...] = value if quarter == 0 else summed[...] + value
+        if quarter == 3:
+            drive(step)
+
     def drive(step):
-        for copy in fetch(step):
-            copy.wait()
-        driven = mm(normed[...], chunks[step]).astype(BF16)
+        driven = summed[...].astype(BF16)
         driven_ref[:, 256 * step : 256 * step + 256] = driven
         for j in range(8):
             pairs_ref[8 * step + j] = driven[:, 32 * j : 32 * j + 32]
@@ -157,7 +165,7 @@
     units = [(pair, k) for pair in range(32) for k in range(2)]
     for n in range(len(units) + LAG):
         if n in DRIVE_AT:
-            drive(DRIVE_AT.index(n))
+            gather_in(*divmod(DRIVE_AT.index(n), 4))
         if n < len(units):
             pull(*units[n])
         if n >= LAG:
@@ -371,7 +379,7 @@
         sends[0][64:72, :] = span
         return
     here = lax.axis_index("z")
-    partners = (here + 1 - 2 * (here % 2), (here + 2) % 4, 3 - here)
+    partners = ((here + 2) % 4, 3 - here, here + 1 - 2 * (here % 2))
     for partner, send in zip(partners, sends):
         keep_states(send, 0, pick(partner > here, totals[0], totals[1]))
         send[32:40, :] = span
@@ -506,7 +514,7 @@
         ],
         scratch_shapes=[
             VMEM((ROWS, D), BF16), VMEM((3, ROWS, ROWS), F32), VMEM((CHUNKS, D, 256), BF16), VMEM((2, 256, ROWS), BF16),
-            VMEM((8, 2, ROWS, 256), BF16),
+            VMEM((ROWS, 256), F32), VMEM((8, 2, ROWS, 256), BF16),
             pltpu.SemaphoreType.DMA((CHUNKS,)), pltpu.SemaphoreType.DMA((CHUNKS,)),
         ],
         compiler_params=params(12),
@@ -530,13 +538,18 @@
 
     swap = [(0, 1), (1, 0)]
     swaps = ([(0, 1), (1, 0), (2, 3), (3, 2)], [(0, 2), (2, 0), (1, 3), (3, 1)], [(0, 3), (3, 0), (1, 2), (2, 1)])
+
+    def trade(values, axis, order, weights=()):
+        found = piece_between(values[order[0]], tuple(lax.ppermute(values[n], axis, swaps[n]) for n in order), weights)
+        return tuple(found[order.index(n)] for n in range(3))
+
     four = VMEM((4, 72, 128), F32)
     keep = ends[0]
     partner = piece_between(keep, lax.ppermute(ends[1], "c", swap))
     (total,) = simple(pair_kernel, "pair", [(72, 128)], (keep, partner, pars))
     befores = []
     for axis in ("y", "x"):
-        others = piece_between(total, tuple(lax.ppermute(total, axis, pairs) for pairs in swaps))
+        others = trade((total,) * 3, axis, (0, 2, 1))
         *totals, before = simple(
             functools.partial(group_kernel, axis), f"group_{axis}",
             [(72, 128)] * (axis == "y") + [(40, 128)] * (3 * (axis == "x")) + [(8, 16, 128)],
@@ -544,10 +557,7 @@
         )
         total = totals[0]
         befores.append(before)
-    others = piece_between(
-        total, tuple(lax.ppermute(value, "z", pairs) for value, pairs in zip(totals, swaps)),
-        (hbm(glu_weight), hbm(out_weight)),
-    )
+    others = trade(totals[2:] + totals[:2], "z", (1, 2, 0), (hbm(glu_weight), hbm(out_weight)))
     glu_here, outw_here = pieces[-1][3:]
     mine, theirs = simple(
         enter_kernel, "enter", [(4, 16, 128), (4, 16, 128)],

time: 46.1 us -> 43.9 us (0.952)
  waiting for transfers between devices: 2.6 us -> 1.39 us
  starting transfers between devices: 18.4 us -> 17.8 us
    ppermute x9, waiting for transfers between devices: 2.59 us -> 1.38 us  [trade(): lax.ppermute(values[n], axis, swaps[n])]
    ppermute x1, starting transfers between devices: 4.99 us -> 4.32 us  [local(): other = piece_between(theirs, lax.ppermute(theirs, 'c', swap))]
  transfers between devices with their start and end apart: 11 -> 11, of which waited for: 3 -> 3; matrix products, arithmetic and copies ran while one was open for 0% -> 0% of each run, Pallas kernels for 25% -> 26%
where the time goes in v10:
time: 43.9 us; the launch traced here: 43.8 us
  Pallas kernels  24.4 us (56%)
  starting transfers between devices  17.8 us (41%)
  waiting for transfers between devices  1.39 us (3%)
    ppermute x9, starting transfers between devices, trade(): lax.ppermute(values[n], axis, swaps[n])  12 us
    pallas_call x5, Pallas kernels, run_local(): pl.pallas_call(functools.partial(local_kernel, 4 * start, 4 * size, count...  11.3 us
    pallas_call x1, Pallas kernels, local(): pl.pallas_call(end_kernel, name='ends', in_specs=[spec, spec, spec, dista...  9.4 us
    ppermute x1, starting transfers between devices, local(): other = piece_between(theirs, lax.ppermute(theirs, 'c', swap))  4.32 us
    pallas_call x1, Pallas kernels, local(): pl.pallas_call(final_kernel, name='final', in_specs=[spec] * len(args), o...  3.25 us
    ppermute x1, starting transfers between devices, local(): partner = piece_between(keep, lax.ppermute(ends[1], 'c', swap))  1.46 us
    ppermute x9, waiting for transfers between devices, trade(): lax.ppermute(values[n], axis, swaps[n])  1.38 us
  transfers between devices with their start and end apart: 11, of which 3 were waited for; matrix products, arithmetic and copies ran while one was open for 0% of the time, Pallas kernels for 26%

profile of v10, /device:TPU:1, one launch (start us, length us, event | category | flops | bytes accessed | tf_op | source)
XLA Modules:
  0.0 43.8 jit_solution(1827368578272663872)
XLA Ops:
  0.0 0.0 copy-start
  0.0 9.4 %ends.1 = (bf16[128,1024]{1,0:T(8,128)(2,1)S(1)}, bf16[32,128,32]{2,1,0:T(8,128)(2,1)S(1)}, f32[2,72,128]{2,1,0:T(8,128)S(1)}, f32[2,2,32,128]{3,2,1,0:T(8,128)S...) custom-call(bf16[128,2048]{1,0:T(8,128)(2,1)} %tokens.1, ...), custom_call_target="tpu_custom_call" | custom-call | tf_op jit(solution)/shard_map/ends/pallas_call | solution.py:506
  9.4 1.5 %collective-permute-start = (f32[72,128]{1,0:T(8,128)S(1)}, f32[72,128]{1,0:T(8,128)S(1)}, u32[]{:S(2)}, u32[]{:S(2)}) collective-permute-start(f32[72,128]{1,0:T(8,128)S(1)} %get-tuple-element.135), channel_id=1, source_target_pairs={{0,1},{1,0},{2,3},{3,2},{4,5},{5,4},{6,7},{7,6},{8,9},{9,8},{10,11... | collective-permute-start | bytes 110600 | tf_op jit(solution)/shard_map/ppermute | solution.py:548
  10.9 0.0 copy-done
  10.9 1.5 %local_0.1 = (f32[4,128,32]{2,1,0:T(8,128)S(1)}, bf16[4,2,128,256]{3,2,1,0:T(8,128)(2,1)S(1)}, f32[4,2,2,32,128]{4,3,2,1,0:T(8,128)S(1)}) custom-call(f32[2,128,128]{2,1,0:T(8,128)S(1)} %get-tuple-element.70.within, f32[32,2,128,128]{3,2,1,0:T(8,128)S(1)} %get-tuple-element.71.damps, bf16[32,128,32]{2,1,0:T(8,128)(2,1)S(1)} %get-tuple-element.112.driven, ...), custom_call_target="tpu_custom_call" | custom-call | flops 500000000 | bytes 2097152 | tf_op jit(solution)/shard_map/local_0/pallas_call | solution.py:464
  12.4 0.0 collective-permute-done.other
  12.4 3.1 %collective-permute-start.3 = (f32[72,128]{1,0:T(8,128)S(1)}, f32[72,128]{1,0:T(8,128)S(1)}, u32[]{:S(2)}, u32[]{:S(2)}) collective-permute-start(f32[72,128]{1,0:T(8,128)S(1)} %pair.1.own), channel_id=1, source_target_pairs={{0,4},{4,0},{2,6},{6,2},{1,5},{5,1},{3,7},{7,3},{8,12},{12,8},{10,... | collective-permute-start | bytes 110600 | tf_op jit(solution)/shard_map/ppermute | solution.py:543
  15.5 0.8 %collective-permute-start.2 = (f32[72,128]{1,0:T(8,128)S(1)}, f32[72,128]{1,0:T(8,128)S(1)}, u32[]{:S(2)}, u32[]{:S(2)}) collective-permute-start(f32[72,128]{1,0:T(8,128)S(1)} %pair.1.own), channel_id=1, source_target_pairs={{0,6},{6,0},{2,4},{4,2},{1,7},{7,1},{3,5},{5,3},{8,14},{14,8},{10,... | collective-permute-start | bytes 110600 | tf_op jit(solution)/shard_map/ppermute | solution.py:543
  16.3 0.0 collective-permute-start.1
  16.3 2.8 %local_1.1 = (f32[8,128,32]{2,1,0:T(8,128)S(1)}, bf16[8,2,128,256]{3,2,1,0:T(8,128)(2,1)S(1)}, f32[8,2,2,32,128]{4,3,2,1,0:T(8,128)S(1)}) custom-call(f32[2,128,128]{2,1,0:T(8,128)S(1)} %get-tuple-element.70.within, f32[32,2,128,128]{3,2,1,0:T(8,128)S(1)} %get-tuple-element.71.damps, bf16[32,128,32]{2,1,0:T(8,128)(2,1)S(1)} %get-tuple-element.112.driven, ...), custom_call_target="tpu_custom_call" | custom-call | flops 1000000000 | bytes 4194304 | tf_op jit(solution)/shard_map/local_1/pallas_call | solution.py:464
  19.1 0.0 collective-permute-done.3.two
  19.1 0.4 %collective-permute-done.2.three = f32[72,128]{1,0:T(8,128)S(1)} collective-permute-done((f32[72,128]{1,0:T(8,128)S(1)}, f32[72,128]{1,0:T(8,128)S(1)}, u32[]{:S(2)}, u32[]{:S(2)}) %collective-permute-start.2) | collective-permute-done | bytes 36896 | tf_op jit(solution)/shard_map/ppermute | solution.py:543
  19.6 0.0 collective-permute-done.1.one
  19.6 0.1 group_y.1
  19.7 2.8 %collective-permute-start.6 = (f32[72,128]{1,0:T(8,128)S(1)}, f32[72,128]{1,0:T(8,128)S(1)}, u32[]{:S(2)}, u32[]{:S(2)}) collective-permute-start(f32[72,128]{1,0:T(8,128)S(1)} %get-tuple-element.88.own), channel_id=1, source_target_pairs={{0,16},{16,0},{8,24},{24,8},{1,17},{17,1},{9,25},{25,9},{2,18},{18... | collective-permute-start | bytes 110600 | tf_op jit(solution)/shard_map/ppermute | solution.py:543
  22.5 0.9 %collective-permute-start.5 = (f32[72,128]{1,0:T(8,128)S(1)}, f32[72,128]{1,0:T(8,128)S(1)}, u32[]{:S(2)}, u32[]{:S(2)}) collective-permute-start(f32[72,128]{1,0:T(8,128)S(1)} %get-tuple-element.88.own), channel_id=1, source_target_pairs={{0,24},{24,0},{8,16},{16,8},{1,25},{25,1},{9,17},{17,9},{2,26},{26... | collective-permute-start | bytes 110600 | tf_op jit(solution)/shard_map/ppermute | solution.py:543
  23.4 0.0 collective-permute-start.4
  23.4 2.8 %local_3.1 = (f32[8,128,32]{2,1,0:T(8,128)S(1)}, bf16[8,2,128,256]{3,2,1,0:T(8,128)(2,1)S(1)}, f32[8,2,2,32,128]{4,3,2,1,0:T(8,128)S(1)}) custom-call(f32[2,128,128]{2,1,0:T(8,128)S(1)} %get-tuple-element.70.within, f32[32,2,128,128]{3,2,1,0:T(8,128)S(1)} %get-tuple-element.71.damps, bf16[32,128,32]{2,1,0:T(8,128)(2,1)S(1)} %get-tuple-element.112.driven, ...), custom_call_target="tpu_custom_call" | custom-call | flops 1000000000 | bytes 4194304 | tf_op jit(solution)/shard_map/local_3/pallas_call | solution.py:464
  26.2 0.0 collective-permute-done.6.two
  26.2 0.4 collective-permute-done.5.three
  26.5 0.0 collective-permute-done.4.one
  26.5 0.1 group_x.1
  26.7 3.7 %collective-permute-start.7 = (f32[40,128]{1,0:T(8,128)S(1)}, f32[40,128]{1,0:T(8,128)S(1)}, u32[]{:S(2)}, u32[]{:S(2)}) collective-permute-start(f32[40,128]{1,0:T(8,128)S(1)} %get-tuple-element.96), channel_id=1, source_target_pairs={{0,64},{64,0},{32,96},{96,32},{1,65},{65,1},{33,97},{97,33},{2,66}... | collective-permute-start | bytes 61448 | tf_op jit(solution)/shard_map/ppermute | solution.py:543
  30.4 0.4 collective-permute-start.8
  30.8 0.3 collective-permute-start.9
  31.1 2.8 %local_5.1 = (f32[8,128,32]{2,1,0:T(8,128)S(1)}, bf16[8,2,128,256]{3,2,1,0:T(8,128)(2,1)S(1)}, f32[8,2,2,32,128]{4,3,2,1,0:T(8,128)S(1)}, bf16[1024,1024]{1,0:T(8,128)(2,1)S(1)}, bf16[1024,2048]{1,0:T(8,128)(2,1)S(1)}) custom-call(f32[2,128,128]{2,1,0:T(8,128)S(1)} %get-tuple-element.70.within, f32[32,2,128,128]{3,2,1,0:T(8,128)S(1)} %get-tuple-element.71.damps, ...), custom_call_target="tpu_custom_call" | custom-call | flops 1000000000 | bytes 4194304 | tf_op jit(solution)/shard_map/local_5/pallas_call | solution.py:464
  33.9 0.5 %collective-permute-done.8.three = f32[40,128]{1,0:T(8,128)S(1)} collective-permute-done((f32[40,128]{1,0:T(8,128)S(1)}, f32[40,128]{1,0:T(8,128)S(1)}, u32[]{:S(2)}, u32[]{:S(2)}) %collective-permute-start.8) | collective-permute-done | bytes 20512 | tf_op jit(solution)/shard_map/ppermute | solution.py:543
  34.5 0.0 collective-permute-done.9.one
  34.5 0.0 collective-permute-done.7.two
  34.5 0.1 enter.1
  34.6 0.0 copy-start.1
  34.7 0.0 copy-start.2
  34.7 0.0 copy-start.3
  34.7 4.3 %collective-permute-start.10 = (f32[4,16,128]{2,1,0:T(8,128)S(1)}, f32[4,16,128]{2,1,0:T(8,128)S(1)}, u32[]{:S(2)}, u32[]{:S(2)}) collective-permute-start(f32[4,16,128]{2,1,0:T(8,128)S(1)} %get-tuple-element.111), channel_id=1, source_target_pairs={{0,1},{1,0},{2,3},{3,2},{4,5},{5,4},{6,7},{7,6},{8,9},{9,8},{10,11... | collective-permute-start | bytes 98312 | tf_op jit(solution)/shard_map/ppermute | solution.py:566
  39.0 1.5 %local_7.1 = (f32[4,128,32]{2,1,0:T(8,128)S(1)}, bf16[4,2,128,256]{3,2,1,0:T(8,128)(2,1)S(1)}, f32[4,2,2,32,128]{4,3,2,1,0:T(8,128)S(1)}) custom-call(f32[2,128,128]{2,1,0:T(8,128)S(1)} %get-tuple-element.70.within, f32[32,2,128,128]{3,2,1,0:T(8,128)S(1)} %get-tuple-element.71.damps, bf16[32,128,32]{2,1,0:T(8,128)(2,1)S(1)} %get-tuple-element.112.driven, ...), custom_call_target="tpu_custom_call" | custom-call | flops 500000000 | bytes 2097152 | tf_op jit(solution)/shard_map/local_7/pallas_call | solution.py:464
  40.5 0.0 collective-permute-done.10.refs_1_
  40.5 0.0 copy-done.1
  40.5 0.0 copy-done.2
  40.5 0.0 copy-done.3
  40.5 3.2 %final.1 = bf16[128,2048]{1,0:T(8,128)(2,1)} custom-call(f32[4,16,128]{2,1,0:T(8,128)S(1)} %get-tuple-element.110.refs_0_, f32[4,16,128]{2,1,0:T(8,128)S(1)} %collective-permute-done.10.refs_1_, f32[4,128,32]{2,1,0:T(8,128)S(1)} %get-tuple-element.117.refs_2_, f32[8,128,32]{2,1,0:T(8,128)S(1)} %get-tuple-element.118.refs_3_, ...), custom_call_target="tpu_custom_call" | custom-call | tf_op jit(solution)/shard_map/final/pallas_call | solution.py:573
  (2 shorter events, 0.1 us)
Async XLA Ops:
  0.0 10.9 %copy-start = (f32[2,2,64,16,64]{4,3,2,1,0:T(8,128)S(1)}, f32[2,2,64,16,64]{4,3,2,1,0:T(8,128)}, u32[]{:S(2)}) copy-start(f32[2,2,64,16,64]{4,3,2,1,0:T(8,128)} %readout.9) | copy-start | bytes 3145732
  9.4 2.9 %collective-permute-start = (f32[72,128]{1,0:T(8,128)S(1)}, f32[72,128]{1,0:T(8,128)S(1)}, u32[]{:S(2)}, u32[]{:S(2)}) collective-permute-start(f32[72,128]{1,0:T(8,128)S(1)} %get-tuple-element.135), channel_id=1, source_target_pairs={{0,1},{1,0},{2,3},{3,2},{4,5},{5,4},{6,7},{7,6},{8,9},{9,8},{10,11... | collective-permute-start | bytes 110600 | tf_op jit(solution)/shard_map/ppermute | solution.py:548
  12.4 6.7 %collective-permute-start.3 = (f32[72,128]{1,0:T(8,128)S(1)}, f32[72,128]{1,0:T(8,128)S(1)}, u32[]{:S(2)}, u32[]{:S(2)}) collective-permute-start(f32[72,128]{1,0:T(8,128)S(1)} %pair.1.own), channel_id=1, source_target_pairs={{0,4},{4,0},{2,6},{6,2},{1,5},{5,1},{3,7},{7,3},{8,12},{12,8},{10,... | collective-permute-start | bytes 110600 | tf_op jit(solution)/shard_map/ppermute | solution.py:543
  15.5 4.0 %collective-permute-start.2 = (f32[72,128]{1,0:T(8,128)S(1)}, f32[72,128]{1,0:T(8,128)S(1)}, u32[]{:S(2)}, u32[]{:S(2)}) collective-permute-start(f32[72,128]{1,0:T(8,128)S(1)} %pair.1.own), channel_id=1, source_target_pairs={{0,6},{6,0},{2,4},{4,2},{1,7},{7,1},{3,5},{5,3},{8,14},{14,8},{10,... | collective-permute-start | bytes 110600 | tf_op jit(solution)/shard_map/ppermute | solution.py:543
  16.3 3.2 %collective-permute-start.1 = (f32[72,128]{1,0:T(8,128)S(1)}, f32[72,128]{1,0:T(8,128)S(1)}, u32[]{:S(2)}, u32[]{:S(2)}) collective-permute-start(f32[72,128]{1,0:T(8,128)S(1)} %pair.1.own), channel_id=1, source_target_pairs={{0,2},{2,0},{4,6},{6,4},{1,3},{3,1},{5,7},{7,5},{8,10},{10,8},{12,... | collective-permute-start | bytes 110600 | tf_op jit(solution)/shard_map/ppermute | solution.py:543
  19.7 6.5 %collective-permute-start.6 = (f32[72,128]{1,0:T(8,128)S(1)}, f32[72,128]{1,0:T(8,128)S(1)}, u32[]{:S(2)}, u32[]{:S(2)}) collective-permute-start(f32[72,128]{1,0:T(8,128)S(1)} %get-tuple-element.88.own), channel_id=1, source_target_pairs={{0,16},{16,0},{8,24},{24,8},{1,17},{17,1},{9,25},{25,9},{2,18},{18... | collective-permute-start | bytes 110600 | tf_op jit(solution)/shard_map/ppermute | solution.py:543
  22.5 4.0 %collective-permute-start.5 = (f32[72,128]{1,0:T(8,128)S(1)}, f32[72,128]{1,0:T(8,128)S(1)}, u32[]{:S(2)}, u32[]{:S(2)}) collective-permute-start(f32[72,128]{1,0:T(8,128)S(1)} %get-tuple-element.88.own), channel_id=1, source_target_pairs={{0,24},{24,0},{8,16},{16,8},{1,25},{25,1},{9,17},{17,9},{2,26},{26... | collective-permute-start | bytes 110600 | tf_op jit(solution)/shard_map/ppermute | solution.py:543
  23.4 3.2 %collective-permute-start.4 = (f32[72,128]{1,0:T(8,128)S(1)}, f32[72,128]{1,0:T(8,128)S(1)}, u32[]{:S(2)}, u32[]{:S(2)}) collective-permute-start(f32[72,128]{1,0:T(8,128)S(1)} %get-tuple-element.88.own), channel_id=1, source_target_pairs={{0,8},{8,0},{16,24},{24,16},{1,9},{9,1},{17,25},{25,17},{2,10},{10... | collective-permute-start | bytes 110600 | tf_op jit(solution)/shard_map/ppermute | solution.py:543
  26.7 7.8 %collective-permute-start.7 = (f32[40,128]{1,0:T(8,128)S(1)}, f32[40,128]{1,0:T(8,128)S(1)}, u32[]{:S(2)}, u32[]{:S(2)}) collective-permute-start(f32[40,128]{1,0:T(8,128)S(1)} %get-tuple-element.96), channel_id=1, source_target_pairs={{0,64},{64,0},{32,96},{96,32},{1,65},{65,1},{33,97},{97,33},{2,66}... | collective-permute-start | bytes 61448 | tf_op jit(solution)/shard_map/ppermute | solution.py:543
  30.4 4.1 %collective-permute-start.8 = (f32[40,128]{1,0:T(8,128)S(1)}, f32[40,128]{1,0:T(8,128)S(1)}, u32[]{:S(2)}, u32[]{:S(2)}) collective-permute-start(f32[40,128]{1,0:T(8,128)S(1)} %get-tuple-element.103), channel_id=1, source_target_pairs={{0,96},{96,0},{32,64},{64,32},{1,97},{97,1},{33,65},{65,33},{2,98}... | collective-permute-start | bytes 61448 | tf_op jit(solution)/shard_map/ppermute | solution.py:543
  30.8 3.7 %collective-permute-start.9 = (f32[40,128]{1,0:T(8,128)S(1)}, f32[40,128]{1,0:T(8,128)S(1)}, u32[]{:S(2)}, u32[]{:S(2)}) collective-permute-start(f32[40,128]{1,0:T(8,128)S(1)} %get-tuple-element.104), channel_id=1, source_target_pairs={{0,32},{32,0},{64,96},{96,64},{1,33},{33,1},{65,97},{97,65},{2,34}... | collective-permute-start | bytes 61448 | tf_op jit(solution)/shard_map/ppermute | solution.py:543
  34.6 5.8 %copy-start.1 = (f32[2048]{0:T(1024)S(1)}, f32[2048]{0:T(1024)}, u32[]{:S(2)}) copy-start(f32[2048]{0:T(1024)} %param.25) | copy-start | bytes 24580
  34.7 5.8 %copy-start.2 = (f32[1024]{0:T(1024)S(1)}, f32[1024]{0:T(1024)}, u32[]{:S(2)}) copy-start(f32[1024]{0:T(1024)} %param.21) | copy-start | bytes 12292
  34.7 5.8 %copy-start.3 = (f32[1024]{0:T(1024)S(1)}, f32[1024]{0:T(1024)}, u32[]{:S(2)}) copy-start(f32[1024]{0:T(1024)} %param.23) | copy-start | bytes 12292
  34.7 5.8 %collective-permute-start.10 = (f32[4,16,128]{2,1,0:T(8,128)S(1)}, f32[4,16,128]{2,1,0:T(8,128)S(1)}, u32[]{:S(2)}, u32[]{:S(2)}) collective-permute-start(f32[4,16,128]{2,1,0:T(8,128)S(1)} %get-tuple-element.111), channel_id=1, source_target_pairs={{0,1},{1,0},{2,3},{3,2},{4,5},{5,4},{6,7},{7,6},{8,9},{9,8},{10,11... | collective-permute-start | bytes 98312 | tf_op jit(solution)/shard_map/ppermute | solution.py:566

commit v11 on v10

--- a/solution.py
+++ b/solution.py
@@ -13,8 +13,10 @@
 D = 2048
 CHANNELS = 1024
 CHUNKS = 4
-LAG = 12
-DRIVE_AT = (6, 7, 8, 9, 13, 16, 19, 22, 29, 32, 35, 38, 45, 48, 51, 54)
+FINISH_AT = 24
+LAG = 6
+NORM_AT = 18
+DRIVE_AT = (18, 19, 20, 21, 22, 24, 26, 28, 30, 33, 36, 39, 41, 44, 47, 50)
 SPAN = 16
 SPANS = ROWS // SPAN
 SLOTS = 6
@@ -84,7 +86,7 @@
 
 def end_kernel(
     tokens, elapsed, gain, weight, inputs, angle, rate,
-    driven_ref, pairs_ref, ends_ref, pars_ref, damp_ref, within_ref, inputs_ref, normed, times, chunks, flipped, summed, pulls, weight_sems, input_sems,
+    driven_ref, pairs_ref, ends_ref, pars_ref, damp_ref, within_ref, inputs_ref, raw, normed, times, chunks, flipped, summed, pulls, weight_sems, input_sems, token_sem,
 ):
     core = lax.axis_index("c")
 
@@ -96,9 +98,19 @@
             pltpu.make_async_copy(inputs.at[:, :, pl.ds(16 * i, 16)], inputs_ref.at[:, :, pl.ds(16 * i, 16)], input_sems.at[i]),
         )
 
-    for i in range(CHUNKS):
-        for copy in fetch(i):
-            copy.start()
+    def norm():
+        token_copy.wait()
+        for r in range(0, ROWS, 16):
+            x = raw[r : r + 16, :].astype(F32)
+            scale = lax.rsqrt(jnp.mean(x * x, axis=-1, keepdims=True) + EPSILON)
+            normed[r : r + 16, :] = (x * scale * gain[...]).astype(BF16)
+
+    token_copy = pltpu.make_async_copy(tokens, raw, token_sem)
+    token_copy.start()
+    fetched = [fetch(i) for i in range(CHUNKS)]
+    for n in range(2):
+        for copies in fetched:
+            copies[n].start()
     steps = column_of(elapsed[...])
     parts = in_parts(steps)
     row, col = iotas((ROWS, ROWS))
@@ -111,16 +123,12 @@
     total = sums_of(jnp.ones((8, ROWS), F32), parts)
     ends_ref[0, 64:] = total
     ends_ref[1, 64:] = total
-    for r in range(0, ROWS, 16):
-        x = tokens[r : r + 16, :].astype(F32)
-        scale = lax.rsqrt(jnp.mean(x * x, axis=-1, keepdims=True) + EPSILON)
-        normed[r : r + 16, :] = (x * scale * gain[...]).astype(BF16)
     first = lax.broadcasted_iota(jnp.int32, (16, 128), 1) < 64
 
     def gather_in(step, quarter):
-        if quarter == 0:
-            for copy in fetch(step):
-                copy.wait()
+        if quarter == 0 and step == 0:
+            for copies in fetched:
+                copies[0].wait()
         cut = slice(512 * quarter, 512 * quarter + 512)
         value = mm(normed[:, cut], chunks[step, cut, :])
         summed[...] = value if quarter == 0 else summed[...] + value
@@ -146,11 +154,11 @@
         damp_ref[pair, k] = damp
         amp = jnp.exp2(after * (f * -LOG2E)) * damp
         tilted = amp * s
-        pulls[pair % 8, k, :, :128] = (amp - tilted * s).astype(BF16)
-        pulls[pair % 8, k, :, 128:] = (tilted * c).astype(BF16)
+        pulls[pair % 16, k, :, :128] = (amp - tilted * s).astype(BF16)
+        pulls[pair % 16, k, :, 128:] = (tilted * c).astype(BF16)
 
     def finish(pair, k):
-        mixed = mm(flipped[pair // 8 % 2, 32 * (pair % 8) : 32 * (pair % 8) + 32], pulls[pair % 8, k])
+        mixed = mm(flipped[pair // 8 % 2, 32 * (pair % 8) : 32 * (pair % 8) + 32], pulls[pair % 16, k])
         m_re = jnp.where(first, mixed[:16, :128], mixed[16:, :128])
         m_im = jnp.where(first, mixed[:16, 128:], mixed[16:, 128:])
         b_re, b_im = (
@@ -163,13 +171,21 @@
         ends_ref[away, at + 16 : at + 17, :] = jnp.sum(b_re * m_im + b_im * m_re, axis=0, keepdims=True)
 
     units = [(pair, k) for pair in range(32) for k in range(2)]
+    done = 0
     for n in range(len(units) + LAG):
+        if n == NORM_AT:
+            norm()
         if n in DRIVE_AT:
             gather_in(*divmod(DRIVE_AT.index(n), 4))
         if n < len(units):
             pull(*units[n])
-        if n >= LAG:
-            finish(*units[n - LAG])
+        if n == FINISH_AT:
+            for copies in fetched:
+                copies[1].wait()
+        for _ in range(2):
+            if done < len(units) and FINISH_AT <= n and done <= n - LAG:
+                finish(*units[done])
+                done += 1
 
 
 def shifted_rows(x, by, fill):
@@ -506,16 +522,16 @@
     driven, pairs, ends, pars, damps, within, inputs_here = pl.pallas_call(
         end_kernel,
         name="ends",
-        in_specs=[spec, spec, spec, distant, distant, spec, spec],
+        in_specs=[distant, spec, spec, distant, distant, spec, spec],
         out_specs=[spec] * 7,
         out_shape=[
             sds((ROWS, CHANNELS), BF16), sds((32, ROWS, 32), BF16), sds((2, 72, 128)), sds((2, 2, 32, 128)),
             sds((32, 2, ROWS, ROWS)), sds((2, ROWS, ROWS)), sds((2, 2, 64, 16, 64), BF16),
         ],
         scratch_shapes=[
-            VMEM((ROWS, D), BF16), VMEM((3, ROWS, ROWS), F32), VMEM((CHUNKS, D, 256), BF16), VMEM((2, 256, ROWS), BF16),
-            VMEM((ROWS, 256), F32), VMEM((8, 2, ROWS, 256), BF16),
-            pltpu.SemaphoreType.DMA((CHUNKS,)), pltpu.SemaphoreType.DMA((CHUNKS,)),
+            VMEM((ROWS, D), BF16), VMEM((ROWS, D), BF16), VMEM((3, ROWS, ROWS), F32), VMEM((CHUNKS, D, 256), BF16), VMEM((2, 256, ROWS), BF16),
+            VMEM((ROWS, 256), F32), VMEM((16, 2, ROWS, 256), BF16),
+            pltpu.SemaphoreType.DMA((CHUNKS,)), pltpu.SemaphoreType.DMA((CHUNKS,)), pltpu.SemaphoreType.DMA,
         ],
         compiler_params=params(12),
     )(

time: 43.9 us -> 43.4 us (0.989)
  no operation moved by 1% of the time
where the time goes in v11:
time: 43.4 us; the launch traced here: 43.3 us
  Pallas kernels  24.1 us (56%)
  starting transfers between devices  17.5 us (40%)
  waiting for transfers between devices  1.39 us (3%)
    ppermute x9, starting transfers between devices, trade(): lax.ppermute(values[n], axis, swaps[n])  12 us
    pallas_call x5, Pallas kernels, run_local(): pl.pallas_call(functools.partial(local_kernel, 4 * start, 4 * size, count...  11.3 us
    pallas_call x1, Pallas kernels, local(): pl.pallas_call(end_kernel, name='ends', in_specs=[distant, spec, spec, di...  9.13 us
    ppermute x1, starting transfers between devices, local(): other = piece_between(theirs, lax.ppermute(theirs, 'c', swap))  4.1 us
    pallas_call x1, Pallas kernels, local(): pl.pallas_call(final_kernel, name='final', in_specs=[spec] * len(args), o...  3.23 us
    ppermute x1, starting transfers between devices, local(): partner = piece_between(keep, lax.ppermute(ends[1], 'c', swap))  1.46 us
    ppermute x9, waiting for transfers between devices, trade(): lax.ppermute(values[n], axis, swaps[n])  1.39 us
  transfers between devices with their start and end apart: 11, of which 3 were waited for; matrix products, arithmetic and copies ran while one was open for 0% of the time, Pallas kernels for 26%

profile of v11, /device:TPU:1, one launch (start us, length us, event | category | flops | bytes accessed | tf_op | source)
XLA Modules:
  0.0 43.3 jit_solution(14024421553905795684)
XLA Ops:
  0.0 0.0 copy-start
  0.0 9.1 %ends.1 = (bf16[128,1024]{1,0:T(8,128)(2,1)S(1)}, bf16[32,128,32]{2,1,0:T(8,128)(2,1)S(1)}, f32[2,72,128]{2,1,0:T(8,128)S(1)}, f32[2,2,32,128]{3,2,1,0:T(8,128)S...) custom-call(bf16[128,2048]{1,0:T(8,128)(2,1)} %tokens.1, ...), custom_call_target="tpu_custom_call" | custom-call | tf_op jit(solution)/shard_map/ends/pallas_call | solution.py:522
  9.2 1.5 %collective-permute-start = (f32[72,128]{1,0:T(8,128)S(1)}, f32[72,128]{1,0:T(8,128)S(1)}, u32[]{:S(2)}, u32[]{:S(2)}) collective-permute-start(f32[72,128]{1,0:T(8,128)S(1)} %get-tuple-element.135), channel_id=1, source_target_pairs={{0,1},{1,0},{2,3},{3,2},{4,5},{5,4},{6,7},{7,6},{8,9},{9,8},{10,11... | collective-permute-start | bytes 110600 | tf_op jit(solution)/shard_map/ppermute | solution.py:564
  10.6 0.0 copy-done
  10.6 1.5 %local_0.1 = (f32[4,128,32]{2,1,0:T(8,128)S(1)}, bf16[4,2,128,256]{3,2,1,0:T(8,128)(2,1)S(1)}, f32[4,2,2,32,128]{4,3,2,1,0:T(8,128)S(1)}) custom-call(f32[2,128,128]{2,1,0:T(8,128)S(1)} %get-tuple-element.70.within, f32[32,2,128,128]{3,2,1,0:T(8,128)S(1)} %get-tuple-element.71.damps, bf16[32,128,32]{2,1,0:T(8,128)(2,1)S(1)} %get-tuple-element.112.driven, ...), custom_call_target="tpu_custom_call" | custom-call | flops 500000000 | bytes 2097152 | tf_op jit(solution)/shard_map/local_0/pallas_call | solution.py:480
  12.1 0.0 collective-permute-done.other
  12.2 3.1 %collective-permute-start.3 = (f32[72,128]{1,0:T(8,128)S(1)}, f32[72,128]{1,0:T(8,128)S(1)}, u32[]{:S(2)}, u32[]{:S(2)}) collective-permute-start(f32[72,128]{1,0:T(8,128)S(1)} %pair.1.own), channel_id=1, source_target_pairs={{0,4},{4,0},{2,6},{6,2},{1,5},{5,1},{3,7},{7,3},{8,12},{12,8},{10,... | collective-permute-start | bytes 110600 | tf_op jit(solution)/shard_map/ppermute | solution.py:559
  15.3 0.8 %collective-permute-start.2 = (f32[72,128]{1,0:T(8,128)S(1)}, f32[72,128]{1,0:T(8,128)S(1)}, u32[]{:S(2)}, u32[]{:S(2)}) collective-permute-start(f32[72,128]{1,0:T(8,128)S(1)} %pair.1.own), channel_id=1, source_target_pairs={{0,6},{6,0},{2,4},{4,2},{1,7},{7,1},{3,5},{5,3},{8,14},{14,8},{10,... | collective-permute-start | bytes 110600 | tf_op jit(solution)/shard_map/ppermute | solution.py:559
  16.0 0.0 collective-permute-start.1
  16.0 2.8 %local_1.1 = (f32[8,128,32]{2,1,0:T(8,128)S(1)}, bf16[8,2,128,256]{3,2,1,0:T(8,128)(2,1)S(1)}, f32[8,2,2,32,128]{4,3,2,1,0:T(8,128)S(1)}) custom-call(f32[2,128,128]{2,1,0:T(8,128)S(1)} %get-tuple-element.70.within, f32[32,2,128,128]{3,2,1,0:T(8,128)S(1)} %get-tuple-element.71.damps, bf16[32,128,32]{2,1,0:T(8,128)(2,1)S(1)} %get-tuple-element.112.driven, ...), custom_call_target="tpu_custom_call" | custom-call | flops 1000000000 | bytes 4194304 | tf_op jit(solution)/shard_map/local_1/pallas_call | solution.py:480
  18.8 0.0 collective-permute-done.3.two
  18.8 0.5 %collective-permute-done.2.three = f32[72,128]{1,0:T(8,128)S(1)} collective-permute-done((f32[72,128]{1,0:T(8,128)S(1)}, f32[72,128]{1,0:T(8,128)S(1)}, u32[]{:S(2)}, u32[]{:S(2)}) %collective-permute-start.2) | collective-permute-done | bytes 36896 | tf_op jit(solution)/shard_map/ppermute | solution.py:559
  19.3 0.0 collective-permute-done.1.one
  19.3 0.1 group_y.1
  19.4 2.8 %collective-permute-start.6 = (f32[72,128]{1,0:T(8,128)S(1)}, f32[72,128]{1,0:T(8,128)S(1)}, u32[]{:S(2)}, u32[]{:S(2)}) collective-permute-start(f32[72,128]{1,0:T(8,128)S(1)} %get-tuple-element.88.own), channel_id=1, source_target_pairs={{0,16},{16,0},{8,24},{24,8},{1,17},{17,1},{9,25},{25,9},{2,18},{18... | collective-permute-start | bytes 110600 | tf_op jit(solution)/shard_map/ppermute | solution.py:559
  22.2 0.9 %collective-permute-start.5 = (f32[72,128]{1,0:T(8,128)S(1)}, f32[72,128]{1,0:T(8,128)S(1)}, u32[]{:S(2)}, u32[]{:S(2)}) collective-permute-start(f32[72,128]{1,0:T(8,128)S(1)} %get-tuple-element.88.own), channel_id=1, source_target_pairs={{0,24},{24,0},{8,16},{16,8},{1,25},{25,1},{9,17},{17,9},{2,26},{26... | collective-permute-start | bytes 110600 | tf_op jit(solution)/shard_map/ppermute | solution.py:559
  23.1 0.0 collective-permute-start.4
  23.1 2.8 %local_3.1 = (f32[8,128,32]{2,1,0:T(8,128)S(1)}, bf16[8,2,128,256]{3,2,1,0:T(8,128)(2,1)S(1)}, f32[8,2,2,32,128]{4,3,2,1,0:T(8,128)S(1)}) custom-call(f32[2,128,128]{2,1,0:T(8,128)S(1)} %get-tuple-element.70.within, f32[32,2,128,128]{3,2,1,0:T(8,128)S(1)} %get-tuple-element.71.damps, bf16[32,128,32]{2,1,0:T(8,128)(2,1)S(1)} %get-tuple-element.112.driven, ...), custom_call_target="tpu_custom_call" | custom-call | flops 1000000000 | bytes 4194304 | tf_op jit(solution)/shard_map/local_3/pallas_call | solution.py:480
  25.9 0.0 collective-permute-done.6.two
  25.9 0.4 collective-permute-done.5.three
  26.3 0.0 collective-permute-done.4.one
  26.3 0.1 group_x.1
  26.4 3.7 %collective-permute-start.7 = (f32[40,128]{1,0:T(8,128)S(1)}, f32[40,128]{1,0:T(8,128)S(1)}, u32[]{:S(2)}, u32[]{:S(2)}) collective-permute-start(f32[40,128]{1,0:T(8,128)S(1)} %get-tuple-element.96), channel_id=1, source_target_pairs={{0,64},{64,0},{32,96},{96,32},{1,65},{65,1},{33,97},{97,33},{2,66}... | collective-permute-start | bytes 61448 | tf_op jit(solution)/shard_map/ppermute | solution.py:559
  30.1 0.4 %collective-permute-start.8 = (f32[40,128]{1,0:T(8,128)S(1)}, f32[40,128]{1,0:T(8,128)S(1)}, u32[]{:S(2)}, u32[]{:S(2)}) collective-permute-start(f32[40,128]{1,0:T(8,128)S(1)} %get-tuple-element.103), channel_id=1, source_target_pairs={{0,96},{96,0},{32,64},{64,32},{1,97},{97,1},{33,65},{65,33},{2,98}... | collective-permute-start | bytes 61448 | tf_op jit(solution)/shard_map/ppermute | solution.py:559
  30.5 0.3 collective-permute-start.9
  30.8 2.8 %local_5.1 = (f32[8,128,32]{2,1,0:T(8,128)S(1)}, bf16[8,2,128,256]{3,2,1,0:T(8,128)(2,1)S(1)}, f32[8,2,2,32,128]{4,3,2,1,0:T(8,128)S(1)}, bf16[1024,1024]{1,0:T(8,128)(2,1)S(1)}, bf16[1024,2048]{1,0:T(8,128)(2,1)S(1)}) custom-call(f32[2,128,128]{2,1,0:T(8,128)S(1)} %get-tuple-element.70.within, f32[32,2,128,128]{3,2,1,0:T(8,128)S(1)} %get-tuple-element.71.damps, ...), custom_call_target="tpu_custom_call" | custom-call | flops 1000000000 | bytes 4194304 | tf_op jit(solution)/shard_map/local_5/pallas_call | solution.py:480
  33.7 0.6 %collective-permute-done.8.three = f32[40,128]{1,0:T(8,128)S(1)} collective-permute-done((f32[40,128]{1,0:T(8,128)S(1)}, f32[40,128]{1,0:T(8,128)S(1)}, u32[]{:S(2)}, u32[]{:S(2)}) %collective-permute-start.8) | collective-permute-done | bytes 20512 | tf_op jit(solution)/shard_map/ppermute | solution.py:559
  34.2 0.0 collective-permute-done.9.one
  34.2 0.0 collective-permute-done.7.two
  34.2 0.1 enter.1
  34.4 0.0 copy-start.1
  34.4 0.0 copy-start.2
  34.4 0.0 copy-start.3
  34.4 4.1 %collective-permute-start.10 = (f32[4,16,128]{2,1,0:T(8,128)S(1)}, f32[4,16,128]{2,1,0:T(8,128)S(1)}, u32[]{:S(2)}, u32[]{:S(2)}) collective-permute-start(f32[4,16,128]{2,1,0:T(8,128)S(1)} %get-tuple-element.111), channel_id=1, source_target_pairs={{0,1},{1,0},{2,3},{3,2},{4,5},{5,4},{6,7},{7,6},{8,9},{9,8},{10,11... | collective-permute-start | bytes 98312 | tf_op jit(solution)/shard_map/ppermute | solution.py:582
  38.5 1.5 %local_7.1 = (f32[4,128,32]{2,1,0:T(8,128)S(1)}, bf16[4,2,128,256]{3,2,1,0:T(8,128)(2,1)S(1)}, f32[4,2,2,32,128]{4,3,2,1,0:T(8,128)S(1)}) custom-call(f32[2,128,128]{2,1,0:T(8,128)S(1)} %get-tuple-element.70.within, f32[32,2,128,128]{3,2,1,0:T(8,128)S(1)} %get-tuple-element.71.damps, bf16[32,128,32]{2,1,0:T(8,128)(2,1)S(1)} %get-tuple-element.112.driven, ...), custom_call_target="tpu_custom_call" | custom-call | flops 500000000 | bytes 2097152 | tf_op jit(solution)/shard_map/local_7/pallas_call | solution.py:480
  40.0 0.0 collective-permute-done.10.refs_1_
  40.0 0.0 copy-done.1
  40.0 0.0 copy-done.2
  40.0 0.0 copy-done.3
  40.0 3.2 %final.1 = bf16[128,2048]{1,0:T(8,128)(2,1)} custom-call(f32[4,16,128]{2,1,0:T(8,128)S(1)} %get-tuple-element.110.refs_0_, f32[4,16,128]{2,1,0:T(8,128)S(1)} %collective-permute-done.10.refs_1_, f32[4,128,32]{2,1,0:T(8,128)S(1)} %get-tuple-element.117.refs_2_, f32[8,128,32]{2,1,0:T(8,128)S(1)} %get-tuple-element.118.refs_3_, ...), custom_call_target="tpu_custom_call" | custom-call | tf_op jit(solution)/shard_map/final/pallas_call | solution.py:589
  (2 shorter events, 0.1 us)
Async XLA Ops:
  0.0 10.6 %copy-start = (f32[2,2,64,16,64]{4,3,2,1,0:T(8,128)S(1)}, f32[2,2,64,16,64]{4,3,2,1,0:T(8,128)}, u32[]{:S(2)}) copy-start(f32[2,2,64,16,64]{4,3,2,1,0:T(8,128)} %readout.9) | copy-start | bytes 3145732
  9.2 2.9 %collective-permute-start = (f32[72,128]{1,0:T(8,128)S(1)}, f32[72,128]{1,0:T(8,128)S(1)}, u32[]{:S(2)}, u32[]{:S(2)}) collective-permute-start(f32[72,128]{1,0:T(8,128)S(1)} %get-tuple-element.135), channel_id=1, source_target_pairs={{0,1},{1,0},{2,3},{3,2},{4,5},{5,4},{6,7},{7,6},{8,9},{9,8},{10,11... | collective-permute-start | bytes 110600 | tf_op jit(solution)/shard_map/ppermute | solution.py:564
  12.2 6.7 %collective-permute-start.3 = (f32[72,128]{1,0:T(8,128)S(1)}, f32[72,128]{1,0:T(8,128)S(1)}, u32[]{:S(2)}, u32[]{:S(2)}) collective-permute-start(f32[72,128]{1,0:T(8,128)S(1)} %pair.1.own), channel_id=1, source_target_pairs={{0,4},{4,0},{2,6},{6,2},{1,5},{5,1},{3,7},{7,3},{8,12},{12,8},{10,... | collective-permute-start | bytes 110600 | tf_op jit(solution)/shard_map/ppermute | solution.py:559
  15.3 4.0 %collective-permute-start.2 = (f32[72,128]{1,0:T(8,128)S(1)}, f32[72,128]{1,0:T(8,128)S(1)}, u32[]{:S(2)}, u32[]{:S(2)}) collective-permute-start(f32[72,128]{1,0:T(8,128)S(1)} %pair.1.own), channel_id=1, source_target_pairs={{0,6},{6,0},{2,4},{4,2},{1,7},{7,1},{3,5},{5,3},{8,14},{14,8},{10,... | collective-permute-start | bytes 110600 | tf_op jit(solution)/shard_map/ppermute | solution.py:559
  16.0 3.2 %collective-permute-start.1 = (f32[72,128]{1,0:T(8,128)S(1)}, f32[72,128]{1,0:T(8,128)S(1)}, u32[]{:S(2)}, u32[]{:S(2)}) collective-permute-start(f32[72,128]{1,0:T(8,128)S(1)} %pair.1.own), channel_id=1, source_target_pairs={{0,2},{2,0},{4,6},{6,4},{1,3},{3,1},{5,7},{7,5},{8,10},{10,8},{12,... | collective-permute-start | bytes 110600 | tf_op jit(solution)/shard_map/ppermute | solution.py:559
  19.4 6.5 %collective-permute-start.6 = (f32[72,128]{1,0:T(8,128)S(1)}, f32[72,128]{1,0:T(8,128)S(1)}, u32[]{:S(2)}, u32[]{:S(2)}) collective-permute-start(f32[72,128]{1,0:T(8,128)S(1)} %get-tuple-element.88.own), channel_id=1, source_target_pairs={{0,16},{16,0},{8,24},{24,8},{1,17},{17,1},{9,25},{25,9},{2,18},{18... | collective-permute-start | bytes 110600 | tf_op jit(solution)/shard_map/ppermute | solution.py:559
  22.2 4.0 %collective-permute-start.5 = (f32[72,128]{1,0:T(8,128)S(1)}, f32[72,128]{1,0:T(8,128)S(1)}, u32[]{:S(2)}, u32[]{:S(2)}) collective-permute-start(f32[72,128]{1,0:T(8,128)S(1)} %get-tuple-element.88.own), channel_id=1, source_target_pairs={{0,24},{24,0},{8,16},{16,8},{1,25},{25,1},{9,17},{17,9},{2,26},{26... | collective-permute-start | bytes 110600 | tf_op jit(solution)/shard_map/ppermute | solution.py:559
  23.1 3.2 %collective-permute-start.4 = (f32[72,128]{1,0:T(8,128)S(1)}, f32[72,128]{1,0:T(8,128)S(1)}, u32[]{:S(2)}, u32[]{:S(2)}) collective-permute-start(f32[72,128]{1,0:T(8,128)S(1)} %get-tuple-element.88.own), channel_id=1, source_target_pairs={{0,8},{8,0},{16,24},{24,16},{1,9},{9,1},{17,25},{25,17},{2,10},{10... | collective-permute-start | bytes 110600 | tf_op jit(solution)/shard_map/ppermute | solution.py:559
  26.4 7.8 %collective-permute-start.7 = (f32[40,128]{1,0:T(8,128)S(1)}, f32[40,128]{1,0:T(8,128)S(1)}, u32[]{:S(2)}, u32[]{:S(2)}) collective-permute-start(f32[40,128]{1,0:T(8,128)S(1)} %get-tuple-element.96), channel_id=1, source_target_pairs={{0,64},{64,0},{32,96},{96,32},{1,65},{65,1},{33,97},{97,33},{2,66}... | collective-permute-start | bytes 61448 | tf_op jit(solution)/shard_map/ppermute | solution.py:559
  30.1 4.1 %collective-permute-start.8 = (f32[40,128]{1,0:T(8,128)S(1)}, f32[40,128]{1,0:T(8,128)S(1)}, u32[]{:S(2)}, u32[]{:S(2)}) collective-permute-start(f32[40,128]{1,0:T(8,128)S(1)} %get-tuple-element.103), channel_id=1, source_target_pairs={{0,96},{96,0},{32,64},{64,32},{1,97},{97,1},{33,65},{65,33},{2,98}... | collective-permute-start | bytes 61448 | tf_op jit(solution)/shard_map/ppermute | solution.py:559
  30.5 3.7 %collective-permute-start.9 = (f32[40,128]{1,0:T(8,128)S(1)}, f32[40,128]{1,0:T(8,128)S(1)}, u32[]{:S(2)}, u32[]{:S(2)}) collective-permute-start(f32[40,128]{1,0:T(8,128)S(1)} %get-tuple-element.104), channel_id=1, source_target_pairs={{0,32},{32,0},{64,96},{96,64},{1,33},{33,1},{65,97},{97,65},{2,34}... | collective-permute-start | bytes 61448 | tf_op jit(solution)/shard_map/ppermute | solution.py:559
  34.4 5.6 %copy-start.1 = (f32[2048]{0:T(1024)S(1)}, f32[2048]{0:T(1024)}, u32[]{:S(2)}) copy-start(f32[2048]{0:T(1024)} %param.25) | copy-start | bytes 24580
  34.4 5.6 %copy-start.2 = (f32[1024]{0:T(1024)S(1)}, f32[1024]{0:T(1024)}, u32[]{:S(2)}) copy-start(f32[1024]{0:T(1024)} %param.21) | copy-start | bytes 12292
  34.4 5.6 %copy-start.3 = (f32[1024]{0:T(1024)S(1)}, f32[1024]{0:T(1024)}, u32[]{:S(2)}) copy-start(f32[1024]{0:T(1024)} %param.23) | copy-start | bytes 12292
  34.4 5.6 %collective-permute-start.10 = (f32[4,16,128]{2,1,0:T(8,128)S(1)}, f32[4,16,128]{2,1,0:T(8,128)S(1)}, u32[]{:S(2)}, u32[]{:S(2)}) collective-permute-start(f32[4,16,128]{2,1,0:T(8,128)S(1)} %get-tuple-element.111), channel_id=1, source_target_pairs={{0,1},{1,0},{2,3},{3,2},{4,5},{5,4},{6,7},{7,6},{8,9},{9,8},{10,11... | collective-permute-start | bytes 98312 | tf_op jit(solution)/shard_map/ppermute | solution.py:582

commit v12 on v11

--- a/solution.py
+++ b/solution.py
@@ -13,10 +13,10 @@
 D = 2048
 CHANNELS = 1024
 CHUNKS = 4
-FINISH_AT = 24
+FINISH_AT = 20
 LAG = 6
-NORM_AT = 18
-DRIVE_AT = (18, 19, 20, 21, 22, 24, 26, 28, 30, 33, 36, 39, 41, 44, 47, 50)
+NORM_AT = 14
+DRIVE_AT = (14, 15, 16, 17, 18, 20, 22, 24, 26, 29, 32, 35, 37, 40, 43, 46)
 SPAN = 16
 SPANS = ROWS // SPAN
 SLOTS = 6
@@ -429,7 +429,7 @@
     count = len(PIECES)
     own, other = refs[:2]
     nears, prefixes, tables = (refs[2 + count * n : 2 + count * n + count] for n in range(3))
-    driven, skip, glu, glu_bias, outw, out_gain, out_ref, entering, response = refs[2 + 3 * count :]
+    driven, skip, glu, glu_bias, outw, out_gain, out_ref, entering, response, staged, sems = refs[2 + 3 * count :]
     core = lax.axis_index("c")
     entering[core] = own[...]
     entering[1 - core] = other[...]
@@ -462,8 +462,15 @@
     gate = mm(active.astype(BF16), glu[...]) + glu_bias[...]
     gated = (active * jax.nn.sigmoid(gate)).astype(BF16)
     projected = mm(gated, outw[...])
-    scale = lax.rsqrt(jnp.mean(projected * projected, axis=-1, keepdims=True) + EPSILON)
-    out_ref[...] = (projected * scale * out_gain[...]).astype(BF16)
+    copies = []
+    for n, r in enumerate(range(0, ROWS, 32)):
+        rows = projected[r : r + 32, :]
+        scale = lax.rsqrt(jnp.mean(rows * rows, axis=-1, keepdims=True) + EPSILON)
+        staged[r : r + 32, :] = (rows * scale * out_gain[...]).astype(BF16)
+        copies.append(pltpu.make_async_copy(staged.at[r : r + 32, :], out_ref.at[r : r + 32, :], sems.at[n]))
+        copies[n].start()
+    for copy in copies:
+        copy.wait()
 
 
 def sds(shape, dtype=F32):
@@ -590,9 +597,12 @@
         final_kernel,
         name="final",
         in_specs=[spec] * len(args),
-        out_specs=spec,
+        out_specs=pl.BlockSpec(memory_space=pltpu.HBM),
         out_shape=sds((ROWS, D), BF16),
-        scratch_shapes=[VMEM((2, 4, 16, 128), F32), VMEM((ROWS, CHANNELS), F32)],
+        scratch_shapes=[
+            VMEM((2, 4, 16, 128), F32), VMEM((ROWS, CHANNELS), F32), VMEM((ROWS, D), BF16),
+            pltpu.SemaphoreType.DMA((4,)),
+        ],
         compiler_params=params(12),
     )(*args)
 

time: 43.4 us -> 43.7 us (level)
  no operation moved by 1% of the time
where the time goes in v12:
time: 43.7 us; the launch traced here: 43.6 us
  Pallas kernels  24.3 us (56%)
  starting transfers between devices  17.5 us (40%)
  waiting for transfers between devices  1.39 us (3%)
    ppermute x9, starting transfers between devices, trade(): lax.ppermute(values[n], axis, swaps[n])  12 us
    pallas_call x5, Pallas kernels, run_local(): pl.pallas_call(functools.partial(local_kernel, 4 * start, 4 * size, count...  11.3 us
    pallas_call x1, Pallas kernels, local(): pl.pallas_call(end_kernel, name='ends', in_specs=[distant, spec, spec, di...  9.35 us
    ppermute x1, starting transfers between devices, local(): other = piece_between(theirs, lax.ppermute(theirs, 'c', swap))  4.1 us
    pallas_call x1, Pallas kernels, local(): pl.pallas_call(final_kernel, name='final', in_specs=[spec] * len(args), o...  3.2 us
    ppermute x1, starting transfers between devices, local(): partner = piece_between(keep, lax.ppermute(ends[1], 'c', swap))  1.46 us
    ppermute x9, waiting for transfers between devices, trade(): lax.ppermute(values[n], axis, swaps[n])  1.39 us
  transfers between devices with their start and end apart: 11, of which 3 were waited for; matrix products, arithmetic and copies ran while one was open for 0% of the time, Pallas kernels for 26%

profile of v12, /device:TPU:1, one launch (start us, length us, event | category | flops | bytes accessed | tf_op | source)
XLA Modules:
  0.0 43.6 jit_solution(2420337660105227321)
XLA Ops:
  0.0 0.0 copy-start
  0.0 9.3 %ends.1 = (bf16[128,1024]{1,0:T(8,128)(2,1)S(1)}, bf16[32,128,32]{2,1,0:T(8,128)(2,1)S(1)}, f32[2,72,128]{2,1,0:T(8,128)S(1)}, f32[2,2,32,128]{3,2,1,0:T(8,128)S...) custom-call(bf16[128,2048]{1,0:T(8,128)(2,1)} %tokens.1, ...), custom_call_target="tpu_custom_call" | custom-call | tf_op jit(solution)/shard_map/ends/pallas_call | solution.py:529
  9.4 1.5 %collective-permute-start = (f32[72,128]{1,0:T(8,128)S(1)}, f32[72,128]{1,0:T(8,128)S(1)}, u32[]{:S(2)}, u32[]{:S(2)}) collective-permute-start(f32[72,128]{1,0:T(8,128)S(1)} %get-tuple-element.135), channel_id=1, source_target_pairs={{0,1},{1,0},{2,3},{3,2},{4,5},{5,4},{6,7},{7,6},{8,9},{9,8},{10,11... | collective-permute-start | bytes 110600 | tf_op jit(solution)/shard_map/ppermute | solution.py:571
  10.8 0.0 copy-done
  10.8 1.5 %local_0.1 = (f32[4,128,32]{2,1,0:T(8,128)S(1)}, bf16[4,2,128,256]{3,2,1,0:T(8,128)(2,1)S(1)}, f32[4,2,2,32,128]{4,3,2,1,0:T(8,128)S(1)}) custom-call(f32[2,128,128]{2,1,0:T(8,128)S(1)} %get-tuple-element.70.within, f32[32,2,128,128]{3,2,1,0:T(8,128)S(1)} %get-tuple-element.71.damps, bf16[32,128,32]{2,1,0:T(8,128)(2,1)S(1)} %get-tuple-element.112.driven, ...), custom_call_target="tpu_custom_call" | custom-call | flops 500000000 | bytes 2097152 | tf_op jit(solution)/shard_map/local_0/pallas_call | solution.py:487
  12.3 0.0 collective-permute-done.other
  12.4 3.1 %collective-permute-start.3 = (f32[72,128]{1,0:T(8,128)S(1)}, f32[72,128]{1,0:T(8,128)S(1)}, u32[]{:S(2)}, u32[]{:S(2)}) collective-permute-start(f32[72,128]{1,0:T(8,128)S(1)} %pair.1.own), channel_id=1, source_target_pairs={{0,4},{4,0},{2,6},{6,2},{1,5},{5,1},{3,7},{7,3},{8,12},{12,8},{10,... | collective-permute-start | bytes 110600 | tf_op jit(solution)/shard_map/ppermute | solution.py:566
  15.5 0.8 %collective-permute-start.2 = (f32[72,128]{1,0:T(8,128)S(1)}, f32[72,128]{1,0:T(8,128)S(1)}, u32[]{:S(2)}, u32[]{:S(2)}) collective-permute-start(f32[72,128]{1,0:T(8,128)S(1)} %pair.1.own), channel_id=1, source_target_pairs={{0,6},{6,0},{2,4},{4,2},{1,7},{7,1},{3,5},{5,3},{8,14},{14,8},{10,... | collective-permute-start | bytes 110600 | tf_op jit(solution)/shard_map/ppermute | solution.py:566
  16.3 0.0 collective-permute-start.1
  16.3 2.8 %local_1.1 = (f32[8,128,32]{2,1,0:T(8,128)S(1)}, bf16[8,2,128,256]{3,2,1,0:T(8,128)(2,1)S(1)}, f32[8,2,2,32,128]{4,3,2,1,0:T(8,128)S(1)}) custom-call(f32[2,128,128]{2,1,0:T(8,128)S(1)} %get-tuple-element.70.within, f32[32,2,128,128]{3,2,1,0:T(8,128)S(1)} %get-tuple-element.71.damps, bf16[32,128,32]{2,1,0:T(8,128)(2,1)S(1)} %get-tuple-element.112.driven, ...), custom_call_target="tpu_custom_call" | custom-call | flops 1000000000 | bytes 4194304 | tf_op jit(solution)/shard_map/local_1/pallas_call | solution.py:487
  19.0 0.0 collective-permute-done.3.two
  19.0 0.5 %collective-permute-done.2.three = f32[72,128]{1,0:T(8,128)S(1)} collective-permute-done((f32[72,128]{1,0:T(8,128)S(1)}, f32[72,128]{1,0:T(8,128)S(1)}, u32[]{:S(2)}, u32[]{:S(2)}) %collective-permute-start.2) | collective-permute-done | bytes 36896 | tf_op jit(solution)/shard_map/ppermute | solution.py:566
  19.5 0.0 collective-permute-done.1.one
  19.5 0.1 group_y.1
  19.6 2.8 %collective-permute-start.6 = (f32[72,128]{1,0:T(8,128)S(1)}, f32[72,128]{1,0:T(8,128)S(1)}, u32[]{:S(2)}, u32[]{:S(2)}) collective-permute-start(f32[72,128]{1,0:T(8,128)S(1)} %get-tuple-element.88.own), channel_id=1, source_target_pairs={{0,16},{16,0},{8,24},{24,8},{1,17},{17,1},{9,25},{25,9},{2,18},{18... | collective-permute-start | bytes 110600 | tf_op jit(solution)/shard_map/ppermute | solution.py:566
  22.5 0.9 %collective-permute-start.5 = (f32[72,128]{1,0:T(8,128)S(1)}, f32[72,128]{1,0:T(8,128)S(1)}, u32[]{:S(2)}, u32[]{:S(2)}) collective-permute-start(f32[72,128]{1,0:T(8,128)S(1)} %get-tuple-element.88.own), channel_id=1, source_target_pairs={{0,24},{24,0},{8,16},{16,8},{1,25},{25,1},{9,17},{17,9},{2,26},{26... | collective-permute-start | bytes 110600 | tf_op jit(solution)/shard_map/ppermute | solution.py:566
  23.3 0.0 collective-permute-start.4
  23.3 2.8 %local_3.1 = (f32[8,128,32]{2,1,0:T(8,128)S(1)}, bf16[8,2,128,256]{3,2,1,0:T(8,128)(2,1)S(1)}, f32[8,2,2,32,128]{4,3,2,1,0:T(8,128)S(1)}) custom-call(f32[2,128,128]{2,1,0:T(8,128)S(1)} %get-tuple-element.70.within, f32[32,2,128,128]{3,2,1,0:T(8,128)S(1)} %get-tuple-element.71.damps, bf16[32,128,32]{2,1,0:T(8,128)(2,1)S(1)} %get-tuple-element.112.driven, ...), custom_call_target="tpu_custom_call" | custom-call | flops 1000000000 | bytes 4194304 | tf_op jit(solution)/shard_map/local_3/pallas_call | solution.py:487
  26.1 0.0 collective-permute-done.6.two
  26.1 0.4 collective-permute-done.5.three
  26.5 0.0 collective-permute-done.4.one
  26.5 0.1 group_x.1
  26.6 3.7 %collective-permute-start.7 = (f32[40,128]{1,0:T(8,128)S(1)}, f32[40,128]{1,0:T(8,128)S(1)}, u32[]{:S(2)}, u32[]{:S(2)}) collective-permute-start(f32[40,128]{1,0:T(8,128)S(1)} %get-tuple-element.96), channel_id=1, source_target_pairs={{0,64},{64,0},{32,96},{96,32},{1,65},{65,1},{33,97},{97,33},{2,66}... | collective-permute-start | bytes 61448 | tf_op jit(solution)/shard_map/ppermute | solution.py:566
  30.3 0.4 collective-permute-start.8
  30.7 0.3 collective-permute-start.9
  31.0 2.8 %local_5.1 = (f32[8,128,32]{2,1,0:T(8,128)S(1)}, bf16[8,2,128,256]{3,2,1,0:T(8,128)(2,1)S(1)}, f32[8,2,2,32,128]{4,3,2,1,0:T(8,128)S(1)}, bf16[1024,1024]{1,0:T(8,128)(2,1)S(1)}, bf16[1024,2048]{1,0:T(8,128)(2,1)S(1)}) custom-call(f32[2,128,128]{2,1,0:T(8,128)S(1)} %get-tuple-element.70.within, f32[32,2,128,128]{3,2,1,0:T(8,128)S(1)} %get-tuple-element.71.damps, ...), custom_call_target="tpu_custom_call" | custom-call | flops 1000000000 | bytes 4194304 | tf_op jit(solution)/shard_map/local_5/pallas_call | solution.py:487
  33.9 0.6 %collective-permute-done.8.three = f32[40,128]{1,0:T(8,128)S(1)} collective-permute-done((f32[40,128]{1,0:T(8,128)S(1)}, f32[40,128]{1,0:T(8,128)S(1)}, u32[]{:S(2)}, u32[]{:S(2)}) %collective-permute-start.8) | collective-permute-done | bytes 20512 | tf_op jit(solution)/shard_map/ppermute | solution.py:566
  34.4 0.0 collective-permute-done.9.one
  34.5 0.0 collective-permute-done.7.two
  34.5 0.1 enter.1
  34.6 0.0 copy-start.1
  34.6 0.0 copy-start.2
  34.6 0.0 copy-start.3
  34.6 4.1 %collective-permute-start.10 = (f32[4,16,128]{2,1,0:T(8,128)S(1)}, f32[4,16,128]{2,1,0:T(8,128)S(1)}, u32[]{:S(2)}, u32[]{:S(2)}) collective-permute-start(f32[4,16,128]{2,1,0:T(8,128)S(1)} %get-tuple-element.111), channel_id=1, source_target_pairs={{0,1},{1,0},{2,3},{3,2},{4,5},{5,4},{6,7},{7,6},{8,9},{9,8},{10,11... | collective-permute-start | bytes 98312 | tf_op jit(solution)/shard_map/ppermute | solution.py:589
  38.7 1.5 %local_7.1 = (f32[4,128,32]{2,1,0:T(8,128)S(1)}, bf16[4,2,128,256]{3,2,1,0:T(8,128)(2,1)S(1)}, f32[4,2,2,32,128]{4,3,2,1,0:T(8,128)S(1)}) custom-call(f32[2,128,128]{2,1,0:T(8,128)S(1)} %get-tuple-element.70.within, f32[32,2,128,128]{3,2,1,0:T(8,128)S(1)} %get-tuple-element.71.damps, bf16[32,128,32]{2,1,0:T(8,128)(2,1)S(1)} %get-tuple-element.112.driven, ...), custom_call_target="tpu_custom_call" | custom-call | flops 500000000 | bytes 2097152 | tf_op jit(solution)/shard_map/local_7/pallas_call | solution.py:487
  40.2 0.0 collective-permute-done.10.refs_1_
  40.2 0.0 copy-done.1
  40.2 0.0 copy-done.2
  40.2 0.0 copy-done.3
  40.2 3.2 %final.1 = bf16[128,2048]{1,0:T(8,128)(2,1)} custom-call(f32[4,16,128]{2,1,0:T(8,128)S(1)} %get-tuple-element.110.refs_0_, f32[4,16,128]{2,1,0:T(8,128)S(1)} %collective-permute-done.10.refs_1_, f32[4,128,32]{2,1,0:T(8,128)S(1)} %get-tuple-element.117.refs_2_, f32[8,128,32]{2,1,0:T(8,128)S(1)} %get-tuple-element.118.refs_3_, ...), custom_call_target="tpu_custom_call" | custom-call | tf_op jit(solution)/shard_map/final/pallas_call | solution.py:596
  (2 shorter events, 0.1 us)
Async XLA Ops:
  0.0 10.8 %copy-start = (f32[2,2,64,16,64]{4,3,2,1,0:T(8,128)S(1)}, f32[2,2,64,16,64]{4,3,2,1,0:T(8,128)}, u32[]{:S(2)}) copy-start(f32[2,2,64,16,64]{4,3,2,1,0:T(8,128)} %readout.9) | copy-start | bytes 3145732
  9.4 2.9 %collective-permute-start = (f32[72,128]{1,0:T(8,128)S(1)}, f32[72,128]{1,0:T(8,128)S(1)}, u32[]{:S(2)}, u32[]{:S(2)}) collective-permute-start(f32[72,128]{1,0:T(8,128)S(1)} %get-tuple-element.135), channel_id=1, source_target_pairs={{0,1},{1,0},{2,3},{3,2},{4,5},{5,4},{6,7},{7,6},{8,9},{9,8},{10,11... | collective-permute-start | bytes 110600 | tf_op jit(solution)/shard_map/ppermute | solution.py:571
  12.4 6.7 %collective-permute-start.3 = (f32[72,128]{1,0:T(8,128)S(1)}, f32[72,128]{1,0:T(8,128)S(1)}, u32[]{:S(2)}, u32[]{:S(2)}) collective-permute-start(f32[72,128]{1,0:T(8,128)S(1)} %pair.1.own), channel_id=1, source_target_pairs={{0,4},{4,0},{2,6},{6,2},{1,5},{5,1},{3,7},{7,3},{8,12},{12,8},{10,... | collective-permute-start | bytes 110600 | tf_op jit(solution)/shard_map/ppermute | solution.py:566
  15.5 4.0 %collective-permute-start.2 = (f32[72,128]{1,0:T(8,128)S(1)}, f32[72,128]{1,0:T(8,128)S(1)}, u32[]{:S(2)}, u32[]{:S(2)}) collective-permute-start(f32[72,128]{1,0:T(8,128)S(1)} %pair.1.own), channel_id=1, source_target_pairs={{0,6},{6,0},{2,4},{4,2},{1,7},{7,1},{3,5},{5,3},{8,14},{14,8},{10,... | collective-permute-start | bytes 110600 | tf_op jit(solution)/shard_map/ppermute | solution.py:566
  16.3 3.2 %collective-permute-start.1 = (f32[72,128]{1,0:T(8,128)S(1)}, f32[72,128]{1,0:T(8,128)S(1)}, u32[]{:S(2)}, u32[]{:S(2)}) collective-permute-start(f32[72,128]{1,0:T(8,128)S(1)} %pair.1.own), channel_id=1, source_target_pairs={{0,2},{2,0},{4,6},{6,4},{1,3},{3,1},{5,7},{7,5},{8,10},{10,8},{12,... | collective-permute-start | bytes 110600 | tf_op jit(solution)/shard_map/ppermute | solution.py:566
  19.6 6.5 %collective-permute-start.6 = (f32[72,128]{1,0:T(8,128)S(1)}, f32[72,128]{1,0:T(8,128)S(1)}, u32[]{:S(2)}, u32[]{:S(2)}) collective-permute-start(f32[72,128]{1,0:T(8,128)S(1)} %get-tuple-element.88.own), channel_id=1, source_target_pairs={{0,16},{16,0},{8,24},{24,8},{1,17},{17,1},{9,25},{25,9},{2,18},{18... | collective-permute-start | bytes 110600 | tf_op jit(solution)/shard_map/ppermute | solution.py:566
  22.5 4.0 %collective-permute-start.5 = (f32[72,128]{1,0:T(8,128)S(1)}, f32[72,128]{1,0:T(8,128)S(1)}, u32[]{:S(2)}, u32[]{:S(2)}) collective-permute-start(f32[72,128]{1,0:T(8,128)S(1)} %get-tuple-element.88.own), channel_id=1, source_target_pairs={{0,24},{24,0},{8,16},{16,8},{1,25},{25,1},{9,17},{17,9},{2,26},{26... | collective-permute-start | bytes 110600 | tf_op jit(solution)/shard_map/ppermute | solution.py:566
  23.3 3.2 %collective-permute-start.4 = (f32[72,128]{1,0:T(8,128)S(1)}, f32[72,128]{1,0:T(8,128)S(1)}, u32[]{:S(2)}, u32[]{:S(2)}) collective-permute-start(f32[72,128]{1,0:T(8,128)S(1)} %get-tuple-element.88.own), channel_id=1, source_target_pairs={{0,8},{8,0},{16,24},{24,16},{1,9},{9,1},{17,25},{25,17},{2,10},{10... | collective-permute-start | bytes 110600 | tf_op jit(solution)/shard_map/ppermute | solution.py:566
  26.6 7.8 %collective-permute-start.7 = (f32[40,128]{1,0:T(8,128)S(1)}, f32[40,128]{1,0:T(8,128)S(1)}, u32[]{:S(2)}, u32[]{:S(2)}) collective-permute-start(f32[40,128]{1,0:T(8,128)S(1)} %get-tuple-element.96), channel_id=1, source_target_pairs={{0,64},{64,0},{32,96},{96,32},{1,65},{65,1},{33,97},{97,33},{2,66}... | collective-permute-start | bytes 61448 | tf_op jit(solution)/shard_map/ppermute | solution.py:566
  30.3 4.1 %collective-permute-start.8 = (f32[40,128]{1,0:T(8,128)S(1)}, f32[40,128]{1,0:T(8,128)S(1)}, u32[]{:S(2)}, u32[]{:S(2)}) collective-permute-start(f32[40,128]{1,0:T(8,128)S(1)} %get-tuple-element.103), channel_id=1, source_target_pairs={{0,96},{96,0},{32,64},{64,32},{1,97},{97,1},{33,65},{65,33},{2,98}... | collective-permute-start | bytes 61448 | tf_op jit(solution)/shard_map/ppermute | solution.py:566
  30.7 3.7 %collective-permute-start.9 = (f32[40,128]{1,0:T(8,128)S(1)}, f32[40,128]{1,0:T(8,128)S(1)}, u32[]{:S(2)}, u32[]{:S(2)}) collective-permute-start(f32[40,128]{1,0:T(8,128)S(1)} %get-tuple-element.104), channel_id=1, source_target_pairs={{0,32},{32,0},{64,96},{96,64},{1,33},{33,1},{65,97},{97,65},{2,34}... | collective-permute-start | bytes 61448 | tf_op jit(solution)/shard_map/ppermute | solution.py:566
  34.6 5.6 %copy-start.1 = (f32[2048]{0:T(1024)S(1)}, f32[2048]{0:T(1024)}, u32[]{:S(2)}) copy-start(f32[2048]{0:T(1024)} %param.25) | copy-start | bytes 24580
  34.6 5.6 %copy-start.2 = (f32[1024]{0:T(1024)S(1)}, f32[1024]{0:T(1024)}, u32[]{:S(2)}) copy-start(f32[1024]{0:T(1024)} %param.21) | copy-start | bytes 12292
  34.6 5.6 %copy-start.3 = (f32[1024]{0:T(1024)S(1)}, f32[1024]{0:T(1024)}, u32[]{:S(2)}) copy-start(f32[1024]{0:T(1024)} %param.23) | copy-start | bytes 12292
  34.6 5.6 %collective-permute-start.10 = (f32[4,16,128]{2,1,0:T(8,128)S(1)}, f32[4,16,128]{2,1,0:T(8,128)S(1)}, u32[]{:S(2)}, u32[]{:S(2)}) collective-permute-start(f32[4,16,128]{2,1,0:T(8,128)S(1)} %get-tuple-element.111), channel_id=1, source_target_pairs={{0,1},{1,0},{2,3},{3,2},{4,5},{5,4},{6,7},{7,6},{8,9},{9,8},{10,11... | collective-permute-start | bytes 98312 | tf_op jit(solution)/shard_map/ppermute | solution.py:589

commit v13 on v12

--- a/solution.py
+++ b/solution.py
@@ -13,10 +13,10 @@
 D = 2048
 CHANNELS = 1024
 CHUNKS = 4
-FINISH_AT = 20
+FINISH_AT = 30
 LAG = 6
-NORM_AT = 14
-DRIVE_AT = (14, 15, 16, 17, 18, 20, 22, 24, 26, 29, 32, 35, 37, 40, 43, 46)
+NORM_AT = 24
+DRIVE_AT = (24, 25, 26, 27, 28, 30, 32, 34, 36, 38, 40, 42, 46, 48, 50, 52)
 SPAN = 16
 SPANS = ROWS // SPAN
 SLOTS = 6

time: 43.7 us -> 43.7 us (level)
  no operation moved by 1% of the time
where the time goes in v13:
time: 43.7 us; the launch traced here: 43.6 us
  Pallas kernels  24.3 us (56%)
  starting transfers between devices  17.5 us (40%)
  waiting for transfers between devices  1.38 us (3%)
    ppermute x9, starting transfers between devices, trade(): lax.ppermute(values[n], axis, swaps[n])  12 us
    pallas_call x5, Pallas kernels, run_local(): pl.pallas_call(functools.partial(local_kernel, 4 * start, 4 * size, count...  11.3 us
    pallas_call x1, Pallas kernels, local(): pl.pallas_call(end_kernel, name='ends', in_specs=[distant, spec, spec, di...  9.3 us
    ppermute x1, starting transfers between devices, local(): other = piece_between(theirs, lax.ppermute(theirs, 'c', swap))  4.1 us
    pallas_call x1, Pallas kernels, local(): pl.pallas_call(final_kernel, name='final', in_specs=[spec] * len(args), o...  3.2 us
    ppermute x1, starting transfers between devices, local(): partner = piece_between(keep, lax.ppermute(ends[1], 'c', swap))  1.46 us
    ppermute x9, waiting for transfers between devices, trade(): lax.ppermute(values[n], axis, swaps[n])  1.37 us
  transfers between devices with their start and end apart: 11, of which 3 were waited for; matrix products, arithmetic and copies ran while one was open for 0% of the time, Pallas kernels for 26%

profile of v13, /device:TPU:1, one launch (start us, length us, event | category | flops | bytes accessed | tf_op | source)
XLA Modules:
  0.0 43.6 jit_solution(14433409532230157037)
XLA Ops:
  0.0 0.0 copy-start
  0.0 9.3 %ends.1 = (bf16[128,1024]{1,0:T(8,128)(2,1)S(1)}, bf16[32,128,32]{2,1,0:T(8,128)(2,1)S(1)}, f32[2,72,128]{2,1,0:T(8,128)S(1)}, f32[2,2,32,128]{3,2,1,0:T(8,128)S...) custom-call(bf16[128,2048]{1,0:T(8,128)(2,1)} %tokens.1, ...), custom_call_target="tpu_custom_call" | custom-call | tf_op jit(solution)/shard_map/ends/pallas_call | solution.py:529
  9.3 1.5 %collective-permute-start = (f32[72,128]{1,0:T(8,128)S(1)}, f32[72,128]{1,0:T(8,128)S(1)}, u32[]{:S(2)}, u32[]{:S(2)}) collective-permute-start(f32[72,128]{1,0:T(8,128)S(1)} %get-tuple-element.135), channel_id=1, source_target_pairs={{0,1},{1,0},{2,3},{3,2},{4,5},{5,4},{6,7},{7,6},{8,9},{9,8},{10,11... | collective-permute-start | bytes 110600 | tf_op jit(solution)/shard_map/ppermute | solution.py:571
  10.8 0.0 copy-done
  10.8 1.5 %local_0.1 = (f32[4,128,32]{2,1,0:T(8,128)S(1)}, bf16[4,2,128,256]{3,2,1,0:T(8,128)(2,1)S(1)}, f32[4,2,2,32,128]{4,3,2,1,0:T(8,128)S(1)}) custom-call(f32[2,128,128]{2,1,0:T(8,128)S(1)} %get-tuple-element.70.within, f32[32,2,128,128]{3,2,1,0:T(8,128)S(1)} %get-tuple-element.71.damps, bf16[32,128,32]{2,1,0:T(8,128)(2,1)S(1)} %get-tuple-element.112.driven, ...), custom_call_target="tpu_custom_call" | custom-call | flops 500000000 | bytes 2097152 | tf_op jit(solution)/shard_map/local_0/pallas_call | solution.py:487
  12.3 0.0 collective-permute-done.other
  12.3 3.1 %collective-permute-start.3 = (f32[72,128]{1,0:T(8,128)S(1)}, f32[72,128]{1,0:T(8,128)S(1)}, u32[]{:S(2)}, u32[]{:S(2)}) collective-permute-start(f32[72,128]{1,0:T(8,128)S(1)} %pair.1.own), channel_id=1, source_target_pairs={{0,4},{4,0},{2,6},{6,2},{1,5},{5,1},{3,7},{7,3},{8,12},{12,8},{10,... | collective-permute-start | bytes 110600 | tf_op jit(solution)/shard_map/ppermute | solution.py:566
  15.4 0.8 %collective-permute-start.2 = (f32[72,128]{1,0:T(8,128)S(1)}, f32[72,128]{1,0:T(8,128)S(1)}, u32[]{:S(2)}, u32[]{:S(2)}) collective-permute-start(f32[72,128]{1,0:T(8,128)S(1)} %pair.1.own), channel_id=1, source_target_pairs={{0,6},{6,0},{2,4},{4,2},{1,7},{7,1},{3,5},{5,3},{8,14},{14,8},{10,... | collective-permute-start | bytes 110600 | tf_op jit(solution)/shard_map/ppermute | solution.py:566
  16.2 0.0 collective-permute-start.1
  16.2 2.8 %local_1.1 = (f32[8,128,32]{2,1,0:T(8,128)S(1)}, bf16[8,2,128,256]{3,2,1,0:T(8,128)(2,1)S(1)}, f32[8,2,2,32,128]{4,3,2,1,0:T(8,128)S(1)}) custom-call(f32[2,128,128]{2,1,0:T(8,128)S(1)} %get-tuple-element.70.within, f32[32,2,128,128]{3,2,1,0:T(8,128)S(1)} %get-tuple-element.71.damps, bf16[32,128,32]{2,1,0:T(8,128)(2,1)S(1)} %get-tuple-element.112.driven, ...), custom_call_target="tpu_custom_call" | custom-call | flops 1000000000 | bytes 4194304 | tf_op jit(solution)/shard_map/local_1/pallas_call | solution.py:487
  19.0 0.0 collective-permute-done.3.two
  19.0 0.4 %collective-permute-done.2.three = f32[72,128]{1,0:T(8,128)S(1)} collective-permute-done((f32[72,128]{1,0:T(8,128)S(1)}, f32[72,128]{1,0:T(8,128)S(1)}, u32[]{:S(2)}, u32[]{:S(2)}) %collective-permute-start.2) | collective-permute-done | bytes 36896 | tf_op jit(solution)/shard_map/ppermute | solution.py:566
  19.5 0.0 collective-permute-done.1.one
  19.5 0.1 group_y.1
  19.6 2.8 %collective-permute-start.6 = (f32[72,128]{1,0:T(8,128)S(1)}, f32[72,128]{1,0:T(8,128)S(1)}, u32[]{:S(2)}, u32[]{:S(2)}) collective-permute-start(f32[72,128]{1,0:T(8,128)S(1)} %get-tuple-element.88.own), channel_id=1, source_target_pairs={{0,16},{16,0},{8,24},{24,8},{1,17},{17,1},{9,25},{25,9},{2,18},{18... | collective-permute-start | bytes 110600 | tf_op jit(solution)/shard_map/ppermute | solution.py:566
  22.4 0.9 %collective-permute-start.5 = (f32[72,128]{1,0:T(8,128)S(1)}, f32[72,128]{1,0:T(8,128)S(1)}, u32[]{:S(2)}, u32[]{:S(2)}) collective-permute-start(f32[72,128]{1,0:T(8,128)S(1)} %get-tuple-element.88.own), channel_id=1, source_target_pairs={{0,24},{24,0},{8,16},{16,8},{1,25},{25,1},{9,17},{17,9},{2,26},{26... | collective-permute-start | bytes 110600 | tf_op jit(solution)/shard_map/ppermute | solution.py:566
  23.3 0.0 collective-permute-start.4
  23.3 2.8 %local_3.1 = (f32[8,128,32]{2,1,0:T(8,128)S(1)}, bf16[8,2,128,256]{3,2,1,0:T(8,128)(2,1)S(1)}, f32[8,2,2,32,128]{4,3,2,1,0:T(8,128)S(1)}) custom-call(f32[2,128,128]{2,1,0:T(8,128)S(1)} %get-tuple-element.70.within, f32[32,2,128,128]{3,2,1,0:T(8,128)S(1)} %get-tuple-element.71.damps, bf16[32,128,32]{2,1,0:T(8,128)(2,1)S(1)} %get-tuple-element.112.driven, ...), custom_call_target="tpu_custom_call" | custom-call | flops 1000000000 | bytes 4194304 | tf_op jit(solution)/shard_map/local_3/pallas_call | solution.py:487
  26.1 0.0 collective-permute-done.6.two
  26.1 0.4 collective-permute-done.5.three
  26.4 0.0 collective-permute-done.4.one
  26.4 0.1 group_x.1
  26.6 3.7 %collective-permute-start.7 = (f32[40,128]{1,0:T(8,128)S(1)}, f32[40,128]{1,0:T(8,128)S(1)}, u32[]{:S(2)}, u32[]{:S(2)}) collective-permute-start(f32[40,128]{1,0:T(8,128)S(1)} %get-tuple-element.96), channel_id=1, source_target_pairs={{0,64},{64,0},{32,96},{96,32},{1,65},{65,1},{33,97},{97,33},{2,66}... | collective-permute-start | bytes 61448 | tf_op jit(solution)/shard_map/ppermute | solution.py:566
  30.3 0.4 collective-permute-start.8
  30.7 0.3 collective-permute-start.9
  31.0 2.8 %local_5.1 = (f32[8,128,32]{2,1,0:T(8,128)S(1)}, bf16[8,2,128,256]{3,2,1,0:T(8,128)(2,1)S(1)}, f32[8,2,2,32,128]{4,3,2,1,0:T(8,128)S(1)}, bf16[1024,1024]{1,0:T(8,128)(2,1)S(1)}, bf16[1024,2048]{1,0:T(8,128)(2,1)S(1)}) custom-call(f32[2,128,128]{2,1,0:T(8,128)S(1)} %get-tuple-element.70.within, f32[32,2,128,128]{3,2,1,0:T(8,128)S(1)} %get-tuple-element.71.damps, ...), custom_call_target="tpu_custom_call" | custom-call | flops 1000000000 | bytes 4194304 | tf_op jit(solution)/shard_map/local_5/pallas_call | solution.py:487
  33.9 0.5 %collective-permute-done.8.three = f32[40,128]{1,0:T(8,128)S(1)} collective-permute-done((f32[40,128]{1,0:T(8,128)S(1)}, f32[40,128]{1,0:T(8,128)S(1)}, u32[]{:S(2)}, u32[]{:S(2)}) %collective-permute-start.8) | collective-permute-done | bytes 20512 | tf_op jit(solution)/shard_map/ppermute | solution.py:566
  34.4 0.0 collective-permute-done.9.one
  34.4 0.0 collective-permute-done.7.two
  34.4 0.1 enter.1
  34.5 0.0 copy-start.1
  34.6 0.0 copy-start.2
  34.6 0.0 copy-start.3
  34.6 4.1 %collective-permute-start.10 = (f32[4,16,128]{2,1,0:T(8,128)S(1)}, f32[4,16,128]{2,1,0:T(8,128)S(1)}, u32[]{:S(2)}, u32[]{:S(2)}) collective-permute-start(f32[4,16,128]{2,1,0:T(8,128)S(1)} %get-tuple-element.111), channel_id=1, source_target_pairs={{0,1},{1,0},{2,3},{3,2},{4,5},{5,4},{6,7},{7,6},{8,9},{9,8},{10,11... | collective-permute-start | bytes 98312 | tf_op jit(solution)/shard_map/ppermute | solution.py:589
  38.7 1.5 %local_7.1 = (f32[4,128,32]{2,1,0:T(8,128)S(1)}, bf16[4,2,128,256]{3,2,1,0:T(8,128)(2,1)S(1)}, f32[4,2,2,32,128]{4,3,2,1,0:T(8,128)S(1)}) custom-call(f32[2,128,128]{2,1,0:T(8,128)S(1)} %get-tuple-element.70.within, f32[32,2,128,128]{3,2,1,0:T(8,128)S(1)} %get-tuple-element.71.damps, bf16[32,128,32]{2,1,0:T(8,128)(2,1)S(1)} %get-tuple-element.112.driven, ...), custom_call_target="tpu_custom_call" | custom-call | flops 500000000 | bytes 2097152 | tf_op jit(solution)/shard_map/local_7/pallas_call | solution.py:487
  40.2 0.0 collective-permute-done.10.refs_1_
  40.2 0.0 copy-done.1
  40.2 0.0 copy-done.2
  40.2 0.0 copy-done.3
  40.2 3.2 %final.1 = bf16[128,2048]{1,0:T(8,128)(2,1)} custom-call(f32[4,16,128]{2,1,0:T(8,128)S(1)} %get-tuple-element.110.refs_0_, f32[4,16,128]{2,1,0:T(8,128)S(1)} %collective-permute-done.10.refs_1_, f32[4,128,32]{2,1,0:T(8,128)S(1)} %get-tuple-element.117.refs_2_, f32[8,128,32]{2,1,0:T(8,128)S(1)} %get-tuple-element.118.refs_3_, ...), custom_call_target="tpu_custom_call" | custom-call | tf_op jit(solution)/shard_map/final/pallas_call | solution.py:596
  (2 shorter events, 0.1 us)
Async XLA Ops:
  0.0 10.8 %copy-start = (f32[2,2,64,16,64]{4,3,2,1,0:T(8,128)S(1)}, f32[2,2,64,16,64]{4,3,2,1,0:T(8,128)}, u32[]{:S(2)}) copy-start(f32[2,2,64,16,64]{4,3,2,1,0:T(8,128)} %readout.9) | copy-start | bytes 3145732
  9.3 2.9 %collective-permute-start = (f32[72,128]{1,0:T(8,128)S(1)}, f32[72,128]{1,0:T(8,128)S(1)}, u32[]{:S(2)}, u32[]{:S(2)}) collective-permute-start(f32[72,128]{1,0:T(8,128)S(1)} %get-tuple-element.135), channel_id=1, source_target_pairs={{0,1},{1,0},{2,3},{3,2},{4,5},{5,4},{6,7},{7,6},{8,9},{9,8},{10,11... | collective-permute-start | bytes 110600 | tf_op jit(solution)/shard_map/ppermute | solution.py:571
  12.3 6.7 %collective-permute-start.3 = (f32[72,128]{1,0:T(8,128)S(1)}, f32[72,128]{1,0:T(8,128)S(1)}, u32[]{:S(2)}, u32[]{:S(2)}) collective-permute-start(f32[72,128]{1,0:T(8,128)S(1)} %pair.1.own), channel_id=1, source_target_pairs={{0,4},{4,0},{2,6},{6,2},{1,5},{5,1},{3,7},{7,3},{8,12},{12,8},{10,... | collective-permute-start | bytes 110600 | tf_op jit(solution)/shard_map/ppermute | solution.py:566
  15.4 4.0 %collective-permute-start.2 = (f32[72,128]{1,0:T(8,128)S(1)}, f32[72,128]{1,0:T(8,128)S(1)}, u32[]{:S(2)}, u32[]{:S(2)}) collective-permute-start(f32[72,128]{1,0:T(8,128)S(1)} %pair.1.own), channel_id=1, source_target_pairs={{0,6},{6,0},{2,4},{4,2},{1,7},{7,1},{3,5},{5,3},{8,14},{14,8},{10,... | collective-permute-start | bytes 110600 | tf_op jit(solution)/shard_map/ppermute | solution.py:566
  16.2 3.2 %collective-permute-start.1 = (f32[72,128]{1,0:T(8,128)S(1)}, f32[72,128]{1,0:T(8,128)S(1)}, u32[]{:S(2)}, u32[]{:S(2)}) collective-permute-start(f32[72,128]{1,0:T(8,128)S(1)} %pair.1.own), channel_id=1, source_target_pairs={{0,2},{2,0},{4,6},{6,4},{1,3},{3,1},{5,7},{7,5},{8,10},{10,8},{12,... | collective-permute-start | bytes 110600 | tf_op jit(solution)/shard_map/ppermute | solution.py:566
  19.6 6.5 %collective-permute-start.6 = (f32[72,128]{1,0:T(8,128)S(1)}, f32[72,128]{1,0:T(8,128)S(1)}, u32[]{:S(2)}, u32[]{:S(2)}) collective-permute-start(f32[72,128]{1,0:T(8,128)S(1)} %get-tuple-element.88.own), channel_id=1, source_target_pairs={{0,16},{16,0},{8,24},{24,8},{1,17},{17,1},{9,25},{25,9},{2,18},{18... | collective-permute-start | bytes 110600 | tf_op jit(solution)/shard_map/ppermute | solution.py:566
  22.4 4.0 %collective-permute-start.5 = (f32[72,128]{1,0:T(8,128)S(1)}, f32[72,128]{1,0:T(8,128)S(1)}, u32[]{:S(2)}, u32[]{:S(2)}) collective-permute-start(f32[72,128]{1,0:T(8,128)S(1)} %get-tuple-element.88.own), channel_id=1, source_target_pairs={{0,24},{24,0},{8,16},{16,8},{1,25},{25,1},{9,17},{17,9},{2,26},{26... | collective-permute-start | bytes 110600 | tf_op jit(solution)/shard_map/ppermute | solution.py:566
  23.3 3.2 %collective-permute-start.4 = (f32[72,128]{1,0:T(8,128)S(1)}, f32[72,128]{1,0:T(8,128)S(1)}, u32[]{:S(2)}, u32[]{:S(2)}) collective-permute-start(f32[72,128]{1,0:T(8,128)S(1)} %get-tuple-element.88.own), channel_id=1, source_target_pairs={{0,8},{8,0},{16,24},{24,16},{1,9},{9,1},{17,25},{25,17},{2,10},{10... | collective-permute-start | bytes 110600 | tf_op jit(solution)/shard_map/ppermute | solution.py:566
  26.6 7.8 %collective-permute-start.7 = (f32[40,128]{1,0:T(8,128)S(1)}, f32[40,128]{1,0:T(8,128)S(1)}, u32[]{:S(2)}, u32[]{:S(2)}) collective-permute-start(f32[40,128]{1,0:T(8,128)S(1)} %get-tuple-element.96), channel_id=1, source_target_pairs={{0,64},{64,0},{32,96},{96,32},{1,65},{65,1},{33,97},{97,33},{2,66}... | collective-permute-start | bytes 61448 | tf_op jit(solution)/shard_map/ppermute | solution.py:566
  30.3 4.1 %collective-permute-start.8 = (f32[40,128]{1,0:T(8,128)S(1)}, f32[40,128]{1,0:T(8,128)S(1)}, u32[]{:S(2)}, u32[]{:S(2)}) collective-permute-start(f32[40,128]{1,0:T(8,128)S(1)} %get-tuple-element.103), channel_id=1, source_target_pairs={{0,96},{96,0},{32,64},{64,32},{1,97},{97,1},{33,65},{65,33},{2,98}... | collective-permute-start | bytes 61448 | tf_op jit(solution)/shard_map/ppermute | solution.py:566
  30.7 3.7 %collective-permute-start.9 = (f32[40,128]{1,0:T(8,128)S(1)}, f32[40,128]{1,0:T(8,128)S(1)}, u32[]{:S(2)}, u32[]{:S(2)}) collective-permute-start(f32[40,128]{1,0:T(8,128)S(1)} %get-tuple-element.104), channel_id=1, source_target_pairs={{0,32},{32,0},{64,96},{96,64},{1,33},{33,1},{65,97},{97,65},{2,34}... | collective-permute-start | bytes 61448 | tf_op jit(solution)/shard_map/ppermute | solution.py:566
  34.5 5.6 %copy-start.1 = (f32[2048]{0:T(1024)S(1)}, f32[2048]{0:T(1024)}, u32[]{:S(2)}) copy-start(f32[2048]{0:T(1024)} %param.25) | copy-start | bytes 24580
  34.6 5.6 %copy-start.2 = (f32[1024]{0:T(1024)S(1)}, f32[1024]{0:T(1024)}, u32[]{:S(2)}) copy-start(f32[1024]{0:T(1024)} %param.21) | copy-start | bytes 12292
  34.6 5.6 %copy-start.3 = (f32[1024]{0:T(1024)S(1)}, f32[1024]{0:T(1024)}, u32[]{:S(2)}) copy-start(f32[1024]{0:T(1024)} %param.23) | copy-start | bytes 12292
  34.6 5.6 %collective-permute-start.10 = (f32[4,16,128]{2,1,0:T(8,128)S(1)}, f32[4,16,128]{2,1,0:T(8,128)S(1)}, u32[]{:S(2)}, u32[]{:S(2)}) collective-permute-start(f32[4,16,128]{2,1,0:T(8,128)S(1)} %get-tuple-element.111), channel_id=1, source_target_pairs={{0,1},{1,0},{2,3},{3,2},{4,5},{5,4},{6,7},{7,6},{8,9},{9,8},{10,11... | collective-permute-start | bytes 98312 | tf_op jit(solution)/shard_map/ppermute | solution.py:589
